TPU v7x, 512 devices: a whole 4x8x8 slice. The times are simulated.
512 devices in a mesh: ep: 32 (over z, x), tp: 16 (over y, core).
Axes of the slice: x: 4, y: 8, z: 8, core: 2. Of those that a mesh axis runs over, the one named last changes fastest.
Arguments:
- pool_input: bfloat16 [8192, 2048], P('ep', 'tp'), may hold values from -6 to 6
- pool_map: bfloat16 [16, 128, 128], replicated, may hold values from -0.5 to 0.5
- pool_scale: float32 [2048], replicated, may hold values from 0.1 to 1.9
- out_proj: bfloat16 [2048, 4096], P('tp'), may hold values from -0.125 to 0.125
- moe_input: bfloat16 [4096, 4096], P('ep'), may hold values from -6 to 6
- norm_gain: float32 [4096], replicated, may hold values from 0.1 to 1.9
- routes: int32 [4096, 4], P('ep'), may hold values from 0 to 31, all different within a row; in each aligned block of 128 rows (0 to 127, 128 to 255, ...) at most 24 rows name the same one
- route_weights: float32 [4096, 4], P('ep'), may hold values from 0.1 to 1
- expert_gate: bfloat16 [32, 4096, 1024], P('ep', None, 'tp'), may hold values from -0.09375 to 0.09375
- expert_up: bfloat16 [32, 4096, 1024], P('ep', None, 'tp'), may hold values from -0.09375 to 0.09375
- expert_down: bfloat16 [32, 1024, 4096], P('ep', None, 'tp'), may hold values from -0.1875 to 0.1875
- shared_gate: bfloat16 [4096, 512], P(None, 'tp'), may hold values from -0.09375 to 0.09375
- shared_up: bfloat16 [4096, 512], P(None, 'tp'), may hold values from -0.09375 to 0.09375
- shared_down: bfloat16 [512, 4096], P('tp'), may hold values from -0.25 to 0.25
Outputs:
- mixer_output: bfloat16 [8192, 4096], P('ep', 'tp')
- moe_output: bfloat16 [4096, 4096], P('ep', 'tp')
Inputs may be any that keep to these rules, and one draw needn't show every extreme that they name: `routes`: each row names 4 different experts. In each aligned block of 128 rows no expert is named by more than 24 rows, a bound that some block reaches.
All inputs are finite; a program needn't handle non-finite values.
Results may differ from a plain program's by a relative error of at most 0.017.
Values may be sent and summed in bfloat16 or wider, within the bound.
No kernel may reach another device: no remote copies, remote signals or barrier semaphores. Data moves between devices by JAX's collectives and lax.ppermute only.
A program may use at most 64 MiB of HBM per device.

v0:
```python
import jax
import jax.numpy as jnp
from jax import lax
from jax.sharding import PartitionSpec as P

windows = (2, 4, 8, 16)
reach_back = 15
eps = 1e-05


def passed_along(block, axis, distance):
    devices = range(lax.axis_size(axis))
    route = [(i - distance, i) for i in devices if i - distance in devices]
    return lax.ppermute(block, axis, route)


def sent_to_all(x, axis):
    devices = lax.axis_size(axis)
    return lax.all_to_all(jnp.broadcast_to(x[None], (devices, *x.shape)), axis, 0, 0, tiled=True)


def joined_along(pieces, dim):
    shape = list(pieces.shape[1:])
    shape[dim] *= pieces.shape[0]
    return jnp.moveaxis(pieces, 0, dim).reshape(shape)


def gathered_copies(x, axis, dim):
    pieces = sent_to_all(x, axis)
    return joined_along(pieces, dim)


def in_one_piece(arrays, axis, dim, along):
    both = jnp.concatenate(arrays, axis=along)
    out, at, done = (lax.psum_scatter(both, axis, scatter_dimension=dim, tiled=True), 0, [])
    for a in arrays:
        done.append(lax.slice_in_dim(out, at, at + a.shape[along], axis=along))
        at += a.shape[along]
    return tuple(done)


def pool_branch(pool_input, pool_map, pool_scale, out_proj):
    row_count = pool_input.shape[0]
    channels = pool_input.shape[1]
    group_dim = pool_map.shape[1]
    local_groups = channels // group_dim
    tp_rank = lax.axis_index("tp")
    ep_rank = lax.axis_index("ep")
    earlier_rows = passed_along(pool_input[row_count - reach_back :], "ep", 1)
    values = pool_input.astype(jnp.float32)
    extended = jnp.concatenate([earlier_rows.astype(jnp.float32), values], axis=0)
    position = (ep_rank * row_count + jnp.arange(row_count, dtype=jnp.int32)).astype(jnp.float32)
    group_ids = tp_rank * local_groups + jnp.arange(channels, dtype=jnp.int32) // group_dim
    group_kind = group_ids % 4
    running = jnp.zeros((row_count, channels), jnp.float32)
    pooled = -values
    for lag_step in range(reach_back + 1):
        running = running + extended[reach_back - lag_step : reach_back - lag_step + row_count]
        if lag_step + 1 in windows:
            kind_id = windows.index(lag_step + 1)
            counts = jnp.minimum(position + 1.0, float(lag_step + 1))
            select = (group_kind == kind_id).astype(jnp.float32)
            pooled = pooled + select[None, :] * running / counts[:, None]
    pooled = pooled.astype(jnp.bfloat16)
    my_maps = lax.dynamic_slice_in_dim(pool_map, tp_rank * local_groups, local_groups, 0)
    my_scale = lax.dynamic_slice_in_dim(pool_scale, tp_rank * channels, channels, 0)
    mapped = jnp.einsum(
        "rgc,gcd->rgd",
        pooled.reshape(row_count, local_groups, group_dim),
        my_maps,
        preferred_element_type=jnp.float32,
    )
    group_out = (mapped.reshape(row_count, channels) * my_scale[None, :]).astype(jnp.bfloat16)
    return jnp.dot(group_out, out_proj, preferred_element_type=jnp.float32)


def dispatch_rows(routes, expert_count, capacity):
    tok_count, top_count = routes.shape
    flat_ids = routes.reshape(tok_count * top_count)
    one_hot = (flat_ids[:, None] == jnp.arange(expert_count, dtype=jnp.int32)[None, :]).astype(
        jnp.int32
    )
    earlier = jnp.cumsum(one_hot, axis=0) - one_hot
    slot_ids = jnp.sum(earlier * one_hot, axis=1)
    return (flat_ids * capacity + slot_ids).reshape(tok_count, top_count)


def per_device(
    pool_input,
    pool_map,
    pool_scale,
    out_proj,
    moe_input,
    norm_gain,
    routes,
    route_weights,
    expert_gate,
    expert_up,
    expert_down,
    shared_gate,
    shared_up,
    shared_down,
):
    mixer_part = pool_branch(pool_input, pool_map, pool_scale, out_proj)
    values = moe_input.astype(jnp.float32)
    centre = values - jnp.mean(values, axis=1, keepdims=True)
    variance = jnp.mean(centre * centre, axis=1, keepdims=True)
    normed = (centre * lax.rsqrt(variance + eps) * norm_gain[None, :]).astype(jnp.bfloat16)
    expert_count = lax.axis_size("ep")
    tok_count = moe_input.shape[0]
    top_count = routes.shape[1]
    capacity = (3 * tok_count * top_count + 2 * expert_count - 1) // (2 * expert_count)
    slot_index = dispatch_rows(routes, expert_count, capacity)
    buffer_len = expert_count * capacity
    targets = jnp.arange(buffer_len, dtype=jnp.int32)[:, None]
    placing = jnp.zeros((buffer_len, tok_count), jnp.float32)
    for top_step in range(top_count):
        placing = placing + (targets == slot_index[None, :, top_step]).astype(jnp.float32)
    outgoing = jnp.dot(
        placing.astype(jnp.bfloat16), normed, preferred_element_type=jnp.float32
    ).astype(jnp.bfloat16)
    gate_weight = expert_gate[0]
    up_weight = expert_up[0]
    down_weight = expert_down[0]
    tp_rank = lax.axis_index("tp")
    slice_width = outgoing.shape[1] // lax.axis_size("tp")
    my_slice = lax.dynamic_slice_in_dim(outgoing, tp_rank * slice_width, slice_width, 1)
    arrived = lax.all_to_all(my_slice, "ep", split_axis=0, concat_axis=0, tiled=True)
    shard_cols = lax.all_gather(arrived, "tp", axis=1, tiled=True)
    gate_val = jnp.dot(shard_cols, gate_weight, preferred_element_type=jnp.float32)
    up_val = jnp.dot(shard_cols, up_weight, preferred_element_type=jnp.float32)
    hidden = (jax.nn.silu(gate_val) * up_val).astype(jnp.bfloat16)
    expert_result = jnp.dot(
        gathered_copies(hidden, "tp", 1), down_weight, preferred_element_type=jnp.float32
    ).astype(jnp.bfloat16)
    returned = lax.all_to_all(expert_result, "ep", split_axis=0, concat_axis=0, tiled=True)
    routed = jnp.zeros((tok_count, returned.shape[1]), jnp.float32)
    for top_step in range(top_count):
        picked = returned[slot_index[:, top_step]].astype(jnp.float32)
        routed = routed + route_weights[:, top_step, None] * picked
    shared_gate_val = jnp.dot(normed, shared_gate, preferred_element_type=jnp.float32)
    shared_up_val = jnp.dot(normed, shared_up, preferred_element_type=jnp.float32)
    shared_hidden = (jax.nn.silu(shared_gate_val) * shared_up_val).astype(jnp.bfloat16)
    shared_part = jnp.dot(shared_hidden, shared_down, preferred_element_type=jnp.float32)
    mixer_sum, shared_sum = tuple(
        (
            part.astype(jnp.float32)
            for part in in_one_piece(
                (mixer_part.astype(jnp.bfloat16), shared_part.astype(jnp.bfloat16)), "tp", 1, 0
            )
        )
    )
    return (mixer_sum.astype(jnp.bfloat16), (routed + shared_sum).astype(jnp.bfloat16))


def solution(mesh):
    return jax.shard_map(
        per_device,
        mesh=mesh,
        in_specs=(
            P("ep", "tp"),
            P(),
            P(),
            P("tp", None),
            P("ep", None),
            P(),
            P("ep", None),
            P("ep", None),
            P("ep", None, "tp"),
            P("ep", None, "tp"),
            P("ep", None, "tp"),
            P(None, "tp"),
            P(None, "tp"),
            P("tp", None),
        ),
        out_specs=(P("ep", "tp"), P("ep", "tp")),
        check_vma=False,
    )
```

profile of v0, /device:TPU:1, one launch (start us, length us, event | category | flops | bytes accessed | tf_op | source)
XLA Modules:
  0.0 197.1 jit_solution(10955667984421792337)
XLA Ops:
  7.2 0.9 copy.27
  8.4 1.2 reduce-window.6
  9.6 0.2 slice_reduce_fusion
  9.8 0.1 fusion.55
  10.0 0.1 reduce_sum.32
  10.1 0.7 multiply_add_fusion
  10.8 1.5 convert_reduce_fusion
  12.3 0.4 fusion.2
  12.8 1.9 fusion.13
  14.8 27.4 %all_to_all.29 = bf16[32,24,256]{2,1,0:T(8,128)(2,1)} all-to-all(bf16[32,24,256]{2,1,0:T(8,128)(2,1)S(1)} %bitcast.88), channel_id=1, replica_groups=mesh['ep'=32,'tp'=16] {'ep'}, dimensions={0} | all-to-all | bytes 786432 | tf_op jit(solution)/shard_map/all_to_all | solution.py:128
  42.3 2.3 %collective-permute-start = (bf16[15,128]{1,0:T(8,128)(2,1)S(1)}, bf16[15,128]{1,0:T(8,128)(2,1)S(1)}, u32[]{:S(2)}, u32[]{:S(2)}) collective-permute-start(bf16[15,128]{1,0:T(8,128)(2,1)S(1)} %slice.88), channel_id=1, source_target_pairs={{0,16},{16,32},{32,48},{48,64},{64,80},{80,96},{96,112},{112,128},... | collective-permute-start | bytes 11528 | tf_op jit(solution)/shard_map/ppermute | solution.py:14
  44.7 0.5 compare_convert_fusion
  45.2 0.5 fusion.102
  45.7 2.4 %convolution_convert_fusion.1 = bf16[128,4096]{1,0:T(8,128)(2,1)S(1)} fusion(bf16[32,4096]{1,0:T(8,128)(2,1)S(1)} %copy-done.5, bf16[4096,32]{0,1:T(8,128)(2,1)} %param.26, f32[128,32]{0,1:T(8,128)S(1)} %fusion.102, bf16[128,4096]{1,0:T(8,128)(2,1)S(1)} %copy-done.2, f32[4096]{0:T(1024)S(1)} %copy-done.7, f32[128]{0:T(128)S(1)} %add_rsqrt_fusion, ...), kind=kOutput, calls=%fused_computation.5 | convolution fusion | flops 70279168 | bytes 2655232 | tf_op jit(solution)/shard_map/dot_general | solution.py:144
  48.2 0.8 dynamic_slice.10
  49.0 3.3 %convolution_convert_fusion = bf16[256,4096]{1,0:T(8,128)(2,1)} fusion(bf16[128,4096]{1,0:T(8,128)(2,1)S(1)} %copy-done, f32[256,128]{1,0:T(8,128)S(1)} %convert_element_type.122, f32[15,128]{1,0:T(8,128)S(1)} %convert_element_type.124, f32[128]{0:T(128)S(1)} %dynamic_slice.10, f32[256]{0:T(256)S(1)} %get-tuple-element.18, f32[128]{0:T(128)} %get-tuple-element.14, ...), kind=kOutput, calls=%fused_computation.4 | convolution fusion | flops 279379968 | bytes 3323908 | tf_op jit(solution)/shard_map/dot_general | solution.py:74
  52.2 3.6 %pad_maximum_fusion = bf16[384,4096]{1,0:T(8,128)(2,1)} fusion(bf16[128,4096]{1,0:T(8,128)(2,1)S(1)} %convolution_convert_fusion.1, bf16[256,4096]{1,0:T(8,128)(2,1)} %convolution_convert_fusion), kind=kLoop, calls=%fused_computation.6 | loop fusion | flops 6291456 | bytes 6291456 | tf_op jit(solution)/shard_map/concatenate | solution.py:34
  55.8 44.0 %all-gather.2.cloned.1.call-done = bf16[768,4096]{1,0:T(8,128)(2,1)} async-done(((bf16[768,256]{1,0:T(8,128)(2,1)}), bf16[768,4096]{1,0:T(8,128)(2,1)}) %all-gather.2.cloned.1.call-update) | async-done | bytes 6291472 | tf_op jit(solution)/shard_map/all_gather | solution.py:129
  99.8 5.0 %fusion.11 = f32[768,64]{0,1:T(8,128)S(1)} fusion(bf16[768,4096]{1,0:T(8,128)(2,1)} %all-gather.2.cloned.1.call-done, bf16[1,4096,64]{1,2,0:T(8,128)(2,1)S(1)} %copy-done.4), kind=kOutput, calls=%fused_computation.39 | convolution fusion | flops 402653184 | bytes 7012352 | tf_op jit(solution)/shard_map/dot_general | solution.py:130
  104.8 2.1 %fusion.5 = bf16[768,64]{0,1:T(8,128)(2,1)S(1)} fusion(bf16[768,4096]{1,0:T(8,128)(2,1)S(1)} %copy-done.1, bf16[1,4096,64]{1,2,0:T(8,128)(2,1)S(1)} %copy-done.3, f32[768,64]{0,1:T(8,128)S(1)} %fusion.11), kind=kOutput, calls=%fused_computation.16 | convolution fusion | flops 402948096 | bytes 7110656 | tf_op jit(solution)/shard_map/dot_general | solution.py:131
  106.9 0.1 broadcast_in_dim.2
  107.0 52.2 %all_to_all.30 = bf16[16,768,64]{1,2,0:T(8,128)(2,1)S(1)} all-to-all(bf16[16,768,64]{1,2,0:T(8,128)(2,1)S(1)} %broadcast_in_dim.2), channel_id=1, replica_groups=mesh['ep'=32,'tp'=16] {'tp'}, dimensions={0} | all-to-all | bytes 3145728 | tf_op jit(solution)/shard_map/all_to_all | solution.py:19
  159.3 1.4 convolution_convert_fusion.2
  160.6 9.9 %all-to-all-start.2 = ((bf16[32,24,256]{2,1,0:T(8,128)(2,1)}), bf16[32,24,256]{2,1,0:T(8,128)(2,1)S(1)}, u32[]{:S(2)}, u32[]{:S(2)}) async-start(bf16[32,24,256]{2,1,0:T(8,128)(2,1)} %bitcast.17), calls=%async_computation.3 | async-start | bytes 786432 | tf_op jit(solution)/shard_map/all_to_all | solution.py:136
  170.6 11.8 %reduce-scatter.2.cloned.1.call-done = bf16[384,256]{1,0:T(8,128)(2,1)} async-done(((bf16[384,4096]{1,0:T(8,128)(2,1)}), bf16[384,256]{1,0:T(8,128)(2,1)}) %reduce-scatter.2.cloned.1.call-update) | async-done | bytes 196624 | tf_op jit(solution)/shard_map/reduce_scatter | solution.py:35
  182.4 1.6 slice.152
  183.9 1.3 all-to-all-done.2
  185.2 0.8 gather_fusion
  186.1 0.8 gather_fusion.1
  186.9 0.8 gather_fusion.2
  187.8 0.8 gather_fusion.3
  188.6 1.6 add_convert_fusion.2
  (46 shorter events, 0.6 us)
Async XLA Ops:
  7.2 41.8 %copy-start = (bf16[128,4096]{1,0:T(8,128)(2,1)S(1)}, bf16[128,4096]{1,0:T(8,128)(2,1)}, u32[]{:S(2)}) copy-start(bf16[128,4096]{1,0:T(8,128)(2,1)} %param.17) | copy-start | bytes 3145732
  7.2 5.1 %copy-start.2 = (bf16[128,4096]{1,0:T(8,128)(2,1)S(1)}, bf16[128,4096]{1,0:T(8,128)(2,1)}, u32[]{:S(2)}) copy-start(bf16[128,4096]{1,0:T(8,128)(2,1)} %param.18) | copy-start | bytes 3145732
  7.2 5.6 %copy-start.7 = (f32[4096]{0:T(1024)S(1)}, f32[4096]{0:T(1024)}, u32[]{:S(2)}) copy-start(f32[4096]{0:T(1024)} %param.19) | copy-start | bytes 49156
  7.2 92.6 %all-gather.2.cloned.1.call-start = ((), (), s32[]{:S(2)}) async-start(), calls=%async_computation.5 | async-start | bytes 6684672 | tf_op jit(solution)/shard_map/all_gather | solution.py:129
  12.8 29.6 %copy-start.6 = (bf16[256,128]{1,0:T(8,128)(2,1)S(1)}, bf16[256,128]{1,0:T(8,128)(2,1)}, u32[]{:S(2)}) copy-start(bf16[256,128]{1,0:T(8,128)(2,1)} %param.14) | copy-start | bytes 196612
  12.8 32.4 %copy-start.10 = (bf16[4096,32]{0,1:T(8,128)(2,1)S(1)}, bf16[4096,32]{0,1:T(8,128)(2,1)}, u32[]{:S(2)}) copy-start(bf16[4096,32]{0,1:T(8,128)(2,1)} %param.25) | copy-start | bytes 786436
  14.7 31.0 %copy-start.5 = (bf16[32,4096]{1,0:T(8,128)(2,1)S(1)}, bf16[32,4096]{1,0:T(8,128)(2,1)}, u32[]{:S(2)}) copy-start(bf16[32,4096]{1,0:T(8,128)(2,1)} %param.27) | copy-start | bytes 786436
  42.3 140.1 %reduce-scatter.2.cloned.1.call-start = ((), (), s32[]{:S(2)}) async-start(), calls=%async_computation.4 | async-start | bytes 3342336 | tf_op jit(solution)/shard_map/reduce_scatter | solution.py:35
  42.3 6.6 %collective-permute-start = (bf16[15,128]{1,0:T(8,128)(2,1)S(1)}, bf16[15,128]{1,0:T(8,128)(2,1)S(1)}, u32[]{:S(2)}, u32[]{:S(2)}) collective-permute-start(bf16[15,128]{1,0:T(8,128)(2,1)S(1)} %slice.88), channel_id=1, source_target_pairs={{0,16},{16,32},{32,48},{48,64},{64,80},{80,96},{96,112},{112,128},... | collective-permute-start | bytes 11528 | tf_op jit(solution)/shard_map/ppermute | solution.py:14
  55.8 44.0 %copy-start.4 = (bf16[1,4096,64]{1,2,0:T(8,128)(2,1)S(1)}, bf16[1,4096,64]{1,2,0:T(8,128)(2,1)}, u32[]{:S(2)}) copy-start(bf16[1,4096,64]{1,2,0:T(8,128)(2,1)} %param.22) | copy-start | bytes 1572868
  55.8 48.9 %copy-start.3 = (bf16[1,4096,64]{1,2,0:T(8,128)(2,1)S(1)}, bf16[1,4096,64]{1,2,0:T(8,128)(2,1)}, u32[]{:S(2)}) copy-start(bf16[1,4096,64]{1,2,0:T(8,128)(2,1)} %param.23) | copy-start | bytes 1572868
  99.8 5.0 %copy-start.1 = (bf16[768,4096]{1,0:T(8,128)(2,1)S(1)}, bf16[768,4096]{1,0:T(8,128)(2,1)}, u32[]{:S(2)}) copy-start(bf16[768,4096]{1,0:T(8,128)(2,1)} %all-gather.2.cloned.1.call-done) | copy-start | bytes 18874372
  106.9 52.4 %copy-start.9 = (bf16[1,1024,256]{2,1,0:T(8,128)(2,1)S(1)}, bf16[1,1024,256]{2,1,0:T(8,128)(2,1)}, u32[]{:S(2)}) copy-start(bf16[1,1024,256]{2,1,0:T(8,128)(2,1)} %param.24) | copy-start | bytes 1572868
  159.3 11.3 %copy-start.8 = (f32[128,4]{0,1:T(4,128)S(1)}, f32[128,4]{0,1:T(4,128)}, u32[]{:S(2)}) copy-start(f32[128,4]{0,1:T(4,128)} %param.21) | copy-start | bytes 6148
  160.6 24.6 %all-to-all-start.2 = ((bf16[32,24,256]{2,1,0:T(8,128)(2,1)}), bf16[32,24,256]{2,1,0:T(8,128)(2,1)S(1)}, u32[]{:S(2)}, u32[]{:S(2)}) async-start(bf16[32,24,256]{2,1,0:T(8,128)(2,1)} %bitcast.17), calls=%async_computation.3 | async-start | bytes 786432 | tf_op jit(solution)/shard_map/all_to_all | solution.py:136
Sparse Core Ops, SparseCore 0:
  42.4 57.3 all-gather.1
  102.7 79.6 reduce-scatter.1
where the time goes:
time: 198 us; the launch traced here: 197 us
  blocking collectives  79.7 us (40%)
  waiting for transfers between devices  57.1 us (29%)
  matrix products  16.5 us (8%)
  between operations  14.3 us (7%)
  starting transfers between devices  12.3 us (6%)
  other arithmetic  9.7 us (5%)
  local copies, waits for them, and re-layouts  7.53 us (4%)
    all_to_all x1, blocking collectives, sent_to_all(): lax.all_to_all(jnp.broadcast_to(x[None], (devices, *x.shape)), axis, 0, 0...  52.2 us
    all_gather x1, waiting for transfers between devices, per_device(): shard_cols = lax.all_gather(arrived, 'tp', axis=1, tiled=True)  44 us
    all_to_all x1, blocking collectives, per_device(): lax.all_to_all(my_slice, 'ep', split_axis=0, concat_axis=0, tiled=True)  27.4 us
    reduce_scatter x1, waiting for transfers between devices, in_one_piece(): lax.psum_scatter(both, axis, scatter_dimension=dim, tiled=True)  11.8 us
    all_to_all x1, starting transfers between devices, per_device(): lax.all_to_all(expert_result, 'ep', split_axis=0, concat_axis=0, tiled=True)  9.89 us
    dot_general x1, matrix products, per_device(): jnp.dot(shard_cols, gate_weight, preferred_element_type=jnp.float32)  4.96 us
  transfers between devices with their start and end apart: 4, of which 3 were waited for; matrix products, arithmetic and copies ran while one was open for 11% of the time, Pallas kernels for 0%

commit v1 on v0

v1 whole, which is shorter than its diff:
```python
import jax
import jax.numpy as jnp
from jax import lax
from jax.sharding import PartitionSpec as P

windows = (2, 4, 8, 16)
reach_back = 15
eps = 1e-05
f32 = jnp.float32
bf16 = jnp.bfloat16


def halo(block):
    devices = range(lax.axis_size("ep"))
    return lax.ppermute(block, "ep", [(i - 1, i) for i in devices if i > 0])


def along_y(x, step):
    n = lax.axis_size("tp")
    return lax.ppermute(x, "tp", [(i, (i + 2 * step) % n) for i in range(n)])


def to_partner(x):
    n = lax.axis_size("tp")
    return lax.ppermute(x, "tp", [(i, i ^ 1) for i in range(n)])


def tdot(a, b):
    return lax.dot_general(a, b, (((1,), (1,)), ((), ())), preferred_element_type=f32)


def pool_group_out(pool_input, earlier_rows, pool_map, pool_scale, tp_rank, ep_rank):
    row_count, channels = pool_input.shape
    group_dim = pool_map.shape[1]
    local_groups = channels // group_dim
    values = pool_input.astype(f32)
    extended = jnp.concatenate([earlier_rows.astype(f32), values], axis=0)
    position = (ep_rank * row_count + jnp.arange(row_count, dtype=jnp.int32)).astype(f32)
    group_ids = tp_rank * local_groups + jnp.arange(channels, dtype=jnp.int32) // group_dim
    group_kind = group_ids % 4
    running = jnp.zeros((row_count, channels), f32)
    pooled = -values
    for lag_step in range(reach_back + 1):
        running = running + extended[reach_back - lag_step : reach_back - lag_step + row_count]
        if lag_step + 1 in windows:
            kind_id = windows.index(lag_step + 1)
            counts = jnp.minimum(position + 1.0, float(lag_step + 1))
            select = (group_kind == kind_id).astype(f32)
            pooled = pooled + select[None, :] * running / counts[:, None]
    pooled = pooled.astype(bf16)
    my_maps = lax.dynamic_slice_in_dim(pool_map, tp_rank * local_groups, local_groups, 0)
    my_scale = lax.dynamic_slice_in_dim(pool_scale, tp_rank * channels, channels, 0)
    mapped = jnp.einsum(
        "rgc,gcd->rgd",
        pooled.reshape(row_count, local_groups, group_dim),
        my_maps,
        preferred_element_type=f32,
    )
    return (mapped.reshape(row_count, channels) * my_scale[None, :]).astype(bf16)


def per_device(
    pool_input,
    pool_map,
    pool_scale,
    out_proj,
    moe_input,
    norm_gain,
    routes,
    route_weights,
    expert_gate,
    expert_up,
    expert_down,
    shared_gate,
    shared_up,
    shared_down,
):
    tp_rank = lax.axis_index("tp")
    ep_rank = lax.axis_index("ep")
    tp_size = lax.axis_size("tp")
    expert_count = lax.axis_size("ep")
    y_size = tp_size // 2
    core = tp_rank % 2
    y = tp_rank // 2
    tok_count, width = moe_input.shape
    top_count = routes.shape[1]
    capacity = (3 * tok_count * top_count + 2 * expert_count - 1) // (2 * expert_count)
    buffer_len = expert_count * capacity
    slice_width = width // tp_size
    row_count = pool_input.shape[0]

    earlier_rows = halo(pool_input[row_count - reach_back :])

    routes_t = routes.T
    experts = jnp.arange(expert_count, dtype=jnp.int32)[:, None]
    named = jnp.zeros((expert_count, tok_count), f32)
    weight_t = jnp.zeros((expert_count, tok_count), f32)
    for k in range(top_count):
        hit = routes_t[k][None, :] == experts
        named = named + hit.astype(f32)
        weight_t = weight_t + jnp.where(hit, route_weights.T[k][None, :], 0.0)
    before = jnp.arange(tok_count)[:, None] < jnp.arange(tok_count)[None, :]
    earlier = jnp.dot(named.astype(bf16), before.astype(bf16), preferred_element_type=f32)
    slot = jnp.where(named > 0, earlier, -1.0)
    slots = jnp.arange(capacity, dtype=f32)[None, :, None]
    match = slot[:, None, :] == slots
    placing = match.astype(bf16).reshape(buffer_len, tok_count)
    combine = jnp.where(match, weight_t[:, None, :], 0.0).astype(bf16).reshape(buffer_len, tok_count)

    values = moe_input.astype(f32)
    mean = jnp.mean(values, axis=1, keepdims=True)
    centre = values - mean
    rstd = lax.rsqrt(jnp.mean(centre * centre, axis=1, keepdims=True) + eps)
    at = tp_rank * slice_width
    mine = lax.dynamic_slice_in_dim(moe_input, at, slice_width, 1).astype(f32)
    my_gain = lax.dynamic_slice_in_dim(norm_gain, at, slice_width, 0)
    normed_slice = ((mine - mean) * rstd * my_gain[None, :]).astype(bf16)
    outgoing = jnp.dot(placing, normed_slice, preferred_element_type=f32).astype(bf16)
    arrived = lax.all_to_all(outgoing, "ep", split_axis=0, concat_axis=0, tiled=True)

    gate_up = jnp.concatenate([expert_gate[0].T, expert_up[0].T], axis=0)
    hid = gate_up.shape[0]

    def feature_slices(side):
        pieces = []
        for j in range(y_size):
            lo = 2 * j * slice_width
            even = gate_up[:, lo : lo + slice_width]
            odd = gate_up[:, lo + slice_width : lo + 2 * slice_width]
            pieces.append(jnp.where(side == 0, even, odd))
        return jnp.stack(pieces)

    own_weights = feature_slices(core)
    partner_weights = to_partner(feature_slices(1 - core))
    weights = jnp.concatenate([own_weights, partner_weights], axis=1)

    def product(rows, offset):
        w = lax.dynamic_index_in_dim(weights, (y + offset) % y_size, 0, keepdims=False)
        return tdot(w, rows)

    half = buffer_len // 2
    sums = []
    ups = [rows for rows in (arrived[:half], arrived[half:])]
    downs = list(ups)
    sums = [product(rows, 0) for rows in ups]
    reach_up = (y_size // 2, y_size // 2 - 1)
    for step in range(1, y_size // 2 + 1):
        for h in range(2):
            if step <= reach_up[h]:
                ups[h] = along_y(ups[h], 1)
                sums[h] = sums[h] + product(ups[h], -step)
            if step <= reach_up[1 - h]:
                downs[h] = along_y(downs[h], -1)
                sums[h] = sums[h] + product(downs[h], step)
    partial = jnp.concatenate(sums, axis=1)
    full = partial[:hid] + to_partner(partial[hid:])
    units = hid // 2
    hidden = (jax.nn.silu(full[:units]) * full[units:]).astype(bf16)

    order = [None] * y_size
    order[0] = hidden
    up = down = hidden
    for step in range(1, y_size // 2 + 1):
        up = along_y(up, 1)
        order[y_size - step] = up
        if step < y_size // 2:
            down = along_y(down, -1)
            order[step] = down
    own_hidden = jnp.concatenate(order, axis=0)
    other_hidden = to_partner(own_hidden)
    down_weight = expert_down[0].reshape(y_size, 2, units, slice_width)

    def down_rows(side):
        pieces = []
        for j in range(y_size):
            block = lax.dynamic_index_in_dim(down_weight, (y + j) % y_size, 0, keepdims=False)
            pieces.append(jnp.where(side == 0, block[0], block[1]))
        return jnp.concatenate(pieces, axis=0)

    def down_product(h, w):
        return lax.dot_general(h, w, (((0,), (0,)), ((), ())), preferred_element_type=f32)

    expert_result = down_product(own_hidden, down_rows(core))
    expert_result = expert_result + down_product(other_hidden, down_rows(1 - core))
    returned = lax.all_to_all(expert_result.astype(bf16), "ep", split_axis=0, concat_axis=0, tiled=True)
    routed = lax.dot_general(combine, returned, (((0,), (0,)), ((), ())), preferred_element_type=f32)

    group_out = pool_group_out(pool_input, earlier_rows, pool_map, pool_scale, tp_rank, ep_rank)
    normed = (centre * rstd * norm_gain[None, :]).astype(bf16)
    shared_gate_val = jnp.dot(normed, shared_gate, preferred_element_type=f32)
    shared_up_val = jnp.dot(normed, shared_up, preferred_element_type=f32)
    shared_hidden = (jax.nn.silu(shared_gate_val) * shared_up_val).astype(bf16)

    def columns(weight, side):
        pieces = []
        for j in range(y_size):
            begin = (((y + j) % y_size) * 2 + side) * slice_width
            pieces.append(lax.dynamic_slice_in_dim(weight, begin, slice_width, 1))
        return jnp.concatenate(pieces, axis=1)

    def projected(side):
        top = jnp.dot(group_out, columns(out_proj, side), preferred_element_type=f32)
        bottom = jnp.dot(shared_hidden, columns(shared_down, side), preferred_element_type=f32)
        return jnp.concatenate([top.astype(bf16), bottom.astype(bf16)], axis=0)

    from_partner = to_partner(projected(1 - core))
    kept = projected(core)

    def part(j):
        lo = j * slice_width
        return kept[:, lo : lo + slice_width].astype(f32) + from_partner[:, lo : lo + slice_width].astype(f32)

    up = down = None
    for step in range(y_size // 2):
        j = y_size // 2 - step
        up = part(j) if up is None else part(j) + up.astype(f32)
        up = along_y(up.astype(bf16), 1)
        if step < y_size // 2 - 1:
            j = y_size // 2 + 1 + step
            down = part(j) if down is None else part(j) + down.astype(f32)
            down = along_y(down.astype(bf16), -1)
    total = part(0) + up.astype(f32) + down.astype(f32)
    return (total[:row_count].astype(bf16), (routed + total[row_count:]).astype(bf16))


def solution(mesh):
    return jax.shard_map(
        per_device,
        mesh=mesh,
        in_specs=(
            P("ep", "tp"),
            P(),
            P(),
            P("tp", None),
            P("ep", None),
            P(),
            P("ep", None),
            P("ep", None),
            P("ep", None, "tp"),
            P("ep", None, "tp"),
            P("ep", None, "tp"),
            P(None, "tp"),
            P(None, "tp"),
            P("tp", None),
        ),
        out_specs=(P("ep", "tp"), P("ep", "tp")),
        check_vma=False,
    )
```

time: 198 us -> 226 us (1.14)
  starting transfers between devices: 12.3 us -> 129 us
  blocking collectives: 79.7 us -> 0 us
  waiting for transfers between devices: 57.1 us -> 17.8 us
  local copies, waits for them, and re-layouts: 7.53 us -> 31.6 us
  other arithmetic: 9.7 us -> 26 us
  between operations: 14.3 us -> 2 us
    ppermute x1 -> x33, starting transfers between devices: 2.31 us -> 113 us  [the longest x28 84.8 us: along_y(): return lax.ppermute(x, 'tp', [(i, (i + 2 * step) % n) for i in range(n)])]
    all_to_all x2 -> x0, blocking collectives: 79.7 us -> none  [the longest x1 52.2 us: sent_to_all(): lax.all_to_all(jnp.broadcast_to(x[None], (devices, *x.shape)), axis, 0, 0...]
    all_gather x1 -> x0, waiting for transfers between devices: 44 us -> none  [per_device(): shard_cols = lax.all_gather(arrived, 'tp', axis=1, tiled=True)]
    unnamed x23 -> x90, local copies, waits for them, and re-layouts: 0.98 us -> 23 us
    ppermute x1 -> x33, waiting for transfers between devices: 0.01 us -> 16.2 us  [the longest x28 16.2 us: along_y(): return lax.ppermute(x, 'tp', [(i, (i + 2 * step) % n) for i in range(n)])]
    unnamed x0 -> x27, other arithmetic: none -> 12.3 us
    reduce_scatter x1 -> x0, waiting for transfers between devices: 11.8 us -> none  [in_one_piece(): lax.psum_scatter(both, axis, scatter_dimension=dim, tiled=True)]
    all_to_all x1 -> x2, starting transfers between devices: 9.89 us -> 16.3 us  [the longest x1 8.59 us: per_device(): lax.all_to_all(expert_result.astype(bf16), 'ep', split_axis=0, concat_axi...]
  transfers between devices with their start and end apart: 4 -> 35, of which waited for: 3 -> 8; matrix products, arithmetic and copies ran while one was open for 11% -> 29% of each run, Pallas kernels for 0% -> 0%
where the time goes in v1:
time: 226 us; the launch traced here: 223 us
  starting transfers between devices  129 us (57%)
  local copies, waits for them, and re-layouts  31.6 us (14%)
  other arithmetic  26 us (12%)
  waiting for transfers between devices  17.8 us (8%)
  matrix products  16.9 us (7%)
    ppermute x28, starting transfers between devices, along_y(): return lax.ppermute(x, 'tp', [(i, (i + 2 * step) % n) for i in range(n)])  84.8 us
    ppermute x4, starting transfers between devices, to_partner(): return lax.ppermute(x, 'tp', [(i, i ^ 1) for i in range(n)])  24.1 us
    unnamed x90, local copies, waits for them, and re-layouts  23 us
    ppermute x28, waiting for transfers between devices, along_y(): return lax.ppermute(x, 'tp', [(i, (i + 2 * step) % n) for i in range(n)])  16.2 us
    unnamed x27, other arithmetic  12.3 us
    all_to_all x1, starting transfers between devices, per_device(): lax.all_to_all(expert_result.astype(bf16), 'ep', split_axis=0, concat_axi...  8.59 us
    all_to_all x1, starting transfers between devices, per_device(): lax.all_to_all(outgoing, 'ep', split_axis=0, concat_axis=0, tiled=True)  7.68 us
    concatenate x4, local copies, waits for them, and re-layouts, columns(): return jnp.concatenate(pieces, axis=1)  5.65 us
  transfers between devices with their start and end apart: 35, of which 8 were waited for; matrix products, arithmetic and copies ran while one was open for 29% of the time, Pallas kernels for 0%

profile of v1, /device:TPU:1, one launch (start us, length us, event | category | flops | bytes accessed | tf_op | source)
XLA Modules:
  0.0 223.2 jit_solution(4651192140991198559)
XLA Ops:
  7.6 8.7 %collective-permute-start.9 = (bf16[8,128,256]{2,1,0:T(8,128)(2,1)}, bf16[8,128,256]{2,1,0:T(8,128)(2,1)S(1)}, u32[]{:S(2)}, u32[]{:S(2)}) collective-permute-start(bf16[8,128,256]{2,1,0:T(8,128)(2,1)} %get-tuple-element.4), channel_id=1, source_target_pairs={{0,1},{1,0},{2,3},{3,2},{4,5},{5,4},{6,7},{7,6},{8,9},{9,8},{10,11... | collective-permute-start | bytes 1572872 | tf_op jit(solution)/shard_map/ppermute | solution.py:25
  18.9 1.9 convolution_convert_fusion.4
  20.9 7.7 %all-to-all-start = ((bf16[32,24,256]{2,1,0:T(8,128)(2,1)}), bf16[32,24,256]{2,1,0:T(8,128)(2,1)S(1)}, u32[]{:S(2)}, u32[]{:S(2)}) async-start(bf16[32,24,256]{2,1,0:T(8,128)(2,1)} %bitcast.232), calls=%async_computation | async-start | bytes 786432 | tf_op jit(solution)/shard_map/all_to_all | solution.py:119
  29.8 3.7 %collective-permute-start = (bf16[15,128]{1,0:T(8,128)(2,1)}, bf16[15,128]{1,0:T(8,128)(2,1)}, u32[]{:S(2)}, u32[]{:S(2)}) collective-permute-start(bf16[15,128]{1,0:T(8,128)(2,1)} %slice.295), channel_id=1, source_target_pairs={{0,16},{16,32},{32,48},{48,64},{64,80},{80,96},{96,112},{112,128},... | collective-permute-start | bytes 11528 | tf_op jit(solution)/shard_map/ppermute | solution.py:15
  34.7 2.6 %fusion.4 = bf16[128,4096]{1,0:T(8,128)(2,1)} fusion(bf16[128,4096]{1,0:T(8,128)(2,1)} %param.18, f32[4096]{0:T(1024)S(1)} %copy-done.15, f32[128]{0:T(128)} %copy-done.29, f32[128]{0:T(128)} %copy-done.18), kind=kLoop, calls=%fused_computation.65 | loop fusion | flops 2621440 | bytes 2114560 | tf_op jit(solution)/shard_map/convert_element_type | solution.py:189
  80.5 5.1 %collective-permute-start.11 = (bf16[384,256]{1,0:T(8,128)(2,1)S(1)}, bf16[384,256]{1,0:T(8,128)(2,1)S(1)}, u32[]{:S(2)}, u32[]{:S(2)}) collective-permute-start(bf16[384,256]{1,0:T(8,128)(2,1)S(1)} %bitcast.236), channel_id=1, source_target_pairs={{0,14},{1,15},{2,0},{3,1},{4,2},{5,3},{6,4},{7,5},{8,6},{9,7},{10,... | collective-permute-start | bytes 589832 | tf_op jit(solution)/shard_map/ppermute | solution.py:20
  85.6 3.0 %collective-permute-start.18 = (bf16[384,256]{1,0:T(8,128)(2,1)S(1)}, bf16[384,256]{1,0:T(8,128)(2,1)S(1)}, u32[]{:S(2)}, u32[]{:S(2)}) collective-permute-start(bf16[384,256]{1,0:T(8,128)(2,1)S(1)} %bitcast.233), channel_id=1, source_target_pairs={{0,14},{1,15},{2,0},{3,1},{4,2},{5,3},{6,4},{7,5},{8,6},{9,7},{10,... | collective-permute-start | bytes 589832 | tf_op jit(solution)/shard_map/ppermute | solution.py:20
  89.7 3.3 %collective-permute-start.1 = (bf16[384,2048]{1,0:T(8,128)(2,1)S(1)}, bf16[384,2048]{1,0:T(8,128)(2,1)S(1)}, u32[]{:S(2)}, u32[]{:S(2)}) collective-permute-start(bf16[384,2048]{1,0:T(8,128)(2,1)S(1)} %pad_maximum_fusion), channel_id=1, source_target_pairs={{0,1},{1,0},{2,3},{3,2},{4,5},{5,4},{6,7},{7,6},{8,9},{9,8},{10,11... | collective-permute-start | bytes 4718600 | tf_op jit(solution)/shard_map/ppermute | solution.py:25
  93.1 2.3 %collective-permute-start.10 = (bf16[384,256]{1,0:T(8,128)(2,1)S(1)}, bf16[384,256]{1,0:T(8,128)(2,1)S(1)}, u32[]{:S(2)}, u32[]{:S(2)}) collective-permute-start(bf16[384,256]{1,0:T(8,128)(2,1)S(1)} %bitcast.237), channel_id=1, source_target_pairs={{0,2},{1,3},{2,4},{3,5},{4,6},{5,7},{6,8},{7,9},{8,10},{9,11},{10,... | collective-permute-start | bytes 589832 | tf_op jit(solution)/shard_map/ppermute | solution.py:20
  95.4 1.9 collective-permute-start.17
  97.3 4.6 %collective-permute-start.13 = (bf16[384,256]{1,0:T(8,128)(2,1)S(1)}, bf16[384,256]{1,0:T(8,128)(2,1)S(1)}, u32[]{:S(2)}, u32[]{:S(2)}) collective-permute-start(bf16[384,256]{1,0:T(8,128)(2,1)S(1)} %collective-permute-done.11), channel_id=1, source_target_pairs={{0,14},{1,15},{2,0},{3,1},{4,2},{5,3},{6,4},{7,5},{8,6},{9,7},{10,... | collective-permute-start | bytes 589832 | tf_op jit(solution)/shard_map/ppermute | solution.py:20
  101.9 3.0 %collective-permute-start.20 = (bf16[384,256]{1,0:T(8,128)(2,1)S(1)}, bf16[384,256]{1,0:T(8,128)(2,1)S(1)}, u32[]{:S(2)}, u32[]{:S(2)}) collective-permute-start(bf16[384,256]{1,0:T(8,128)(2,1)S(1)} %collective-permute-done.18), channel_id=1, source_target_pairs={{0,14},{1,15},{2,0},{3,1},{4,2},{5,3},{6,4},{7,5},{8,6},{9,7},{10,... | collective-permute-start | bytes 589832 | tf_op jit(solution)/shard_map/ppermute | solution.py:20
  105.4 2.3 %collective-permute-start.12 = (bf16[384,256]{1,0:T(8,128)(2,1)S(1)}, bf16[384,256]{1,0:T(8,128)(2,1)S(1)}, u32[]{:S(2)}, u32[]{:S(2)}) collective-permute-start(bf16[384,256]{1,0:T(8,128)(2,1)S(1)} %collective-permute-done.10), channel_id=1, source_target_pairs={{0,2},{1,3},{2,4},{3,5},{4,6},{5,7},{6,8},{7,9},{8,10},{9,11},{10,... | collective-permute-start | bytes 589832 | tf_op jit(solution)/shard_map/ppermute | solution.py:20
  108.3 1.9 collective-permute-start.19
  110.7 4.6 %collective-permute-start.15 = (bf16[384,256]{1,0:T(8,128)(2,1)S(1)}, bf16[384,256]{1,0:T(8,128)(2,1)S(1)}, u32[]{:S(2)}, u32[]{:S(2)}) collective-permute-start(bf16[384,256]{1,0:T(8,128)(2,1)S(1)} %collective-permute-done.13), channel_id=1, source_target_pairs={{0,14},{1,15},{2,0},{3,1},{4,2},{5,3},{6,4},{7,5},{8,6},{9,7},{10,... | collective-permute-start | bytes 589832 | tf_op jit(solution)/shard_map/ppermute | solution.py:20
  115.3 1.9 collective-permute-start.14
  117.5 4.6 %collective-permute-start.22 = (bf16[384,256]{1,0:T(8,128)(2,1)S(1)}, bf16[384,256]{1,0:T(8,128)(2,1)S(1)}, u32[]{:S(2)}, u32[]{:S(2)}) collective-permute-start(bf16[384,256]{1,0:T(8,128)(2,1)S(1)} %collective-permute-done.20), channel_id=1, source_target_pairs={{0,14},{1,15},{2,0},{3,1},{4,2},{5,3},{6,4},{7,5},{8,6},{9,7},{10,... | collective-permute-start | bytes 589832 | tf_op jit(solution)/shard_map/ppermute | solution.py:20
  127.0 4.6 %collective-permute-start.23 = (bf16[384,256]{1,0:T(8,128)(2,1)S(1)}, bf16[384,256]{1,0:T(8,128)(2,1)S(1)}, u32[]{:S(2)}, u32[]{:S(2)}) collective-permute-start(bf16[384,256]{1,0:T(8,128)(2,1)S(1)} %collective-permute-done.22), channel_id=1, source_target_pairs={{0,14},{1,15},{2,0},{3,1},{4,2},{5,3},{6,4},{7,5},{8,6},{9,7},{10,... | collective-permute-start | bytes 589832 | tf_op jit(solution)/shard_map/ppermute | solution.py:20
  134.8 5.6 %collective-permute-start.24 = (f32[128,768]{1,0:T(8,128)S(1)}, f32[128,768]{1,0:T(8,128)S(1)}, u32[]{:S(2)}, u32[]{:S(2)}) collective-permute-start(f32[128,768]{1,0:T(8,128)S(1)} %pad_maximum_fusion.1), channel_id=1, source_target_pairs={{0,1},{1,0},{2,3},{3,2},{4,5},{5,4},{6,7},{7,6},{8,9},{9,8},{10,11... | collective-permute-start | bytes 1179656 | tf_op jit(solution)/shard_map/ppermute | solution.py:25
  141.0 3.3 %collective-permute-start.2 = (bf16[384,256]{1,0:T(8,128)(2,1)S(1)}, bf16[384,256]{1,0:T(8,128)(2,1)S(1)}, u32[]{:S(2)}, u32[]{:S(2)}) collective-permute-start(bf16[384,256]{1,0:T(8,128)(2,1)S(1)} %add_convert_fusion.6), channel_id=1, source_target_pairs={{0,2},{1,3},{2,4},{3,5},{4,6},{5,7},{6,8},{7,9},{8,10},{9,11},{10,... | collective-permute-start | bytes 589832 | tf_op jit(solution)/shard_map/ppermute | solution.py:20
  144.4 4.0 %collective-permute-start.25 = (bf16[64,768]{1,0:T(8,128)(2,1)S(1)}, bf16[64,768]{1,0:T(8,128)(2,1)S(1)}, u32[]{:S(2)}, u32[]{:S(2)}) collective-permute-start(bf16[64,768]{1,0:T(8,128)(2,1)S(1)} %get-tuple-element.3), channel_id=1, source_target_pairs={{0,14},{1,15},{2,0},{3,1},{4,2},{5,3},{6,4},{7,5},{8,6},{9,7},{10,... | collective-permute-start | bytes 294920 | tf_op jit(solution)/shard_map/ppermute | solution.py:20
  151.6 2.0 collective-permute-start.3
  153.7 4.5 %collective-permute-start.26 = (bf16[64,768]{1,0:T(8,128)(2,1)S(1)}, bf16[64,768]{1,0:T(8,128)(2,1)S(1)}, u32[]{:S(2)}, u32[]{:S(2)}) collective-permute-start(bf16[64,768]{1,0:T(8,128)(2,1)S(1)} %collective-permute-done.25), channel_id=1, source_target_pairs={{0,14},{1,15},{2,0},{3,1},{4,2},{5,3},{6,4},{7,5},{8,6},{9,7},{10,... | collective-permute-start | bytes 294920 | tf_op jit(solution)/shard_map/ppermute | solution.py:20
  160.1 4.6 %collective-permute-start.27 = (bf16[64,768]{1,0:T(8,128)(2,1)S(1)}, bf16[64,768]{1,0:T(8,128)(2,1)S(1)}, u32[]{:S(2)}, u32[]{:S(2)}) collective-permute-start(bf16[64,768]{1,0:T(8,128)(2,1)S(1)} %collective-permute-done.26), channel_id=1, source_target_pairs={{0,14},{1,15},{2,0},{3,1},{4,2},{5,3},{6,4},{7,5},{8,6},{9,7},{10,... | collective-permute-start | bytes 294920 | tf_op jit(solution)/shard_map/ppermute | solution.py:20
  166.7 4.6 %collective-permute-done.30 = bf16[64,768]{1,0:T(8,128)(2,1)S(1)} collective-permute-done((bf16[64,768]{1,0:T(8,128)(2,1)S(1)}, bf16[64,768]{1,0:T(8,128)(2,1)S(1)}, u32[]{:S(2)}, u32[]{:S(2)}) %collective-permute-start.30) | collective-permute-done | bytes 98336 | tf_op jit(solution)/shard_map/ppermute | solution.py:20
  173.3 4.6 %collective-permute-done.31 = bf16[64,768]{1,0:T(8,128)(2,1)S(1)} collective-permute-done((bf16[64,768]{1,0:T(8,128)(2,1)S(1)}, bf16[64,768]{1,0:T(8,128)(2,1)S(1)}, u32[]{:S(2)}, u32[]{:S(2)}) %collective-permute-start.31) | collective-permute-done | bytes 98336 | tf_op jit(solution)/shard_map/ppermute | solution.py:20
  177.9 6.5 %collective-permute-start.32 = (bf16[512,768]{1,0:T(8,128)(2,1)S(1)}, bf16[512,768]{1,0:T(8,128)(2,1)S(1)}, u32[]{:S(2)}, u32[]{:S(2)}) collective-permute-start(bf16[512,768]{1,0:T(8,128)(2,1)S(1)} %constant_dynamic-update-slice_fusion.48), channel_id=1, source_target_pairs={{0,1},{1,0},{2,3},{3,2},{4,5},{5,4},{6,7},{7,6},{8,9},{9,8},{10,11... | collective-permute-start | bytes 2359304 | tf_op jit(solution)/shard_map/ppermute | solution.py:25
  188.9 3.4 %collective-permute-start.4 = (bf16[384,256]{1,0:T(8,128)(2,1)S(1)}, bf16[384,256]{1,0:T(8,128)(2,1)}, u32[]{:S(2)}, u32[]{:S(2)}) collective-permute-start(bf16[384,256]{1,0:T(8,128)(2,1)S(1)} %get-tuple-element.8), channel_id=1, source_target_pairs={{0,2},{1,3},{2,4},{3,5},{4,6},{5,7},{6,8},{7,9},{8,10},{9,11},{10,... | collective-permute-start | bytes 589832 | tf_op jit(solution)/shard_map/ppermute | solution.py:20
  193.8 3.4 %collective-permute-start.7 = (bf16[384,256]{1,0:T(8,128)(2,1)S(1)}, bf16[384,256]{1,0:T(8,128)(2,1)}, u32[]{:S(2)}, u32[]{:S(2)}) collective-permute-start(bf16[384,256]{1,0:T(8,128)(2,1)S(1)} %add_convert_fusion.1), channel_id=1, source_target_pairs={{0,14},{1,15},{2,0},{3,1},{4,2},{5,3},{6,4},{7,5},{8,6},{9,7},{10,... | collective-permute-start | bytes 589832 | tf_op jit(solution)/shard_map/ppermute | solution.py:20
  197.7 2.1 fusion.5
  199.8 8.6 %all-to-all-start.1 = ((bf16[32,24,256]{2,1,0:T(8,128)(2,1)}), bf16[32,24,256]{2,1,0:T(8,128)(2,1)S(1)}, u32[]{:S(2)}, u32[]{:S(2)}) async-start(bf16[32,24,256]{2,1,0:T(8,128)(2,1)} %bitcast.64), calls=%async_computation.1 | async-start | bytes 786432 | tf_op jit(solution)/shard_map/all_to_all | solution.py:185
  211.8 4.6 %collective-permute-start.8 = (bf16[384,256]{1,0:T(8,128)(2,1)S(1)}, bf16[384,256]{1,0:T(8,128)(2,1)S(1)}, u32[]{:S(2)}, u32[]{:S(2)}) collective-permute-start(bf16[384,256]{1,0:T(8,128)(2,1)S(1)} %get-tuple-element.7), channel_id=1, source_target_pairs={{0,14},{1,15},{2,0},{3,1},{4,2},{5,3},{6,4},{7,5},{8,6},{9,7},{10,... | collective-permute-start | bytes 589832 | tf_op jit(solution)/shard_map/ppermute | solution.py:20
  (223 shorter events, 91.6 us)
Async XLA Ops:
  7.6 87.8 %collective-permute-start.9 = (bf16[8,128,256]{2,1,0:T(8,128)(2,1)}, bf16[8,128,256]{2,1,0:T(8,128)(2,1)S(1)}, u32[]{:S(2)}, u32[]{:S(2)}) collective-permute-start(bf16[8,128,256]{2,1,0:T(8,128)(2,1)} %get-tuple-element.4), channel_id=1, source_target_pairs={{0,1},{1,0},{2,3},{3,2},{4,5},{5,4},{6,7},{7,6},{8,9},{9,8},{10,11... | collective-permute-start | bytes 1572872 | tf_op jit(solution)/shard_map/ppermute | solution.py:25
  20.9 59.6 %all-to-all-start = ((bf16[32,24,256]{2,1,0:T(8,128)(2,1)}), bf16[32,24,256]{2,1,0:T(8,128)(2,1)S(1)}, u32[]{:S(2)}, u32[]{:S(2)}) async-start(bf16[32,24,256]{2,1,0:T(8,128)(2,1)} %bitcast.232), calls=%async_computation | async-start | bytes 786432 | tf_op jit(solution)/shard_map/all_to_all | solution.py:119
  29.8 47.4 %collective-permute-start = (bf16[15,128]{1,0:T(8,128)(2,1)}, bf16[15,128]{1,0:T(8,128)(2,1)}, u32[]{:S(2)}, u32[]{:S(2)}) collective-permute-start(bf16[15,128]{1,0:T(8,128)(2,1)} %slice.295), channel_id=1, source_target_pairs={{0,16},{16,32},{32,48},{48,64},{64,80},{80,96},{96,112},{112,128},... | collective-permute-start | bytes 11528 | tf_op jit(solution)/shard_map/ppermute | solution.py:15
  80.5 16.8 %collective-permute-start.11 = (bf16[384,256]{1,0:T(8,128)(2,1)S(1)}, bf16[384,256]{1,0:T(8,128)(2,1)S(1)}, u32[]{:S(2)}, u32[]{:S(2)}) collective-permute-start(bf16[384,256]{1,0:T(8,128)(2,1)S(1)} %bitcast.236), channel_id=1, source_target_pairs={{0,14},{1,15},{2,0},{3,1},{4,2},{5,3},{6,4},{7,5},{8,6},{9,7},{10,... | collective-permute-start | bytes 589832 | tf_op jit(solution)/shard_map/ppermute | solution.py:20
  85.6 16.3 %collective-permute-start.18 = (bf16[384,256]{1,0:T(8,128)(2,1)S(1)}, bf16[384,256]{1,0:T(8,128)(2,1)S(1)}, u32[]{:S(2)}, u32[]{:S(2)}) collective-permute-start(bf16[384,256]{1,0:T(8,128)(2,1)S(1)} %bitcast.233), channel_id=1, source_target_pairs={{0,14},{1,15},{2,0},{3,1},{4,2},{5,3},{6,4},{7,5},{8,6},{9,7},{10,... | collective-permute-start | bytes 589832 | tf_op jit(solution)/shard_map/ppermute | solution.py:20
  89.7 51.1 %collective-permute-start.1 = (bf16[384,2048]{1,0:T(8,128)(2,1)S(1)}, bf16[384,2048]{1,0:T(8,128)(2,1)S(1)}, u32[]{:S(2)}, u32[]{:S(2)}) collective-permute-start(bf16[384,2048]{1,0:T(8,128)(2,1)S(1)} %pad_maximum_fusion), channel_id=1, source_target_pairs={{0,1},{1,0},{2,3},{3,2},{4,5},{5,4},{6,7},{7,6},{8,9},{9,8},{10,11... | collective-permute-start | bytes 4718600 | tf_op jit(solution)/shard_map/ppermute | solution.py:25
  93.1 12.4 %collective-permute-start.10 = (bf16[384,256]{1,0:T(8,128)(2,1)S(1)}, bf16[384,256]{1,0:T(8,128)(2,1)S(1)}, u32[]{:S(2)}, u32[]{:S(2)}) collective-permute-start(bf16[384,256]{1,0:T(8,128)(2,1)S(1)} %bitcast.237), channel_id=1, source_target_pairs={{0,2},{1,3},{2,4},{3,5},{4,6},{5,7},{6,8},{7,9},{8,10},{9,11},{10,... | collective-permute-start | bytes 589832 | tf_op jit(solution)/shard_map/ppermute | solution.py:20
  95.4 12.6 %collective-permute-start.17 = (bf16[384,256]{1,0:T(8,128)(2,1)S(1)}, bf16[384,256]{1,0:T(8,128)(2,1)S(1)}, u32[]{:S(2)}, u32[]{:S(2)}) collective-permute-start(bf16[384,256]{1,0:T(8,128)(2,1)S(1)} %bitcast.234), channel_id=1, source_target_pairs={{0,2},{1,3},{2,4},{3,5},{4,6},{5,7},{6,8},{7,9},{8,10},{9,11},{10,... | collective-permute-start | bytes 589832 | tf_op jit(solution)/shard_map/ppermute | solution.py:20
  97.3 13.4 %collective-permute-start.13 = (bf16[384,256]{1,0:T(8,128)(2,1)S(1)}, bf16[384,256]{1,0:T(8,128)(2,1)S(1)}, u32[]{:S(2)}, u32[]{:S(2)}) collective-permute-start(bf16[384,256]{1,0:T(8,128)(2,1)S(1)} %collective-permute-done.11), channel_id=1, source_target_pairs={{0,14},{1,15},{2,0},{3,1},{4,2},{5,3},{6,4},{7,5},{8,6},{9,7},{10,... | collective-permute-start | bytes 589832 | tf_op jit(solution)/shard_map/ppermute | solution.py:20
  101.9 15.6 %collective-permute-start.20 = (bf16[384,256]{1,0:T(8,128)(2,1)S(1)}, bf16[384,256]{1,0:T(8,128)(2,1)S(1)}, u32[]{:S(2)}, u32[]{:S(2)}) collective-permute-start(bf16[384,256]{1,0:T(8,128)(2,1)S(1)} %collective-permute-done.18), channel_id=1, source_target_pairs={{0,14},{1,15},{2,0},{3,1},{4,2},{5,3},{6,4},{7,5},{8,6},{9,7},{10,... | collective-permute-start | bytes 589832 | tf_op jit(solution)/shard_map/ppermute | solution.py:20
  105.4 9.9 %collective-permute-start.12 = (bf16[384,256]{1,0:T(8,128)(2,1)S(1)}, bf16[384,256]{1,0:T(8,128)(2,1)S(1)}, u32[]{:S(2)}, u32[]{:S(2)}) collective-permute-start(bf16[384,256]{1,0:T(8,128)(2,1)S(1)} %collective-permute-done.10), channel_id=1, source_target_pairs={{0,2},{1,3},{2,4},{3,5},{4,6},{5,7},{6,8},{7,9},{8,10},{9,11},{10,... | collective-permute-start | bytes 589832 | tf_op jit(solution)/shard_map/ppermute | solution.py:20
  108.3 14.1 %collective-permute-start.19 = (bf16[384,256]{1,0:T(8,128)(2,1)S(1)}, bf16[384,256]{1,0:T(8,128)(2,1)S(1)}, u32[]{:S(2)}, u32[]{:S(2)}) collective-permute-start(bf16[384,256]{1,0:T(8,128)(2,1)S(1)} %collective-permute-done.17), channel_id=1, source_target_pairs={{0,2},{1,3},{2,4},{3,5},{4,6},{5,7},{6,8},{7,9},{8,10},{9,11},{10,... | collective-permute-start | bytes 589832 | tf_op jit(solution)/shard_map/ppermute | solution.py:20
  110.7 16.0 %collective-permute-start.15 = (bf16[384,256]{1,0:T(8,128)(2,1)S(1)}, bf16[384,256]{1,0:T(8,128)(2,1)S(1)}, u32[]{:S(2)}, u32[]{:S(2)}) collective-permute-start(bf16[384,256]{1,0:T(8,128)(2,1)S(1)} %collective-permute-done.13), channel_id=1, source_target_pairs={{0,14},{1,15},{2,0},{3,1},{4,2},{5,3},{6,4},{7,5},{8,6},{9,7},{10,... | collective-permute-start | bytes 589832 | tf_op jit(solution)/shard_map/ppermute | solution.py:20
  115.3 9.5 %collective-permute-start.14 = (bf16[384,256]{1,0:T(8,128)(2,1)S(1)}, bf16[384,256]{1,0:T(8,128)(2,1)S(1)}, u32[]{:S(2)}, u32[]{:S(2)}) collective-permute-start(bf16[384,256]{1,0:T(8,128)(2,1)S(1)} %collective-permute-done.12), channel_id=1, source_target_pairs={{0,2},{1,3},{2,4},{3,5},{4,6},{5,7},{6,8},{7,9},{8,10},{9,11},{10,... | collective-permute-start | bytes 589832 | tf_op jit(solution)/shard_map/ppermute | solution.py:20
  117.5 9.5 %collective-permute-start.22 = (bf16[384,256]{1,0:T(8,128)(2,1)S(1)}, bf16[384,256]{1,0:T(8,128)(2,1)S(1)}, u32[]{:S(2)}, u32[]{:S(2)}) collective-permute-start(bf16[384,256]{1,0:T(8,128)(2,1)S(1)} %collective-permute-done.20), channel_id=1, source_target_pairs={{0,14},{1,15},{2,0},{3,1},{4,2},{5,3},{6,4},{7,5},{8,6},{9,7},{10,... | collective-permute-start | bytes 589832 | tf_op jit(solution)/shard_map/ppermute | solution.py:20
  122.4 9.8 %collective-permute-start.21 = (bf16[384,256]{1,0:T(8,128)(2,1)S(1)}, bf16[384,256]{1,0:T(8,128)(2,1)S(1)}, u32[]{:S(2)}, u32[]{:S(2)}) collective-permute-start(bf16[384,256]{1,0:T(8,128)(2,1)S(1)} %collective-permute-done.19), channel_id=1, source_target_pairs={{0,2},{1,3},{2,4},{3,5},{4,6},{5,7},{6,8},{7,9},{8,10},{9,11},{10,... | collective-permute-start | bytes 589832 | tf_op jit(solution)/shard_map/ppermute | solution.py:20
  124.8 9.7 %collective-permute-start.16 = (bf16[384,256]{1,0:T(8,128)(2,1)S(1)}, bf16[384,256]{1,0:T(8,128)(2,1)S(1)}, u32[]{:S(2)}, u32[]{:S(2)}) collective-permute-start(bf16[384,256]{1,0:T(8,128)(2,1)S(1)} %collective-permute-done.14), channel_id=1, source_target_pairs={{0,2},{1,3},{2,4},{3,5},{4,6},{5,7},{6,8},{7,9},{8,10},{9,11},{10,... | collective-permute-start | bytes 589832 | tf_op jit(solution)/shard_map/ppermute | solution.py:20
  127.0 7.2 %collective-permute-start.23 = (bf16[384,256]{1,0:T(8,128)(2,1)S(1)}, bf16[384,256]{1,0:T(8,128)(2,1)S(1)}, u32[]{:S(2)}, u32[]{:S(2)}) collective-permute-start(bf16[384,256]{1,0:T(8,128)(2,1)S(1)} %collective-permute-done.22), channel_id=1, source_target_pairs={{0,14},{1,15},{2,0},{3,1},{4,2},{5,3},{6,4},{7,5},{8,6},{9,7},{10,... | collective-permute-start | bytes 589832 | tf_op jit(solution)/shard_map/ppermute | solution.py:20
  134.8 9.5 %collective-permute-start.24 = (f32[128,768]{1,0:T(8,128)S(1)}, f32[128,768]{1,0:T(8,128)S(1)}, u32[]{:S(2)}, u32[]{:S(2)}) collective-permute-start(f32[128,768]{1,0:T(8,128)S(1)} %pad_maximum_fusion.1), channel_id=1, source_target_pairs={{0,1},{1,0},{2,3},{3,2},{4,5},{5,4},{6,7},{7,6},{8,9},{9,8},{10,11... | collective-permute-start | bytes 1179656 | tf_op jit(solution)/shard_map/ppermute | solution.py:25
  141.0 10.6 %collective-permute-start.2 = (bf16[384,256]{1,0:T(8,128)(2,1)S(1)}, bf16[384,256]{1,0:T(8,128)(2,1)S(1)}, u32[]{:S(2)}, u32[]{:S(2)}) collective-permute-start(bf16[384,256]{1,0:T(8,128)(2,1)S(1)} %add_convert_fusion.6), channel_id=1, source_target_pairs={{0,2},{1,3},{2,4},{3,5},{4,6},{5,7},{6,8},{7,9},{8,10},{9,11},{10,... | collective-permute-start | bytes 589832 | tf_op jit(solution)/shard_map/ppermute | solution.py:20
  144.4 9.2 %collective-permute-start.25 = (bf16[64,768]{1,0:T(8,128)(2,1)S(1)}, bf16[64,768]{1,0:T(8,128)(2,1)S(1)}, u32[]{:S(2)}, u32[]{:S(2)}) collective-permute-start(bf16[64,768]{1,0:T(8,128)(2,1)S(1)} %get-tuple-element.3), channel_id=1, source_target_pairs={{0,14},{1,15},{2,0},{3,1},{4,2},{5,3},{6,4},{7,5},{8,6},{9,7},{10,... | collective-permute-start | bytes 294920 | tf_op jit(solution)/shard_map/ppermute | solution.py:20
  148.5 9.7 %collective-permute-start.28 = (bf16[64,768]{1,0:T(8,128)(2,1)S(1)}, bf16[64,768]{1,0:T(8,128)(2,1)S(1)}, u32[]{:S(2)}, u32[]{:S(2)}) collective-permute-start(bf16[64,768]{1,0:T(8,128)(2,1)S(1)} %get-tuple-element.3), channel_id=1, source_target_pairs={{0,2},{1,3},{2,4},{3,5},{4,6},{5,7},{6,8},{7,9},{8,10},{9,11},{10,... | collective-permute-start | bytes 294920 | tf_op jit(solution)/shard_map/ppermute | solution.py:20
  151.6 33.6 %collective-permute-start.3 = (bf16[384,256]{1,0:T(8,128)(2,1)S(1)}, bf16[384,256]{1,0:T(8,128)(2,1)S(1)}, u32[]{:S(2)}, u32[]{:S(2)}) collective-permute-start(bf16[384,256]{1,0:T(8,128)(2,1)S(1)} %add_convert_fusion.5), channel_id=1, source_target_pairs={{0,2},{1,3},{2,4},{3,5},{4,6},{5,7},{6,8},{7,9},{8,10},{9,11},{10,... | collective-permute-start | bytes 589832 | tf_op jit(solution)/shard_map/ppermute | solution.py:20
  158.2 6.6 %collective-permute-start.29 = (bf16[64,768]{1,0:T(8,128)(2,1)S(1)}, bf16[64,768]{1,0:T(8,128)(2,1)S(1)}, u32[]{:S(2)}, u32[]{:S(2)}) collective-permute-start(bf16[64,768]{1,0:T(8,128)(2,1)S(1)} %collective-permute-done.28), channel_id=1, source_target_pairs={{0,2},{1,3},{2,4},{3,5},{4,6},{5,7},{6,8},{7,9},{8,10},{9,11},{10,... | collective-permute-start | bytes 294920 | tf_op jit(solution)/shard_map/ppermute | solution.py:20
  160.1 13.1 %collective-permute-start.27 = (bf16[64,768]{1,0:T(8,128)(2,1)S(1)}, bf16[64,768]{1,0:T(8,128)(2,1)S(1)}, u32[]{:S(2)}, u32[]{:S(2)}) collective-permute-start(bf16[64,768]{1,0:T(8,128)(2,1)S(1)} %collective-permute-done.26), channel_id=1, source_target_pairs={{0,14},{1,15},{2,0},{3,1},{4,2},{5,3},{6,4},{7,5},{8,6},{9,7},{10,... | collective-permute-start | bytes 294920 | tf_op jit(solution)/shard_map/ppermute | solution.py:20
  177.9 19.3 %collective-permute-start.32 = (bf16[512,768]{1,0:T(8,128)(2,1)S(1)}, bf16[512,768]{1,0:T(8,128)(2,1)S(1)}, u32[]{:S(2)}, u32[]{:S(2)}) collective-permute-start(bf16[512,768]{1,0:T(8,128)(2,1)S(1)} %constant_dynamic-update-slice_fusion.48), channel_id=1, source_target_pairs={{0,1},{1,0},{2,3},{3,2},{4,5},{5,4},{6,7},{7,6},{8,9},{9,8},{10,11... | collective-permute-start | bytes 2359304 | tf_op jit(solution)/shard_map/ppermute | solution.py:25
  185.4 8.3 %collective-permute-start.6 = (bf16[384,256]{1,0:T(8,128)(2,1)S(1)}, bf16[384,256]{1,0:T(8,128)(2,1)S(1)}, u32[]{:S(2)}, u32[]{:S(2)}) collective-permute-start(bf16[384,256]{1,0:T(8,128)(2,1)S(1)} %get-tuple-element.9), channel_id=1, source_target_pairs={{0,14},{1,15},{2,0},{3,1},{4,2},{5,3},{6,4},{7,5},{8,6},{9,7},{10,... | collective-permute-start | bytes 589832 | tf_op jit(solution)/shard_map/ppermute | solution.py:20
  188.9 19.6 %collective-permute-start.4 = (bf16[384,256]{1,0:T(8,128)(2,1)S(1)}, bf16[384,256]{1,0:T(8,128)(2,1)}, u32[]{:S(2)}, u32[]{:S(2)}) collective-permute-start(bf16[384,256]{1,0:T(8,128)(2,1)S(1)} %get-tuple-element.8), channel_id=1, source_target_pairs={{0,2},{1,3},{2,4},{3,5},{4,6},{5,7},{6,8},{7,9},{8,10},{9,11},{10,... | collective-permute-start | bytes 589832 | tf_op jit(solution)/shard_map/ppermute | solution.py:20
  193.8 14.7 %collective-permute-start.7 = (bf16[384,256]{1,0:T(8,128)(2,1)S(1)}, bf16[384,256]{1,0:T(8,128)(2,1)}, u32[]{:S(2)}, u32[]{:S(2)}) collective-permute-start(bf16[384,256]{1,0:T(8,128)(2,1)S(1)} %add_convert_fusion.1), channel_id=1, source_target_pairs={{0,14},{1,15},{2,0},{3,1},{4,2},{5,3},{6,4},{7,5},{8,6},{9,7},{10,... | collective-permute-start | bytes 589832 | tf_op jit(solution)/shard_map/ppermute | solution.py:20
  199.8 22.5 %all-to-all-start.1 = ((bf16[32,24,256]{2,1,0:T(8,128)(2,1)}), bf16[32,24,256]{2,1,0:T(8,128)(2,1)S(1)}, u32[]{:S(2)}, u32[]{:S(2)}) async-start(bf16[32,24,256]{2,1,0:T(8,128)(2,1)} %bitcast.64), calls=%async_computation.1 | async-start | bytes 786432 | tf_op jit(solution)/shard_map/all_to_all | solution.py:185
  209.9 8.4 %collective-permute-start.5 = (bf16[384,256]{1,0:T(8,128)(2,1)S(1)}, bf16[384,256]{1,0:T(8,128)(2,1)S(1)}, u32[]{:S(2)}, u32[]{:S(2)}) collective-permute-start(bf16[384,256]{1,0:T(8,128)(2,1)S(1)} %get-tuple-element.6), channel_id=1, source_target_pairs={{0,2},{1,3},{2,4},{3,5},{4,6},{5,7},{6,8},{7,9},{8,10},{9,11},{10,... | collective-permute-start | bytes 589832 | tf_op jit(solution)/shard_map/ppermute | solution.py:20
  211.8 7.2 %collective-permute-start.8 = (bf16[384,256]{1,0:T(8,128)(2,1)S(1)}, bf16[384,256]{1,0:T(8,128)(2,1)S(1)}, u32[]{:S(2)}, u32[]{:S(2)}) collective-permute-start(bf16[384,256]{1,0:T(8,128)(2,1)S(1)} %get-tuple-element.7), channel_id=1, source_target_pairs={{0,14},{1,15},{2,0},{3,1},{4,2},{5,3},{6,4},{7,5},{8,6},{9,7},{10,... | collective-permute-start | bytes 589832 | tf_op jit(solution)/shard_map/ppermute | solution.py:20
  (37 other events, 368.6 us)

commit v2 on v1

--- a/solution.py
+++ b/solution.py
@@ -1,6 +1,8 @@
 import jax
 import jax.numpy as jnp
 from jax import lax
+from jax.experimental import pallas as pl
+from jax.experimental.pallas import tpu as pltpu
 from jax.sharding import PartitionSpec as P
 
 windows = (2, 4, 8, 16)
@@ -27,6 +29,69 @@
 
 def tdot(a, b):
     return lax.dot_general(a, b, (((1,), (1,)), ((), ())), preferred_element_type=f32)
+
+
+def gate_up_kernel(index, gate_own, up_own, gate_out, up_out, own, out):
+    units = gate_own.shape[0]
+    own[0, :units] = gate_own[...]
+    own[0, units:] = up_own[...]
+    out[0, :units] = gate_out[...]
+    out[0, units:] = up_out[...]
+
+
+def gate_up_blocks(index, gate_t, up_t, slice_width):
+    units = gate_t.shape[0]
+    count = index.shape[1]
+    block = (units, slice_width)
+    own = pl.BlockSpec(block, lambda j, index: (0, index[0, j]))
+    out = pl.BlockSpec(block, lambda j, index: (0, index[1, j]))
+    result = pl.BlockSpec((1, 2 * units, slice_width), lambda j, index: (j, 0, 0))
+    shape = jax.ShapeDtypeStruct((count, 2 * units, slice_width), bf16)
+    return pl.pallas_call(
+        gate_up_kernel,
+        grid_spec=pltpu.PrefetchScalarGridSpec(
+            num_scalar_prefetch=1, grid=(count,), in_specs=[own, own, out, out], out_specs=[result, result]
+        ),
+        out_shape=[shape, shape],
+    )(index, gate_t, up_t, gate_t, up_t)
+
+
+def project_kernel(index, group, hidden, proj_own, proj_out, down_own, down_out, own, out):
+    rows = group.shape[0]
+    for proj, down, to in ((proj_own, down_own, own), (proj_out, down_out, out)):
+        to[0, :rows] = jnp.dot(group[...], proj[...], preferred_element_type=f32).astype(bf16)
+        to[0, rows:] = jnp.dot(hidden[...], down[...], preferred_element_type=f32).astype(bf16)
+
+
+def projected_blocks(index, group_out, shared_hidden, out_proj, shared_down, slice_width):
+    count = index.shape[1]
+    rows = group_out.shape[0] + shared_hidden.shape[0]
+
+    def whole(a):
+        return pl.BlockSpec(a.shape, lambda j, index: (0, 0))
+
+    def columns(a, side):
+        return pl.BlockSpec((a.shape[0], slice_width), lambda j, index: (0, index[side, j]))
+
+    result = pl.BlockSpec((1, rows, slice_width), lambda j, index: (j, 0, 0))
+    shape = jax.ShapeDtypeStruct((count, rows, slice_width), bf16)
+    return pl.pallas_call(
+        project_kernel,
+        grid_spec=pltpu.PrefetchScalarGridSpec(
+            num_scalar_prefetch=1,
+            grid=(count,),
+            in_specs=[
+                whole(group_out),
+                whole(shared_hidden),
+                columns(out_proj, 0),
+                columns(out_proj, 1),
+                columns(shared_down, 0),
+                columns(shared_down, 1),
+            ],
+            out_specs=[result, result],
+        ),
+        out_shape=[shape, shape],
+    )(index, group_out, shared_hidden, out_proj, out_proj, shared_down, shared_down)
 
 
 def pool_group_out(pool_input, earlier_rows, pool_map, pool_scale, tp_rank, ep_rank):
@@ -111,78 +176,64 @@
     mean = jnp.mean(values, axis=1, keepdims=True)
     centre = values - mean
     rstd = lax.rsqrt(jnp.mean(centre * centre, axis=1, keepdims=True) + eps)
-    at = tp_rank * slice_width
-    mine = lax.dynamic_slice_in_dim(moe_input, at, slice_width, 1).astype(f32)
-    my_gain = lax.dynamic_slice_in_dim(norm_gain, at, slice_width, 0)
-    normed_slice = ((mine - mean) * rstd * my_gain[None, :]).astype(bf16)
-    outgoing = jnp.dot(placing, normed_slice, preferred_element_type=f32).astype(bf16)
-    arrived = lax.all_to_all(outgoing, "ep", split_axis=0, concat_axis=0, tiled=True)
-
-    gate_up = jnp.concatenate([expert_gate[0].T, expert_up[0].T], axis=0)
-    hid = gate_up.shape[0]
-
-    def feature_slices(side):
-        pieces = []
-        for j in range(y_size):
-            lo = 2 * j * slice_width
-            even = gate_up[:, lo : lo + slice_width]
-            odd = gate_up[:, lo + slice_width : lo + 2 * slice_width]
-            pieces.append(jnp.where(side == 0, even, odd))
-        return jnp.stack(pieces)
-
-    own_weights = feature_slices(core)
-    partner_weights = to_partner(feature_slices(1 - core))
-    weights = jnp.concatenate([own_weights, partner_weights], axis=1)
-
-    def product(rows, offset):
-        w = lax.dynamic_index_in_dim(weights, (y + offset) % y_size, 0, keepdims=False)
-        return tdot(w, rows)
-
-    half = buffer_len // 2
-    sums = []
-    ups = [rows for rows in (arrived[:half], arrived[half:])]
-    downs = list(ups)
-    sums = [product(rows, 0) for rows in ups]
-    reach_up = (y_size // 2, y_size // 2 - 1)
-    for step in range(1, y_size // 2 + 1):
-        for h in range(2):
-            if step <= reach_up[h]:
-                ups[h] = along_y(ups[h], 1)
-                sums[h] = sums[h] + product(ups[h], -step)
-            if step <= reach_up[1 - h]:
-                downs[h] = along_y(downs[h], -1)
-                sums[h] = sums[h] + product(downs[h], step)
-    partial = jnp.concatenate(sums, axis=1)
-    full = partial[:hid] + to_partner(partial[hid:])
-    units = hid // 2
+
+    def outgoing(far):
+        at = (((y + far) % y_size) * 2 + core) * slice_width
+        mine = lax.dynamic_slice_in_dim(moe_input, at, slice_width, 1).astype(f32)
+        gain = lax.dynamic_slice_in_dim(norm_gain, at, slice_width, 0)
+        normed_slice = ((mine - mean) * rstd * gain[None, :]).astype(bf16)
+        return jnp.dot(placing, normed_slice, preferred_element_type=f32).astype(bf16)
+
+    def exchanged(rows):
+        return lax.all_to_all(rows, "ep", split_axis=0, concat_axis=0, tiled=True)
+
+    near = exchanged(outgoing(0))
+    far = exchanged(outgoing(y_size // 2))
+
+    turn = (y + jnp.arange(y_size, dtype=jnp.int32)) % y_size
+    index = jnp.stack([turn * 2 + core, turn * 2 + 1 - core]).astype(jnp.int32)
+    own_weights, to_send = gate_up_blocks(index, expert_gate[0].T, expert_up[0].T, slice_width)
+    partner_weights = to_partner(to_send)
+    units = expert_gate.shape[2]
+
+    sums = [0.0, 0.0]
+
+    def add_product(rows, j):
+        sums[0] = sums[0] + tdot(own_weights[j % y_size], rows)
+        sums[1] = sums[1] + tdot(partner_weights[j % y_size], rows)
+
+    up = along_y(near, 1)
+    down = along_y(near, -1)
+    add_product(near, 0)
+    up_two = along_y(up, 1)
+    down_two = along_y(down, -1)
+    add_product(up, -1)
+    add_product(down, 1)
+    up_far = along_y(far, 1)
+    down_far = along_y(far, -1)
+    add_product(far, 4)
+    add_product(up_two, -2)
+    add_product(down_two, 2)
+    add_product(up_far, 3)
+    add_product(down_far, -3)
+    full = sums[0] + to_partner(sums[1])
     hidden = (jax.nn.silu(full[:units]) * full[units:]).astype(bf16)
 
-    order = [None] * y_size
-    order[0] = hidden
-    up = down = hidden
-    for step in range(1, y_size // 2 + 1):
-        up = along_y(up, 1)
-        order[y_size - step] = up
-        if step < y_size // 2:
-            down = along_y(down, -1)
-            order[step] = down
-    own_hidden = jnp.concatenate(order, axis=0)
+    copies = jnp.broadcast_to(hidden[None], (y_size, *hidden.shape))
+    groups = [[2 * i + c for i in range(y_size)] for c in range(2)]
+    own_hidden = lax.all_to_all(copies, "tp", 0, 0, axis_index_groups=groups, tiled=True)
     other_hidden = to_partner(own_hidden)
     down_weight = expert_down[0].reshape(y_size, 2, units, slice_width)
 
-    def down_rows(side):
-        pieces = []
-        for j in range(y_size):
-            block = lax.dynamic_index_in_dim(down_weight, (y + j) % y_size, 0, keepdims=False)
-            pieces.append(jnp.where(side == 0, block[0], block[1]))
-        return jnp.concatenate(pieces, axis=0)
-
-    def down_product(h, w):
-        return lax.dot_general(h, w, (((0,), (0,)), ((), ())), preferred_element_type=f32)
-
-    expert_result = down_product(own_hidden, down_rows(core))
-    expert_result = expert_result + down_product(other_hidden, down_rows(1 - core))
-    returned = lax.all_to_all(expert_result.astype(bf16), "ep", split_axis=0, concat_axis=0, tiled=True)
+    def down_product(h, side):
+        w = lax.dynamic_index_in_dim(down_weight, side, 1, keepdims=False)
+        w = w.reshape(y_size * units, slice_width)
+        return lax.dot_general(
+            h.reshape(y_size * units, buffer_len), w, (((0,), (0,)), ((), ())), preferred_element_type=f32
+        )
+
+    expert_result = down_product(own_hidden, core) + down_product(other_hidden, 1 - core)
+    returned = exchanged(expert_result.astype(bf16))
     routed = lax.dot_general(combine, returned, (((0,), (0,)), ((), ())), preferred_element_type=f32)
 
     group_out = pool_group_out(pool_input, earlier_rows, pool_map, pool_scale, tp_rank, ep_rank)
@@ -191,24 +242,11 @@
     shared_up_val = jnp.dot(normed, shared_up, preferred_element_type=f32)
     shared_hidden = (jax.nn.silu(shared_gate_val) * shared_up_val).astype(bf16)
 
-    def columns(weight, side):
-        pieces = []
-        for j in range(y_size):
-            begin = (((y + j) % y_size) * 2 + side) * slice_width
-            pieces.append(lax.dynamic_slice_in_dim(weight, begin, slice_width, 1))
-        return jnp.concatenate(pieces, axis=1)
-
-    def projected(side):
-        top = jnp.dot(group_out, columns(out_proj, side), preferred_element_type=f32)
-        bottom = jnp.dot(shared_hidden, columns(shared_down, side), preferred_element_type=f32)
-        return jnp.concatenate([top.astype(bf16), bottom.astype(bf16)], axis=0)
-
-    from_partner = to_partner(projected(1 - core))
-    kept = projected(core)
+    kept, sent = projected_blocks(index, group_out, shared_hidden, out_proj, shared_down, slice_width)
+    from_partner = to_partner(sent)
 
     def part(j):
-        lo = j * slice_width
-        return kept[:, lo : lo + slice_width].astype(f32) + from_partner[:, lo : lo + slice_width].astype(f32)
+        return kept[j].astype(f32) + from_partner[j].astype(f32)
 
     up = down = None
     for step in range(y_size // 2):

time: 226 us -> 185 us (0.82)
  the two profiles are of different devices: /device:TPU:1 before, /device:TPU:8 now
where the time goes in v2:
time: 185 us; the launch traced here: 182 us
  starting transfers between devices  92.7 us (50%)
  waiting for transfers between devices  40.4 us (22%)
  matrix products  19.7 us (11%)
  Pallas kernels  12.7 us (7%)
  other arithmetic  11.9 us (6%)
  local copies, waits for them, and re-layouts  3.53 us (2%)
    ppermute x13, starting transfers between devices, along_y(): return lax.ppermute(x, 'tp', [(i, (i + 2 * step) % n) for i in range(n)])  41.7 us
    ppermute x13, waiting for transfers between devices, along_y(): return lax.ppermute(x, 'tp', [(i, (i + 2 * step) % n) for i in range(n)])  35.5 us
    all_to_all x3, starting transfers between devices, exchanged(): return lax.all_to_all(rows, 'ep', split_axis=0, concat_axis=0, tiled=True)  30.8 us
    dot_general x16, matrix products, tdot(): lax.dot_general(a, b, (((1,), (1,)), ((), ())), preferred_element_type=f32)  11.3 us
    all_to_all x1, starting transfers between devices, per_device(): lax.all_to_all(copies, 'tp', 0, 0, axis_index_groups=groups, tiled=True)  8.67 us
    ppermute x4, starting transfers between devices, to_partner(): return lax.ppermute(x, 'tp', [(i, i ^ 1) for i in range(n)])  7.79 us
    pallas_call x1, Pallas kernels, projected_blocks(): pl.pallas_call(project_kernel, grid_spec=pltpu.PrefetchScalarGridSpec(num...  7.16 us
    convert_element_type x4, other arithmetic, per_device(): up = along_y(up.astype(bf16), 1)  6.65 us
  transfers between devices with their start and end apart: 22, of which 10 were waited for; matrix products, arithmetic and copies ran while one was open for 16% of the time, Pallas kernels for 7%

profile of v2, /device:TPU:8, one launch (start us, length us, event | category | flops | bytes accessed | tf_op | source)
XLA Modules:
  0.0 182.2 jit_solution(10387732435922981822)
XLA Ops:
  5.1 13.3 %all-to-all-start = ((bf16[32,24,256]{2,1,0:T(8,128)(2,1)}), bf16[32,24,256]{2,1,0:T(8,128)(2,1)S(1)}, u32[]{:S(2)}, u32[]{:S(2)}) async-start(bf16[32,24,256]{2,1,0:T(8,128)(2,1)} %bitcast.28), calls=%async_computation | async-start | bytes 786432 | tf_op jit(solution)/shard_map/all_to_all | solution.py:188
  19.1 5.5 %shard_map.150 = (bf16[8,128,256]{2,1,0:T(8,128)(2,1)}, bf16[8,128,256]{2,1,0:T(8,128)(2,1)}) custom-call(s32[2,8]{1,0:T(2,128)} %pad_add_fusion.index, bf16[64,4096]{1,0:T(8,128)(2,1)} %bitcast.165, bf16[64,4096]{1,0:T(8,128)(2,1)} %bitcast.167, bf16[64,4096]{1,0:T(8,128)(2,1)} %bitcast.166, bf16[64,4096]{1,0:T(8,128)(2,1)} %bitcast.168), custom_call_target="tpu_custom_call" | custom-call | tf_op jit(solution)/shard_map/pallas_call | solution.py:50
  24.6 2.0 %collective-permute-start.15 = (bf16[8,128,256]{2,1,0:T(8,128)(2,1)}, bf16[8,128,256]{2,1,0:T(8,128)(2,1)}, u32[]{:S(2)}, u32[]{:S(2)}) collective-permute-start(bf16[8,128,256]{2,1,0:T(8,128)(2,1)} %get-tuple-element.9), channel_id=1, source_target_pairs={{0,1},{1,0},{2,3},{3,2},{4,5},{5,4},{6,7},{7,6},{8,9},{9,8},{10,11... | collective-permute-start | bytes 1572872 | tf_op jit(solution)/shard_map/ppermute | solution.py:27
  26.6 3.7 %collective-permute-start = (bf16[15,128]{1,0:T(8,128)(2,1)S(1)}, bf16[15,128]{1,0:T(8,128)(2,1)S(1)}, u32[]{:S(2)}, u32[]{:S(2)}) collective-permute-start(bf16[15,128]{1,0:T(8,128)(2,1)S(1)} %slice.181), channel_id=1, source_target_pairs={{0,16},{16,32},{32,48},{48,64},{64,80},{80,96},{96,112},{112,128},... | collective-permute-start | bytes 11528 | tf_op jit(solution)/shard_map/ppermute | solution.py:17
  33.7 7.7 %all-to-all-start.1 = ((bf16[32,24,256]{2,1,0:T(8,128)(2,1)}), bf16[32,24,256]{2,1,0:T(8,128)(2,1)S(1)}, u32[]{:S(2)}, u32[]{:S(2)}) async-start(bf16[32,24,256]{2,1,0:T(8,128)(2,1)} %bitcast.33), calls=%async_computation.1 | async-start | bytes 786432 | tf_op jit(solution)/shard_map/all_to_all | solution.py:188
  44.4 7.2 %shard_map.149 = (bf16[8,384,256]{2,1,0:T(8,128)(2,1)}, bf16[8,384,256]{2,1,0:T(8,128)(2,1)}) custom-call(s32[2,8]{1,0:T(2,128)} %pad_add_fusion.index, bf16[256,128]{1,0:T(8,128)(2,1)} %fusion.17.group, bf16[128,32]{1,0:T(8,128)(2,1)} %fusion.18.hidden, bf16[128,4096]{1,0:T(8,128)(2,1)} %proj_out.1, bf16[128,4096]{1,0:T(8,128)(2,1)} %proj_out.1, ...), custom_call_target="tpu_custom_call" | custom-call | tf_op jit(solution)/shard_map/pallas_call | solution.py:78
  51.5 1.9 %collective-permute-start.1 = (bf16[8,384,256]{2,1,0:T(8,128)(2,1)}, bf16[8,384,256]{2,1,0:T(8,128)(2,1)}, u32[]{:S(2)}, u32[]{:S(2)}) collective-permute-start(bf16[8,384,256]{2,1,0:T(8,128)(2,1)} %get-tuple-element.7), channel_id=1, source_target_pairs={{0,1},{1,0},{2,3},{3,2},{4,5},{5,4},{6,7},{7,6},{8,9},{9,8},{10,11... | collective-permute-start | bytes 4718600 | tf_op jit(solution)/shard_map/ppermute | solution.py:27
  53.5 3.5 %collective-permute-start.9 = (bf16[768,256]{1,0:T(8,128)(2,1)S(1)}, bf16[768,256]{1,0:T(8,128)(2,1)S(1)}, u32[]{:S(2)}, u32[]{:S(2)}) collective-permute-start(bf16[768,256]{1,0:T(8,128)(2,1)S(1)} %bitcast.160), channel_id=1, source_target_pairs={{0,2},{1,3},{2,4},{3,5},{4,6},{5,7},{6,8},{7,9},{8,10},{9,11},{10,... | collective-permute-start | bytes 1179656 | tf_op jit(solution)/shard_map/ppermute | solution.py:22
  57.0 2.4 %collective-permute-start.10 = (bf16[768,256]{1,0:T(8,128)(2,1)S(1)}, bf16[768,256]{1,0:T(8,128)(2,1)S(1)}, u32[]{:S(2)}, u32[]{:S(2)}) collective-permute-start(bf16[768,256]{1,0:T(8,128)(2,1)S(1)} %bitcast.161), channel_id=1, source_target_pairs={{0,14},{1,15},{2,0},{3,1},{4,2},{5,3},{6,4},{7,5},{8,6},{9,7},{10,... | collective-permute-start | bytes 1179656 | tf_op jit(solution)/shard_map/ppermute | solution.py:22
  59.3 3.8 %collective-permute-start.14 = (bf16[768,256]{1,0:T(8,128)(2,1)S(1)}, bf16[768,256]{1,0:T(8,128)(2,1)S(1)}, u32[]{:S(2)}, u32[]{:S(2)}) collective-permute-start(bf16[768,256]{1,0:T(8,128)(2,1)S(1)} %bitcast.156), channel_id=1, source_target_pairs={{0,14},{1,15},{2,0},{3,1},{4,2},{5,3},{6,4},{7,5},{8,6},{9,7},{10,... | collective-permute-start | bytes 1179656 | tf_op jit(solution)/shard_map/ppermute | solution.py:22
  63.8 2.0 %collective-permute-start.13 = (bf16[768,256]{1,0:T(8,128)(2,1)S(1)}, bf16[768,256]{1,0:T(8,128)(2,1)S(1)}, u32[]{:S(2)}, u32[]{:S(2)}) collective-permute-start(bf16[768,256]{1,0:T(8,128)(2,1)S(1)} %bitcast.158), channel_id=1, source_target_pairs={{0,2},{1,3},{2,4},{3,5},{4,6},{5,7},{6,8},{7,9},{8,10},{9,11},{10,... | collective-permute-start | bytes 1179656 | tf_op jit(solution)/shard_map/ppermute | solution.py:22
  66.9 3.9 %collective-permute-done.10 = bf16[768,256]{1,0:T(8,128)(2,1)S(1)} collective-permute-done((bf16[768,256]{1,0:T(8,128)(2,1)S(1)}, bf16[768,256]{1,0:T(8,128)(2,1)S(1)}, u32[]{:S(2)}, u32[]{:S(2)}) %collective-permute-start.10) | collective-permute-done | bytes 393248 | tf_op jit(solution)/shard_map/ppermute | solution.py:22
  70.8 2.3 %collective-permute-start.12 = (bf16[768,256]{1,0:T(8,128)(2,1)S(1)}, bf16[768,256]{1,0:T(8,128)(2,1)S(1)}, u32[]{:S(2)}, u32[]{:S(2)}) collective-permute-start(bf16[768,256]{1,0:T(8,128)(2,1)S(1)} %collective-permute-done.10), channel_id=1, source_target_pairs={{0,14},{1,15},{2,0},{3,1},{4,2},{5,3},{6,4},{7,5},{8,6},{9,7},{10,... | collective-permute-start | bytes 1179656 | tf_op jit(solution)/shard_map/ppermute | solution.py:22
  74.3 3.8 %collective-permute-start.11 = (bf16[768,256]{1,0:T(8,128)(2,1)S(1)}, bf16[768,256]{1,0:T(8,128)(2,1)S(1)}, u32[]{:S(2)}, u32[]{:S(2)}) collective-permute-start(bf16[768,256]{1,0:T(8,128)(2,1)S(1)} %collective-permute-done.9), channel_id=1, source_target_pairs={{0,2},{1,3},{2,4},{3,5},{4,6},{5,7},{6,8},{7,9},{8,10},{9,11},{10,... | collective-permute-start | bytes 1179656 | tf_op jit(solution)/shard_map/ppermute | solution.py:22
  83.6 3.4 %collective-permute-done.12 = bf16[768,256]{1,0:T(8,128)(2,1)S(1)} collective-permute-done((bf16[768,256]{1,0:T(8,128)(2,1)S(1)}, bf16[768,256]{1,0:T(8,128)(2,1)S(1)}, u32[]{:S(2)}, u32[]{:S(2)}) %collective-permute-start.12) | collective-permute-done | bytes 393248 | tf_op jit(solution)/shard_map/ppermute | solution.py:22
  89.2 1.9 %collective-permute-start.16 = (f32[128,768]{1,0:T(8,128)S(1)}, f32[128,768]{1,0:T(8,128)S(1)}, u32[]{:S(2)}, u32[]{:S(2)}) collective-permute-start(f32[128,768]{1,0:T(8,128)S(1)} %fusion.15), channel_id=1, source_target_pairs={{0,1},{1,0},{2,3},{3,2},{4,5},{5,4},{6,7},{7,6},{8,9},{9,8},{10,11... | collective-permute-start | bytes 1179656 | tf_op jit(solution)/shard_map/ppermute | solution.py:27
  94.2 8.7 %all-to-all-start.2 = ((bf16[8,64,768]{2,1,0:T(8,128)(2,1)}), bf16[8,64,768]{2,1,0:T(8,128)(2,1)S(1)}, u32[]{:S(2)}, u32[]{:S(2)}) async-start(bf16[8,64,768]{2,1,0:T(8,128)(2,1)} %broadcast_in_dim.89), calls=%async_computation.2 | async-start | bytes 1572864 | tf_op jit(solution)/shard_map/all_to_all | solution.py:224
  102.8 1.9 %fusion.25 = (bf16[384,256]{1,0:T(8,128)(2,1)S(1)}, bf16[384,256]{1,0:T(8,128)(2,1)}) fusion(bf16[8,384,256]{2,1,0:T(8,128)(2,1)} %collective-permute-done.1, bf16[8,384,256]{2,1,0:T(8,128)(2,1)S(1)} %copy-done.2), kind=kLoop, calls=%fused_computation.65 | loop fusion | flops 786432 | bytes 1179648 | tf_op jit(solution)/shard_map/convert_element_type | solution.py:255
  104.7 3.4 %collective-permute-start.2 = (bf16[384,256]{1,0:T(8,128)(2,1)S(1)}, bf16[384,256]{1,0:T(8,128)(2,1)S(1)}, u32[]{:S(2)}, u32[]{:S(2)}) collective-permute-start(bf16[384,256]{1,0:T(8,128)(2,1)S(1)} %get-tuple-element.12), channel_id=1, source_target_pairs={{0,2},{1,3},{2,4},{3,5},{4,6},{5,7},{6,8},{7,9},{8,10},{9,11},{10,... | collective-permute-start | bytes 589832 | tf_op jit(solution)/shard_map/ppermute | solution.py:22
  108.1 16.8 %collective-permute-done.2 = bf16[384,256]{1,0:T(8,128)(2,1)S(1)} collective-permute-done((bf16[384,256]{1,0:T(8,128)(2,1)S(1)}, bf16[384,256]{1,0:T(8,128)(2,1)S(1)}, u32[]{:S(2)}, u32[]{:S(2)}) %collective-permute-start.2) | collective-permute-done | bytes 196640 | tf_op jit(solution)/shard_map/ppermute | solution.py:22
  126.5 3.4 %collective-permute-start.3 = (bf16[384,256]{1,0:T(8,128)(2,1)}, bf16[384,256]{1,0:T(8,128)(2,1)}, u32[]{:S(2)}, u32[]{:S(2)}) collective-permute-start(bf16[384,256]{1,0:T(8,128)(2,1)} %fusion.21), channel_id=1, source_target_pairs={{0,2},{1,3},{2,4},{3,5},{4,6},{5,7},{6,8},{7,9},{8,10},{9,11},{10,... | collective-permute-start | bytes 589832 | tf_op jit(solution)/shard_map/ppermute | solution.py:22
  129.9 3.4 %collective-permute-start.6 = (bf16[384,256]{1,0:T(8,128)(2,1)}, bf16[384,256]{1,0:T(8,128)(2,1)}, u32[]{:S(2)}, u32[]{:S(2)}) collective-permute-start(bf16[384,256]{1,0:T(8,128)(2,1)} %get-tuple-element.13), channel_id=1, source_target_pairs={{0,14},{1,15},{2,0},{3,1},{4,2},{5,3},{6,4},{7,5},{8,6},{9,7},{10,... | collective-permute-start | bytes 589832 | tf_op jit(solution)/shard_map/ppermute | solution.py:22
  133.3 1.9 %collective-permute-start.17 = (bf16[8,64,768]{2,1,0:T(8,128)(2,1)S(1)}, bf16[8,64,768]{2,1,0:T(8,128)(2,1)}, u32[]{:S(2)}, u32[]{:S(2)}) collective-permute-start(bf16[8,64,768]{2,1,0:T(8,128)(2,1)S(1)} %all-to-all-done.2), channel_id=1, source_target_pairs={{0,1},{1,0},{2,3},{3,2},{4,5},{5,4},{6,7},{7,6},{8,9},{9,8},{10,11... | collective-permute-start | bytes 2359304 | tf_op jit(solution)/shard_map/ppermute | solution.py:27
  137.6 3.1 %collective-permute-start.4 = (bf16[384,256]{1,0:T(8,128)(2,1)}, bf16[384,256]{1,0:T(8,128)(2,1)}, u32[]{:S(2)}, u32[]{:S(2)}) collective-permute-start(bf16[384,256]{1,0:T(8,128)(2,1)} %fusion.22), channel_id=1, source_target_pairs={{0,2},{1,3},{2,4},{3,5},{4,6},{5,7},{6,8},{7,9},{8,10},{9,11},{10,... | collective-permute-start | bytes 589832 | tf_op jit(solution)/shard_map/ppermute | solution.py:22
  140.8 7.2 %collective-permute-done.4 = bf16[384,256]{1,0:T(8,128)(2,1)} collective-permute-done((bf16[384,256]{1,0:T(8,128)(2,1)}, bf16[384,256]{1,0:T(8,128)(2,1)}, u32[]{:S(2)}, u32[]{:S(2)}) %collective-permute-start.4) | collective-permute-done | bytes 196640 | tf_op jit(solution)/shard_map/ppermute | solution.py:22
  149.4 4.9 %collective-permute-start.7 = (bf16[384,256]{1,0:T(8,128)(2,1)S(1)}, bf16[384,256]{1,0:T(8,128)(2,1)S(1)}, u32[]{:S(2)}, u32[]{:S(2)}) collective-permute-start(bf16[384,256]{1,0:T(8,128)(2,1)S(1)} %get-tuple-element.11), channel_id=1, source_target_pairs={{0,14},{1,15},{2,0},{3,1},{4,2},{5,3},{6,4},{7,5},{8,6},{9,7},{10,... | collective-permute-start | bytes 589832 | tf_op jit(solution)/shard_map/ppermute | solution.py:22
  154.7 2.3 %fusion.5 = bf16[768,256]{1,0:T(8,128)(2,1)} fusion(f32[768,256]{1,0:T(8,128)S(1)} %fusion.125, bf16[512,768]{1,0:T(8,128)(2,1)} %bitcast.50, bf16[512,256]{1,0:T(8,128)(2,1)S(1)} %bitcast.169), kind=kOutput, calls=%fused_computation.8 | convolution fusion | flops 201719808 | bytes 2228224 | tf_op jit(solution)/shard_map/dot_general | solution.py:231
  157.0 9.8 %all-to-all-start.3 = ((bf16[32,24,256]{2,1,0:T(8,128)(2,1)}), bf16[32,24,256]{2,1,0:T(8,128)(2,1)S(1)}, u32[]{:S(2)}, u32[]{:S(2)}) async-start(bf16[32,24,256]{2,1,0:T(8,128)(2,1)} %bitcast.52), calls=%async_computation.3 | async-start | bytes 786432 | tf_op jit(solution)/shard_map/all_to_all | solution.py:188
  166.8 1.9 %collective-permute-start.5 = (bf16[384,256]{1,0:T(8,128)(2,1)S(1)}, bf16[384,256]{1,0:T(8,128)(2,1)S(1)}, u32[]{:S(2)}, u32[]{:S(2)}) collective-permute-start(bf16[384,256]{1,0:T(8,128)(2,1)S(1)} %get-tuple-element.10), channel_id=1, source_target_pairs={{0,2},{1,3},{2,4},{3,5},{4,6},{5,7},{6,8},{7,9},{8,10},{9,11},{10,... | collective-permute-start | bytes 589832 | tf_op jit(solution)/shard_map/ppermute | solution.py:22
  169.7 3.9 %collective-permute-start.8 = (bf16[384,256]{1,0:T(8,128)(2,1)S(1)}, bf16[384,256]{1,0:T(8,128)(2,1)S(1)}, u32[]{:S(2)}, u32[]{:S(2)}) collective-permute-start(bf16[384,256]{1,0:T(8,128)(2,1)S(1)} %fusion.20), channel_id=1, source_target_pairs={{0,14},{1,15},{2,0},{3,1},{4,2},{5,3},{6,4},{7,5},{8,6},{9,7},{10,... | collective-permute-start | bytes 589832 | tf_op jit(solution)/shard_map/ppermute | solution.py:22
  174.4 2.9 %collective-permute-done.8 = bf16[384,256]{1,0:T(8,128)(2,1)S(1)} collective-permute-done((bf16[384,256]{1,0:T(8,128)(2,1)S(1)}, bf16[384,256]{1,0:T(8,128)(2,1)S(1)}, u32[]{:S(2)}, u32[]{:S(2)}) %collective-permute-start.8) | collective-permute-done | bytes 196640 | tf_op jit(solution)/shard_map/ppermute | solution.py:22
  179.0 2.3 %all-to-all-done.3 = bf16[32,24,256]{2,1,0:T(8,128)(2,1)S(1)} async-done(((bf16[32,24,256]{2,1,0:T(8,128)(2,1)}), bf16[32,24,256]{2,1,0:T(8,128)(2,1)S(1)}, u32[]{:S(2)}, u32[]{:S(2)}) %all-to-all-start.3) | async-done | bytes 393248 | tf_op jit(solution)/shard_map/all_to_all | solution.py:188
  (107 shorter events, 34.8 us)
Async XLA Ops:
  0.6 42.7 %copy-start = (bf16[16,128,128]{2,1,0:T(8,128)(2,1)S(1)}, bf16[16,128,128]{2,1,0:T(8,128)(2,1)}, u32[]{:S(2)}) copy-start(bf16[16,128,128]{2,1,0:T(8,128)(2,1)} %param.15) | copy-start | bytes 1572868
  5.1 21.5 %copy-start.6 = (bf16[256,128]{1,0:T(8,128)(2,1)S(1)}, bf16[256,128]{1,0:T(8,128)(2,1)}, u32[]{:S(2)}) copy-start(bf16[256,128]{1,0:T(8,128)(2,1)} %param.14) | copy-start | bytes 196612
  5.1 28.6 %all-to-all-start = ((bf16[32,24,256]{2,1,0:T(8,128)(2,1)}), bf16[32,24,256]{2,1,0:T(8,128)(2,1)S(1)}, u32[]{:S(2)}, u32[]{:S(2)}) async-start(bf16[32,24,256]{2,1,0:T(8,128)(2,1)} %bitcast.28), calls=%async_computation | async-start | bytes 786432 | tf_op jit(solution)/shard_map/all_to_all | solution.py:188
  24.6 39.2 %collective-permute-start.15 = (bf16[8,128,256]{2,1,0:T(8,128)(2,1)}, bf16[8,128,256]{2,1,0:T(8,128)(2,1)}, u32[]{:S(2)}, u32[]{:S(2)}) collective-permute-start(bf16[8,128,256]{2,1,0:T(8,128)(2,1)} %get-tuple-element.9), channel_id=1, source_target_pairs={{0,1},{1,0},{2,3},{3,2},{4,5},{5,4},{6,7},{7,6},{8,9},{9,8},{10,11... | collective-permute-start | bytes 1572872 | tf_op jit(solution)/shard_map/ppermute | solution.py:27
  26.6 16.7 %collective-permute-start = (bf16[15,128]{1,0:T(8,128)(2,1)S(1)}, bf16[15,128]{1,0:T(8,128)(2,1)S(1)}, u32[]{:S(2)}, u32[]{:S(2)}) collective-permute-start(bf16[15,128]{1,0:T(8,128)(2,1)S(1)} %slice.181), channel_id=1, source_target_pairs={{0,16},{16,32},{32,48},{48,64},{64,80},{80,96},{96,112},{112,128},... | collective-permute-start | bytes 11528 | tf_op jit(solution)/shard_map/ppermute | solution.py:17
  33.7 25.6 %all-to-all-start.1 = ((bf16[32,24,256]{2,1,0:T(8,128)(2,1)}), bf16[32,24,256]{2,1,0:T(8,128)(2,1)S(1)}, u32[]{:S(2)}, u32[]{:S(2)}) async-start(bf16[32,24,256]{2,1,0:T(8,128)(2,1)} %bitcast.33), calls=%async_computation.1 | async-start | bytes 786432 | tf_op jit(solution)/shard_map/all_to_all | solution.py:188
  44.4 18.8 %copy-start.4 = (bf16[8,128,256]{2,1,0:T(8,128)(2,1)S(1)}, bf16[8,128,256]{2,1,0:T(8,128)(2,1)}, u32[]{:S(2)}) copy-start(bf16[8,128,256]{2,1,0:T(8,128)(2,1)} %get-tuple-element.8) | copy-start | bytes 1572868
  51.5 51.3 %collective-permute-start.1 = (bf16[8,384,256]{2,1,0:T(8,128)(2,1)}, bf16[8,384,256]{2,1,0:T(8,128)(2,1)}, u32[]{:S(2)}, u32[]{:S(2)}) collective-permute-start(bf16[8,384,256]{2,1,0:T(8,128)(2,1)} %get-tuple-element.7), channel_id=1, source_target_pairs={{0,1},{1,0},{2,3},{3,2},{4,5},{5,4},{6,7},{7,6},{8,9},{9,8},{10,11... | collective-permute-start | bytes 4718600 | tf_op jit(solution)/shard_map/ppermute | solution.py:27
  53.5 20.9 %collective-permute-start.9 = (bf16[768,256]{1,0:T(8,128)(2,1)S(1)}, bf16[768,256]{1,0:T(8,128)(2,1)S(1)}, u32[]{:S(2)}, u32[]{:S(2)}) collective-permute-start(bf16[768,256]{1,0:T(8,128)(2,1)S(1)} %bitcast.160), channel_id=1, source_target_pairs={{0,2},{1,3},{2,4},{3,5},{4,6},{5,7},{6,8},{7,9},{8,10},{9,11},{10,... | collective-permute-start | bytes 1179656 | tf_op jit(solution)/shard_map/ppermute | solution.py:22
  57.0 13.9 %collective-permute-start.10 = (bf16[768,256]{1,0:T(8,128)(2,1)S(1)}, bf16[768,256]{1,0:T(8,128)(2,1)S(1)}, u32[]{:S(2)}, u32[]{:S(2)}) collective-permute-start(bf16[768,256]{1,0:T(8,128)(2,1)S(1)} %bitcast.161), channel_id=1, source_target_pairs={{0,14},{1,15},{2,0},{3,1},{4,2},{5,3},{6,4},{7,5},{8,6},{9,7},{10,... | collective-permute-start | bytes 1179656 | tf_op jit(solution)/shard_map/ppermute | solution.py:22
  59.3 21.7 %collective-permute-start.14 = (bf16[768,256]{1,0:T(8,128)(2,1)S(1)}, bf16[768,256]{1,0:T(8,128)(2,1)S(1)}, u32[]{:S(2)}, u32[]{:S(2)}) collective-permute-start(bf16[768,256]{1,0:T(8,128)(2,1)S(1)} %bitcast.156), channel_id=1, source_target_pairs={{0,14},{1,15},{2,0},{3,1},{4,2},{5,3},{6,4},{7,5},{8,6},{9,7},{10,... | collective-permute-start | bytes 1179656 | tf_op jit(solution)/shard_map/ppermute | solution.py:22
  63.8 18.7 %collective-permute-start.13 = (bf16[768,256]{1,0:T(8,128)(2,1)S(1)}, bf16[768,256]{1,0:T(8,128)(2,1)S(1)}, u32[]{:S(2)}, u32[]{:S(2)}) collective-permute-start(bf16[768,256]{1,0:T(8,128)(2,1)S(1)} %bitcast.158), channel_id=1, source_target_pairs={{0,2},{1,3},{2,4},{3,5},{4,6},{5,7},{6,8},{7,9},{8,10},{9,11},{10,... | collective-permute-start | bytes 1179656 | tf_op jit(solution)/shard_map/ppermute | solution.py:22
  70.8 16.1 %collective-permute-start.12 = (bf16[768,256]{1,0:T(8,128)(2,1)S(1)}, bf16[768,256]{1,0:T(8,128)(2,1)S(1)}, u32[]{:S(2)}, u32[]{:S(2)}) collective-permute-start(bf16[768,256]{1,0:T(8,128)(2,1)S(1)} %collective-permute-done.10), channel_id=1, source_target_pairs={{0,14},{1,15},{2,0},{3,1},{4,2},{5,3},{6,4},{7,5},{8,6},{9,7},{10,... | collective-permute-start | bytes 1179656 | tf_op jit(solution)/shard_map/ppermute | solution.py:22
  74.3 13.7 %collective-permute-start.11 = (bf16[768,256]{1,0:T(8,128)(2,1)S(1)}, bf16[768,256]{1,0:T(8,128)(2,1)S(1)}, u32[]{:S(2)}, u32[]{:S(2)}) collective-permute-start(bf16[768,256]{1,0:T(8,128)(2,1)S(1)} %collective-permute-done.9), channel_id=1, source_target_pairs={{0,2},{1,3},{2,4},{3,5},{4,6},{5,7},{6,8},{7,9},{8,10},{9,11},{10,... | collective-permute-start | bytes 1179656 | tf_op jit(solution)/shard_map/ppermute | solution.py:22
  89.2 3.6 %collective-permute-start.16 = (f32[128,768]{1,0:T(8,128)S(1)}, f32[128,768]{1,0:T(8,128)S(1)}, u32[]{:S(2)}, u32[]{:S(2)}) collective-permute-start(f32[128,768]{1,0:T(8,128)S(1)} %fusion.15), channel_id=1, source_target_pairs={{0,1},{1,0},{2,3},{3,2},{4,5},{5,4},{6,7},{7,6},{8,9},{9,8},{10,11... | collective-permute-start | bytes 1179656 | tf_op jit(solution)/shard_map/ppermute | solution.py:27
  93.1 9.7 %copy-start.2 = (bf16[8,384,256]{2,1,0:T(8,128)(2,1)S(1)}, bf16[8,384,256]{2,1,0:T(8,128)(2,1)}, u32[]{:S(2)}) copy-start(bf16[8,384,256]{2,1,0:T(8,128)(2,1)} %get-tuple-element.6) | copy-start | bytes 4718596
  94.2 39.1 %all-to-all-start.2 = ((bf16[8,64,768]{2,1,0:T(8,128)(2,1)}), bf16[8,64,768]{2,1,0:T(8,128)(2,1)S(1)}, u32[]{:S(2)}, u32[]{:S(2)}) async-start(bf16[8,64,768]{2,1,0:T(8,128)(2,1)} %broadcast_in_dim.89), calls=%async_computation.2 | async-start | bytes 1572864 | tf_op jit(solution)/shard_map/all_to_all | solution.py:224
  102.8 37.9 %copy-start.3 = (bf16[1,1024,256]{2,1,0:T(8,128)(2,1)S(1)}, bf16[1,1024,256]{2,1,0:T(8,128)(2,1)}, u32[]{:S(2)}) copy-start(bf16[1,1024,256]{2,1,0:T(8,128)(2,1)} %param.24) | copy-start | bytes 1572868
  104.7 20.2 %collective-permute-start.2 = (bf16[384,256]{1,0:T(8,128)(2,1)S(1)}, bf16[384,256]{1,0:T(8,128)(2,1)S(1)}, u32[]{:S(2)}, u32[]{:S(2)}) collective-permute-start(bf16[384,256]{1,0:T(8,128)(2,1)S(1)} %get-tuple-element.12), channel_id=1, source_target_pairs={{0,2},{1,3},{2,4},{3,5},{4,6},{5,7},{6,8},{7,9},{8,10},{9,11},{10,... | collective-permute-start | bytes 589832 | tf_op jit(solution)/shard_map/ppermute | solution.py:22
  126.5 9.3 %collective-permute-start.3 = (bf16[384,256]{1,0:T(8,128)(2,1)}, bf16[384,256]{1,0:T(8,128)(2,1)}, u32[]{:S(2)}, u32[]{:S(2)}) collective-permute-start(bf16[384,256]{1,0:T(8,128)(2,1)} %fusion.21), channel_id=1, source_target_pairs={{0,2},{1,3},{2,4},{3,5},{4,6},{5,7},{6,8},{7,9},{8,10},{9,11},{10,... | collective-permute-start | bytes 589832 | tf_op jit(solution)/shard_map/ppermute | solution.py:22
  129.9 10.9 %collective-permute-start.6 = (bf16[384,256]{1,0:T(8,128)(2,1)}, bf16[384,256]{1,0:T(8,128)(2,1)}, u32[]{:S(2)}, u32[]{:S(2)}) collective-permute-start(bf16[384,256]{1,0:T(8,128)(2,1)} %get-tuple-element.13), channel_id=1, source_target_pairs={{0,14},{1,15},{2,0},{3,1},{4,2},{5,3},{6,4},{7,5},{8,6},{9,7},{10,... | collective-permute-start | bytes 589832 | tf_op jit(solution)/shard_map/ppermute | solution.py:22
  133.3 21.4 %collective-permute-start.17 = (bf16[8,64,768]{2,1,0:T(8,128)(2,1)S(1)}, bf16[8,64,768]{2,1,0:T(8,128)(2,1)}, u32[]{:S(2)}, u32[]{:S(2)}) collective-permute-start(bf16[8,64,768]{2,1,0:T(8,128)(2,1)S(1)} %all-to-all-done.2), channel_id=1, source_target_pairs={{0,1},{1,0},{2,3},{3,2},{4,5},{5,4},{6,7},{7,6},{8,9},{9,8},{10,11... | collective-permute-start | bytes 2359304 | tf_op jit(solution)/shard_map/ppermute | solution.py:27
  137.6 10.4 %collective-permute-start.4 = (bf16[384,256]{1,0:T(8,128)(2,1)}, bf16[384,256]{1,0:T(8,128)(2,1)}, u32[]{:S(2)}, u32[]{:S(2)}) collective-permute-start(bf16[384,256]{1,0:T(8,128)(2,1)} %fusion.22), channel_id=1, source_target_pairs={{0,2},{1,3},{2,4},{3,5},{4,6},{5,7},{6,8},{7,9},{8,10},{9,11},{10,... | collective-permute-start | bytes 589832 | tf_op jit(solution)/shard_map/ppermute | solution.py:22
  149.4 19.4 %collective-permute-start.7 = (bf16[384,256]{1,0:T(8,128)(2,1)S(1)}, bf16[384,256]{1,0:T(8,128)(2,1)S(1)}, u32[]{:S(2)}, u32[]{:S(2)}) collective-permute-start(bf16[384,256]{1,0:T(8,128)(2,1)S(1)} %get-tuple-element.11), channel_id=1, source_target_pairs={{0,14},{1,15},{2,0},{3,1},{4,2},{5,3},{6,4},{7,5},{8,6},{9,7},{10,... | collective-permute-start | bytes 589832 | tf_op jit(solution)/shard_map/ppermute | solution.py:22
  154.6 12.2 %copy-start.8 = (f32[128,4]{0,1:T(4,128)S(1)}, f32[128,4]{0,1:T(4,128)}, u32[]{:S(2)}) copy-start(f32[128,4]{0,1:T(4,128)} %param.21) | copy-start | bytes 6148
  154.7 19.0 %copy-start.10 = (s32[128]{0:T(128)S(1)}, s32[128]{0:T(128)}, u32[]{:S(2)}) copy-start(s32[128]{0:T(128)} %copy-done.9) | copy-start | bytes 1540
  154.7 19.0 %copy-start.12 = (s32[128]{0:T(128)S(1)}, s32[128]{0:T(128)}, u32[]{:S(2)}) copy-start(s32[128]{0:T(128)} %copy-done.11) | copy-start | bytes 1540
  154.7 19.0 %copy-start.14 = (s32[128]{0:T(128)S(1)}, s32[128]{0:T(128)}, u32[]{:S(2)}) copy-start(s32[128]{0:T(128)} %copy-done.13) | copy-start | bytes 1540
  154.7 19.0 %copy-start.16 = (s32[128]{0:T(128)S(1)}, s32[128]{0:T(128)}, u32[]{:S(2)}) copy-start(s32[128]{0:T(128)} %copy-done.15) | copy-start | bytes 1540
  157.0 24.3 %all-to-all-start.3 = ((bf16[32,24,256]{2,1,0:T(8,128)(2,1)}), bf16[32,24,256]{2,1,0:T(8,128)(2,1)S(1)}, u32[]{:S(2)}, u32[]{:S(2)}) async-start(bf16[32,24,256]{2,1,0:T(8,128)(2,1)} %bitcast.52), calls=%async_computation.3 | async-start | bytes 786432 | tf_op jit(solution)/shard_map/all_to_all | solution.py:188
  166.8 7.6 %collective-permute-start.5 = (bf16[384,256]{1,0:T(8,128)(2,1)S(1)}, bf16[384,256]{1,0:T(8,128)(2,1)S(1)}, u32[]{:S(2)}, u32[]{:S(2)}) collective-permute-start(bf16[384,256]{1,0:T(8,128)(2,1)S(1)} %get-tuple-element.10), channel_id=1, source_target_pairs={{0,2},{1,3},{2,4},{3,5},{4,6},{5,7},{6,8},{7,9},{8,10},{9,11},{10,... | collective-permute-start | bytes 589832 | tf_op jit(solution)/shard_map/ppermute | solution.py:22
  169.7 7.6 %collective-permute-start.8 = (bf16[384,256]{1,0:T(8,128)(2,1)S(1)}, bf16[384,256]{1,0:T(8,128)(2,1)S(1)}, u32[]{:S(2)}, u32[]{:S(2)}) collective-permute-start(bf16[384,256]{1,0:T(8,128)(2,1)S(1)} %fusion.20), channel_id=1, source_target_pairs={{0,14},{1,15},{2,0},{3,1},{4,2},{5,3},{6,4},{7,5},{8,6},{9,7},{10,... | collective-permute-start | bytes 589832 | tf_op jit(solution)/shard_map/ppermute | solution.py:22
  (8 other events, 35.6 us)

commit v3 on v2

v3 whole, which is shorter than its diff:
```python
import jax
import jax.numpy as jnp
from jax import lax
from jax.experimental import pallas as pl
from jax.experimental.pallas import tpu as pltpu
from jax.sharding import PartitionSpec as P


windows = (2, 4, 8, 16)
reach_back = 15
eps = 1e-05
f32 = jnp.float32
bf16 = jnp.bfloat16


def halo(block):
    devices = range(lax.axis_size("ep"))
    return lax.ppermute(block, "ep", [(i - 1, i) for i in devices if i > 0])


def along_y(x, step):
    n = lax.axis_size("tp")
    return lax.ppermute(x, "tp", [(i, (i + 2 * step) % n) for i in range(n)])


def to_partner(x):
    n = lax.axis_size("tp")
    return lax.ppermute(x, "tp", [(i, i ^ 1) for i in range(n)])


def tdot(a, b):
    return lax.dot_general(a, b, (((1,), (1,)), ((), ())), preferred_element_type=f32)


def lanes(block, width):
    return pl.ds(pl.multiple_of(block * width, width), width)


def local_kernel(body, index, operands, out_shape):
    vmem = pl.BlockSpec(memory_space=pltpu.VMEM)
    smem = pl.BlockSpec(memory_space=pltpu.SMEM)
    several = isinstance(out_shape, list)
    return pl.pallas_call(
        body,
        in_specs=[smem] + [vmem] * len(operands),
        out_specs=[vmem] * len(out_shape) if several else vmem,
        out_shape=out_shape,
    )(index, *operands)


def weight_kernel(index, gate, up, partner_gate, partner_up, blocks):
    count, _, width = blocks.shape
    units = gate.shape[0]
    for j in range(count):
        at = lanes(index[0, j], width)
        for i, source in enumerate((gate, up, partner_gate, partner_up)):
            blocks[j, i * units : (i + 1) * units] = source[:, at]


def project_kernel(index, group, hidden, proj, down, own, out):
    rows = group.shape[0]
    count, _, width = own.shape
    for side, to in ((1, out), (0, own)):
        for j in range(count):
            at = lanes(index[side, j], width)
            to[j, :rows] = jnp.dot(group[...], proj[:, at], preferred_element_type=f32).astype(bf16)
            to[j, rows:] = jnp.dot(hidden[...], down[:, at], preferred_element_type=f32).astype(bf16)


def after(x, event):
    return lax.optimization_barrier((x, event))[0]


def pool_group_out(pool_input, earlier_rows, pool_map, pool_scale, tp_rank, ep_rank):
    row_count, channels = pool_input.shape
    group_dim = pool_map.shape[1]
    local_groups = channels // group_dim
    values = pool_input.astype(f32)
    extended = jnp.concatenate([earlier_rows.astype(f32), values], axis=0)
    position = (ep_rank * row_count + jnp.arange(row_count, dtype=jnp.int32)).astype(f32)
    group_ids = tp_rank * local_groups + jnp.arange(channels, dtype=jnp.int32) // group_dim
    group_kind = group_ids % 4
    running = jnp.zeros((row_count, channels), f32)
    pooled = -values
    for lag_step in range(reach_back + 1):
        running = running + extended[reach_back - lag_step : reach_back - lag_step + row_count]
        if lag_step + 1 in windows:
            kind_id = windows.index(lag_step + 1)
            counts = jnp.minimum(position + 1.0, float(lag_step + 1))
            select = (group_kind == kind_id).astype(f32)
            pooled = pooled + select[None, :] * running / counts[:, None]
    pooled = pooled.astype(bf16)
    my_maps = lax.dynamic_slice_in_dim(pool_map, tp_rank * local_groups, local_groups, 0)
    my_scale = lax.dynamic_slice_in_dim(pool_scale, tp_rank * channels, channels, 0)
    mapped = jnp.einsum(
        "rgc,gcd->rgd",
        pooled.reshape(row_count, local_groups, group_dim),
        my_maps,
        preferred_element_type=f32,
    )
    return (mapped.reshape(row_count, channels) * my_scale[None, :]).astype(bf16)


def per_device(
    pool_input,
    pool_map,
    pool_scale,
    out_proj,
    moe_input,
    norm_gain,
    routes,
    route_weights,
    expert_gate,
    expert_up,
    expert_down,
    shared_gate,
    shared_up,
    shared_down,
):
    tp_rank = lax.axis_index("tp")
    ep_rank = lax.axis_index("ep")
    tp_size = lax.axis_size("tp")
    expert_count = lax.axis_size("ep")
    y_size = tp_size // 2
    core = tp_rank % 2
    y = tp_rank // 2
    tok_count, width = moe_input.shape
    top_count = routes.shape[1]
    capacity = (3 * tok_count * top_count + 2 * expert_count - 1) // (2 * expert_count)
    buffer_len = expert_count * capacity
    slice_width = width // tp_size
    row_count = pool_input.shape[0]

    earlier_rows = halo(pool_input[row_count - reach_back :])

    routes_t = routes.T
    experts = jnp.arange(expert_count, dtype=jnp.int32)[:, None]
    named = jnp.zeros((expert_count, tok_count), f32)
    weight_t = jnp.zeros((expert_count, tok_count), f32)
    for k in range(top_count):
        hit = routes_t[k][None, :] == experts
        named = named + hit.astype(f32)
        weight_t = weight_t + jnp.where(hit, route_weights.T[k][None, :], 0.0)
    before = jnp.arange(tok_count)[:, None] < jnp.arange(tok_count)[None, :]
    earlier = jnp.dot(named.astype(bf16), before.astype(bf16), preferred_element_type=f32)
    slot = jnp.where(named > 0, earlier, -1.0)
    slots = jnp.arange(capacity, dtype=f32)[None, :, None]
    match = slot[:, None, :] == slots
    placing = match.astype(bf16).reshape(buffer_len, tok_count)
    combine = jnp.where(match, weight_t[:, None, :], 0.0).astype(bf16).reshape(buffer_len, tok_count)

    values = moe_input.astype(f32)
    mean = jnp.mean(values, axis=1, keepdims=True)
    centre = values - mean
    rstd = lax.rsqrt(jnp.mean(centre * centre, axis=1, keepdims=True) + eps)

    def normed_slice(far):
        at = (((y + far) % y_size) * 2 + core) * slice_width
        mine = lax.dynamic_slice_in_dim(moe_input, at, slice_width, 1).astype(f32)
        gain = lax.dynamic_slice_in_dim(norm_gain, at, slice_width, 0)
        return ((mine - mean) * rstd * gain[None, :]).astype(bf16)

    def exchanged(rows):
        return lax.all_to_all(rows, "ep", split_axis=0, concat_axis=0, tiled=True)

    both = jnp.concatenate([normed_slice(0), normed_slice(y_size // 2)], axis=1)
    outgoing = jnp.dot(placing, both, preferred_element_type=f32).astype(bf16)
    arrived = exchanged(outgoing)
    pool_input = after(pool_input, outgoing)
    turn = (y + jnp.arange(y_size, dtype=jnp.int32)) % y_size
    index = jnp.stack([turn * 2 + core, turn * 2 + 1 - core]).astype(jnp.int32)

    group_out = pool_group_out(pool_input, earlier_rows, pool_map, pool_scale, tp_rank, ep_rank)
    normed = (centre * rstd * norm_gain[None, :]).astype(bf16)
    shared_gate_val = jnp.dot(normed, shared_gate, preferred_element_type=f32)
    shared_up_val = jnp.dot(normed, shared_up, preferred_element_type=f32)
    shared_hidden = (jax.nn.silu(shared_gate_val) * shared_up_val).astype(bf16)

    shape = jax.ShapeDtypeStruct((y_size, row_count + tok_count, slice_width), bf16)
    kept, sent = local_kernel(project_kernel, index, (group_out, shared_hidden, out_proj, shared_down), [shape, shape])
    from_partner = to_partner(sent)


    gate_t = expert_gate[0].T
    up_t = expert_up[0].T
    units = gate_t.shape[0]
    blocks = jax.ShapeDtypeStruct((y_size, 4 * units, slice_width), bf16)
    weights = local_kernel(weight_kernel, index, (gate_t, up_t, to_partner(gate_t), to_partner(up_t)), blocks)

    def part(j):
        return kept[j].astype(f32) + from_partner[j].astype(f32)

    def reduced(rs_up, rs_down, step):
        rs_up = (part(4 - step) + rs_up.astype(f32)).astype(bf16)
        rs_down = (part(5 + step) + rs_down.astype(f32)).astype(bf16)
        rs_up, rs_down = lax.optimization_barrier((rs_up, rs_down))
        return along_y(rs_up, 1), along_y(rs_down, -1)

    arrived = after(arrived, (from_partner, weights))
    near = arrived[:, :slice_width]
    far = arrived[:, slice_width:]

    def product(rows, j):
        return tdot(weights[j % y_size], rows)

    up = along_y(near, 1)
    down = along_y(near, -1)
    up_far = along_y(far, 1)
    down_far = along_y(far, -1)
    up_two = along_y(up, 1)
    down_two = along_y(down, -1)
    rs_up = along_y(part(4).astype(bf16), 1)
    rs_down = along_y(part(5).astype(bf16), -1)
    rs_up, rs_down = lax.optimization_barrier((rs_up, rs_down))
    rs_up, rs_down = reduced(rs_up, rs_down, 1)
    summed = product(near, 0) + product(far, 4)
    summed = summed + product(up, -1) + product(down, 1)
    summed = summed + product(up_far, 3) + product(down_far, -3)
    summed = summed + product(up_two, -2) + product(down_two, 2)
    full = summed[: 2 * units] + to_partner(summed[2 * units :])
    hidden = (jax.nn.silu(full[:units]) * full[units:]).astype(bf16)


    copies = jnp.broadcast_to(hidden[None], (y_size, *hidden.shape))
    groups = [[2 * i + c for i in range(y_size)] for c in range(2)]
    own_hidden = lax.all_to_all(copies, "tp", 0, 0, axis_index_groups=groups, tiled=True)
    rs_up, rs_down = after((rs_up, rs_down), own_hidden)
    rs_up, rs_down = reduced(rs_up, rs_down, 2)
    other_hidden = to_partner(own_hidden)
    down_weight = expert_down[0].reshape(y_size, 2, units, slice_width)

    def down_product(h, side):
        w = lax.dynamic_index_in_dim(down_weight, side, 1, keepdims=False)
        w = w.reshape(y_size * units, slice_width)
        return lax.dot_general(
            h.reshape(y_size * units, buffer_len), w, (((0,), (0,)), ((), ())), preferred_element_type=f32
        )

    expert_result = down_product(own_hidden, core) + down_product(other_hidden, 1 - core)
    expert_result = expert_result.astype(bf16)
    returned = exchanged(expert_result)
    rs_up = along_y((part(1) + rs_up.astype(f32)).astype(bf16), 1)
    routed = lax.dot_general(combine, returned, (((0,), (0,)), ((), ())), preferred_element_type=f32)

    total = part(0) + rs_up.astype(f32) + rs_down.astype(f32)
    return (total[:row_count].astype(bf16), (routed + total[row_count:]).astype(bf16))


def solution(mesh):
    return jax.shard_map(
        per_device,
        mesh=mesh,
        in_specs=(
            P("ep", "tp"),
            P(),
            P(),
            P("tp", None),
            P("ep", None),
            P(),
            P("ep", None),
            P("ep", None),
            P("ep", None, "tp"),
            P("ep", None, "tp"),
            P("ep", None, "tp"),
            P(None, "tp"),
            P(None, "tp"),
            P("tp", None),
        ),
        out_specs=(P("ep", "tp"), P("ep", "tp")),
        check_vma=False,
    )
```

time: 185 us -> 172 us (0.930)
  the two profiles are of different devices: /device:TPU:8 before, /device:TPU:1 now
where the time goes in v3:
time: 172 us; the launch traced here: 169 us
  starting transfers between devices  81.5 us (47%)
  waiting for transfers between devices  54.9 us (32%)
  other arithmetic  10 us (6%)
  matrix products  9.92 us (6%)
  Pallas kernels  6.31 us (4%)
  local copies, waits for them, and re-layouts  5.07 us (3%)
    ppermute x13, starting transfers between devices, along_y(): return lax.ppermute(x, 'tp', [(i, (i + 2 * step) % n) for i in range(n)])  41.2 us
    ppermute x13, waiting for transfers between devices, along_y(): return lax.ppermute(x, 'tp', [(i, (i + 2 * step) % n) for i in range(n)])  39.4 us
    ppermute x5, starting transfers between devices, to_partner(): return lax.ppermute(x, 'tp', [(i, i ^ 1) for i in range(n)])  18.1 us
    all_to_all x2, starting transfers between devices, exchanged(): return lax.all_to_all(rows, 'ep', split_axis=0, concat_axis=0, tiled=True)  14.5 us
    all_to_all x2, waiting for transfers between devices, exchanged(): return lax.all_to_all(rows, 'ep', split_axis=0, concat_axis=0, tiled=True)  12.5 us
    pallas_call x2, Pallas kernels, local_kernel(): pl.pallas_call(body, in_specs=[smem] + [vmem] * len(operands), out_specs=...  6.31 us
    ppermute x1, starting transfers between devices, halo(): return lax.ppermute(block, 'ep', [(i - 1, i) for i in devices if i > 0])  3.92 us
    all_to_all x1, starting transfers between devices, per_device(): lax.all_to_all(copies, 'tp', 0, 0, axis_index_groups=groups, tiled=True)  3.8 us
  transfers between devices with their start and end apart: 22, of which 10 were waited for; matrix products, arithmetic and copies ran while one was open for 11% of the time, Pallas kernels for 2%

profile of v3, /device:TPU:1, one launch (start us, length us, event | category | flops | bytes accessed | tf_op | source)
XLA Modules:
  0.0 169.1 jit_solution(3393945230280148945)
XLA Ops:
  1.5 3.9 %collective-permute-start = (bf16[15,128]{1,0:T(8,128)(2,1)S(1)}, bf16[15,128]{1,0:T(8,128)(2,1)S(1)}, u32[]{:S(2)}, u32[]{:S(2)}) collective-permute-start(bf16[15,128]{1,0:T(8,128)(2,1)S(1)} %slice.173), channel_id=1, source_target_pairs={{0,16},{16,32},{32,48},{48,64},{64,80},{80,96},{96,112},{112,128},... | collective-permute-start | bytes 11528 | tf_op jit(solution)/shard_map/ppermute | solution.py:18
  13.7 3.6 %shard_map.149 = (bf16[8,384,256]{2,1,0:T(8,128)(2,1)}, bf16[8,384,256]{2,1,0:T(8,128)(2,1)}) custom-call(s32[2,8]{1,0:T(2,128)} %pad_add_fusion.index, bf16[256,128]{1,0:T(8,128)(2,1)} %fusion.12.group, bf16[128,32]{1,0:T(8,128)(2,1)} %fusion.13.hidden, bf16[128,4096]{1,0:T(8,128)(2,1)} %proj.1, bf16[32,4096]{1,0:T(8,128)(2,1)} %down.1), custom_call_target="tpu_custom_call" | custom-call | tf_op jit(solution)/shard_map/pallas_call | solution.py:43
  17.3 6.1 %collective-permute-start.1 = (bf16[8,384,256]{2,1,0:T(8,128)(2,1)}, bf16[8,384,256]{2,1,0:T(8,128)(2,1)}, u32[]{:S(2)}, u32[]{:S(2)}) collective-permute-start(bf16[8,384,256]{2,1,0:T(8,128)(2,1)} %get-tuple-element.16), channel_id=1, source_target_pairs={{0,1},{1,0},{2,3},{3,2},{4,5},{5,4},{6,7},{7,6},{8,9},{9,8},{10,11... | collective-permute-start | bytes 4718600 | tf_op jit(solution)/shard_map/ppermute | solution.py:28
  23.4 9.4 %all-to-all-start = ((bf16[32,24,512]{2,1,0:T(8,128)(2,1)}), bf16[32,24,512]{2,1,0:T(8,128)(2,1)S(1)}, u32[]{:S(2)}, u32[]{:S(2)}) async-start(bf16[32,24,512]{2,1,0:T(8,128)(2,1)} %bitcast.24), calls=%async_computation | async-start | bytes 1572864 | tf_op jit(solution)/shard_map/all_to_all | solution.py:164
  32.8 2.2 %collective-permute-start.6 = (bf16[64,4096]{1,0:T(8,128)(2,1)S(1)}, bf16[64,4096]{1,0:T(8,128)(2,1)S(1)}, u32[]{:S(2)}, u32[]{:S(2)}) collective-permute-start(bf16[64,4096]{1,0:T(8,128)(2,1)S(1)} %bitcast.127), channel_id=1, source_target_pairs={{0,1},{1,0},{2,3},{3,2},{4,5},{5,4},{6,7},{7,6},{8,9},{9,8},{10,11... | collective-permute-start | bytes 1572872 | tf_op jit(solution)/shard_map/ppermute | solution.py:28
  35.0 2.1 %collective-permute-start.7 = (bf16[64,4096]{1,0:T(8,128)(2,1)S(1)}, bf16[64,4096]{1,0:T(8,128)(2,1)S(1)}, u32[]{:S(2)}, u32[]{:S(2)}) collective-permute-start(bf16[64,4096]{1,0:T(8,128)(2,1)S(1)} %bitcast.129), channel_id=1, source_target_pairs={{0,1},{1,0},{2,3},{3,2},{4,5},{5,4},{6,7},{7,6},{8,9},{9,8},{10,11... | collective-permute-start | bytes 1572872 | tf_op jit(solution)/shard_map/ppermute | solution.py:28
  39.7 2.7 %shard_map.150 = bf16[8,256,256]{2,1,0:T(8,128)(2,1)} custom-call(s32[2,8]{1,0:T(2,128)} %pad_add_fusion.index, bf16[64,4096]{1,0:T(8,128)(2,1)} %bitcast.126, bf16[64,4096]{1,0:T(8,128)(2,1)} %bitcast.128, bf16[64,4096]{1,0:T(8,128)(2,1)} %copy-done.7, bf16[64,4096]{1,0:T(8,128)(2,1)} %copy-done.8), custom_call_target="tpu_custom_call" | custom-call | tf_op jit(solution)/shard_map/pallas_call | solution.py:43
  42.4 12.5 %all-to-all-done = bf16[32,24,512]{2,1,0:T(8,128)(2,1)S(1)} async-done(((bf16[32,24,512]{2,1,0:T(8,128)(2,1)}), bf16[32,24,512]{2,1,0:T(8,128)(2,1)S(1)}, u32[]{:S(2)}, u32[]{:S(2)}) %all-to-all-start) | async-done | bytes 786464 | tf_op jit(solution)/shard_map/all_to_all | solution.py:164
  55.0 5.1 %collective-permute-start.9 = (bf16[768,256]{1,0:T(8,128)(2,1)S(1)}, bf16[768,256]{1,0:T(8,128)(2,1)S(1)}, u32[]{:S(2)}, u32[]{:S(2)}) collective-permute-start(bf16[768,256]{1,0:T(8,128)(2,1)S(1)} %get-tuple-element.35), channel_id=1, source_target_pairs={{0,14},{1,15},{2,0},{3,1},{4,2},{5,3},{6,4},{7,5},{8,6},{9,7},{10,... | collective-permute-start | bytes 1179656 | tf_op jit(solution)/shard_map/ppermute | solution.py:23
  60.1 1.9 %collective-permute-start.8 = (bf16[768,256]{1,0:T(8,128)(2,1)S(1)}, bf16[768,256]{1,0:T(8,128)(2,1)S(1)}, u32[]{:S(2)}, u32[]{:S(2)}) collective-permute-start(bf16[768,256]{1,0:T(8,128)(2,1)S(1)} %get-tuple-element.35), channel_id=1, source_target_pairs={{0,2},{1,3},{2,4},{3,5},{4,6},{5,7},{6,8},{7,9},{8,10},{9,11},{10,... | collective-permute-start | bytes 1179656 | tf_op jit(solution)/shard_map/ppermute | solution.py:23
  62.0 1.9 %collective-permute-start.10 = (bf16[768,256]{1,0:T(8,128)(2,1)S(1)}, bf16[768,256]{1,0:T(8,128)(2,1)S(1)}, u32[]{:S(2)}, u32[]{:S(2)}) collective-permute-start(bf16[768,256]{1,0:T(8,128)(2,1)S(1)} %get-tuple-element.34), channel_id=1, source_target_pairs={{0,2},{1,3},{2,4},{3,5},{4,6},{5,7},{6,8},{7,9},{8,10},{9,11},{10,... | collective-permute-start | bytes 1179656 | tf_op jit(solution)/shard_map/ppermute | solution.py:23
  63.9 4.6 %collective-permute-start.11 = (bf16[768,256]{1,0:T(8,128)(2,1)S(1)}, bf16[768,256]{1,0:T(8,128)(2,1)S(1)}, u32[]{:S(2)}, u32[]{:S(2)}) collective-permute-start(bf16[768,256]{1,0:T(8,128)(2,1)S(1)} %get-tuple-element.34), channel_id=1, source_target_pairs={{0,14},{1,15},{2,0},{3,1},{4,2},{5,3},{6,4},{7,5},{8,6},{9,7},{10,... | collective-permute-start | bytes 1179656 | tf_op jit(solution)/shard_map/ppermute | solution.py:23
  68.8 3.6 %collective-permute-start.13 = (bf16[768,256]{1,0:T(8,128)(2,1)S(1)}, bf16[768,256]{1,0:T(8,128)(2,1)S(1)}, u32[]{:S(2)}, u32[]{:S(2)}) collective-permute-start(bf16[768,256]{1,0:T(8,128)(2,1)S(1)} %collective-permute-done.9), channel_id=1, source_target_pairs={{0,14},{1,15},{2,0},{3,1},{4,2},{5,3},{6,4},{7,5},{8,6},{9,7},{10,... | collective-permute-start | bytes 1179656 | tf_op jit(solution)/shard_map/ppermute | solution.py:23
  72.5 1.9 %collective-permute-start.12 = (bf16[768,256]{1,0:T(8,128)(2,1)S(1)}, bf16[768,256]{1,0:T(8,128)(2,1)S(1)}, u32[]{:S(2)}, u32[]{:S(2)}) collective-permute-start(bf16[768,256]{1,0:T(8,128)(2,1)S(1)} %collective-permute-done.8), channel_id=1, source_target_pairs={{0,2},{1,3},{2,4},{3,5},{4,6},{5,7},{6,8},{7,9},{8,10},{9,11},{10,... | collective-permute-start | bytes 1179656 | tf_op jit(solution)/shard_map/ppermute | solution.py:23
  75.0 5.6 %collective-permute-done.10 = bf16[768,256]{1,0:T(8,128)(2,1)S(1)} collective-permute-done((bf16[768,256]{1,0:T(8,128)(2,1)S(1)}, bf16[768,256]{1,0:T(8,128)(2,1)S(1)}, u32[]{:S(2)}, u32[]{:S(2)}) %collective-permute-start.10) | collective-permute-done | bytes 393248 | tf_op jit(solution)/shard_map/ppermute | solution.py:23
  83.8 5.3 %collective-permute-done.12 = bf16[768,256]{1,0:T(8,128)(2,1)S(1)} collective-permute-done((bf16[768,256]{1,0:T(8,128)(2,1)S(1)}, bf16[768,256]{1,0:T(8,128)(2,1)S(1)}, u32[]{:S(2)}, u32[]{:S(2)}) %collective-permute-start.12) | collective-permute-done | bytes 393248 | tf_op jit(solution)/shard_map/ppermute | solution.py:23
  89.4 4.4 %collective-permute-start.14 = (f32[128,768]{1,0:T(8,128)S(1)}, f32[128,768]{1,0:T(8,128)S(1)}, u32[]{:S(2)}, u32[]{:S(2)}) collective-permute-start(f32[128,768]{1,0:T(8,128)S(1)} %slice.269), channel_id=1, source_target_pairs={{0,1},{1,0},{2,3},{3,2},{4,5},{5,4},{6,7},{7,6},{8,9},{9,8},{10,11... | collective-permute-start | bytes 1179656 | tf_op jit(solution)/shard_map/ppermute | solution.py:28
  96.2 3.8 %all-to-all-start.1 = ((bf16[8,64,768]{2,1,0:T(8,128)(2,1)}), bf16[8,64,768]{2,1,0:T(8,128)(2,1)S(1)}, u32[]{:S(2)}, u32[]{:S(2)}) async-start(bf16[8,64,768]{2,1,0:T(8,128)(2,1)} %broadcast_in_dim.79), calls=%async_computation.1 | async-start | bytes 1572864 | tf_op jit(solution)/shard_map/all_to_all | solution.py:226
  101.2 3.4 %collective-permute-start.2 = (bf16[384,256]{1,0:T(8,128)(2,1)S(1)}, bf16[384,256]{1,0:T(8,128)(2,1)S(1)}, u32[]{:S(2)}, u32[]{:S(2)}) collective-permute-start(bf16[384,256]{1,0:T(8,128)(2,1)S(1)} %get-tuple-element.31), channel_id=1, source_target_pairs={{0,2},{1,3},{2,4},{3,5},{4,6},{5,7},{6,8},{7,9},{8,10},{9,11},{10,... | collective-permute-start | bytes 589832 | tf_op jit(solution)/shard_map/ppermute | solution.py:23
  104.6 3.1 %collective-permute-start.3 = (bf16[384,256]{1,0:T(8,128)(2,1)S(1)}, bf16[384,256]{1,0:T(8,128)(2,1)}, u32[]{:S(2)}, u32[]{:S(2)}) collective-permute-start(bf16[384,256]{1,0:T(8,128)(2,1)S(1)} %get-tuple-element.30), channel_id=1, source_target_pairs={{0,14},{1,15},{2,0},{3,1},{4,2},{5,3},{6,4},{7,5},{8,6},{9,7},{10,... | collective-permute-start | bytes 589832 | tf_op jit(solution)/shard_map/ppermute | solution.py:23
  107.7 16.5 %collective-permute-done.2 = bf16[384,256]{1,0:T(8,128)(2,1)S(1)} collective-permute-done((bf16[384,256]{1,0:T(8,128)(2,1)S(1)}, bf16[384,256]{1,0:T(8,128)(2,1)S(1)}, u32[]{:S(2)}, u32[]{:S(2)}) %collective-permute-start.2) | collective-permute-done | bytes 196640 | tf_op jit(solution)/shard_map/ppermute | solution.py:23
  124.9 3.3 %collective-permute-start.18 = (bf16[8,64,768]{2,1,0:T(8,128)(2,1)S(1)}, bf16[8,64,768]{2,1,0:T(8,128)(2,1)}, u32[]{:S(2)}, u32[]{:S(2)}) collective-permute-start(bf16[8,64,768]{2,1,0:T(8,128)(2,1)S(1)} %all-to-all-done.1), channel_id=1, source_target_pairs={{0,1},{1,0},{2,3},{3,2},{4,5},{5,4},{6,7},{7,6},{8,9},{9,8},{10,11... | collective-permute-start | bytes 2359304 | tf_op jit(solution)/shard_map/ppermute | solution.py:28
  128.2 2.1 %fusion.15 = (bf16[384,256]{1,0:T(8,128)(2,1)}, bf16[384,256]{1,0:T(8,128)(2,1)}) fusion(bf16[384,256]{1,0:T(8,128)(2,1)} %collective-permute-done.3, bf16[8,384,256]{2,1,0:T(8,128)(2,1)} %collective-permute-done.1, bf16[8,384,256]{2,1,0:T(8,128)(2,1)S(1)} %copy-done.3, bf16[384,256]{1,0:T(8,128)(2,1)} %copy-done.10), kind=kLoop, calls=%fused_computation.42 | loop fusion | flops 1179648 | bytes 1572864 | tf_op jit(solution)/shard_map/convert_element_type | solution.py:195
  130.3 1.9 %collective-permute-start.4 = (bf16[384,256]{1,0:T(8,128)(2,1)}, bf16[384,256]{1,0:T(8,128)(2,1)}, u32[]{:S(2)}, u32[]{:S(2)}) collective-permute-start(bf16[384,256]{1,0:T(8,128)(2,1)} %get-tuple-element.19), channel_id=1, source_target_pairs={{0,2},{1,3},{2,4},{3,5},{4,6},{5,7},{6,8},{7,9},{8,10},{9,11},{10,... | collective-permute-start | bytes 589832 | tf_op jit(solution)/shard_map/ppermute | solution.py:23
  132.2 4.6 %collective-permute-start.5 = (bf16[384,256]{1,0:T(8,128)(2,1)}, bf16[384,256]{1,0:T(8,128)(2,1)}, u32[]{:S(2)}, u32[]{:S(2)}) collective-permute-start(bf16[384,256]{1,0:T(8,128)(2,1)} %get-tuple-element.20), channel_id=1, source_target_pairs={{0,14},{1,15},{2,0},{3,1},{4,2},{5,3},{6,4},{7,5},{8,6},{9,7},{10,... | collective-permute-start | bytes 589832 | tf_op jit(solution)/shard_map/ppermute | solution.py:23
  136.9 3.3 %collective-permute-done.4 = bf16[384,256]{1,0:T(8,128)(2,1)} collective-permute-done((bf16[384,256]{1,0:T(8,128)(2,1)}, bf16[384,256]{1,0:T(8,128)(2,1)}, u32[]{:S(2)}, u32[]{:S(2)}) %collective-permute-start.4) | collective-permute-done | bytes 196640 | tf_op jit(solution)/shard_map/ppermute | solution.py:23
  142.5 3.2 %collective-permute-start.15 = (bf16[384,256]{1,0:T(8,128)(2,1)S(1)}, bf16[384,256]{1,0:T(8,128)(2,1)S(1)}, u32[]{:S(2)}, u32[]{:S(2)}) collective-permute-start(bf16[384,256]{1,0:T(8,128)(2,1)S(1)} %get-tuple-element.24), channel_id=1, source_target_pairs={{0,2},{1,3},{2,4},{3,5},{4,6},{5,7},{6,8},{7,9},{8,10},{9,11},{10,... | collective-permute-start | bytes 589832 | tf_op jit(solution)/shard_map/ppermute | solution.py:23
  146.1 2.3 %fusion.10 = bf16[768,256]{1,0:T(8,128)(2,1)} fusion(f32[768,256]{1,0:T(8,128)S(1)} %fusion.96, bf16[512,768]{1,0:T(8,128)(2,1)} %bitcast.42, bf16[512,256]{1,0:T(8,128)(2,1)S(1)} %bitcast.123), kind=kOutput, calls=%fused_computation.16 | convolution fusion | flops 201719808 | bytes 2228224 | tf_op jit(solution)/shard_map/dot_general | solution.py:235
  148.4 5.1 %all-to-all-start.2 = ((bf16[32,24,256]{2,1,0:T(8,128)(2,1)}), bf16[32,24,256]{2,1,0:T(8,128)(2,1)S(1)}, u32[]{:S(2)}, u32[]{:S(2)}) async-start(bf16[32,24,256]{2,1,0:T(8,128)(2,1)} %bitcast.44), calls=%async_computation.2 | async-start | bytes 786432 | tf_op jit(solution)/shard_map/all_to_all | solution.py:164
  153.6 4.0 %collective-permute-start.17 = (bf16[384,256]{1,0:T(8,128)(2,1)S(1)}, bf16[384,256]{1,0:T(8,128)(2,1)S(1)}, u32[]{:S(2)}, u32[]{:S(2)}) collective-permute-start(bf16[384,256]{1,0:T(8,128)(2,1)S(1)} %get-tuple-element.25), channel_id=1, source_target_pairs={{0,14},{1,15},{2,0},{3,1},{4,2},{5,3},{6,4},{7,5},{8,6},{9,7},{10,... | collective-permute-start | bytes 589832 | tf_op jit(solution)/shard_map/ppermute | solution.py:23
  158.6 1.9 %collective-permute-start.16 = (bf16[384,256]{1,0:T(8,128)(2,1)S(1)}, bf16[384,256]{1,0:T(8,128)(2,1)S(1)}, u32[]{:S(2)}, u32[]{:S(2)}) collective-permute-start(bf16[384,256]{1,0:T(8,128)(2,1)S(1)} %fusion.18), channel_id=1, source_target_pairs={{0,2},{1,3},{2,4},{3,5},{4,6},{5,7},{6,8},{7,9},{8,10},{9,11},{10,... | collective-permute-start | bytes 589832 | tf_op jit(solution)/shard_map/ppermute | solution.py:23
  160.6 6.0 %collective-permute-done.16 = bf16[384,256]{1,0:T(8,128)(2,1)S(1)} collective-permute-done((bf16[384,256]{1,0:T(8,128)(2,1)S(1)}, bf16[384,256]{1,0:T(8,128)(2,1)S(1)}, u32[]{:S(2)}, u32[]{:S(2)}) %collective-permute-start.16) | collective-permute-done | bytes 196640 | tf_op jit(solution)/shard_map/ppermute | solution.py:23
  (97 shorter events, 26.4 us)
Async XLA Ops:
  0.6 12.1 %copy-start = (bf16[16,128,128]{2,1,0:T(8,128)(2,1)S(1)}, bf16[16,128,128]{2,1,0:T(8,128)(2,1)}, u32[]{:S(2)}) copy-start(bf16[16,128,128]{2,1,0:T(8,128)(2,1)} %param.15) | copy-start | bytes 1572868
  0.6 6.4 %copy-start.1 = (bf16[128,4096]{1,0:T(8,128)(2,1)S(1)}, bf16[128,4096]{1,0:T(8,128)(2,1)}, u32[]{:S(2)}) copy-start(bf16[128,4096]{1,0:T(8,128)(2,1)} %param.18) | copy-start | bytes 3145732
  0.7 6.8 %copy-start.13 = (s32[128,4]{0,1:T(4,128)S(1)}, s32[128,4]{0,1:T(4,128)}, u32[]{:S(2)}) copy-start(s32[128,4]{0,1:T(4,128)} %param.20) | copy-start | bytes 6148
  0.7 6.9 %copy-start.12 = (f32[4096]{0:T(1024)S(1)}, f32[4096]{0:T(1024)}, u32[]{:S(2)}) copy-start(f32[4096]{0:T(1024)} %param.19) | copy-start | bytes 49156
  1.5 11.2 %collective-permute-start = (bf16[15,128]{1,0:T(8,128)(2,1)S(1)}, bf16[15,128]{1,0:T(8,128)(2,1)S(1)}, u32[]{:S(2)}, u32[]{:S(2)}) collective-permute-start(bf16[15,128]{1,0:T(8,128)(2,1)S(1)} %slice.173), channel_id=1, source_target_pairs={{0,16},{16,32},{32,48},{48,64},{64,80},{80,96},{96,112},{112,128},... | collective-permute-start | bytes 11528 | tf_op jit(solution)/shard_map/ppermute | solution.py:18
  13.7 19.1 %copy-start.5 = (bf16[1,4096,64]{1,2,0:T(8,128)(2,1)S(1)}, bf16[1,4096,64]{1,2,0:T(8,128)(2,1)}, u32[]{:S(2)}) copy-start(bf16[1,4096,64]{1,2,0:T(8,128)(2,1)} %param.22) | copy-start | bytes 1572868
  13.7 21.3 %copy-start.6 = (bf16[1,4096,64]{1,2,0:T(8,128)(2,1)S(1)}, bf16[1,4096,64]{1,2,0:T(8,128)(2,1)}, u32[]{:S(2)}) copy-start(bf16[1,4096,64]{1,2,0:T(8,128)(2,1)} %param.23) | copy-start | bytes 1572868
  17.3 37.6 %collective-permute-start.1 = (bf16[8,384,256]{2,1,0:T(8,128)(2,1)}, bf16[8,384,256]{2,1,0:T(8,128)(2,1)}, u32[]{:S(2)}, u32[]{:S(2)}) collective-permute-start(bf16[8,384,256]{2,1,0:T(8,128)(2,1)} %get-tuple-element.16), channel_id=1, source_target_pairs={{0,1},{1,0},{2,3},{3,2},{4,5},{5,4},{6,7},{7,6},{8,9},{9,8},{10,11... | collective-permute-start | bytes 4718600 | tf_op jit(solution)/shard_map/ppermute | solution.py:28
  23.4 31.5 %all-to-all-start = ((bf16[32,24,512]{2,1,0:T(8,128)(2,1)}), bf16[32,24,512]{2,1,0:T(8,128)(2,1)S(1)}, u32[]{:S(2)}, u32[]{:S(2)}) async-start(bf16[32,24,512]{2,1,0:T(8,128)(2,1)} %bitcast.24), calls=%async_computation | async-start | bytes 1572864 | tf_op jit(solution)/shard_map/all_to_all | solution.py:164
  32.8 4.4 %collective-permute-start.6 = (bf16[64,4096]{1,0:T(8,128)(2,1)S(1)}, bf16[64,4096]{1,0:T(8,128)(2,1)S(1)}, u32[]{:S(2)}, u32[]{:S(2)}) collective-permute-start(bf16[64,4096]{1,0:T(8,128)(2,1)S(1)} %bitcast.127), channel_id=1, source_target_pairs={{0,1},{1,0},{2,3},{3,2},{4,5},{5,4},{6,7},{7,6},{8,9},{9,8},{10,11... | collective-permute-start | bytes 1572872 | tf_op jit(solution)/shard_map/ppermute | solution.py:28
  35.0 3.8 %collective-permute-start.7 = (bf16[64,4096]{1,0:T(8,128)(2,1)S(1)}, bf16[64,4096]{1,0:T(8,128)(2,1)S(1)}, u32[]{:S(2)}, u32[]{:S(2)}) collective-permute-start(bf16[64,4096]{1,0:T(8,128)(2,1)S(1)} %bitcast.129), channel_id=1, source_target_pairs={{0,1},{1,0},{2,3},{3,2},{4,5},{5,4},{6,7},{7,6},{8,9},{9,8},{10,11... | collective-permute-start | bytes 1572872 | tf_op jit(solution)/shard_map/ppermute | solution.py:28
  42.4 26.1 %copy-start.2 = (bf16[8,256,256]{2,1,0:T(8,128)(2,1)S(1)}, bf16[8,256,256]{2,1,0:T(8,128)(2,1)}, u32[]{:S(2)}) copy-start(bf16[8,256,256]{2,1,0:T(8,128)(2,1)} %shard_map.150) | copy-start | bytes 3145732
  55.0 13.9 %collective-permute-start.9 = (bf16[768,256]{1,0:T(8,128)(2,1)S(1)}, bf16[768,256]{1,0:T(8,128)(2,1)S(1)}, u32[]{:S(2)}, u32[]{:S(2)}) collective-permute-start(bf16[768,256]{1,0:T(8,128)(2,1)S(1)} %get-tuple-element.35), channel_id=1, source_target_pairs={{0,14},{1,15},{2,0},{3,1},{4,2},{5,3},{6,4},{7,5},{8,6},{9,7},{10,... | collective-permute-start | bytes 1179656 | tf_op jit(solution)/shard_map/ppermute | solution.py:23
  60.1 12.4 %collective-permute-start.8 = (bf16[768,256]{1,0:T(8,128)(2,1)S(1)}, bf16[768,256]{1,0:T(8,128)(2,1)S(1)}, u32[]{:S(2)}, u32[]{:S(2)}) collective-permute-start(bf16[768,256]{1,0:T(8,128)(2,1)S(1)} %get-tuple-element.35), channel_id=1, source_target_pairs={{0,2},{1,3},{2,4},{3,5},{4,6},{5,7},{6,8},{7,9},{8,10},{9,11},{10,... | collective-permute-start | bytes 1179656 | tf_op jit(solution)/shard_map/ppermute | solution.py:23
  62.0 18.6 %collective-permute-start.10 = (bf16[768,256]{1,0:T(8,128)(2,1)S(1)}, bf16[768,256]{1,0:T(8,128)(2,1)S(1)}, u32[]{:S(2)}, u32[]{:S(2)}) collective-permute-start(bf16[768,256]{1,0:T(8,128)(2,1)S(1)} %get-tuple-element.34), channel_id=1, source_target_pairs={{0,2},{1,3},{2,4},{3,5},{4,6},{5,7},{6,8},{7,9},{8,10},{9,11},{10,... | collective-permute-start | bytes 1179656 | tf_op jit(solution)/shard_map/ppermute | solution.py:23
  63.9 17.0 %collective-permute-start.11 = (bf16[768,256]{1,0:T(8,128)(2,1)S(1)}, bf16[768,256]{1,0:T(8,128)(2,1)S(1)}, u32[]{:S(2)}, u32[]{:S(2)}) collective-permute-start(bf16[768,256]{1,0:T(8,128)(2,1)S(1)} %get-tuple-element.34), channel_id=1, source_target_pairs={{0,14},{1,15},{2,0},{3,1},{4,2},{5,3},{6,4},{7,5},{8,6},{9,7},{10,... | collective-permute-start | bytes 1179656 | tf_op jit(solution)/shard_map/ppermute | solution.py:23
  68.8 14.6 %collective-permute-start.13 = (bf16[768,256]{1,0:T(8,128)(2,1)S(1)}, bf16[768,256]{1,0:T(8,128)(2,1)S(1)}, u32[]{:S(2)}, u32[]{:S(2)}) collective-permute-start(bf16[768,256]{1,0:T(8,128)(2,1)S(1)} %collective-permute-done.9), channel_id=1, source_target_pairs={{0,14},{1,15},{2,0},{3,1},{4,2},{5,3},{6,4},{7,5},{8,6},{9,7},{10,... | collective-permute-start | bytes 1179656 | tf_op jit(solution)/shard_map/ppermute | solution.py:23
  72.5 16.6 %collective-permute-start.12 = (bf16[768,256]{1,0:T(8,128)(2,1)S(1)}, bf16[768,256]{1,0:T(8,128)(2,1)S(1)}, u32[]{:S(2)}, u32[]{:S(2)}) collective-permute-start(bf16[768,256]{1,0:T(8,128)(2,1)S(1)} %collective-permute-done.8), channel_id=1, source_target_pairs={{0,2},{1,3},{2,4},{3,5},{4,6},{5,7},{6,8},{7,9},{8,10},{9,11},{10,... | collective-permute-start | bytes 1179656 | tf_op jit(solution)/shard_map/ppermute | solution.py:23
  89.4 5.8 %collective-permute-start.14 = (f32[128,768]{1,0:T(8,128)S(1)}, f32[128,768]{1,0:T(8,128)S(1)}, u32[]{:S(2)}, u32[]{:S(2)}) collective-permute-start(f32[128,768]{1,0:T(8,128)S(1)} %slice.269), channel_id=1, source_target_pairs={{0,1},{1,0},{2,3},{3,2},{4,5},{5,4},{6,7},{7,6},{8,9},{9,8},{10,11... | collective-permute-start | bytes 1179656 | tf_op jit(solution)/shard_map/ppermute | solution.py:28
  95.2 4.8 %copy-start.3 = (bf16[8,384,256]{2,1,0:T(8,128)(2,1)S(1)}, bf16[8,384,256]{2,1,0:T(8,128)(2,1)}, u32[]{:S(2)}) copy-start(bf16[8,384,256]{2,1,0:T(8,128)(2,1)} %get-tuple-element.15) | copy-start | bytes 4718596
  96.2 28.7 %all-to-all-start.1 = ((bf16[8,64,768]{2,1,0:T(8,128)(2,1)}), bf16[8,64,768]{2,1,0:T(8,128)(2,1)S(1)}, u32[]{:S(2)}, u32[]{:S(2)}) async-start(bf16[8,64,768]{2,1,0:T(8,128)(2,1)} %broadcast_in_dim.79), calls=%async_computation.1 | async-start | bytes 1572864 | tf_op jit(solution)/shard_map/all_to_all | solution.py:226
  100.0 36.8 %copy-start.4 = (bf16[1,1024,256]{2,1,0:T(8,128)(2,1)S(1)}, bf16[1,1024,256]{2,1,0:T(8,128)(2,1)}, u32[]{:S(2)}) copy-start(bf16[1,1024,256]{2,1,0:T(8,128)(2,1)} %param.24) | copy-start | bytes 1572868
  101.2 23.0 %collective-permute-start.2 = (bf16[384,256]{1,0:T(8,128)(2,1)S(1)}, bf16[384,256]{1,0:T(8,128)(2,1)S(1)}, u32[]{:S(2)}, u32[]{:S(2)}) collective-permute-start(bf16[384,256]{1,0:T(8,128)(2,1)S(1)} %get-tuple-element.31), channel_id=1, source_target_pairs={{0,2},{1,3},{2,4},{3,5},{4,6},{5,7},{6,8},{7,9},{8,10},{9,11},{10,... | collective-permute-start | bytes 589832 | tf_op jit(solution)/shard_map/ppermute | solution.py:23
  104.6 20.3 %collective-permute-start.3 = (bf16[384,256]{1,0:T(8,128)(2,1)S(1)}, bf16[384,256]{1,0:T(8,128)(2,1)}, u32[]{:S(2)}, u32[]{:S(2)}) collective-permute-start(bf16[384,256]{1,0:T(8,128)(2,1)S(1)} %get-tuple-element.30), channel_id=1, source_target_pairs={{0,14},{1,15},{2,0},{3,1},{4,2},{5,3},{6,4},{7,5},{8,6},{9,7},{10,... | collective-permute-start | bytes 589832 | tf_op jit(solution)/shard_map/ppermute | solution.py:23
  124.9 21.2 %collective-permute-start.18 = (bf16[8,64,768]{2,1,0:T(8,128)(2,1)S(1)}, bf16[8,64,768]{2,1,0:T(8,128)(2,1)}, u32[]{:S(2)}, u32[]{:S(2)}) collective-permute-start(bf16[8,64,768]{2,1,0:T(8,128)(2,1)S(1)} %all-to-all-done.1), channel_id=1, source_target_pairs={{0,1},{1,0},{2,3},{3,2},{4,5},{5,4},{6,7},{7,6},{8,9},{9,8},{10,11... | collective-permute-start | bytes 2359304 | tf_op jit(solution)/shard_map/ppermute | solution.py:28
  130.3 9.9 %collective-permute-start.4 = (bf16[384,256]{1,0:T(8,128)(2,1)}, bf16[384,256]{1,0:T(8,128)(2,1)}, u32[]{:S(2)}, u32[]{:S(2)}) collective-permute-start(bf16[384,256]{1,0:T(8,128)(2,1)} %get-tuple-element.19), channel_id=1, source_target_pairs={{0,2},{1,3},{2,4},{3,5},{4,6},{5,7},{6,8},{7,9},{8,10},{9,11},{10,... | collective-permute-start | bytes 589832 | tf_op jit(solution)/shard_map/ppermute | solution.py:23
  132.2 8.8 %collective-permute-start.5 = (bf16[384,256]{1,0:T(8,128)(2,1)}, bf16[384,256]{1,0:T(8,128)(2,1)}, u32[]{:S(2)}, u32[]{:S(2)}) collective-permute-start(bf16[384,256]{1,0:T(8,128)(2,1)} %get-tuple-element.20), channel_id=1, source_target_pairs={{0,14},{1,15},{2,0},{3,1},{4,2},{5,3},{6,4},{7,5},{8,6},{9,7},{10,... | collective-permute-start | bytes 589832 | tf_op jit(solution)/shard_map/ppermute | solution.py:23
  142.5 15.1 %collective-permute-start.15 = (bf16[384,256]{1,0:T(8,128)(2,1)S(1)}, bf16[384,256]{1,0:T(8,128)(2,1)S(1)}, u32[]{:S(2)}, u32[]{:S(2)}) collective-permute-start(bf16[384,256]{1,0:T(8,128)(2,1)S(1)} %get-tuple-element.24), channel_id=1, source_target_pairs={{0,2},{1,3},{2,4},{3,5},{4,6},{5,7},{6,8},{7,9},{8,10},{9,11},{10,... | collective-permute-start | bytes 589832 | tf_op jit(solution)/shard_map/ppermute | solution.py:23
  146.1 7.4 %copy-start.14 = (f32[128,4]{0,1:T(4,128)S(1)}, f32[128,4]{0,1:T(4,128)}, u32[]{:S(2)}) copy-start(f32[128,4]{0,1:T(4,128)} %param.21) | copy-start | bytes 6148
  148.4 19.8 %all-to-all-start.2 = ((bf16[32,24,256]{2,1,0:T(8,128)(2,1)}), bf16[32,24,256]{2,1,0:T(8,128)(2,1)S(1)}, u32[]{:S(2)}, u32[]{:S(2)}) async-start(bf16[32,24,256]{2,1,0:T(8,128)(2,1)} %bitcast.44), calls=%async_computation.2 | async-start | bytes 786432 | tf_op jit(solution)/shard_map/all_to_all | solution.py:164
  153.6 7.0 %collective-permute-start.17 = (bf16[384,256]{1,0:T(8,128)(2,1)S(1)}, bf16[384,256]{1,0:T(8,128)(2,1)S(1)}, u32[]{:S(2)}, u32[]{:S(2)}) collective-permute-start(bf16[384,256]{1,0:T(8,128)(2,1)S(1)} %get-tuple-element.25), channel_id=1, source_target_pairs={{0,14},{1,15},{2,0},{3,1},{4,2},{5,3},{6,4},{7,5},{8,6},{9,7},{10,... | collective-permute-start | bytes 589832 | tf_op jit(solution)/shard_map/ppermute | solution.py:23
  158.6 7.9 %collective-permute-start.16 = (bf16[384,256]{1,0:T(8,128)(2,1)S(1)}, bf16[384,256]{1,0:T(8,128)(2,1)S(1)}, u32[]{:S(2)}, u32[]{:S(2)}) collective-permute-start(bf16[384,256]{1,0:T(8,128)(2,1)S(1)} %fusion.18), channel_id=1, source_target_pairs={{0,2},{1,3},{2,4},{3,5},{4,6},{5,7},{6,8},{7,9},{8,10},{9,11},{10,... | collective-permute-start | bytes 589832 | tf_op jit(solution)/shard_map/ppermute | solution.py:23
  (6 other events, 8.6 us)

commit v4 on v3

--- a/solution.py
+++ b/solution.py
@@ -185,7 +185,9 @@
     up_t = expert_up[0].T
     units = gate_t.shape[0]
     blocks = jax.ShapeDtypeStruct((y_size, 4 * units, slice_width), bf16)
-    weights = local_kernel(weight_kernel, index, (gate_t, up_t, to_partner(gate_t), to_partner(up_t)), blocks)
+    partner_gate = to_partner(gate_t)
+    partner_up = to_partner(up_t)
+    weights = local_kernel(weight_kernel, index, (gate_t, up_t, partner_gate, partner_up), blocks)
 
     def part(j):
         return kept[j].astype(f32) + from_partner[j].astype(f32)
@@ -196,7 +198,6 @@
         rs_up, rs_down = lax.optimization_barrier((rs_up, rs_down))
         return along_y(rs_up, 1), along_y(rs_down, -1)
 
-    arrived = after(arrived, (from_partner, weights))
     near = arrived[:, :slice_width]
     far = arrived[:, slice_width:]
 
@@ -224,7 +225,6 @@
     copies = jnp.broadcast_to(hidden[None], (y_size, *hidden.shape))
     groups = [[2 * i + c for i in range(y_size)] for c in range(2)]
     own_hidden = lax.all_to_all(copies, "tp", 0, 0, axis_index_groups=groups, tiled=True)
-    rs_up, rs_down = after((rs_up, rs_down), own_hidden)
     rs_up, rs_down = reduced(rs_up, rs_down, 2)
     other_hidden = to_partner(own_hidden)
     down_weight = expert_down[0].reshape(y_size, 2, units, slice_width)

time: 172 us -> 165 us (0.959)
  waiting for transfers between devices: 54.9 us -> 41.9 us
  starting transfers between devices: 81.5 us -> 85.4 us
  matrix products: 9.92 us -> 12.9 us
    ppermute x13, waiting for transfers between devices: 39.4 us -> 31.5 us  [along_y(): return lax.ppermute(x, 'tp', [(i, (i + 2 * step) % n) for i in range(n)])]
    all_to_all x2, starting transfers between devices: 14.5 us -> 19.5 us  [exchanged(): return lax.all_to_all(rows, 'ep', split_axis=0, concat_axis=0, tiled=True)]
    ppermute x5, waiting for transfers between devices: 2.98 us -> 0.01 us  [to_partner(): return lax.ppermute(x, 'tp', [(i, i ^ 1) for i in range(n)])]
    dot_general x8, matrix products: 2.44 us -> 5.41 us  [tdot(): lax.dot_general(a, b, (((1,), (1,)), ((), ())), preferred_element_type=f32)]
    all_to_all x2, waiting for transfers between devices: 12.5 us -> 10.4 us  [exchanged(): return lax.all_to_all(rows, 'ep', split_axis=0, concat_axis=0, tiled=True)]
  transfers between devices with their start and end apart: 22 -> 22, of which waited for: 10 -> 7; matrix products, arithmetic and copies ran while one was open for 11% -> 13% of each run, Pallas kernels for 2% -> 4%
where the time goes in v4:
time: 165 us; the launch traced here: 163 us
  starting transfers between devices  85.4 us (52%)
  waiting for transfers between devices  41.9 us (25%)
  matrix products  12.9 us (8%)
  other arithmetic  10.1 us (6%)
  Pallas kernels  6.27 us (4%)
  local copies, waits for them, and re-layouts  4.88 us (3%)
    ppermute x13, starting transfers between devices, along_y(): return lax.ppermute(x, 'tp', [(i, (i + 2 * step) % n) for i in range(n)])  42.3 us
    ppermute x13, waiting for transfers between devices, along_y(): return lax.ppermute(x, 'tp', [(i, (i + 2 * step) % n) for i in range(n)])  31.5 us
    all_to_all x2, starting transfers between devices, exchanged(): return lax.all_to_all(rows, 'ep', split_axis=0, concat_axis=0, tiled=True)  19.5 us
    ppermute x5, starting transfers between devices, to_partner(): return lax.ppermute(x, 'tp', [(i, i ^ 1) for i in range(n)])  16.4 us
    all_to_all x2, waiting for transfers between devices, exchanged(): return lax.all_to_all(rows, 'ep', split_axis=0, concat_axis=0, tiled=True)  10.4 us
    pallas_call x2, Pallas kernels, local_kernel(): pl.pallas_call(body, in_specs=[smem] + [vmem] * len(operands), out_specs=...  6.27 us
    dot_general x8, matrix products, tdot(): lax.dot_general(a, b, (((1,), (1,)), ((), ())), preferred_element_type=f32)  5.41 us
    all_to_all x1, starting transfers between devices, per_device(): lax.all_to_all(copies, 'tp', 0, 0, axis_index_groups=groups, tiled=True)  3.8 us
  transfers between devices with their start and end apart: 22, of which 7 were waited for; matrix products, arithmetic and copies ran while one was open for 13% of the time, Pallas kernels for 4%

profile of v4, /device:TPU:1, one launch (start us, length us, event | category | flops | bytes accessed | tf_op | source)
XLA Modules:
  0.0 162.8 jit_solution(2007664981119133548)
XLA Ops:
  0.7 1.6 convert_reduce_fusion
  4.7 13.7 %all-to-all-start = ((bf16[32,24,512]{2,1,0:T(8,128)(2,1)}), bf16[32,24,512]{2,1,0:T(8,128)(2,1)S(1)}, u32[]{:S(2)}, u32[]{:S(2)}) async-start(bf16[32,24,512]{2,1,0:T(8,128)(2,1)} %bitcast.30), calls=%async_computation | async-start | bytes 1572864 | tf_op jit(solution)/shard_map/all_to_all | solution.py:164
  18.4 2.9 %collective-permute-start.10 = (bf16[64,4096]{1,0:T(8,128)(2,1)S(1)}, bf16[64,4096]{1,0:T(8,128)(2,1)}, u32[]{:S(2)}, u32[]{:S(2)}) collective-permute-start(bf16[64,4096]{1,0:T(8,128)(2,1)S(1)} %bitcast.129), channel_id=1, source_target_pairs={{0,1},{1,0},{2,3},{3,2},{4,5},{5,4},{6,7},{7,6},{8,9},{9,8},{10,11... | collective-permute-start | bytes 1572872 | tf_op jit(solution)/shard_map/ppermute | solution.py:28
  21.3 1.9 %collective-permute-start.9 = (bf16[64,4096]{1,0:T(8,128)(2,1)S(1)}, bf16[64,4096]{1,0:T(8,128)(2,1)}, u32[]{:S(2)}, u32[]{:S(2)}) collective-permute-start(bf16[64,4096]{1,0:T(8,128)(2,1)S(1)} %bitcast.127), channel_id=1, source_target_pairs={{0,1},{1,0},{2,3},{3,2},{4,5},{5,4},{6,7},{7,6},{8,9},{9,8},{10,11... | collective-permute-start | bytes 1572872 | tf_op jit(solution)/shard_map/ppermute | solution.py:28
  23.2 3.4 %collective-permute-start = (bf16[15,128]{1,0:T(8,128)(2,1)S(1)}, bf16[15,128]{1,0:T(8,128)(2,1)S(1)}, u32[]{:S(2)}, u32[]{:S(2)}) collective-permute-start(bf16[15,128]{1,0:T(8,128)(2,1)S(1)} %slice.173), channel_id=1, source_target_pairs={{0,16},{16,32},{32,48},{48,64},{64,80},{80,96},{96,112},{112,128},... | collective-permute-start | bytes 11528 | tf_op jit(solution)/shard_map/ppermute | solution.py:18
  29.1 10.4 %all-to-all-done = bf16[32,24,512]{2,1,0:T(8,128)(2,1)S(1)} async-done(((bf16[32,24,512]{2,1,0:T(8,128)(2,1)}), bf16[32,24,512]{2,1,0:T(8,128)(2,1)S(1)}, u32[]{:S(2)}, u32[]{:S(2)}) %all-to-all-start) | async-done | bytes 786464 | tf_op jit(solution)/shard_map/all_to_all | solution.py:164
  40.4 5.1 %collective-permute-start.12 = (bf16[768,256]{1,0:T(8,128)(2,1)}, bf16[768,256]{1,0:T(8,128)(2,1)}, u32[]{:S(2)}, u32[]{:S(2)}) collective-permute-start(bf16[768,256]{1,0:T(8,128)(2,1)} %get-tuple-element.29), channel_id=1, source_target_pairs={{0,14},{1,15},{2,0},{3,1},{4,2},{5,3},{6,4},{7,5},{8,6},{9,7},{10,... | collective-permute-start | bytes 1179656 | tf_op jit(solution)/shard_map/ppermute | solution.py:23
  45.5 1.9 %collective-permute-start.11 = (bf16[768,256]{1,0:T(8,128)(2,1)}, bf16[768,256]{1,0:T(8,128)(2,1)}, u32[]{:S(2)}, u32[]{:S(2)}) collective-permute-start(bf16[768,256]{1,0:T(8,128)(2,1)} %get-tuple-element.29), channel_id=1, source_target_pairs={{0,2},{1,3},{2,4},{3,5},{4,6},{5,7},{6,8},{7,9},{8,10},{9,11},{10,... | collective-permute-start | bytes 1179656 | tf_op jit(solution)/shard_map/ppermute | solution.py:23
  48.0 2.7 %shard_map.150 = bf16[8,256,256]{2,1,0:T(8,128)(2,1)} custom-call(s32[2,8]{1,0:T(2,128)} %pad_add_fusion.index, bf16[64,4096]{1,0:T(8,128)(2,1)} %bitcast.126, bf16[64,4096]{1,0:T(8,128)(2,1)} %bitcast.128, bf16[64,4096]{1,0:T(8,128)(2,1)} %collective-permute-done.9.partner_gate, bf16[64,4096]{1,0:T(8,128)(2,1)} %collective-permute-done.10.partner_up), custom_call_target="tpu_custom_call" | custom-call | tf_op jit(solution)/shard_map/pallas_call | solution.py:43
  50.7 4.7 %collective-permute-start.14 = (bf16[768,256]{1,0:T(8,128)(2,1)S(1)}, bf16[768,256]{1,0:T(8,128)(2,1)S(1)}, u32[]{:S(2)}, u32[]{:S(2)}) collective-permute-start(bf16[768,256]{1,0:T(8,128)(2,1)S(1)} %copy-done.7), channel_id=1, source_target_pairs={{0,14},{1,15},{2,0},{3,1},{4,2},{5,3},{6,4},{7,5},{8,6},{9,7},{10,... | collective-permute-start | bytes 1179656 | tf_op jit(solution)/shard_map/ppermute | solution.py:23
  55.4 1.9 %collective-permute-start.13 = (bf16[768,256]{1,0:T(8,128)(2,1)S(1)}, bf16[768,256]{1,0:T(8,128)(2,1)S(1)}, u32[]{:S(2)}, u32[]{:S(2)}) collective-permute-start(bf16[768,256]{1,0:T(8,128)(2,1)S(1)} %copy-done.7), channel_id=1, source_target_pairs={{0,2},{1,3},{2,4},{3,5},{4,6},{5,7},{6,8},{7,9},{8,10},{9,11},{10,... | collective-permute-start | bytes 1179656 | tf_op jit(solution)/shard_map/ppermute | solution.py:23
  58.6 4.6 %collective-permute-start.16 = (bf16[768,256]{1,0:T(8,128)(2,1)}, bf16[768,256]{1,0:T(8,128)(2,1)S(1)}, u32[]{:S(2)}, u32[]{:S(2)}) collective-permute-start(bf16[768,256]{1,0:T(8,128)(2,1)} %collective-permute-done.12), channel_id=1, source_target_pairs={{0,14},{1,15},{2,0},{3,1},{4,2},{5,3},{6,4},{7,5},{8,6},{9,7},{10,... | collective-permute-start | bytes 1179656 | tf_op jit(solution)/shard_map/ppermute | solution.py:23
  63.2 1.9 %collective-permute-start.15 = (bf16[768,256]{1,0:T(8,128)(2,1)}, bf16[768,256]{1,0:T(8,128)(2,1)S(1)}, u32[]{:S(2)}, u32[]{:S(2)}) collective-permute-start(bf16[768,256]{1,0:T(8,128)(2,1)} %collective-permute-done.11), channel_id=1, source_target_pairs={{0,2},{1,3},{2,4},{3,5},{4,6},{5,7},{6,8},{7,9},{8,10},{9,11},{10,... | collective-permute-start | bytes 1179656 | tf_op jit(solution)/shard_map/ppermute | solution.py:23
  69.3 4.6 %collective-permute-done.15 = bf16[768,256]{1,0:T(8,128)(2,1)S(1)} collective-permute-done((bf16[768,256]{1,0:T(8,128)(2,1)}, bf16[768,256]{1,0:T(8,128)(2,1)S(1)}, u32[]{:S(2)}, u32[]{:S(2)}) %collective-permute-start.15) | collective-permute-done | bytes 393248 | tf_op jit(solution)/shard_map/ppermute | solution.py:23
  74.3 6.4 %collective-permute-start.17 = (f32[128,768]{1,0:T(8,128)S(1)}, f32[128,768]{1,0:T(8,128)S(1)}, u32[]{:S(2)}, u32[]{:S(2)}) collective-permute-start(f32[128,768]{1,0:T(8,128)S(1)} %slice.273), channel_id=1, source_target_pairs={{0,1},{1,0},{2,3},{3,2},{4,5},{5,4},{6,7},{7,6},{8,9},{9,8},{10,11... | collective-permute-start | bytes 1179656 | tf_op jit(solution)/shard_map/ppermute | solution.py:28
  82.6 3.6 %shard_map.149 = (bf16[8,384,256]{2,1,0:T(8,128)(2,1)}, bf16[8,384,256]{2,1,0:T(8,128)(2,1)}) custom-call(s32[2,8]{1,0:T(2,128)} %pad_add_fusion.index, bf16[256,128]{1,0:T(8,128)(2,1)} %fusion.12.group, bf16[128,32]{1,0:T(8,128)(2,1)} %fusion.13.hidden, bf16[128,4096]{1,0:T(8,128)(2,1)} %proj.1, bf16[32,4096]{1,0:T(8,128)(2,1)} %down.1), custom_call_target="tpu_custom_call" | custom-call | tf_op jit(solution)/shard_map/pallas_call | solution.py:43
  86.2 1.9 %collective-permute-start.1 = (bf16[8,384,256]{2,1,0:T(8,128)(2,1)}, bf16[8,384,256]{2,1,0:T(8,128)(2,1)}, u32[]{:S(2)}, u32[]{:S(2)}) collective-permute-start(bf16[8,384,256]{2,1,0:T(8,128)(2,1)} %get-tuple-element.13), channel_id=1, source_target_pairs={{0,1},{1,0},{2,3},{3,2},{4,5},{5,4},{6,7},{7,6},{8,9},{9,8},{10,11... | collective-permute-start | bytes 4718600 | tf_op jit(solution)/shard_map/ppermute | solution.py:28
  89.2 3.8 %all-to-all-start.1 = ((bf16[8,64,768]{2,1,0:T(8,128)(2,1)}), bf16[8,64,768]{2,1,0:T(8,128)(2,1)S(1)}, u32[]{:S(2)}, u32[]{:S(2)}) async-start(bf16[8,64,768]{2,1,0:T(8,128)(2,1)} %broadcast_in_dim.89), calls=%async_computation.1 | async-start | bytes 1572864 | tf_op jit(solution)/shard_map/all_to_all | solution.py:227
  94.2 3.4 %collective-permute-start.2 = (bf16[384,256]{1,0:T(8,128)(2,1)S(1)}, bf16[384,256]{1,0:T(8,128)(2,1)S(1)}, u32[]{:S(2)}, u32[]{:S(2)}) collective-permute-start(bf16[384,256]{1,0:T(8,128)(2,1)S(1)} %get-tuple-element.25), channel_id=1, source_target_pairs={{0,2},{1,3},{2,4},{3,5},{4,6},{5,7},{6,8},{7,9},{8,10},{9,11},{10,... | collective-permute-start | bytes 589832 | tf_op jit(solution)/shard_map/ppermute | solution.py:23
  97.6 3.1 %collective-permute-start.3 = (bf16[384,256]{1,0:T(8,128)(2,1)S(1)}, bf16[384,256]{1,0:T(8,128)(2,1)}, u32[]{:S(2)}, u32[]{:S(2)}) collective-permute-start(bf16[384,256]{1,0:T(8,128)(2,1)S(1)} %get-tuple-element.24), channel_id=1, source_target_pairs={{0,14},{1,15},{2,0},{3,1},{4,2},{5,3},{6,4},{7,5},{8,6},{9,7},{10,... | collective-permute-start | bytes 589832 | tf_op jit(solution)/shard_map/ppermute | solution.py:23
  100.7 16.5 %collective-permute-done.2 = bf16[384,256]{1,0:T(8,128)(2,1)S(1)} collective-permute-done((bf16[384,256]{1,0:T(8,128)(2,1)S(1)}, bf16[384,256]{1,0:T(8,128)(2,1)S(1)}, u32[]{:S(2)}, u32[]{:S(2)}) %collective-permute-start.2) | collective-permute-done | bytes 196640 | tf_op jit(solution)/shard_map/ppermute | solution.py:23
  117.9 3.3 %collective-permute-start.18 = (bf16[8,64,768]{2,1,0:T(8,128)(2,1)S(1)}, bf16[8,64,768]{2,1,0:T(8,128)(2,1)}, u32[]{:S(2)}, u32[]{:S(2)}) collective-permute-start(bf16[8,64,768]{2,1,0:T(8,128)(2,1)S(1)} %all-to-all-done.1), channel_id=1, source_target_pairs={{0,1},{1,0},{2,3},{3,2},{4,5},{5,4},{6,7},{7,6},{8,9},{9,8},{10,11... | collective-permute-start | bytes 2359304 | tf_op jit(solution)/shard_map/ppermute | solution.py:28
  121.2 2.1 %fusion.15 = (bf16[384,256]{1,0:T(8,128)(2,1)}, bf16[384,256]{1,0:T(8,128)(2,1)}) fusion(bf16[384,256]{1,0:T(8,128)(2,1)} %collective-permute-done.3, bf16[8,384,256]{2,1,0:T(8,128)(2,1)} %collective-permute-done.1, bf16[8,384,256]{2,1,0:T(8,128)(2,1)S(1)} %copy-done.3, bf16[384,256]{1,0:T(8,128)(2,1)} %copy-done.9), kind=kLoop, calls=%fused_computation.42 | loop fusion | flops 1179648 | bytes 1572864 | tf_op jit(solution)/shard_map/convert_element_type | solution.py:197
  123.3 1.9 %collective-permute-start.4 = (bf16[384,256]{1,0:T(8,128)(2,1)}, bf16[384,256]{1,0:T(8,128)(2,1)}, u32[]{:S(2)}, u32[]{:S(2)}) collective-permute-start(bf16[384,256]{1,0:T(8,128)(2,1)} %get-tuple-element.16), channel_id=1, source_target_pairs={{0,2},{1,3},{2,4},{3,5},{4,6},{5,7},{6,8},{7,9},{8,10},{9,11},{10,... | collective-permute-start | bytes 589832 | tf_op jit(solution)/shard_map/ppermute | solution.py:23
  125.2 4.6 %collective-permute-start.5 = (bf16[384,256]{1,0:T(8,128)(2,1)}, bf16[384,256]{1,0:T(8,128)(2,1)}, u32[]{:S(2)}, u32[]{:S(2)}) collective-permute-start(bf16[384,256]{1,0:T(8,128)(2,1)} %get-tuple-element.17), channel_id=1, source_target_pairs={{0,14},{1,15},{2,0},{3,1},{4,2},{5,3},{6,4},{7,5},{8,6},{9,7},{10,... | collective-permute-start | bytes 589832 | tf_op jit(solution)/shard_map/ppermute | solution.py:23
  129.9 3.3 %collective-permute-done.4 = bf16[384,256]{1,0:T(8,128)(2,1)} collective-permute-done((bf16[384,256]{1,0:T(8,128)(2,1)}, bf16[384,256]{1,0:T(8,128)(2,1)}, u32[]{:S(2)}, u32[]{:S(2)}) %collective-permute-start.4) | collective-permute-done | bytes 196640 | tf_op jit(solution)/shard_map/ppermute | solution.py:23
  135.4 3.2 %collective-permute-start.6 = (bf16[384,256]{1,0:T(8,128)(2,1)S(1)}, bf16[384,256]{1,0:T(8,128)(2,1)S(1)}, u32[]{:S(2)}, u32[]{:S(2)}) collective-permute-start(bf16[384,256]{1,0:T(8,128)(2,1)S(1)} %get-tuple-element.18), channel_id=1, source_target_pairs={{0,2},{1,3},{2,4},{3,5},{4,6},{5,7},{6,8},{7,9},{8,10},{9,11},{10,... | collective-permute-start | bytes 589832 | tf_op jit(solution)/shard_map/ppermute | solution.py:23
  139.1 2.3 %fusion.10 = bf16[768,256]{1,0:T(8,128)(2,1)} fusion(f32[768,256]{1,0:T(8,128)S(1)} %fusion.96, bf16[512,768]{1,0:T(8,128)(2,1)} %bitcast.42, bf16[512,256]{1,0:T(8,128)(2,1)S(1)} %bitcast.123), kind=kOutput, calls=%fused_computation.16 | convolution fusion | flops 201719808 | bytes 2228224 | tf_op jit(solution)/shard_map/dot_general | solution.py:235
  141.4 5.8 %all-to-all-start.2 = ((bf16[32,24,256]{2,1,0:T(8,128)(2,1)}), bf16[32,24,256]{2,1,0:T(8,128)(2,1)S(1)}, u32[]{:S(2)}, u32[]{:S(2)}) async-start(bf16[32,24,256]{2,1,0:T(8,128)(2,1)} %bitcast.44), calls=%async_computation.2 | async-start | bytes 786432 | tf_op jit(solution)/shard_map/all_to_all | solution.py:164
  147.2 4.0 %collective-permute-start.8 = (bf16[384,256]{1,0:T(8,128)(2,1)S(1)}, bf16[384,256]{1,0:T(8,128)(2,1)S(1)}, u32[]{:S(2)}, u32[]{:S(2)}) collective-permute-start(bf16[384,256]{1,0:T(8,128)(2,1)S(1)} %get-tuple-element.19), channel_id=1, source_target_pairs={{0,14},{1,15},{2,0},{3,1},{4,2},{5,3},{6,4},{7,5},{8,6},{9,7},{10,... | collective-permute-start | bytes 589832 | tf_op jit(solution)/shard_map/ppermute | solution.py:23
  152.2 1.9 %collective-permute-start.7 = (bf16[384,256]{1,0:T(8,128)(2,1)S(1)}, bf16[384,256]{1,0:T(8,128)(2,1)S(1)}, u32[]{:S(2)}, u32[]{:S(2)}) collective-permute-start(bf16[384,256]{1,0:T(8,128)(2,1)S(1)} %fusion.18), channel_id=1, source_target_pairs={{0,2},{1,3},{2,4},{3,5},{4,6},{5,7},{6,8},{7,9},{8,10},{9,11},{10,... | collective-permute-start | bytes 589832 | tf_op jit(solution)/shard_map/ppermute | solution.py:23
  154.2 6.0 %collective-permute-done.7 = bf16[384,256]{1,0:T(8,128)(2,1)S(1)} collective-permute-done((bf16[384,256]{1,0:T(8,128)(2,1)S(1)}, bf16[384,256]{1,0:T(8,128)(2,1)S(1)}, u32[]{:S(2)}, u32[]{:S(2)}) %collective-permute-start.7) | collective-permute-done | bytes 196640 | tf_op jit(solution)/shard_map/ppermute | solution.py:23
  (95 shorter events, 23.1 us)
Async XLA Ops:
  0.6 80.9 %copy-start = (bf16[16,128,128]{2,1,0:T(8,128)(2,1)S(1)}, bf16[16,128,128]{2,1,0:T(8,128)(2,1)}, u32[]{:S(2)}) copy-start(bf16[16,128,128]{2,1,0:T(8,128)(2,1)} %param.15) | copy-start | bytes 1572868
  0.7 2.6 %copy-start.11 = (f32[4096]{0:T(1024)S(1)}, f32[4096]{0:T(1024)}, u32[]{:S(2)}) copy-start(f32[4096]{0:T(1024)} %param.19) | copy-start | bytes 49156
  2.7 15.7 %copy-start.6 = (bf16[1,4096,64]{1,2,0:T(8,128)(2,1)S(1)}, bf16[1,4096,64]{1,2,0:T(8,128)(2,1)}, u32[]{:S(2)}) copy-start(bf16[1,4096,64]{1,2,0:T(8,128)(2,1)} %param.23) | copy-start | bytes 1572868
  2.7 18.6 %copy-start.5 = (bf16[1,4096,64]{1,2,0:T(8,128)(2,1)S(1)}, bf16[1,4096,64]{1,2,0:T(8,128)(2,1)}, u32[]{:S(2)}) copy-start(bf16[1,4096,64]{1,2,0:T(8,128)(2,1)} %param.22) | copy-start | bytes 1572868
  2.8 20.5 %copy-start.10 = (bf16[256,128]{1,0:T(8,128)(2,1)S(1)}, bf16[256,128]{1,0:T(8,128)(2,1)}, u32[]{:S(2)}) copy-start(bf16[256,128]{1,0:T(8,128)(2,1)} %param.14) | copy-start | bytes 196612
  4.7 34.8 %all-to-all-start = ((bf16[32,24,512]{2,1,0:T(8,128)(2,1)}), bf16[32,24,512]{2,1,0:T(8,128)(2,1)S(1)}, u32[]{:S(2)}, u32[]{:S(2)}) async-start(bf16[32,24,512]{2,1,0:T(8,128)(2,1)} %bitcast.30), calls=%async_computation | async-start | bytes 1572864 | tf_op jit(solution)/shard_map/all_to_all | solution.py:164
  18.4 29.6 %collective-permute-start.10 = (bf16[64,4096]{1,0:T(8,128)(2,1)S(1)}, bf16[64,4096]{1,0:T(8,128)(2,1)}, u32[]{:S(2)}, u32[]{:S(2)}) collective-permute-start(bf16[64,4096]{1,0:T(8,128)(2,1)S(1)} %bitcast.129), channel_id=1, source_target_pairs={{0,1},{1,0},{2,3},{3,2},{4,5},{5,4},{6,7},{7,6},{8,9},{9,8},{10,11... | collective-permute-start | bytes 1572872 | tf_op jit(solution)/shard_map/ppermute | solution.py:28
  21.3 26.7 %collective-permute-start.9 = (bf16[64,4096]{1,0:T(8,128)(2,1)S(1)}, bf16[64,4096]{1,0:T(8,128)(2,1)}, u32[]{:S(2)}, u32[]{:S(2)}) collective-permute-start(bf16[64,4096]{1,0:T(8,128)(2,1)S(1)} %bitcast.127), channel_id=1, source_target_pairs={{0,1},{1,0},{2,3},{3,2},{4,5},{5,4},{6,7},{7,6},{8,9},{9,8},{10,11... | collective-permute-start | bytes 1572872 | tf_op jit(solution)/shard_map/ppermute | solution.py:28
  23.2 58.3 %collective-permute-start = (bf16[15,128]{1,0:T(8,128)(2,1)S(1)}, bf16[15,128]{1,0:T(8,128)(2,1)S(1)}, u32[]{:S(2)}, u32[]{:S(2)}) collective-permute-start(bf16[15,128]{1,0:T(8,128)(2,1)S(1)} %slice.173), channel_id=1, source_target_pairs={{0,16},{16,32},{32,48},{48,64},{64,80},{80,96},{96,112},{112,128},... | collective-permute-start | bytes 11528 | tf_op jit(solution)/shard_map/ppermute | solution.py:18
  40.4 18.2 %collective-permute-start.12 = (bf16[768,256]{1,0:T(8,128)(2,1)}, bf16[768,256]{1,0:T(8,128)(2,1)}, u32[]{:S(2)}, u32[]{:S(2)}) collective-permute-start(bf16[768,256]{1,0:T(8,128)(2,1)} %get-tuple-element.29), channel_id=1, source_target_pairs={{0,14},{1,15},{2,0},{3,1},{4,2},{5,3},{6,4},{7,5},{8,6},{9,7},{10,... | collective-permute-start | bytes 1179656 | tf_op jit(solution)/shard_map/ppermute | solution.py:23
  45.5 17.7 %collective-permute-start.11 = (bf16[768,256]{1,0:T(8,128)(2,1)}, bf16[768,256]{1,0:T(8,128)(2,1)}, u32[]{:S(2)}, u32[]{:S(2)}) collective-permute-start(bf16[768,256]{1,0:T(8,128)(2,1)} %get-tuple-element.29), channel_id=1, source_target_pairs={{0,2},{1,3},{2,4},{3,5},{4,6},{5,7},{6,8},{7,9},{8,10},{9,11},{10,... | collective-permute-start | bytes 1179656 | tf_op jit(solution)/shard_map/ppermute | solution.py:23
  48.0 2.7 %copy-start.7 = (bf16[768,256]{1,0:T(8,128)(2,1)S(1)}, bf16[768,256]{1,0:T(8,128)(2,1)}, u32[]{:S(2)}) copy-start(bf16[768,256]{1,0:T(8,128)(2,1)} %get-tuple-element.28) | copy-start | bytes 1179652
  50.7 15.7 %copy-start.2 = (bf16[8,256,256]{2,1,0:T(8,128)(2,1)S(1)}, bf16[8,256,256]{2,1,0:T(8,128)(2,1)}, u32[]{:S(2)}) copy-start(bf16[8,256,256]{2,1,0:T(8,128)(2,1)} %shard_map.150) | copy-start | bytes 3145732
  50.7 17.0 %collective-permute-start.14 = (bf16[768,256]{1,0:T(8,128)(2,1)S(1)}, bf16[768,256]{1,0:T(8,128)(2,1)S(1)}, u32[]{:S(2)}, u32[]{:S(2)}) collective-permute-start(bf16[768,256]{1,0:T(8,128)(2,1)S(1)} %copy-done.7), channel_id=1, source_target_pairs={{0,14},{1,15},{2,0},{3,1},{4,2},{5,3},{6,4},{7,5},{8,6},{9,7},{10,... | collective-permute-start | bytes 1179656 | tf_op jit(solution)/shard_map/ppermute | solution.py:23
  55.4 12.7 %collective-permute-start.13 = (bf16[768,256]{1,0:T(8,128)(2,1)S(1)}, bf16[768,256]{1,0:T(8,128)(2,1)S(1)}, u32[]{:S(2)}, u32[]{:S(2)}) collective-permute-start(bf16[768,256]{1,0:T(8,128)(2,1)S(1)} %copy-done.7), channel_id=1, source_target_pairs={{0,2},{1,3},{2,4},{3,5},{4,6},{5,7},{6,8},{7,9},{8,10},{9,11},{10,... | collective-permute-start | bytes 1179656 | tf_op jit(solution)/shard_map/ppermute | solution.py:23
  58.6 10.5 %collective-permute-start.16 = (bf16[768,256]{1,0:T(8,128)(2,1)}, bf16[768,256]{1,0:T(8,128)(2,1)S(1)}, u32[]{:S(2)}, u32[]{:S(2)}) collective-permute-start(bf16[768,256]{1,0:T(8,128)(2,1)} %collective-permute-done.12), channel_id=1, source_target_pairs={{0,14},{1,15},{2,0},{3,1},{4,2},{5,3},{6,4},{7,5},{8,6},{9,7},{10,... | collective-permute-start | bytes 1179656 | tf_op jit(solution)/shard_map/ppermute | solution.py:23
  63.2 10.8 %collective-permute-start.15 = (bf16[768,256]{1,0:T(8,128)(2,1)}, bf16[768,256]{1,0:T(8,128)(2,1)S(1)}, u32[]{:S(2)}, u32[]{:S(2)}) collective-permute-start(bf16[768,256]{1,0:T(8,128)(2,1)} %collective-permute-done.11), channel_id=1, source_target_pairs={{0,2},{1,3},{2,4},{3,5},{4,6},{5,7},{6,8},{7,9},{8,10},{9,11},{10,... | collective-permute-start | bytes 1179656 | tf_op jit(solution)/shard_map/ppermute | solution.py:23
  74.3 13.8 %collective-permute-start.17 = (f32[128,768]{1,0:T(8,128)S(1)}, f32[128,768]{1,0:T(8,128)S(1)}, u32[]{:S(2)}, u32[]{:S(2)}) collective-permute-start(f32[128,768]{1,0:T(8,128)S(1)} %slice.273), channel_id=1, source_target_pairs={{0,1},{1,0},{2,3},{3,2},{4,5},{5,4},{6,7},{7,6},{8,9},{9,8},{10,11... | collective-permute-start | bytes 1179656 | tf_op jit(solution)/shard_map/ppermute | solution.py:28
  86.2 6.9 %collective-permute-start.1 = (bf16[8,384,256]{2,1,0:T(8,128)(2,1)}, bf16[8,384,256]{2,1,0:T(8,128)(2,1)}, u32[]{:S(2)}, u32[]{:S(2)}) collective-permute-start(bf16[8,384,256]{2,1,0:T(8,128)(2,1)} %get-tuple-element.13), channel_id=1, source_target_pairs={{0,1},{1,0},{2,3},{3,2},{4,5},{5,4},{6,7},{7,6},{8,9},{9,8},{10,11... | collective-permute-start | bytes 4718600 | tf_op jit(solution)/shard_map/ppermute | solution.py:28
  88.1 4.9 %copy-start.3 = (bf16[8,384,256]{2,1,0:T(8,128)(2,1)S(1)}, bf16[8,384,256]{2,1,0:T(8,128)(2,1)}, u32[]{:S(2)}) copy-start(bf16[8,384,256]{2,1,0:T(8,128)(2,1)} %get-tuple-element.12) | copy-start | bytes 4718596
  89.2 28.7 %all-to-all-start.1 = ((bf16[8,64,768]{2,1,0:T(8,128)(2,1)}), bf16[8,64,768]{2,1,0:T(8,128)(2,1)S(1)}, u32[]{:S(2)}, u32[]{:S(2)}) async-start(bf16[8,64,768]{2,1,0:T(8,128)(2,1)} %broadcast_in_dim.89), calls=%async_computation.1 | async-start | bytes 1572864 | tf_op jit(solution)/shard_map/all_to_all | solution.py:227
  93.0 36.8 %copy-start.4 = (bf16[1,1024,256]{2,1,0:T(8,128)(2,1)S(1)}, bf16[1,1024,256]{2,1,0:T(8,128)(2,1)}, u32[]{:S(2)}) copy-start(bf16[1,1024,256]{2,1,0:T(8,128)(2,1)} %param.24) | copy-start | bytes 1572868
  94.2 23.0 %collective-permute-start.2 = (bf16[384,256]{1,0:T(8,128)(2,1)S(1)}, bf16[384,256]{1,0:T(8,128)(2,1)S(1)}, u32[]{:S(2)}, u32[]{:S(2)}) collective-permute-start(bf16[384,256]{1,0:T(8,128)(2,1)S(1)} %get-tuple-element.25), channel_id=1, source_target_pairs={{0,2},{1,3},{2,4},{3,5},{4,6},{5,7},{6,8},{7,9},{8,10},{9,11},{10,... | collective-permute-start | bytes 589832 | tf_op jit(solution)/shard_map/ppermute | solution.py:23
  97.6 20.3 %collective-permute-start.3 = (bf16[384,256]{1,0:T(8,128)(2,1)S(1)}, bf16[384,256]{1,0:T(8,128)(2,1)}, u32[]{:S(2)}, u32[]{:S(2)}) collective-permute-start(bf16[384,256]{1,0:T(8,128)(2,1)S(1)} %get-tuple-element.24), channel_id=1, source_target_pairs={{0,14},{1,15},{2,0},{3,1},{4,2},{5,3},{6,4},{7,5},{8,6},{9,7},{10,... | collective-permute-start | bytes 589832 | tf_op jit(solution)/shard_map/ppermute | solution.py:23
  117.9 21.2 %collective-permute-start.18 = (bf16[8,64,768]{2,1,0:T(8,128)(2,1)S(1)}, bf16[8,64,768]{2,1,0:T(8,128)(2,1)}, u32[]{:S(2)}, u32[]{:S(2)}) collective-permute-start(bf16[8,64,768]{2,1,0:T(8,128)(2,1)S(1)} %all-to-all-done.1), channel_id=1, source_target_pairs={{0,1},{1,0},{2,3},{3,2},{4,5},{5,4},{6,7},{7,6},{8,9},{9,8},{10,11... | collective-permute-start | bytes 2359304 | tf_op jit(solution)/shard_map/ppermute | solution.py:28
  123.3 9.9 %collective-permute-start.4 = (bf16[384,256]{1,0:T(8,128)(2,1)}, bf16[384,256]{1,0:T(8,128)(2,1)}, u32[]{:S(2)}, u32[]{:S(2)}) collective-permute-start(bf16[384,256]{1,0:T(8,128)(2,1)} %get-tuple-element.16), channel_id=1, source_target_pairs={{0,2},{1,3},{2,4},{3,5},{4,6},{5,7},{6,8},{7,9},{8,10},{9,11},{10,... | collective-permute-start | bytes 589832 | tf_op jit(solution)/shard_map/ppermute | solution.py:23
  125.2 8.8 %collective-permute-start.5 = (bf16[384,256]{1,0:T(8,128)(2,1)}, bf16[384,256]{1,0:T(8,128)(2,1)}, u32[]{:S(2)}, u32[]{:S(2)}) collective-permute-start(bf16[384,256]{1,0:T(8,128)(2,1)} %get-tuple-element.17), channel_id=1, source_target_pairs={{0,14},{1,15},{2,0},{3,1},{4,2},{5,3},{6,4},{7,5},{8,6},{9,7},{10,... | collective-permute-start | bytes 589832 | tf_op jit(solution)/shard_map/ppermute | solution.py:23
  135.4 15.8 %collective-permute-start.6 = (bf16[384,256]{1,0:T(8,128)(2,1)S(1)}, bf16[384,256]{1,0:T(8,128)(2,1)S(1)}, u32[]{:S(2)}, u32[]{:S(2)}) collective-permute-start(bf16[384,256]{1,0:T(8,128)(2,1)S(1)} %get-tuple-element.18), channel_id=1, source_target_pairs={{0,2},{1,3},{2,4},{3,5},{4,6},{5,7},{6,8},{7,9},{8,10},{9,11},{10,... | collective-permute-start | bytes 589832 | tf_op jit(solution)/shard_map/ppermute | solution.py:23
  139.1 8.1 %copy-start.13 = (f32[128,4]{0,1:T(4,128)S(1)}, f32[128,4]{0,1:T(4,128)}, u32[]{:S(2)}) copy-start(f32[128,4]{0,1:T(4,128)} %param.21) | copy-start | bytes 6148
  141.4 20.5 %all-to-all-start.2 = ((bf16[32,24,256]{2,1,0:T(8,128)(2,1)}), bf16[32,24,256]{2,1,0:T(8,128)(2,1)S(1)}, u32[]{:S(2)}, u32[]{:S(2)}) async-start(bf16[32,24,256]{2,1,0:T(8,128)(2,1)} %bitcast.44), calls=%async_computation.2 | async-start | bytes 786432 | tf_op jit(solution)/shard_map/all_to_all | solution.py:164
  147.2 7.0 %collective-permute-start.8 = (bf16[384,256]{1,0:T(8,128)(2,1)S(1)}, bf16[384,256]{1,0:T(8,128)(2,1)S(1)}, u32[]{:S(2)}, u32[]{:S(2)}) collective-permute-start(bf16[384,256]{1,0:T(8,128)(2,1)S(1)} %get-tuple-element.19), channel_id=1, source_target_pairs={{0,14},{1,15},{2,0},{3,1},{4,2},{5,3},{6,4},{7,5},{8,6},{9,7},{10,... | collective-permute-start | bytes 589832 | tf_op jit(solution)/shard_map/ppermute | solution.py:23
  152.2 7.9 %collective-permute-start.7 = (bf16[384,256]{1,0:T(8,128)(2,1)S(1)}, bf16[384,256]{1,0:T(8,128)(2,1)S(1)}, u32[]{:S(2)}, u32[]{:S(2)}) collective-permute-start(bf16[384,256]{1,0:T(8,128)(2,1)S(1)} %fusion.18), channel_id=1, source_target_pairs={{0,2},{1,3},{2,4},{3,5},{4,6},{5,7},{6,8},{7,9},{8,10},{9,11},{10,... | collective-permute-start | bytes 589832 | tf_op jit(solution)/shard_map/ppermute | solution.py:23
  (5 other events, 6.8 us)

commit v5 on v4

--- a/solution.py
+++ b/solution.py
@@ -18,9 +18,12 @@
     return lax.ppermute(block, "ep", [(i - 1, i) for i in devices if i > 0])
 
 
-def along_y(x, step):
-    n = lax.axis_size("tp")
-    return lax.ppermute(x, "tp", [(i, (i + 2 * step) % n) for i in range(n)])
+def sent(x, targets):
+    n = lax.axis_size("tp") // 2
+    route = []
+    for core, (step, to) in targets.items():
+        route += [(2 * i + core, 2 * ((i + step) % n) + to) for i in range(n)]
+    return lax.ppermute(x, "tp", route)
 
 
 def to_partner(x):
@@ -52,7 +55,7 @@
     count, _, width = blocks.shape
     units = gate.shape[0]
     for j in range(count):
-        at = lanes(index[0, j], width)
+        at = lanes(index[j], width)
         for i, source in enumerate((gate, up, partner_gate, partner_up)):
             blocks[j, i * units : (i + 1) * units] = source[:, at]
 
@@ -154,21 +157,25 @@
     centre = values - mean
     rstd = lax.rsqrt(jnp.mean(centre * centre, axis=1, keepdims=True) + eps)
 
-    def normed_slice(far):
-        at = (((y + far) % y_size) * 2 + core) * slice_width
-        mine = lax.dynamic_slice_in_dim(moe_input, at, slice_width, 1).astype(f32)
-        gain = lax.dynamic_slice_in_dim(norm_gain, at, slice_width, 0)
-        return ((mine - mean) * rstd * gain[None, :]).astype(bf16)
+    home = y + core * (y_size // 2)
+    chip_width = 2 * slice_width
+    at = (home % y_size) * chip_width
+    mine = lax.dynamic_slice_in_dim(moe_input, at, chip_width, 1).astype(f32)
+    gain = lax.dynamic_slice_in_dim(norm_gain, at, chip_width, 0)
+    normed_slice = ((mine - mean) * rstd * gain[None, :]).astype(bf16)
 
     def exchanged(rows):
         return lax.all_to_all(rows, "ep", split_axis=0, concat_axis=0, tiled=True)
 
-    both = jnp.concatenate([normed_slice(0), normed_slice(y_size // 2)], axis=1)
-    outgoing = jnp.dot(placing, both, preferred_element_type=f32).astype(bf16)
+    outgoing = jnp.dot(placing, normed_slice, preferred_element_type=f32).astype(bf16)
     arrived = exchanged(outgoing)
     pool_input = after(pool_input, outgoing)
-    turn = (y + jnp.arange(y_size, dtype=jnp.int32)) % y_size
-    index = jnp.stack([turn * 2 + core, turn * 2 + 1 - core]).astype(jnp.int32)
+    upward = jnp.array([4, 3, 2, 1], jnp.int32)
+    downward = jnp.array([5, 6, 7, 0], jnp.int32)
+    kept_ids = jnp.where(core == 0, upward, downward)
+    sent_ids = jnp.where(core == 0, downward, upward)
+    index = (y + jnp.stack([kept_ids, sent_ids])) % y_size
+    near_index = (home + y_size + jnp.array([0, -1, 1, -2, 2], jnp.int32)) % y_size
 
     group_out = pool_group_out(pool_input, earlier_rows, pool_map, pool_scale, tp_rank, ep_rank)
     normed = (centre * rstd * norm_gain[None, :]).astype(bf16)
@@ -176,48 +183,33 @@
     shared_up_val = jnp.dot(normed, shared_up, preferred_element_type=f32)
     shared_hidden = (jax.nn.silu(shared_gate_val) * shared_up_val).astype(bf16)
 
-    shape = jax.ShapeDtypeStruct((y_size, row_count + tok_count, slice_width), bf16)
-    kept, sent = local_kernel(project_kernel, index, (group_out, shared_hidden, out_proj, shared_down), [shape, shape])
-    from_partner = to_partner(sent)
-
+    shape = jax.ShapeDtypeStruct((y_size // 2, row_count + tok_count, chip_width), bf16)
+    kept, given = local_kernel(project_kernel, index, (group_out, shared_hidden, out_proj, shared_down), [shape, shape])
+    from_partner = to_partner(given)
 
     gate_t = expert_gate[0].T
     up_t = expert_up[0].T
     units = gate_t.shape[0]
-    blocks = jax.ShapeDtypeStruct((y_size, 4 * units, slice_width), bf16)
+    blocks = jax.ShapeDtypeStruct((5, 4 * units, chip_width), bf16)
     partner_gate = to_partner(gate_t)
     partner_up = to_partner(up_t)
-    weights = local_kernel(weight_kernel, index, (gate_t, up_t, partner_gate, partner_up), blocks)
+    weights = local_kernel(weight_kernel, near_index, (gate_t, up_t, partner_gate, partner_up), blocks)
 
     def part(j):
         return kept[j].astype(f32) + from_partner[j].astype(f32)
 
-    def reduced(rs_up, rs_down, step):
-        rs_up = (part(4 - step) + rs_up.astype(f32)).astype(bf16)
-        rs_down = (part(5 + step) + rs_down.astype(f32)).astype(bf16)
-        rs_up, rs_down = lax.optimization_barrier((rs_up, rs_down))
-        return along_y(rs_up, 1), along_y(rs_down, -1)
-
-    near = arrived[:, :slice_width]
-    far = arrived[:, slice_width:]
-
-    def product(rows, j):
-        return tdot(weights[j % y_size], rows)
-
-    up = along_y(near, 1)
-    down = along_y(near, -1)
-    up_far = along_y(far, 1)
-    down_far = along_y(far, -1)
-    up_two = along_y(up, 1)
-    down_two = along_y(down, -1)
-    rs_up = along_y(part(4).astype(bf16), 1)
-    rs_down = along_y(part(5).astype(bf16), -1)
-    rs_up, rs_down = lax.optimization_barrier((rs_up, rs_down))
-    rs_up, rs_down = reduced(rs_up, rs_down, 1)
-    summed = product(near, 0) + product(far, 4)
-    summed = summed + product(up, -1) + product(down, 1)
-    summed = summed + product(up_far, 3) + product(down_far, -3)
-    summed = summed + product(up_two, -2) + product(down_two, 2)
+    def ring_step(x):
+        return sent(x.astype(bf16), {0: (1, 0), 1: (-1, 1)})
+
+    up = sent(arrived, {0: (1, 0), 1: (1, 1)})
+    down = sent(arrived, {0: (-1, 0), 1: (-1, 1)})
+    up_two = sent(up, {0: (1, 0)})
+    down_two = sent(down, {0: (-1, 0)})
+    ring = ring_step(part(0))
+    ring = ring_step(part(1) + ring.astype(f32))
+    summed = tdot(weights[0], arrived)
+    for j, rows in enumerate((up, down, up_two, down_two)):
+        summed = summed + tdot(weights[j + 1], rows)
     full = summed[: 2 * units] + to_partner(summed[2 * units :])
     hidden = (jax.nn.silu(full[:units]) * full[units:]).astype(bf16)
 
@@ -225,7 +217,7 @@
     copies = jnp.broadcast_to(hidden[None], (y_size, *hidden.shape))
     groups = [[2 * i + c for i in range(y_size)] for c in range(2)]
     own_hidden = lax.all_to_all(copies, "tp", 0, 0, axis_index_groups=groups, tiled=True)
-    rs_up, rs_down = reduced(rs_up, rs_down, 2)
+    ring = ring_step(part(2) + ring.astype(f32))
     other_hidden = to_partner(own_hidden)
     down_weight = expert_down[0].reshape(y_size, 2, units, slice_width)
 
@@ -239,10 +231,14 @@
     expert_result = down_product(own_hidden, core) + down_product(other_hidden, 1 - core)
     expert_result = expert_result.astype(bf16)
     returned = exchanged(expert_result)
-    rs_up = along_y((part(1) + rs_up.astype(f32)).astype(bf16), 1)
     routed = lax.dot_general(combine, returned, (((0,), (0,)), ((), ())), preferred_element_type=f32)
 
-    total = part(0) + rs_up.astype(f32) + rs_down.astype(f32)
+    done = part(3) + ring.astype(f32)
+    low = done[:, :slice_width]
+    high = done[:, slice_width:]
+    cross = sent(jnp.where(core == 0, high, low).astype(bf16), {0: (1, 1), 1: (0, 0)})
+    straight = sent(low.astype(bf16), {0: (1, 0)})
+    total = cross.astype(f32) + straight.astype(f32) + jnp.where(core == 0, 0.0, high)
     return (total[:row_count].astype(bf16), (routed + total[row_count:]).astype(bf16))
 
 

time: 165 us -> 162 us (0.982)
  waiting for transfers between devices: 41.9 us -> 45.6 us
  matrix products: 12.9 us -> 9.63 us
    ppermute x13 -> x9, starting transfers between devices: 42.3 us -> 27 us  [sent(): return lax.ppermute(x, 'tp', route)]
    ppermute x5, starting transfers between devices: 16.4 us -> 30.5 us  [to_partner(): return lax.ppermute(x, 'tp', [(i, i ^ 1) for i in range(n)])]
    all_to_all x2, waiting for transfers between devices: 10.4 us -> 14 us  [exchanged(): return lax.all_to_all(rows, 'ep', split_axis=0, concat_axis=0, tiled=True)]
    dot_general x8 -> x5, matrix products: 5.41 us -> 3.22 us  [tdot(): lax.dot_general(a, b, (((1,), (1,)), ((), ())), preferred_element_type=f32)]
    convert_element_type x5 -> x4, other arithmetic: 5.75 us -> 4.35 us  [the longest x3 4.3 us: ring_step(): return sent(x.astype(bf16), {0: (1, 0), 1: (-1, 1)})]
    ppermute x13 -> x9, waiting for transfers between devices: 31.5 us -> 30.3 us  [sent(): return lax.ppermute(x, 'tp', route)]
  transfers between devices with their start and end apart: 22 -> 18, of which waited for: 7 -> 6; matrix products, arithmetic and copies ran while one was open for 13% -> 14% of each run, Pallas kernels for 4% -> 4%
where the time goes in v5:
time: 162 us; the launch traced here: 160 us
  starting transfers between devices  83.8 us (52%)
  waiting for transfers between devices  45.6 us (28%)
  matrix products  9.63 us (6%)
  other arithmetic  9.54 us (6%)
  Pallas kernels  6.27 us (4%)
  local copies, waits for them, and re-layouts  4.38 us (3%)
    ppermute x5, starting transfers between devices, to_partner(): return lax.ppermute(x, 'tp', [(i, i ^ 1) for i in range(n)])  30.5 us
    ppermute x9, waiting for transfers between devices, sent(): return lax.ppermute(x, 'tp', route)  30.3 us
    ppermute x9, starting transfers between devices, sent(): return lax.ppermute(x, 'tp', route)  27 us
    all_to_all x2, starting transfers between devices, exchanged(): return lax.all_to_all(rows, 'ep', split_axis=0, concat_axis=0, tiled=True)  18.5 us
    all_to_all x2, waiting for transfers between devices, exchanged(): return lax.all_to_all(rows, 'ep', split_axis=0, concat_axis=0, tiled=True)  14 us
    pallas_call x2, Pallas kernels, local_kernel(): pl.pallas_call(body, in_specs=[smem] + [vmem] * len(operands), out_specs=...  6.27 us
    convert_element_type x3, other arithmetic, ring_step(): return sent(x.astype(bf16), {0: (1, 0), 1: (-1, 1)})  4.3 us
    ppermute x1, starting transfers between devices, halo(): return lax.ppermute(block, 'ep', [(i - 1, i) for i in devices if i > 0])  3.92 us
  transfers between devices with their start and end apart: 18, of which 6 were waited for; matrix products, arithmetic and copies ran while one was open for 14% of the time, Pallas kernels for 4%

profile of v5, /device:TPU:1, one launch (start us, length us, event | category | flops | bytes accessed | tf_op | source)
XLA Modules:
  0.0 160.5 jit_solution(9308299206346609567)
XLA Ops:
  1.5 3.9 %collective-permute-start = (bf16[15,128]{1,0:T(8,128)(2,1)S(1)}, bf16[15,128]{1,0:T(8,128)(2,1)S(1)}, u32[]{:S(2)}, u32[]{:S(2)}) collective-permute-start(bf16[15,128]{1,0:T(8,128)(2,1)S(1)} %slice.140), channel_id=1, source_target_pairs={{0,16},{16,32},{32,48},{48,64},{64,80},{80,96},{96,112},{112,128},... | collective-permute-start | bytes 11528 | tf_op jit(solution)/shard_map/ppermute | solution.py:18
  6.4 1.5 convert_reduce_fusion
  8.7 1.3 convolution_convert_fusion
  10.0 12.7 %all-to-all-start = ((bf16[32,24,512]{2,1,0:T(8,128)(2,1)}), bf16[32,24,512]{2,1,0:T(8,128)(2,1)S(1)}, u32[]{:S(2)}, u32[]{:S(2)}) async-start(bf16[32,24,512]{2,1,0:T(8,128)(2,1)} %bitcast.28), calls=%async_computation | async-start | bytes 1572864 | tf_op jit(solution)/shard_map/all_to_all | solution.py:168
  22.8 3.1 %collective-permute-start.7 = (bf16[64,4096]{1,0:T(8,128)(2,1)}, bf16[64,4096]{1,0:T(8,128)(2,1)}, u32[]{:S(2)}, u32[]{:S(2)}) collective-permute-start(bf16[64,4096]{1,0:T(8,128)(2,1)} %bitcast.22.gate), channel_id=1, source_target_pairs={{0,1},{1,0},{2,3},{3,2},{4,5},{5,4},{6,7},{7,6},{8,9},{9,8},{10,11... | collective-permute-start | bytes 1572872 | tf_op jit(solution)/shard_map/ppermute | solution.py:31
  25.9 1.9 %collective-permute-start.8 = (bf16[64,4096]{1,0:T(8,128)(2,1)}, bf16[64,4096]{1,0:T(8,128)(2,1)}, u32[]{:S(2)}, u32[]{:S(2)}) collective-permute-start(bf16[64,4096]{1,0:T(8,128)(2,1)} %bitcast.24.up), channel_id=1, source_target_pairs={{0,1},{1,0},{2,3},{3,2},{4,5},{5,4},{6,7},{7,6},{8,9},{9,8},{10,11... | collective-permute-start | bytes 1572872 | tf_op jit(solution)/shard_map/ppermute | solution.py:31
  28.9 1.0 fusion.10.hidden
  29.9 14.0 %all-to-all-done = bf16[32,24,512]{2,1,0:T(8,128)(2,1)S(1)} async-done(((bf16[32,24,512]{2,1,0:T(8,128)(2,1)}), bf16[32,24,512]{2,1,0:T(8,128)(2,1)S(1)}, u32[]{:S(2)}, u32[]{:S(2)}) %all-to-all-start) | async-done | bytes 786464 | tf_op jit(solution)/shard_map/all_to_all | solution.py:168
  43.9 5.1 %collective-permute-start.10 = (bf16[768,512]{1,0:T(8,128)(2,1)S(1)}, bf16[768,512]{1,0:T(8,128)(2,1)}, u32[]{:S(2)}, u32[]{:S(2)}) collective-permute-start(bf16[768,512]{1,0:T(8,128)(2,1)S(1)} %bitcast.98), channel_id=1, source_target_pairs={{0,14},{2,0},{4,2},{6,4},{8,6},{10,8},{12,10},{14,12},{1,15},{3,1}... | collective-permute-start | bytes 2359304 | tf_op jit(solution)/shard_map/ppermute | solution.py:26
  49.0 1.9 %collective-permute-start.9 = (bf16[768,512]{1,0:T(8,128)(2,1)S(1)}, bf16[768,512]{1,0:T(8,128)(2,1)S(1)}, u32[]{:S(2)}, u32[]{:S(2)}) collective-permute-start(bf16[768,512]{1,0:T(8,128)(2,1)S(1)} %bitcast.99), channel_id=1, source_target_pairs={{0,2},{2,4},{4,6},{6,8},{8,10},{10,12},{12,14},{14,0},{1,3},{3,5},... | collective-permute-start | bytes 2359304 | tf_op jit(solution)/shard_map/ppermute | solution.py:26
  53.9 3.5 %shard_map.176 = (bf16[4,384,512]{2,1,0:T(8,128)(2,1)}, bf16[4,384,512]{2,1,0:T(8,128)(2,1)}) custom-call(s32[2,4]{1,0:T(2,128)} %and_select_fusion.3.index, bf16[256,128]{1,0:T(8,128)(2,1)} %fusion.9.group, bf16[128,32]{1,0:T(8,128)(2,1)} %fusion.10.hidden, bf16[128,4096]{1,0:T(8,128)(2,1)} %proj.1, bf16[32,4096]{1,0:T(8,128)(2,1)} %down.1), custom_call_target="tpu_custom_call" | custom-call | tf_op jit(solution)/shard_map/pallas_call | solution.py:46
  57.4 5.0 %collective-permute-start.1 = (bf16[4,384,512]{2,1,0:T(8,128)(2,1)}, bf16[4,384,512]{2,1,0:T(8,128)(2,1)}, u32[]{:S(2)}, u32[]{:S(2)}) collective-permute-start(bf16[4,384,512]{2,1,0:T(8,128)(2,1)} %get-tuple-element.7), channel_id=1, source_target_pairs={{0,1},{1,0},{2,3},{3,2},{4,5},{5,4},{6,7},{7,6},{8,9},{9,8},{10,11... | collective-permute-start | bytes 4718600 | tf_op jit(solution)/shard_map/ppermute | solution.py:31
  62.5 2.7 %shard_map.177 = bf16[5,256,512]{2,1,0:T(8,128)(2,1)} custom-call(s32[5]{0:T(128)} %and_select_fusion.index, bf16[64,4096]{1,0:T(8,128)(2,1)} %bitcast.22.gate, bf16[64,4096]{1,0:T(8,128)(2,1)} %bitcast.24.up, bf16[64,4096]{1,0:T(8,128)(2,1)} %collective-permute-done.7.partner_gate, bf16[64,4096]{1,0:T(8,128)(2,1)} %collective-permute-done.8.partner_up), custom_call_target="tpu_custom_call" | custom-call | tf_op jit(solution)/shard_map/pallas_call | solution.py:46
  66.1 1.9 %collective-permute-done.9 = bf16[768,512]{1,0:T(8,128)(2,1)S(1)} collective-permute-done((bf16[768,512]{1,0:T(8,128)(2,1)S(1)}, bf16[768,512]{1,0:T(8,128)(2,1)S(1)}, u32[]{:S(2)}, u32[]{:S(2)}) %collective-permute-start.9) | collective-permute-done | bytes 786464 | tf_op jit(solution)/shard_map/ppermute | solution.py:26
  68.7 1.6 %fusion.15 = f32[256,768]{1,0:T(8,128)S(1)} fusion(bf16[768,512]{1,0:T(8,128)(2,1)} %collective-permute-done.10, bf16[5,256,512]{2,1,0:T(8,128)(2,1)} %shard_map.177), kind=kOutput, calls=%fused_computation.53 | convolution fusion | flops 201326592 | bytes 1835008 | tf_op jit(solution)/shard_map/dot_general | solution.py:35
  72.1 17.8 %collective-permute-start.13 = (f32[128,768]{1,0:T(8,128)S(1)}, f32[128,768]{1,0:T(8,128)S(1)}, u32[]{:S(2)}, u32[]{:S(2)}) collective-permute-start(f32[128,768]{1,0:T(8,128)S(1)} %slice.222), channel_id=1, source_target_pairs={{0,1},{1,0},{2,3},{3,2},{4,5},{5,4},{6,7},{7,6},{8,9},{9,8},{10,11... | collective-permute-start | bytes 1179656 | tf_op jit(solution)/shard_map/ppermute | solution.py:31
  89.9 1.3 collective-permute-done.13
  92.3 3.8 %all-to-all-start.1 = ((bf16[8,64,768]{2,1,0:T(8,128)(2,1)}), bf16[8,64,768]{2,1,0:T(8,128)(2,1)S(1)}, u32[]{:S(2)}, u32[]{:S(2)}) async-start(bf16[8,64,768]{2,1,0:T(8,128)(2,1)} %broadcast_in_dim.93), calls=%async_computation.1 | async-start | bytes 1572864 | tf_op jit(solution)/shard_map/all_to_all | solution.py:219
  96.1 1.1 fusion.13
  97.3 4.6 %collective-permute-start.2 = (bf16[384,512]{1,0:T(8,128)(2,1)S(1)}, bf16[384,512]{1,0:T(8,128)(2,1)S(1)}, u32[]{:S(2)}, u32[]{:S(2)}) collective-permute-start(bf16[384,512]{1,0:T(8,128)(2,1)S(1)} %fusion.13), channel_id=1, source_target_pairs={{0,2},{2,4},{4,6},{6,8},{8,10},{10,12},{12,14},{14,0},{1,15},{3,1}... | collective-permute-start | bytes 1179656 | tf_op jit(solution)/shard_map/ppermute | solution.py:26
  101.9 18.2 %collective-permute-done.2 = bf16[384,512]{1,0:T(8,128)(2,1)S(1)} collective-permute-done((bf16[384,512]{1,0:T(8,128)(2,1)S(1)}, bf16[384,512]{1,0:T(8,128)(2,1)S(1)}, u32[]{:S(2)}, u32[]{:S(2)}) %collective-permute-start.2) | collective-permute-done | bytes 393248 | tf_op jit(solution)/shard_map/ppermute | solution.py:26
  120.1 1.9 %fusion.11 = bf16[384,512]{1,0:T(8,128)(2,1)} fusion(bf16[384,512]{1,0:T(8,128)(2,1)S(1)} %collective-permute-done.2, bf16[4,384,512]{2,1,0:T(8,128)(2,1)} %collective-permute-done.1, bf16[4,384,512]{2,1,0:T(8,128)(2,1)S(1)} %copy-done.3), kind=kLoop, calls=%fused_computation.36 | loop fusion | flops 1179648 | bytes 1572864 | tf_op jit(solution)/shard_map/convert_element_type | solution.py:202
  122.0 2.8 %collective-permute-start.3 = (bf16[384,512]{1,0:T(8,128)(2,1)}, bf16[384,512]{1,0:T(8,128)(2,1)}, u32[]{:S(2)}, u32[]{:S(2)}) collective-permute-start(bf16[384,512]{1,0:T(8,128)(2,1)} %fusion.11), channel_id=1, source_target_pairs={{0,2},{2,4},{4,6},{6,8},{8,10},{10,12},{12,14},{14,0},{1,15},{3,1}... | collective-permute-start | bytes 1179656 | tf_op jit(solution)/shard_map/ppermute | solution.py:26
  124.8 2.6 %collective-permute-start.14 = (bf16[8,64,768]{2,1,0:T(8,128)(2,1)S(1)}, bf16[8,64,768]{2,1,0:T(8,128)(2,1)S(1)}, u32[]{:S(2)}, u32[]{:S(2)}) collective-permute-start(bf16[8,64,768]{2,1,0:T(8,128)(2,1)S(1)} %all-to-all-done.1), channel_id=1, source_target_pairs={{0,1},{1,0},{2,3},{3,2},{4,5},{5,4},{6,7},{7,6},{8,9},{9,8},{10,11... | collective-permute-start | bytes 2359304 | tf_op jit(solution)/shard_map/ppermute | solution.py:31
  127.5 3.6 %collective-permute-done.3 = bf16[384,512]{1,0:T(8,128)(2,1)} collective-permute-done((bf16[384,512]{1,0:T(8,128)(2,1)}, bf16[384,512]{1,0:T(8,128)(2,1)}, u32[]{:S(2)}, u32[]{:S(2)}) %collective-permute-start.3) | collective-permute-done | bytes 393248 | tf_op jit(solution)/shard_map/ppermute | solution.py:26
  131.1 1.3 fusion.12
  132.4 3.7 %collective-permute-start.4 = (bf16[384,512]{1,0:T(8,128)(2,1)S(1)}, bf16[384,512]{1,0:T(8,128)(2,1)}, u32[]{:S(2)}, u32[]{:S(2)}) collective-permute-start(bf16[384,512]{1,0:T(8,128)(2,1)S(1)} %fusion.12), channel_id=1, source_target_pairs={{0,2},{2,4},{4,6},{6,8},{8,10},{10,12},{12,14},{14,0},{1,15},{3,1}... | collective-permute-start | bytes 1179656 | tf_op jit(solution)/shard_map/ppermute | solution.py:26
  136.5 1.2 fusion.7
  137.7 5.8 %all-to-all-start.2 = ((bf16[32,24,256]{2,1,0:T(8,128)(2,1)}), bf16[32,24,256]{2,1,0:T(8,128)(2,1)S(1)}, u32[]{:S(2)}, u32[]{:S(2)}) async-start(bf16[32,24,256]{2,1,0:T(8,128)(2,1)} %bitcast.39), calls=%async_computation.2 | async-start | bytes 786432 | tf_op jit(solution)/shard_map/all_to_all | solution.py:168
  143.5 1.3 bitcast_add_fusion.2
  145.5 6.7 %collective-permute-start.5 = (bf16[384,256]{1,0:T(8,128)(2,1)S(1)}, bf16[384,256]{1,0:T(8,128)(2,1)S(1)}, u32[]{:S(2)}, u32[]{:S(2)}) collective-permute-start(bf16[384,256]{1,0:T(8,128)(2,1)S(1)} %get-tuple-element.8), channel_id=1, source_target_pairs={{0,3},{2,5},{4,7},{6,9},{8,11},{10,13},{12,15},{14,1},{1,0},{3,2},... | collective-permute-start | bytes 589832 | tf_op jit(solution)/shard_map/ppermute | solution.py:26
  152.2 6.6 %collective-permute-done.5 = bf16[384,256]{1,0:T(8,128)(2,1)S(1)} collective-permute-done((bf16[384,256]{1,0:T(8,128)(2,1)S(1)}, bf16[384,256]{1,0:T(8,128)(2,1)S(1)}, u32[]{:S(2)}, u32[]{:S(2)}) %collective-permute-start.5) | collective-permute-done | bytes 196640 | tf_op jit(solution)/shard_map/ppermute | solution.py:26
  (80 shorter events, 13.6 us)
Async XLA Ops:
  0.6 52.3 %copy-start = (bf16[16,128,128]{2,1,0:T(8,128)(2,1)S(1)}, bf16[16,128,128]{2,1,0:T(8,128)(2,1)}, u32[]{:S(2)}) copy-start(bf16[16,128,128]{2,1,0:T(8,128)(2,1)} %param.18) | copy-start | bytes 1572868
  0.6 7.2 %copy-start.1 = (bf16[128,4096]{1,0:T(8,128)(2,1)S(1)}, bf16[128,4096]{1,0:T(8,128)(2,1)}, u32[]{:S(2)}) copy-start(bf16[128,4096]{1,0:T(8,128)(2,1)} %param.21) | copy-start | bytes 3145732
  0.7 8.0 %copy-start.7 = (f32[4096]{0:T(1024)S(1)}, f32[4096]{0:T(1024)}, u32[]{:S(2)}) copy-start(f32[4096]{0:T(1024)} %param.22) | copy-start | bytes 49156
  1.5 51.4 %collective-permute-start = (bf16[15,128]{1,0:T(8,128)(2,1)S(1)}, bf16[15,128]{1,0:T(8,128)(2,1)S(1)}, u32[]{:S(2)}, u32[]{:S(2)}) collective-permute-start(bf16[15,128]{1,0:T(8,128)(2,1)S(1)} %slice.140), channel_id=1, source_target_pairs={{0,16},{16,32},{32,48},{48,64},{64,80},{80,96},{96,112},{112,128},... | collective-permute-start | bytes 11528 | tf_op jit(solution)/shard_map/ppermute | solution.py:18
  10.0 18.4 %copy-start.5 = (bf16[4096,32]{0,1:T(8,128)(2,1)S(1)}, bf16[4096,32]{0,1:T(8,128)(2,1)}, u32[]{:S(2)}) copy-start(bf16[4096,32]{0,1:T(8,128)(2,1)} %param.28) | copy-start | bytes 786436
  10.0 33.8 %all-to-all-start = ((bf16[32,24,512]{2,1,0:T(8,128)(2,1)}), bf16[32,24,512]{2,1,0:T(8,128)(2,1)S(1)}, u32[]{:S(2)}, u32[]{:S(2)}) async-start(bf16[32,24,512]{2,1,0:T(8,128)(2,1)} %bitcast.28), calls=%async_computation | async-start | bytes 1572864 | tf_op jit(solution)/shard_map/all_to_all | solution.py:168
  22.8 39.7 %collective-permute-start.7 = (bf16[64,4096]{1,0:T(8,128)(2,1)}, bf16[64,4096]{1,0:T(8,128)(2,1)}, u32[]{:S(2)}, u32[]{:S(2)}) collective-permute-start(bf16[64,4096]{1,0:T(8,128)(2,1)} %bitcast.22.gate), channel_id=1, source_target_pairs={{0,1},{1,0},{2,3},{3,2},{4,5},{5,4},{6,7},{7,6},{8,9},{9,8},{10,11... | collective-permute-start | bytes 1572872 | tf_op jit(solution)/shard_map/ppermute | solution.py:31
  25.9 36.6 %collective-permute-start.8 = (bf16[64,4096]{1,0:T(8,128)(2,1)}, bf16[64,4096]{1,0:T(8,128)(2,1)}, u32[]{:S(2)}, u32[]{:S(2)}) collective-permute-start(bf16[64,4096]{1,0:T(8,128)(2,1)} %bitcast.24.up), channel_id=1, source_target_pairs={{0,1},{1,0},{2,3},{3,2},{4,5},{5,4},{6,7},{7,6},{8,9},{9,8},{10,11... | collective-permute-start | bytes 1572872 | tf_op jit(solution)/shard_map/ppermute | solution.py:31
  27.9 1.0 copy-start.11
  28.4 22.5 %copy-start.9 = (s32[4]{0:T(128)S(1)}, s32[4]{0:T(128)}, u32[]{:S(2)}) copy-start(s32[4]{0:T(128)} %constant.148.clone) | copy-start | bytes 52
  28.4 22.5 %copy-start.10 = (s32[4]{0:T(128)S(1)}, s32[4]{0:T(128)}, u32[]{:S(2)}) copy-start(s32[4]{0:T(128)} %constant.149.clone) | copy-start | bytes 52
  28.4 22.5 %copy-start.12 = (s32[5]{0:T(128)S(1)}, s32[5]{0:T(128)}, u32[]{:S(2)}) copy-start(s32[5]{0:T(128)} %constant.150.clone) | copy-start | bytes 64
  28.4 23.7 %copy-start.6 = (bf16[256,128]{1,0:T(8,128)(2,1)S(1)}, bf16[256,128]{1,0:T(8,128)(2,1)}, u32[]{:S(2)}) copy-start(bf16[256,128]{1,0:T(8,128)(2,1)} %param.17) | copy-start | bytes 196612
  43.9 21.4 %collective-permute-start.10 = (bf16[768,512]{1,0:T(8,128)(2,1)S(1)}, bf16[768,512]{1,0:T(8,128)(2,1)}, u32[]{:S(2)}, u32[]{:S(2)}) collective-permute-start(bf16[768,512]{1,0:T(8,128)(2,1)S(1)} %bitcast.98), channel_id=1, source_target_pairs={{0,14},{2,0},{4,2},{6,4},{8,6},{10,8},{12,10},{14,12},{1,15},{3,1}... | collective-permute-start | bytes 2359304 | tf_op jit(solution)/shard_map/ppermute | solution.py:26
  49.0 19.1 %collective-permute-start.9 = (bf16[768,512]{1,0:T(8,128)(2,1)S(1)}, bf16[768,512]{1,0:T(8,128)(2,1)S(1)}, u32[]{:S(2)}, u32[]{:S(2)}) collective-permute-start(bf16[768,512]{1,0:T(8,128)(2,1)S(1)} %bitcast.99), channel_id=1, source_target_pairs={{0,2},{2,4},{4,6},{6,8},{8,10},{10,12},{12,14},{14,0},{1,3},{3,5},... | collective-permute-start | bytes 2359304 | tf_op jit(solution)/shard_map/ppermute | solution.py:26
  57.4 38.7 %collective-permute-start.1 = (bf16[4,384,512]{2,1,0:T(8,128)(2,1)}, bf16[4,384,512]{2,1,0:T(8,128)(2,1)}, u32[]{:S(2)}, u32[]{:S(2)}) collective-permute-start(bf16[4,384,512]{2,1,0:T(8,128)(2,1)} %get-tuple-element.7), channel_id=1, source_target_pairs={{0,1},{1,0},{2,3},{3,2},{4,5},{5,4},{6,7},{7,6},{8,9},{9,8},{10,11... | collective-permute-start | bytes 4718600 | tf_op jit(solution)/shard_map/ppermute | solution.py:31
  65.3 5.1 %copy-start.2 = (bf16[5,256,512]{2,1,0:T(8,128)(2,1)S(1)}, bf16[5,256,512]{2,1,0:T(8,128)(2,1)}, u32[]{:S(2)}) copy-start(bf16[5,256,512]{2,1,0:T(8,128)(2,1)} %shard_map.177) | copy-start | bytes 3932164
  65.3 5.9 %collective-permute-start.12 = (bf16[768,512]{1,0:T(8,128)(2,1)}, bf16[768,512]{1,0:T(8,128)(2,1)S(1)}, u32[]{:S(2)}, u32[]{:S(2)}) collective-permute-start(bf16[768,512]{1,0:T(8,128)(2,1)} %collective-permute-done.10), channel_id=1, source_target_pairs={{0,14},{2,0},{4,2},{6,4},{8,6},{10,8},{12,10},{14,12},{16,30},{18,... | collective-permute-start | bytes 2359304 | tf_op jit(solution)/shard_map/ppermute | solution.py:26
  68.0 3.6 %collective-permute-start.11 = (bf16[768,512]{1,0:T(8,128)(2,1)S(1)}, bf16[768,512]{1,0:T(8,128)(2,1)S(1)}, u32[]{:S(2)}, u32[]{:S(2)}) collective-permute-start(bf16[768,512]{1,0:T(8,128)(2,1)S(1)} %collective-permute-done.9), channel_id=1, source_target_pairs={{0,2},{2,4},{4,6},{6,8},{8,10},{10,12},{12,14},{14,0},{16,18},{18,... | collective-permute-start | bytes 2359304 | tf_op jit(solution)/shard_map/ppermute | solution.py:26
  72.1 19.1 %collective-permute-start.13 = (f32[128,768]{1,0:T(8,128)S(1)}, f32[128,768]{1,0:T(8,128)S(1)}, u32[]{:S(2)}, u32[]{:S(2)}) collective-permute-start(f32[128,768]{1,0:T(8,128)S(1)} %slice.222), channel_id=1, source_target_pairs={{0,1},{1,0},{2,3},{3,2},{4,5},{5,4},{6,7},{7,6},{8,9},{9,8},{10,11... | collective-permute-start | bytes 1179656 | tf_op jit(solution)/shard_map/ppermute | solution.py:31
  91.3 4.9 %copy-start.3 = (bf16[4,384,512]{2,1,0:T(8,128)(2,1)S(1)}, bf16[4,384,512]{2,1,0:T(8,128)(2,1)}, u32[]{:S(2)}) copy-start(bf16[4,384,512]{2,1,0:T(8,128)(2,1)} %get-tuple-element.6) | copy-start | bytes 4718596
  92.3 32.5 %all-to-all-start.1 = ((bf16[8,64,768]{2,1,0:T(8,128)(2,1)}), bf16[8,64,768]{2,1,0:T(8,128)(2,1)S(1)}, u32[]{:S(2)}, u32[]{:S(2)}) async-start(bf16[8,64,768]{2,1,0:T(8,128)(2,1)} %broadcast_in_dim.93), calls=%async_computation.1 | async-start | bytes 1572864 | tf_op jit(solution)/shard_map/all_to_all | solution.py:219
  96.1 31.3 %copy-start.4 = (bf16[1,1024,256]{2,1,0:T(8,128)(2,1)S(1)}, bf16[1,1024,256]{2,1,0:T(8,128)(2,1)}, u32[]{:S(2)}) copy-start(bf16[1,1024,256]{2,1,0:T(8,128)(2,1)} %param.27) | copy-start | bytes 1572868
  97.3 30.2 %copy-start.8 = (f32[128,4]{0,1:T(4,128)S(1)}, f32[128,4]{0,1:T(4,128)}, u32[]{:S(2)}) copy-start(f32[128,4]{0,1:T(4,128)} %param.24) | copy-start | bytes 6148
  97.3 22.8 %collective-permute-start.2 = (bf16[384,512]{1,0:T(8,128)(2,1)S(1)}, bf16[384,512]{1,0:T(8,128)(2,1)S(1)}, u32[]{:S(2)}, u32[]{:S(2)}) collective-permute-start(bf16[384,512]{1,0:T(8,128)(2,1)S(1)} %fusion.13), channel_id=1, source_target_pairs={{0,2},{2,4},{4,6},{6,8},{8,10},{10,12},{12,14},{14,0},{1,15},{3,1}... | collective-permute-start | bytes 1179656 | tf_op jit(solution)/shard_map/ppermute | solution.py:26
  122.0 9.1 %collective-permute-start.3 = (bf16[384,512]{1,0:T(8,128)(2,1)}, bf16[384,512]{1,0:T(8,128)(2,1)}, u32[]{:S(2)}, u32[]{:S(2)}) collective-permute-start(bf16[384,512]{1,0:T(8,128)(2,1)} %fusion.11), channel_id=1, source_target_pairs={{0,2},{2,4},{4,6},{6,8},{8,10},{10,12},{12,14},{14,0},{1,15},{3,1}... | collective-permute-start | bytes 1179656 | tf_op jit(solution)/shard_map/ppermute | solution.py:26
  124.8 11.7 %collective-permute-start.14 = (bf16[8,64,768]{2,1,0:T(8,128)(2,1)S(1)}, bf16[8,64,768]{2,1,0:T(8,128)(2,1)S(1)}, u32[]{:S(2)}, u32[]{:S(2)}) collective-permute-start(bf16[8,64,768]{2,1,0:T(8,128)(2,1)S(1)} %all-to-all-done.1), channel_id=1, source_target_pairs={{0,1},{1,0},{2,3},{3,2},{4,5},{5,4},{6,7},{7,6},{8,9},{9,8},{10,11... | collective-permute-start | bytes 2359304 | tf_op jit(solution)/shard_map/ppermute | solution.py:31
  132.4 11.1 %collective-permute-start.4 = (bf16[384,512]{1,0:T(8,128)(2,1)S(1)}, bf16[384,512]{1,0:T(8,128)(2,1)}, u32[]{:S(2)}, u32[]{:S(2)}) collective-permute-start(bf16[384,512]{1,0:T(8,128)(2,1)S(1)} %fusion.12), channel_id=1, source_target_pairs={{0,2},{2,4},{4,6},{6,8},{8,10},{10,12},{12,14},{14,0},{1,15},{3,1}... | collective-permute-start | bytes 1179656 | tf_op jit(solution)/shard_map/ppermute | solution.py:26
  137.7 21.9 %all-to-all-start.2 = ((bf16[32,24,256]{2,1,0:T(8,128)(2,1)}), bf16[32,24,256]{2,1,0:T(8,128)(2,1)S(1)}, u32[]{:S(2)}, u32[]{:S(2)}) async-start(bf16[32,24,256]{2,1,0:T(8,128)(2,1)} %bitcast.39), calls=%async_computation.2 | async-start | bytes 786432 | tf_op jit(solution)/shard_map/all_to_all | solution.py:168
  144.8 7.4 %collective-permute-start.6 = (bf16[384,256]{1,0:T(8,128)(2,1)S(1)}, bf16[384,256]{1,0:T(8,128)(2,1)S(1)}, u32[]{:S(2)}, u32[]{:S(2)}) collective-permute-start(bf16[384,256]{1,0:T(8,128)(2,1)S(1)} %get-tuple-element.9), channel_id=1, source_target_pairs={{0,2},{2,4},{4,6},{6,8},{8,10},{10,12},{12,14},{14,0},{16,18},{18,... | collective-permute-start | bytes 589832 | tf_op jit(solution)/shard_map/ppermute | solution.py:26
  145.5 13.3 %collective-permute-start.5 = (bf16[384,256]{1,0:T(8,128)(2,1)S(1)}, bf16[384,256]{1,0:T(8,128)(2,1)S(1)}, u32[]{:S(2)}, u32[]{:S(2)}) collective-permute-start(bf16[384,256]{1,0:T(8,128)(2,1)S(1)} %get-tuple-element.8), channel_id=1, source_target_pairs={{0,3},{2,5},{4,7},{6,9},{8,11},{10,13},{12,15},{14,1},{1,0},{3,2},... | collective-permute-start | bytes 589832 | tf_op jit(solution)/shard_map/ppermute | solution.py:26

commit v6 on v5

--- a/solution.py
+++ b/solution.py
@@ -175,7 +175,8 @@
     kept_ids = jnp.where(core == 0, upward, downward)
     sent_ids = jnp.where(core == 0, downward, upward)
     index = (y + jnp.stack([kept_ids, sent_ids])) % y_size
-    near_index = (home + y_size + jnp.array([0, -1, 1, -2, 2], jnp.int32)) % y_size
+    offsets = jnp.where(core == 0, jnp.array([0, -1, 1, -2, 2], jnp.int32), jnp.array([0, 1, -1, 0, 0], jnp.int32))
+    near_index = (home + y_size + offsets) % y_size
 
     group_out = pool_group_out(pool_input, earlier_rows, pool_map, pool_scale, tp_rank, ep_rank)
     normed = (centre * rstd * norm_gain[None, :]).astype(bf16)
@@ -201,14 +202,14 @@
     def ring_step(x):
         return sent(x.astype(bf16), {0: (1, 0), 1: (-1, 1)})
 
-    up = sent(arrived, {0: (1, 0), 1: (1, 1)})
-    down = sent(arrived, {0: (-1, 0), 1: (-1, 1)})
-    up_two = sent(up, {0: (1, 0)})
-    down_two = sent(down, {0: (-1, 0)})
+    one = sent(arrived, {0: (1, 0), 1: (-1, 1)})
+    other = sent(arrived, {0: (-1, 0), 1: (1, 1)})
+    up_two = sent(one, {0: (1, 0)})
+    down_two = sent(other, {0: (-1, 0)})
     ring = ring_step(part(0))
     ring = ring_step(part(1) + ring.astype(f32))
     summed = tdot(weights[0], arrived)
-    for j, rows in enumerate((up, down, up_two, down_two)):
+    for j, rows in enumerate((one, other, up_two, down_two)):
         summed = summed + tdot(weights[j + 1], rows)
     full = summed[: 2 * units] + to_partner(summed[2 * units :])
     hidden = (jax.nn.silu(full[:units]) * full[units:]).astype(bf16)

time: 162 us -> 163 us (level)
  starting transfers between devices: 83.8 us -> 85.5 us
  transfers between devices with their start and end apart: 18 -> 18, of which waited for: 6 -> 6; matrix products, arithmetic and copies ran while one was open for 14% -> 13% of each run, Pallas kernels for 4% -> 4%
where the time goes in v6:
time: 163 us; the launch traced here: 162 us
  starting transfers between devices  85.5 us (52%)
  waiting for transfers between devices  45.8 us (28%)
  matrix products  9.62 us (6%)
  other arithmetic  9.57 us (6%)
  Pallas kernels  6.27 us (4%)
  local copies, waits for them, and re-layouts  4.37 us (3%)
    ppermute x5, starting transfers between devices, to_partner(): return lax.ppermute(x, 'tp', [(i, i ^ 1) for i in range(n)])  32 us
    ppermute x9, waiting for transfers between devices, sent(): return lax.ppermute(x, 'tp', route)  30.5 us
    ppermute x9, starting transfers between devices, sent(): return lax.ppermute(x, 'tp', route)  28.2 us
    all_to_all x2, starting transfers between devices, exchanged(): return lax.all_to_all(rows, 'ep', split_axis=0, concat_axis=0, tiled=True)  17.3 us
    all_to_all x2, waiting for transfers between devices, exchanged(): return lax.all_to_all(rows, 'ep', split_axis=0, concat_axis=0, tiled=True)  13.9 us
    pallas_call x2, Pallas kernels, local_kernel(): pl.pallas_call(body, in_specs=[smem] + [vmem] * len(operands), out_specs=...  6.27 us
    convert_element_type x3, other arithmetic, ring_step(): return sent(x.astype(bf16), {0: (1, 0), 1: (-1, 1)})  4.3 us
    all_to_all x1, starting transfers between devices, per_device(): lax.all_to_all(copies, 'tp', 0, 0, axis_index_groups=groups, tiled=True)  4.11 us
  transfers between devices with their start and end apart: 18, of which 6 were waited for; matrix products, arithmetic and copies ran while one was open for 13% of the time, Pallas kernels for 4%

profile of v6, /device:TPU:1, one launch (start us, length us, event | category | flops | bytes accessed | tf_op | source)
XLA Modules:
  0.0 162.4 jit_solution(1370130558391409106)
XLA Ops:
  1.5 3.9 %collective-permute-start = (bf16[15,128]{1,0:T(8,128)(2,1)S(1)}, bf16[15,128]{1,0:T(8,128)(2,1)S(1)}, u32[]{:S(2)}, u32[]{:S(2)}) collective-permute-start(bf16[15,128]{1,0:T(8,128)(2,1)S(1)} %slice.140), channel_id=1, source_target_pairs={{0,16},{16,32},{32,48},{48,64},{64,80},{80,96},{96,112},{112,128},... | collective-permute-start | bytes 11528 | tf_op jit(solution)/shard_map/ppermute | solution.py:18
  6.4 1.5 convert_reduce_fusion
  8.7 1.3 convolution_convert_fusion
  10.0 12.7 %all-to-all-start = ((bf16[32,24,512]{2,1,0:T(8,128)(2,1)}), bf16[32,24,512]{2,1,0:T(8,128)(2,1)S(1)}, u32[]{:S(2)}, u32[]{:S(2)}) async-start(bf16[32,24,512]{2,1,0:T(8,128)(2,1)} %bitcast.28), calls=%async_computation | async-start | bytes 1572864 | tf_op jit(solution)/shard_map/all_to_all | solution.py:168
  22.8 3.1 %collective-permute-start.7 = (bf16[64,4096]{1,0:T(8,128)(2,1)}, bf16[64,4096]{1,0:T(8,128)(2,1)}, u32[]{:S(2)}, u32[]{:S(2)}) collective-permute-start(bf16[64,4096]{1,0:T(8,128)(2,1)} %bitcast.22.gate), channel_id=1, source_target_pairs={{0,1},{1,0},{2,3},{3,2},{4,5},{5,4},{6,7},{7,6},{8,9},{9,8},{10,11... | collective-permute-start | bytes 1572872 | tf_op jit(solution)/shard_map/ppermute | solution.py:31
  25.9 1.9 %collective-permute-start.8 = (bf16[64,4096]{1,0:T(8,128)(2,1)}, bf16[64,4096]{1,0:T(8,128)(2,1)}, u32[]{:S(2)}, u32[]{:S(2)}) collective-permute-start(bf16[64,4096]{1,0:T(8,128)(2,1)} %bitcast.24.up), channel_id=1, source_target_pairs={{0,1},{1,0},{2,3},{3,2},{4,5},{5,4},{6,7},{7,6},{8,9},{9,8},{10,11... | collective-permute-start | bytes 1572872 | tf_op jit(solution)/shard_map/ppermute | solution.py:31
  28.9 1.0 fusion.10.hidden
  29.9 13.9 %all-to-all-done = bf16[32,24,512]{2,1,0:T(8,128)(2,1)S(1)} async-done(((bf16[32,24,512]{2,1,0:T(8,128)(2,1)}), bf16[32,24,512]{2,1,0:T(8,128)(2,1)S(1)}, u32[]{:S(2)}, u32[]{:S(2)}) %all-to-all-start) | async-done | bytes 786464 | tf_op jit(solution)/shard_map/all_to_all | solution.py:168
  43.9 3.2 %collective-permute-start.10 = (bf16[768,512]{1,0:T(8,128)(2,1)S(1)}, bf16[768,512]{1,0:T(8,128)(2,1)}, u32[]{:S(2)}, u32[]{:S(2)}) collective-permute-start(bf16[768,512]{1,0:T(8,128)(2,1)S(1)} %bitcast.98), channel_id=1, source_target_pairs={{0,14},{2,0},{4,2},{6,4},{8,6},{10,8},{12,10},{14,12},{1,3},{3,5},... | collective-permute-start | bytes 2359304 | tf_op jit(solution)/shard_map/ppermute | solution.py:26
  47.1 3.8 %collective-permute-start.9 = (bf16[768,512]{1,0:T(8,128)(2,1)S(1)}, bf16[768,512]{1,0:T(8,128)(2,1)S(1)}, u32[]{:S(2)}, u32[]{:S(2)}) collective-permute-start(bf16[768,512]{1,0:T(8,128)(2,1)S(1)} %bitcast.99), channel_id=1, source_target_pairs={{0,2},{2,4},{4,6},{6,8},{8,10},{10,12},{12,14},{14,0},{1,15},{3,1}... | collective-permute-start | bytes 2359304 | tf_op jit(solution)/shard_map/ppermute | solution.py:26
  54.0 3.5 %shard_map.185 = (bf16[4,384,512]{2,1,0:T(8,128)(2,1)}, bf16[4,384,512]{2,1,0:T(8,128)(2,1)}) custom-call(s32[2,4]{1,0:T(2,128)} %and_select_fusion.3.index, bf16[256,128]{1,0:T(8,128)(2,1)} %fusion.9.group, bf16[128,32]{1,0:T(8,128)(2,1)} %fusion.10.hidden, bf16[128,4096]{1,0:T(8,128)(2,1)} %proj.1, bf16[32,4096]{1,0:T(8,128)(2,1)} %down.1), custom_call_target="tpu_custom_call" | custom-call | tf_op jit(solution)/shard_map/pallas_call | solution.py:46
  57.5 5.0 %collective-permute-start.1 = (bf16[4,384,512]{2,1,0:T(8,128)(2,1)}, bf16[4,384,512]{2,1,0:T(8,128)(2,1)}, u32[]{:S(2)}, u32[]{:S(2)}) collective-permute-start(bf16[4,384,512]{2,1,0:T(8,128)(2,1)} %get-tuple-element.7), channel_id=1, source_target_pairs={{0,1},{1,0},{2,3},{3,2},{4,5},{5,4},{6,7},{7,6},{8,9},{9,8},{10,11... | collective-permute-start | bytes 4718600 | tf_op jit(solution)/shard_map/ppermute | solution.py:31
  62.6 2.7 %shard_map.186 = bf16[5,256,512]{2,1,0:T(8,128)(2,1)} custom-call(s32[5]{0:T(128)} %and_select_fusion.index, bf16[64,4096]{1,0:T(8,128)(2,1)} %bitcast.22.gate, bf16[64,4096]{1,0:T(8,128)(2,1)} %bitcast.24.up, bf16[64,4096]{1,0:T(8,128)(2,1)} %collective-permute-done.7.partner_gate, bf16[64,4096]{1,0:T(8,128)(2,1)} %collective-permute-done.8.partner_up), custom_call_target="tpu_custom_call" | custom-call | tf_op jit(solution)/shard_map/pallas_call | solution.py:46
  66.1 2.4 %collective-permute-done.9 = bf16[768,512]{1,0:T(8,128)(2,1)S(1)} collective-permute-done((bf16[768,512]{1,0:T(8,128)(2,1)S(1)}, bf16[768,512]{1,0:T(8,128)(2,1)S(1)}, u32[]{:S(2)}, u32[]{:S(2)}) %collective-permute-start.9) | collective-permute-done | bytes 786464 | tf_op jit(solution)/shard_map/ppermute | solution.py:26
  69.2 1.6 fusion.15
  72.5 19.2 %collective-permute-start.13 = (f32[128,768]{1,0:T(8,128)S(1)}, f32[128,768]{1,0:T(8,128)S(1)}, u32[]{:S(2)}, u32[]{:S(2)}) collective-permute-start(f32[128,768]{1,0:T(8,128)S(1)} %slice.222), channel_id=1, source_target_pairs={{0,1},{1,0},{2,3},{3,2},{4,5},{5,4},{6,7},{7,6},{8,9},{9,8},{10,11... | collective-permute-start | bytes 1179656 | tf_op jit(solution)/shard_map/ppermute | solution.py:31
  91.8 1.3 collective-permute-done.13
  94.2 4.1 %all-to-all-start.1 = ((bf16[8,64,768]{2,1,0:T(8,128)(2,1)}), bf16[8,64,768]{2,1,0:T(8,128)(2,1)S(1)}, u32[]{:S(2)}, u32[]{:S(2)}) async-start(bf16[8,64,768]{2,1,0:T(8,128)(2,1)} %broadcast_in_dim.93), calls=%async_computation.1 | async-start | bytes 1572864 | tf_op jit(solution)/shard_map/all_to_all | solution.py:220
  98.3 1.1 fusion.13
  99.5 4.6 %collective-permute-start.2 = (bf16[384,512]{1,0:T(8,128)(2,1)S(1)}, bf16[384,512]{1,0:T(8,128)(2,1)S(1)}, u32[]{:S(2)}, u32[]{:S(2)}) collective-permute-start(bf16[384,512]{1,0:T(8,128)(2,1)S(1)} %fusion.13), channel_id=1, source_target_pairs={{0,2},{2,4},{4,6},{6,8},{8,10},{10,12},{12,14},{14,0},{1,15},{3,1}... | collective-permute-start | bytes 1179656 | tf_op jit(solution)/shard_map/ppermute | solution.py:26
  104.1 18.2 %collective-permute-done.2 = bf16[384,512]{1,0:T(8,128)(2,1)S(1)} collective-permute-done((bf16[384,512]{1,0:T(8,128)(2,1)S(1)}, bf16[384,512]{1,0:T(8,128)(2,1)S(1)}, u32[]{:S(2)}, u32[]{:S(2)}) %collective-permute-start.2) | collective-permute-done | bytes 393248 | tf_op jit(solution)/shard_map/ppermute | solution.py:26
  122.3 1.9 %fusion.11 = bf16[384,512]{1,0:T(8,128)(2,1)} fusion(bf16[384,512]{1,0:T(8,128)(2,1)S(1)} %collective-permute-done.2, bf16[4,384,512]{2,1,0:T(8,128)(2,1)} %collective-permute-done.1, bf16[4,384,512]{2,1,0:T(8,128)(2,1)S(1)} %copy-done.3), kind=kLoop, calls=%fused_computation.36 | loop fusion | flops 1179648 | bytes 1572864 | tf_op jit(solution)/shard_map/convert_element_type | solution.py:203
  124.2 2.8 %collective-permute-start.3 = (bf16[384,512]{1,0:T(8,128)(2,1)}, bf16[384,512]{1,0:T(8,128)(2,1)}, u32[]{:S(2)}, u32[]{:S(2)}) collective-permute-start(bf16[384,512]{1,0:T(8,128)(2,1)} %fusion.11), channel_id=1, source_target_pairs={{0,2},{2,4},{4,6},{6,8},{8,10},{10,12},{12,14},{14,0},{1,15},{3,1}... | collective-permute-start | bytes 1179656 | tf_op jit(solution)/shard_map/ppermute | solution.py:26
  127.0 2.6 %collective-permute-start.14 = (bf16[8,64,768]{2,1,0:T(8,128)(2,1)S(1)}, bf16[8,64,768]{2,1,0:T(8,128)(2,1)S(1)}, u32[]{:S(2)}, u32[]{:S(2)}) collective-permute-start(bf16[8,64,768]{2,1,0:T(8,128)(2,1)S(1)} %all-to-all-done.1), channel_id=1, source_target_pairs={{0,1},{1,0},{2,3},{3,2},{4,5},{5,4},{6,7},{7,6},{8,9},{9,8},{10,11... | collective-permute-start | bytes 2359304 | tf_op jit(solution)/shard_map/ppermute | solution.py:31
  129.7 3.6 %collective-permute-done.3 = bf16[384,512]{1,0:T(8,128)(2,1)} collective-permute-done((bf16[384,512]{1,0:T(8,128)(2,1)}, bf16[384,512]{1,0:T(8,128)(2,1)}, u32[]{:S(2)}, u32[]{:S(2)}) %collective-permute-start.3) | collective-permute-done | bytes 393248 | tf_op jit(solution)/shard_map/ppermute | solution.py:26
  133.3 1.3 fusion.12
  134.6 3.7 %collective-permute-start.4 = (bf16[384,512]{1,0:T(8,128)(2,1)S(1)}, bf16[384,512]{1,0:T(8,128)(2,1)}, u32[]{:S(2)}, u32[]{:S(2)}) collective-permute-start(bf16[384,512]{1,0:T(8,128)(2,1)S(1)} %fusion.12), channel_id=1, source_target_pairs={{0,2},{2,4},{4,6},{6,8},{8,10},{10,12},{12,14},{14,0},{1,15},{3,1}... | collective-permute-start | bytes 1179656 | tf_op jit(solution)/shard_map/ppermute | solution.py:26
  138.8 1.2 fusion.7
  139.9 4.6 %all-to-all-start.2 = ((bf16[32,24,256]{2,1,0:T(8,128)(2,1)}), bf16[32,24,256]{2,1,0:T(8,128)(2,1)S(1)}, u32[]{:S(2)}, u32[]{:S(2)}) async-start(bf16[32,24,256]{2,1,0:T(8,128)(2,1)} %bitcast.39), calls=%async_computation.2 | async-start | bytes 786432 | tf_op jit(solution)/shard_map/all_to_all | solution.py:168
  144.6 1.3 bitcast_add_fusion.2
  146.6 7.8 %collective-permute-start.5 = (bf16[384,256]{1,0:T(8,128)(2,1)S(1)}, bf16[384,256]{1,0:T(8,128)(2,1)S(1)}, u32[]{:S(2)}, u32[]{:S(2)}) collective-permute-start(bf16[384,256]{1,0:T(8,128)(2,1)S(1)} %get-tuple-element.8), channel_id=1, source_target_pairs={{0,3},{2,5},{4,7},{6,9},{8,11},{10,13},{12,15},{14,1},{1,0},{3,2},... | collective-permute-start | bytes 589832 | tf_op jit(solution)/shard_map/ppermute | solution.py:26
  154.4 6.3 %collective-permute-done.5 = bf16[384,256]{1,0:T(8,128)(2,1)S(1)} collective-permute-done((bf16[384,256]{1,0:T(8,128)(2,1)S(1)}, bf16[384,256]{1,0:T(8,128)(2,1)S(1)}, u32[]{:S(2)}, u32[]{:S(2)}) %collective-permute-start.5) | collective-permute-done | bytes 196640 | tf_op jit(solution)/shard_map/ppermute | solution.py:26
  (82 shorter events, 13.6 us)
Async XLA Ops:
  0.6 52.3 %copy-start = (bf16[16,128,128]{2,1,0:T(8,128)(2,1)S(1)}, bf16[16,128,128]{2,1,0:T(8,128)(2,1)}, u32[]{:S(2)}) copy-start(bf16[16,128,128]{2,1,0:T(8,128)(2,1)} %param.19) | copy-start | bytes 1572868
  0.6 7.2 %copy-start.1 = (bf16[128,4096]{1,0:T(8,128)(2,1)S(1)}, bf16[128,4096]{1,0:T(8,128)(2,1)}, u32[]{:S(2)}) copy-start(bf16[128,4096]{1,0:T(8,128)(2,1)} %param.22) | copy-start | bytes 3145732
  0.7 8.0 %copy-start.7 = (f32[4096]{0:T(1024)S(1)}, f32[4096]{0:T(1024)}, u32[]{:S(2)}) copy-start(f32[4096]{0:T(1024)} %param.23) | copy-start | bytes 49156
  1.5 51.4 %collective-permute-start = (bf16[15,128]{1,0:T(8,128)(2,1)S(1)}, bf16[15,128]{1,0:T(8,128)(2,1)S(1)}, u32[]{:S(2)}, u32[]{:S(2)}) collective-permute-start(bf16[15,128]{1,0:T(8,128)(2,1)S(1)} %slice.140), channel_id=1, source_target_pairs={{0,16},{16,32},{32,48},{48,64},{64,80},{80,96},{96,112},{112,128},... | collective-permute-start | bytes 11528 | tf_op jit(solution)/shard_map/ppermute | solution.py:18
  10.0 18.4 %copy-start.5 = (bf16[4096,32]{0,1:T(8,128)(2,1)S(1)}, bf16[4096,32]{0,1:T(8,128)(2,1)}, u32[]{:S(2)}) copy-start(bf16[4096,32]{0,1:T(8,128)(2,1)} %param.29) | copy-start | bytes 786436
  10.0 33.8 %all-to-all-start = ((bf16[32,24,512]{2,1,0:T(8,128)(2,1)}), bf16[32,24,512]{2,1,0:T(8,128)(2,1)S(1)}, u32[]{:S(2)}, u32[]{:S(2)}) async-start(bf16[32,24,512]{2,1,0:T(8,128)(2,1)} %bitcast.28), calls=%async_computation | async-start | bytes 1572864 | tf_op jit(solution)/shard_map/all_to_all | solution.py:168
  22.8 39.8 %collective-permute-start.7 = (bf16[64,4096]{1,0:T(8,128)(2,1)}, bf16[64,4096]{1,0:T(8,128)(2,1)}, u32[]{:S(2)}, u32[]{:S(2)}) collective-permute-start(bf16[64,4096]{1,0:T(8,128)(2,1)} %bitcast.22.gate), channel_id=1, source_target_pairs={{0,1},{1,0},{2,3},{3,2},{4,5},{5,4},{6,7},{7,6},{8,9},{9,8},{10,11... | collective-permute-start | bytes 1572872 | tf_op jit(solution)/shard_map/ppermute | solution.py:31
  25.9 36.6 %collective-permute-start.8 = (bf16[64,4096]{1,0:T(8,128)(2,1)}, bf16[64,4096]{1,0:T(8,128)(2,1)}, u32[]{:S(2)}, u32[]{:S(2)}) collective-permute-start(bf16[64,4096]{1,0:T(8,128)(2,1)} %bitcast.24.up), channel_id=1, source_target_pairs={{0,1},{1,0},{2,3},{3,2},{4,5},{5,4},{6,7},{7,6},{8,9},{9,8},{10,11... | collective-permute-start | bytes 1572872 | tf_op jit(solution)/shard_map/ppermute | solution.py:31
  27.9 1.0 copy-start.13
  28.4 22.5 %copy-start.11 = (s32[4]{0:T(128)S(1)}, s32[4]{0:T(128)}, u32[]{:S(2)}) copy-start(s32[4]{0:T(128)} %constant.150.clone) | copy-start | bytes 52
  28.4 22.5 %copy-start.12 = (s32[4]{0:T(128)S(1)}, s32[4]{0:T(128)}, u32[]{:S(2)}) copy-start(s32[4]{0:T(128)} %constant.151.clone) | copy-start | bytes 52
  28.4 22.5 %copy-start.9 = (s32[5]{0:T(128)S(1)}, s32[5]{0:T(128)}, u32[]{:S(2)}) copy-start(s32[5]{0:T(128)} %constant.152.clone) | copy-start | bytes 64
  28.4 22.5 %copy-start.10 = (s32[5]{0:T(128)S(1)}, s32[5]{0:T(128)}, u32[]{:S(2)}) copy-start(s32[5]{0:T(128)} %constant.153.clone) | copy-start | bytes 64
  28.4 23.7 %copy-start.6 = (bf16[256,128]{1,0:T(8,128)(2,1)S(1)}, bf16[256,128]{1,0:T(8,128)(2,1)}, u32[]{:S(2)}) copy-start(bf16[256,128]{1,0:T(8,128)(2,1)} %param.18) | copy-start | bytes 196612
  43.9 21.4 %collective-permute-start.10 = (bf16[768,512]{1,0:T(8,128)(2,1)S(1)}, bf16[768,512]{1,0:T(8,128)(2,1)}, u32[]{:S(2)}, u32[]{:S(2)}) collective-permute-start(bf16[768,512]{1,0:T(8,128)(2,1)S(1)} %bitcast.98), channel_id=1, source_target_pairs={{0,14},{2,0},{4,2},{6,4},{8,6},{10,8},{12,10},{14,12},{1,3},{3,5},... | collective-permute-start | bytes 2359304 | tf_op jit(solution)/shard_map/ppermute | solution.py:26
  47.1 21.5 %collective-permute-start.9 = (bf16[768,512]{1,0:T(8,128)(2,1)S(1)}, bf16[768,512]{1,0:T(8,128)(2,1)S(1)}, u32[]{:S(2)}, u32[]{:S(2)}) collective-permute-start(bf16[768,512]{1,0:T(8,128)(2,1)S(1)} %bitcast.99), channel_id=1, source_target_pairs={{0,2},{2,4},{4,6},{6,8},{8,10},{10,12},{12,14},{14,0},{1,15},{3,1}... | collective-permute-start | bytes 2359304 | tf_op jit(solution)/shard_map/ppermute | solution.py:26
  57.5 40.8 %collective-permute-start.1 = (bf16[4,384,512]{2,1,0:T(8,128)(2,1)}, bf16[4,384,512]{2,1,0:T(8,128)(2,1)}, u32[]{:S(2)}, u32[]{:S(2)}) collective-permute-start(bf16[4,384,512]{2,1,0:T(8,128)(2,1)} %get-tuple-element.7), channel_id=1, source_target_pairs={{0,1},{1,0},{2,3},{3,2},{4,5},{5,4},{6,7},{7,6},{8,9},{9,8},{10,11... | collective-permute-start | bytes 4718600 | tf_op jit(solution)/shard_map/ppermute | solution.py:31
  65.3 5.6 %copy-start.2 = (bf16[5,256,512]{2,1,0:T(8,128)(2,1)S(1)}, bf16[5,256,512]{2,1,0:T(8,128)(2,1)}, u32[]{:S(2)}) copy-start(bf16[5,256,512]{2,1,0:T(8,128)(2,1)} %shard_map.186) | copy-start | bytes 3932164
  65.3 6.4 %collective-permute-start.12 = (bf16[768,512]{1,0:T(8,128)(2,1)}, bf16[768,512]{1,0:T(8,128)(2,1)S(1)}, u32[]{:S(2)}, u32[]{:S(2)}) collective-permute-start(bf16[768,512]{1,0:T(8,128)(2,1)} %collective-permute-done.10), channel_id=1, source_target_pairs={{0,14},{2,0},{4,2},{6,4},{8,6},{10,8},{12,10},{14,12},{16,30},{18,... | collective-permute-start | bytes 2359304 | tf_op jit(solution)/shard_map/ppermute | solution.py:26
  68.5 3.6 %collective-permute-start.11 = (bf16[768,512]{1,0:T(8,128)(2,1)S(1)}, bf16[768,512]{1,0:T(8,128)(2,1)S(1)}, u32[]{:S(2)}, u32[]{:S(2)}) collective-permute-start(bf16[768,512]{1,0:T(8,128)(2,1)S(1)} %collective-permute-done.9), channel_id=1, source_target_pairs={{0,2},{2,4},{4,6},{6,8},{8,10},{10,12},{12,14},{14,0},{16,18},{18,... | collective-permute-start | bytes 2359304 | tf_op jit(solution)/shard_map/ppermute | solution.py:26
  72.5 20.6 %collective-permute-start.13 = (f32[128,768]{1,0:T(8,128)S(1)}, f32[128,768]{1,0:T(8,128)S(1)}, u32[]{:S(2)}, u32[]{:S(2)}) collective-permute-start(f32[128,768]{1,0:T(8,128)S(1)} %slice.222), channel_id=1, source_target_pairs={{0,1},{1,0},{2,3},{3,2},{4,5},{5,4},{6,7},{7,6},{8,9},{9,8},{10,11... | collective-permute-start | bytes 1179656 | tf_op jit(solution)/shard_map/ppermute | solution.py:31
  93.2 5.2 %copy-start.3 = (bf16[4,384,512]{2,1,0:T(8,128)(2,1)S(1)}, bf16[4,384,512]{2,1,0:T(8,128)(2,1)}, u32[]{:S(2)}) copy-start(bf16[4,384,512]{2,1,0:T(8,128)(2,1)} %get-tuple-element.6) | copy-start | bytes 4718596
  94.2 32.8 %all-to-all-start.1 = ((bf16[8,64,768]{2,1,0:T(8,128)(2,1)}), bf16[8,64,768]{2,1,0:T(8,128)(2,1)S(1)}, u32[]{:S(2)}, u32[]{:S(2)}) async-start(bf16[8,64,768]{2,1,0:T(8,128)(2,1)} %broadcast_in_dim.93), calls=%async_computation.1 | async-start | bytes 1572864 | tf_op jit(solution)/shard_map/all_to_all | solution.py:220
  98.3 31.3 %copy-start.4 = (bf16[1,1024,256]{2,1,0:T(8,128)(2,1)S(1)}, bf16[1,1024,256]{2,1,0:T(8,128)(2,1)}, u32[]{:S(2)}) copy-start(bf16[1,1024,256]{2,1,0:T(8,128)(2,1)} %param.28) | copy-start | bytes 1572868
  99.5 30.2 %copy-start.8 = (f32[128,4]{0,1:T(4,128)S(1)}, f32[128,4]{0,1:T(4,128)}, u32[]{:S(2)}) copy-start(f32[128,4]{0,1:T(4,128)} %param.25) | copy-start | bytes 6148
  99.5 22.8 %collective-permute-start.2 = (bf16[384,512]{1,0:T(8,128)(2,1)S(1)}, bf16[384,512]{1,0:T(8,128)(2,1)S(1)}, u32[]{:S(2)}, u32[]{:S(2)}) collective-permute-start(bf16[384,512]{1,0:T(8,128)(2,1)S(1)} %fusion.13), channel_id=1, source_target_pairs={{0,2},{2,4},{4,6},{6,8},{8,10},{10,12},{12,14},{14,0},{1,15},{3,1}... | collective-permute-start | bytes 1179656 | tf_op jit(solution)/shard_map/ppermute | solution.py:26
  124.2 9.1 %collective-permute-start.3 = (bf16[384,512]{1,0:T(8,128)(2,1)}, bf16[384,512]{1,0:T(8,128)(2,1)}, u32[]{:S(2)}, u32[]{:S(2)}) collective-permute-start(bf16[384,512]{1,0:T(8,128)(2,1)} %fusion.11), channel_id=1, source_target_pairs={{0,2},{2,4},{4,6},{6,8},{8,10},{10,12},{12,14},{14,0},{1,15},{3,1}... | collective-permute-start | bytes 1179656 | tf_op jit(solution)/shard_map/ppermute | solution.py:26
  127.0 11.7 %collective-permute-start.14 = (bf16[8,64,768]{2,1,0:T(8,128)(2,1)S(1)}, bf16[8,64,768]{2,1,0:T(8,128)(2,1)S(1)}, u32[]{:S(2)}, u32[]{:S(2)}) collective-permute-start(bf16[8,64,768]{2,1,0:T(8,128)(2,1)S(1)} %all-to-all-done.1), channel_id=1, source_target_pairs={{0,1},{1,0},{2,3},{3,2},{4,5},{5,4},{6,7},{7,6},{8,9},{9,8},{10,11... | collective-permute-start | bytes 2359304 | tf_op jit(solution)/shard_map/ppermute | solution.py:31
  134.6 10.0 %collective-permute-start.4 = (bf16[384,512]{1,0:T(8,128)(2,1)S(1)}, bf16[384,512]{1,0:T(8,128)(2,1)}, u32[]{:S(2)}, u32[]{:S(2)}) collective-permute-start(bf16[384,512]{1,0:T(8,128)(2,1)S(1)} %fusion.12), channel_id=1, source_target_pairs={{0,2},{2,4},{4,6},{6,8},{8,10},{10,12},{12,14},{14,0},{1,15},{3,1}... | collective-permute-start | bytes 1179656 | tf_op jit(solution)/shard_map/ppermute | solution.py:26
  139.9 21.6 %all-to-all-start.2 = ((bf16[32,24,256]{2,1,0:T(8,128)(2,1)}), bf16[32,24,256]{2,1,0:T(8,128)(2,1)S(1)}, u32[]{:S(2)}, u32[]{:S(2)}) async-start(bf16[32,24,256]{2,1,0:T(8,128)(2,1)} %bitcast.39), calls=%async_computation.2 | async-start | bytes 786432 | tf_op jit(solution)/shard_map/all_to_all | solution.py:168
  145.9 8.6 %collective-permute-start.6 = (bf16[384,256]{1,0:T(8,128)(2,1)S(1)}, bf16[384,256]{1,0:T(8,128)(2,1)S(1)}, u32[]{:S(2)}, u32[]{:S(2)}) collective-permute-start(bf16[384,256]{1,0:T(8,128)(2,1)S(1)} %get-tuple-element.9), channel_id=1, source_target_pairs={{0,2},{2,4},{4,6},{6,8},{8,10},{10,12},{12,14},{14,0},{16,18},{18,... | collective-permute-start | bytes 589832 | tf_op jit(solution)/shard_map/ppermute | solution.py:26
  146.6 14.2 %collective-permute-start.5 = (bf16[384,256]{1,0:T(8,128)(2,1)S(1)}, bf16[384,256]{1,0:T(8,128)(2,1)S(1)}, u32[]{:S(2)}, u32[]{:S(2)}) collective-permute-start(bf16[384,256]{1,0:T(8,128)(2,1)S(1)} %get-tuple-element.8), channel_id=1, source_target_pairs={{0,3},{2,5},{4,7},{6,9},{8,11},{10,13},{12,15},{14,1},{1,0},{3,2},... | collective-permute-start | bytes 589832 | tf_op jit(solution)/shard_map/ppermute | solution.py:26

commit v7 on v6

--- a/solution.py
+++ b/solution.py
@@ -54,10 +54,15 @@
 def weight_kernel(index, gate, up, partner_gate, partner_up, blocks):
     count, _, width = blocks.shape
     units = gate.shape[0]
+    first = index[count] == 0
     for j in range(count):
         at = lanes(index[j], width)
-        for i, source in enumerate((gate, up, partner_gate, partner_up)):
-            blocks[j, i * units : (i + 1) * units] = source[:, at]
+        for i, (own, partner) in enumerate(((gate, partner_gate), (up, partner_up))):
+            mine = own[:, at]
+            other = partner[:, at]
+            low = 2 * i * units
+            blocks[j, low : low + units] = jnp.where(first, mine, other)
+            blocks[j, low + units : low + 2 * units] = jnp.where(first, other, mine)
 
 
 def project_kernel(index, group, hidden, proj, down, own, out):
@@ -177,6 +182,7 @@
     index = (y + jnp.stack([kept_ids, sent_ids])) % y_size
     offsets = jnp.where(core == 0, jnp.array([0, -1, 1, -2, 2], jnp.int32), jnp.array([0, 1, -1, 0, 0], jnp.int32))
     near_index = (home + y_size + offsets) % y_size
+    near_index = jnp.concatenate([near_index, core[None]]).astype(jnp.int32)
 
     group_out = pool_group_out(pool_input, earlier_rows, pool_map, pool_scale, tp_rank, ep_rank)
     normed = (centre * rstd * norm_gain[None, :]).astype(bf16)
@@ -194,10 +200,15 @@
     blocks = jax.ShapeDtypeStruct((5, 4 * units, chip_width), bf16)
     partner_gate = to_partner(gate_t)
     partner_up = to_partner(up_t)
+    own_down = expert_down[0]
+    partner_down = to_partner(own_down)
     weights = local_kernel(weight_kernel, near_index, (gate_t, up_t, partner_gate, partner_up), blocks)
 
     def part(j):
         return kept[j].astype(f32) + from_partner[j].astype(f32)
+
+    def ring_sum(j, ring):
+        return (part(j) + ring.astype(f32)).astype(bf16)
 
     def ring_step(x):
         return sent(x.astype(bf16), {0: (1, 0), 1: (-1, 1)})
@@ -207,29 +218,33 @@
     up_two = sent(one, {0: (1, 0)})
     down_two = sent(other, {0: (-1, 0)})
     ring = ring_step(part(0))
-    ring = ring_step(part(1) + ring.astype(f32))
+    ring = ring_step(ring_sum(1, ring))
     summed = tdot(weights[0], arrived)
     for j, rows in enumerate((one, other, up_two, down_two)):
         summed = summed + tdot(weights[j + 1], rows)
-    full = summed[: 2 * units] + to_partner(summed[2 * units :])
-    hidden = (jax.nn.silu(full[:units]) * full[units:]).astype(bf16)
-
-
-    copies = jnp.broadcast_to(hidden[None], (y_size, *hidden.shape))
-    groups = [[2 * i + c for i in range(y_size)] for c in range(2)]
-    own_hidden = lax.all_to_all(copies, "tp", 0, 0, axis_index_groups=groups, tiled=True)
-    ring = ring_step(part(2) + ring.astype(f32))
-    other_hidden = to_partner(own_hidden)
-    down_weight = expert_down[0].reshape(y_size, 2, units, slice_width)
-
-    def down_product(h, side):
-        w = lax.dynamic_index_in_dim(down_weight, side, 1, keepdims=False)
-        w = w.reshape(y_size * units, slice_width)
-        return lax.dot_general(
-            h.reshape(y_size * units, buffer_len), w, (((0,), (0,)), ((), ())), preferred_element_type=f32
-        )
-
-    expert_result = down_product(own_hidden, core) + down_product(other_hidden, 1 - core)
+    full = summed + to_partner(summed)
+    chip_units = 2 * units
+    hidden = (jax.nn.silu(full[:chip_units]) * full[chip_units:]).astype(bf16)
+
+    half = jnp.where(core == 0, hidden[:units], hidden[units:])
+    pieces = [(half, 0, units)]
+    for distance in range(y_size // 2, 0, -1):
+        block = half if 2 * distance == y_size else hidden
+        route = {0: (distance, 0), 1: (-distance, 1)}
+        pieces.append((sent(block, route), distance, block.shape[0]))
+    own_sum = partner_sum = 0.0
+    for h, distance, rows in pieces:
+        chip = (y + y_size + jnp.where(core == 0, -distance, distance)) % y_size
+        begin = chip * chip_units + (core * units if rows == units else 0)
+
+        def down_product(weight):
+            w = lax.dynamic_slice_in_dim(weight, begin, rows, 0)
+            return lax.dot_general(h, w, (((0,), (0,)), ((), ())), preferred_element_type=f32)
+
+        own_sum = own_sum + down_product(own_down)
+        partner_sum = partner_sum + down_product(partner_down)
+    ring = ring_step(ring_sum(2, ring))
+    expert_result = own_sum + to_partner(partner_sum.astype(bf16)).astype(f32)
     expert_result = expert_result.astype(bf16)
     returned = exchanged(expert_result)
     routed = lax.dot_general(combine, returned, (((0,), (0,)), ((), ())), preferred_element_type=f32)

time: 163 us -> 174 us (1.067)
  waiting for transfers between devices: 45.8 us -> 32.7 us
  starting transfers between devices: 85.5 us -> 97.4 us
  matrix products: 9.62 us -> 21.4 us
  local copies, waits for them, and re-layouts: 4.37 us -> 2.52 us
    dot_general x2 -> x10, matrix products: 1.57 us -> 11.7 us  [down_product(): lax.dot_general(h, w, (((0,), (0,)), ((), ())), preferred_element_type=f32)]
    ppermute x9 -> x13, waiting for transfers between devices: 30.5 us -> 22.6 us  [sent(): return lax.ppermute(x, 'tp', route)]
    all_to_all x2, starting transfers between devices: 17.3 us -> 24.5 us  [exchanged(): return lax.all_to_all(rows, 'ep', split_axis=0, concat_axis=0, tiled=True)]
    all_to_all x2, waiting for transfers between devices: 13.9 us -> 8.47 us  [exchanged(): return lax.all_to_all(rows, 'ep', split_axis=0, concat_axis=0, tiled=True)]
    ppermute x9 -> x13, starting transfers between devices: 28.2 us -> 33.6 us  [sent(): return lax.ppermute(x, 'tp', route)]
    ppermute x5 -> x6, starting transfers between devices: 32 us -> 36.2 us  [to_partner(): return lax.ppermute(x, 'tp', [(i, i ^ 1) for i in range(n)])]
    all_to_all x1 -> x0, starting transfers between devices: 4.11 us -> none  [per_device(): lax.all_to_all(copies, 'tp', 0, 0, axis_index_groups=groups, tiled=True)]
    convert_element_type x3 -> x1, other arithmetic: 4.3 us -> 1.31 us  [ring_step(): return sent(x.astype(bf16), {0: (1, 0), 1: (-1, 1)})]
  transfers between devices with their start and end apart: 18 -> 22, of which waited for: 6 -> 7; matrix products, arithmetic and copies ran while one was open for 13% -> 17% of each run, Pallas kernels for 4% -> 4%
where the time goes in v7:
time: 174 us; the launch traced here: 172 us
  starting transfers between devices  97.4 us (56%)
  waiting for transfers between devices  32.7 us (19%)
  matrix products  21.4 us (12%)
  other arithmetic  10.3 us (6%)
  Pallas kernels  6.28 us (4%)
  local copies, waits for them, and re-layouts  2.52 us (1%)
    ppermute x6, starting transfers between devices, to_partner(): return lax.ppermute(x, 'tp', [(i, i ^ 1) for i in range(n)])  36.2 us
    ppermute x13, starting transfers between devices, sent(): return lax.ppermute(x, 'tp', route)  33.6 us
    all_to_all x2, starting transfers between devices, exchanged(): return lax.all_to_all(rows, 'ep', split_axis=0, concat_axis=0, tiled=True)  24.5 us
    ppermute x13, waiting for transfers between devices, sent(): return lax.ppermute(x, 'tp', route)  22.6 us
    dot_general x10, matrix products, down_product(): lax.dot_general(h, w, (((0,), (0,)), ((), ())), preferred_element_type=f32)  11.7 us
    all_to_all x2, waiting for transfers between devices, exchanged(): return lax.all_to_all(rows, 'ep', split_axis=0, concat_axis=0, tiled=True)  8.47 us
    pallas_call x2, Pallas kernels, local_kernel(): pl.pallas_call(body, in_specs=[smem] + [vmem] * len(operands), out_specs=...  6.28 us
  transfers between devices with their start and end apart: 22, of which 7 were waited for; matrix products, arithmetic and copies ran while one was open for 17% of the time, Pallas kernels for 4%

profile of v7, /device:TPU:1, one launch (start us, length us, event | category | flops | bytes accessed | tf_op | source)
XLA Modules:
  0.0 172.1 jit_solution(4751216675311716019)
XLA Ops:
  1.6 1.5 convert_reduce_fusion
  4.0 1.4 convolution_convert_fusion
  5.3 13.7 %all-to-all-start = ((bf16[32,24,512]{2,1,0:T(8,128)(2,1)}), bf16[32,24,512]{2,1,0:T(8,128)(2,1)S(1)}, u32[]{:S(2)}, u32[]{:S(2)}) async-start(bf16[32,24,512]{2,1,0:T(8,128)(2,1)} %bitcast.29), calls=%async_computation | async-start | bytes 1572864 | tf_op jit(solution)/shard_map/all_to_all | solution.py:173
  19.1 3.1 %collective-permute-start = (bf16[15,128]{1,0:T(8,128)(2,1)S(1)}, bf16[15,128]{1,0:T(8,128)(2,1)S(1)}, u32[]{:S(2)}, u32[]{:S(2)}) collective-permute-start(bf16[15,128]{1,0:T(8,128)(2,1)S(1)} %slice.140), channel_id=1, source_target_pairs={{0,16},{16,32},{32,48},{48,64},{64,80},{80,96},{96,112},{112,128},... | collective-permute-start | bytes 11528 | tf_op jit(solution)/shard_map/ppermute | solution.py:18
  24.1 2.0 %fusion.17.hidden = bf16[128,32]{1,0:T(8,128)(2,1)} fusion(bf16[128,4096]{1,0:T(8,128)(2,1)S(1)} %fusion.4, bf16[4096,32]{0,1:T(8,128)(2,1)} %param.30, f32[128,32]{1,0:T(8,128)S(1)} %fusion.123), kind=kOutput, calls=%fused_computation.28 | convolution fusion | flops 33579008 | bytes 1335296 | tf_op jit(solution)/shard_map/dot_general | solution.py:190
  28.5 3.5 %shard_map.185 = (bf16[4,384,512]{2,1,0:T(8,128)(2,1)}, bf16[4,384,512]{2,1,0:T(8,128)(2,1)}) custom-call(s32[2,4]{1,0:T(2,128)} %and_select_fusion.3.index, bf16[256,128]{1,0:T(8,128)(2,1)} %fusion.16.group, bf16[128,32]{1,0:T(8,128)(2,1)} %fusion.17.hidden, bf16[128,4096]{1,0:T(8,128)(2,1)} %proj.1, bf16[32,4096]{1,0:T(8,128)(2,1)} %down.1), custom_call_target="tpu_custom_call" | custom-call | tf_op jit(solution)/shard_map/pallas_call | solution.py:46
  32.1 3.4 %collective-permute-start.1 = (bf16[4,384,512]{2,1,0:T(8,128)(2,1)}, bf16[4,384,512]{2,1,0:T(8,128)(2,1)}, u32[]{:S(2)}, u32[]{:S(2)}) collective-permute-start(bf16[4,384,512]{2,1,0:T(8,128)(2,1)} %get-tuple-element.7), channel_id=1, source_target_pairs={{0,1},{1,0},{2,3},{3,2},{4,5},{5,4},{6,7},{7,6},{8,9},{9,8},{10,11... | collective-permute-start | bytes 4718600 | tf_op jit(solution)/shard_map/ppermute | solution.py:31
  35.5 4.6 %all-to-all-done = bf16[32,24,512]{2,1,0:T(8,128)(2,1)S(1)} async-done(((bf16[32,24,512]{2,1,0:T(8,128)(2,1)}), bf16[32,24,512]{2,1,0:T(8,128)(2,1)S(1)}, u32[]{:S(2)}, u32[]{:S(2)}) %all-to-all-start) | async-done | bytes 786464 | tf_op jit(solution)/shard_map/all_to_all | solution.py:173
  40.1 3.2 %collective-permute-start.10 = (bf16[768,512]{1,0:T(8,128)(2,1)S(1)}, bf16[768,512]{1,0:T(8,128)(2,1)S(1)}, u32[]{:S(2)}, u32[]{:S(2)}) collective-permute-start(bf16[768,512]{1,0:T(8,128)(2,1)S(1)} %bitcast.115), channel_id=1, source_target_pairs={{0,14},{2,0},{4,2},{6,4},{8,6},{10,8},{12,10},{14,12},{1,3},{3,5},... | collective-permute-start | bytes 2359304 | tf_op jit(solution)/shard_map/ppermute | solution.py:26
  43.3 3.8 %collective-permute-start.9 = (bf16[768,512]{1,0:T(8,128)(2,1)S(1)}, bf16[768,512]{1,0:T(8,128)(2,1)S(1)}, u32[]{:S(2)}, u32[]{:S(2)}) collective-permute-start(bf16[768,512]{1,0:T(8,128)(2,1)S(1)} %bitcast.116), channel_id=1, source_target_pairs={{0,2},{2,4},{4,6},{6,8},{8,10},{10,12},{12,14},{14,0},{1,15},{3,1}... | collective-permute-start | bytes 2359304 | tf_op jit(solution)/shard_map/ppermute | solution.py:26
  47.2 5.0 %collective-permute-start.7 = (bf16[64,4096]{1,0:T(8,128)(2,1)}, bf16[64,4096]{1,0:T(8,128)(2,1)}, u32[]{:S(2)}, u32[]{:S(2)}) collective-permute-start(bf16[64,4096]{1,0:T(8,128)(2,1)} %bitcast.118), channel_id=1, source_target_pairs={{0,1},{1,0},{2,3},{3,2},{4,5},{5,4},{6,7},{7,6},{8,9},{9,8},{10,11... | collective-permute-start | bytes 1572872 | tf_op jit(solution)/shard_map/ppermute | solution.py:31
  52.1 1.9 %collective-permute-start.8 = (bf16[64,4096]{1,0:T(8,128)(2,1)}, bf16[64,4096]{1,0:T(8,128)(2,1)}, u32[]{:S(2)}, u32[]{:S(2)}) collective-permute-start(bf16[64,4096]{1,0:T(8,128)(2,1)} %bitcast.120), channel_id=1, source_target_pairs={{0,1},{1,0},{2,3},{3,2},{4,5},{5,4},{6,7},{7,6},{8,9},{9,8},{10,11... | collective-permute-start | bytes 1572872 | tf_op jit(solution)/shard_map/ppermute | solution.py:31
  54.7 1.6 collective-permute-done.8.partner_up
  56.3 2.7 %shard_map.186 = bf16[5,256,512]{2,1,0:T(8,128)(2,1)} custom-call(s32[6]{0:T(128)} %pad_add_fusion.index, bf16[64,4096]{1,0:T(8,128)(2,1)} %bitcast.119, bf16[64,4096]{1,0:T(8,128)(2,1)} %bitcast.121, bf16[64,4096]{1,0:T(8,128)(2,1)} %collective-permute-done.7.partner_gate, bf16[64,4096]{1,0:T(8,128)(2,1)} %collective-permute-done.8.partner_up), custom_call_target="tpu_custom_call" | custom-call | tf_op jit(solution)/shard_map/pallas_call | solution.py:46
  60.3 4.9 %collective-permute-start.2 = (bf16[384,512]{1,0:T(8,128)(2,1)S(1)}, bf16[384,512]{1,0:T(8,128)(2,1)S(1)}, u32[]{:S(2)}, u32[]{:S(2)}) collective-permute-start(bf16[384,512]{1,0:T(8,128)(2,1)S(1)} %fusion.20), channel_id=1, source_target_pairs={{0,2},{2,4},{4,6},{6,8},{8,10},{10,12},{12,14},{14,0},{1,15},{3,1}... | collective-permute-start | bytes 1179656 | tf_op jit(solution)/shard_map/ppermute | solution.py:26
  69.7 18.4 %collective-permute-start.13 = (f32[256,768]{1,0:T(8,128)S(1)}, f32[256,768]{1,0:T(8,128)}, u32[]{:S(2)}, u32[]{:S(2)}) collective-permute-start(f32[256,768]{1,0:T(8,128)S(1)} %fusion.11), channel_id=1, source_target_pairs={{0,1},{1,0},{2,3},{3,2},{4,5},{5,4},{6,7},{7,6},{8,9},{9,8},{10,11... | collective-permute-start | bytes 2359304 | tf_op jit(solution)/shard_map/ppermute | solution.py:31
  89.3 1.9 %collective-permute-start.3 = (bf16[384,512]{1,0:T(8,128)(2,1)S(1)}, bf16[384,512]{1,0:T(8,128)(2,1)}, u32[]{:S(2)}, u32[]{:S(2)}) collective-permute-start(bf16[384,512]{1,0:T(8,128)(2,1)S(1)} %fusion.18), channel_id=1, source_target_pairs={{0,2},{2,4},{4,6},{6,8},{8,10},{10,12},{12,14},{14,0},{1,15},{3,1}... | collective-permute-start | bytes 1179656 | tf_op jit(solution)/shard_map/ppermute | solution.py:26
  91.3 1.9 %collective-permute-start.18 = (bf16[1024,256]{1,0:T(8,128)(2,1)}, bf16[1024,256]{1,0:T(8,128)(2,1)}, u32[]{:S(2)}, u32[]{:S(2)}) collective-permute-start(bf16[1024,256]{1,0:T(8,128)(2,1)} %bitcast.40), channel_id=1, source_target_pairs={{0,1},{1,0},{2,3},{3,2},{4,5},{5,4},{6,7},{7,6},{8,9},{9,8},{10,11... | collective-permute-start | bytes 1572872 | tf_op jit(solution)/shard_map/ppermute | solution.py:31
  93.4 4.9 %collective-permute-done.3 = bf16[384,512]{1,0:T(8,128)(2,1)} collective-permute-done((bf16[384,512]{1,0:T(8,128)(2,1)S(1)}, bf16[384,512]{1,0:T(8,128)(2,1)}, u32[]{:S(2)}, u32[]{:S(2)}) %collective-permute-start.3) | collective-permute-done | bytes 393248 | tf_op jit(solution)/shard_map/ppermute | solution.py:26
  99.5 2.8 %collective-permute-start.4 = (bf16[384,512]{1,0:T(8,128)(2,1)S(1)}, bf16[384,512]{1,0:T(8,128)(2,1)}, u32[]{:S(2)}, u32[]{:S(2)}) collective-permute-start(bf16[384,512]{1,0:T(8,128)(2,1)S(1)} %fusion.19), channel_id=1, source_target_pairs={{0,2},{2,4},{4,6},{6,8},{8,10},{10,12},{12,14},{14,0},{1,15},{3,1}... | collective-permute-start | bytes 1179656 | tf_op jit(solution)/shard_map/ppermute | solution.py:26
  103.8 1.9 %collective-permute-start.17 = (bf16[128,768]{1,0:T(8,128)(2,1)S(1)}, bf16[128,768]{1,0:T(8,128)(2,1)S(1)}, u32[]{:S(2)}, u32[]{:S(2)}) collective-permute-start(bf16[128,768]{1,0:T(8,128)(2,1)S(1)} %fusion.21), channel_id=1, source_target_pairs={{0,2},{2,4},{4,6},{6,8},{8,10},{10,12},{12,14},{14,0},{1,15},{3,1}... | collective-permute-start | bytes 589832 | tf_op jit(solution)/shard_map/ppermute | solution.py:26
  105.7 4.2 %collective-permute-start.16 = (bf16[128,768]{1,0:T(8,128)(2,1)S(1)}, bf16[128,768]{1,0:T(8,128)(2,1)S(1)}, u32[]{:S(2)}, u32[]{:S(2)}) collective-permute-start(bf16[128,768]{1,0:T(8,128)(2,1)S(1)} %fusion.21), channel_id=1, source_target_pairs={{0,4},{2,6},{4,8},{6,10},{8,12},{10,14},{12,0},{14,2},{1,13},{3,15... | collective-permute-start | bytes 589832 | tf_op jit(solution)/shard_map/ppermute | solution.py:26
  109.9 4.7 %collective-permute-start.14 = (bf16[64,768]{1,0:T(8,128)(2,1)S(1)}, bf16[64,768]{1,0:T(8,128)(2,1)S(1)}, u32[]{:S(2)}, u32[]{:S(2)}) collective-permute-start(bf16[64,768]{1,0:T(8,128)(2,1)S(1)} %slice_select_fusion), channel_id=1, source_target_pairs={{0,8},{2,10},{4,12},{6,14},{8,0},{10,2},{12,4},{14,6},{1,9},{3,11}... | collective-permute-start | bytes 294920 | tf_op jit(solution)/shard_map/ppermute | solution.py:26
  115.6 7.4 %collective-permute-done.14 = bf16[64,768]{1,0:T(8,128)(2,1)S(1)} collective-permute-done((bf16[64,768]{1,0:T(8,128)(2,1)S(1)}, bf16[64,768]{1,0:T(8,128)(2,1)S(1)}, u32[]{:S(2)}, u32[]{:S(2)}) %collective-permute-start.14) | collective-permute-done | bytes 98336 | tf_op jit(solution)/shard_map/ppermute | solution.py:26
  123.0 1.9 %collective-permute-start.15 = (bf16[128,768]{1,0:T(8,128)(2,1)S(1)}, bf16[128,768]{1,0:T(8,128)(2,1)S(1)}, u32[]{:S(2)}, u32[]{:S(2)}) collective-permute-start(bf16[128,768]{1,0:T(8,128)(2,1)S(1)} %fusion.21), channel_id=1, source_target_pairs={{0,6},{2,8},{4,10},{6,12},{8,14},{10,0},{12,2},{14,4},{1,11},{3,13... | collective-permute-start | bytes 589832 | tf_op jit(solution)/shard_map/ppermute | solution.py:26
  129.3 4.7 %collective-permute-done.15 = bf16[128,768]{1,0:T(8,128)(2,1)S(1)} collective-permute-done((bf16[128,768]{1,0:T(8,128)(2,1)S(1)}, bf16[128,768]{1,0:T(8,128)(2,1)S(1)}, u32[]{:S(2)}, u32[]{:S(2)}) %collective-permute-start.15) | collective-permute-done | bytes 196640 | tf_op jit(solution)/shard_map/ppermute | solution.py:26
  136.2 5.6 %collective-permute-start.19 = (bf16[768,256]{1,0:T(8,128)(2,1)S(1)}, bf16[768,256]{1,0:T(8,128)(2,1)S(1)}, u32[]{:S(2)}, u32[]{:S(2)}) collective-permute-start(bf16[768,256]{1,0:T(8,128)(2,1)S(1)} %fusion.14), channel_id=1, source_target_pairs={{0,1},{1,0},{2,3},{3,2},{4,5},{5,4},{6,7},{7,6},{8,9},{9,8},{10,11... | collective-permute-start | bytes 1179656 | tf_op jit(solution)/shard_map/ppermute | solution.py:31
  144.1 1.9 %fusion.13 = bf16[768,256]{1,0:T(8,128)(2,1)} fusion(f32[768,256]{1,0:T(8,128)S(1)} %fusion.66, f32[768,256]{1,0:T(8,128)S(1)} %fusion.68, f32[768,256]{1,0:T(8,128)S(1)} %convolution_add_fusion.2, bf16[128,768]{1,0:T(8,128)(2,1)S(1)} %collective-permute-done.15, bf16[768,256]{1,0:T(8,128)(2,1)S(1)} %collective-permute-done.19, ...), kind=kOutput, calls=%fused_computation.21 | convolution fusion | flops 51511296 | bytes 3407876 | tf_op jit(solution)/shard_map/dot_general | solution.py:242
  146.0 10.8 %all-to-all-start.1 = ((bf16[32,24,256]{2,1,0:T(8,128)(2,1)}), bf16[32,24,256]{2,1,0:T(8,128)(2,1)S(1)}, u32[]{:S(2)}, u32[]{:S(2)}) async-start(bf16[32,24,256]{2,1,0:T(8,128)(2,1)} %bitcast.41), calls=%async_computation.1 | async-start | bytes 786432 | tf_op jit(solution)/shard_map/all_to_all | solution.py:173
  158.2 2.2 %collective-permute-start.5 = (bf16[384,256]{1,0:T(8,128)(2,1)S(1)}, bf16[384,256]{1,0:T(8,128)(2,1)S(1)}, u32[]{:S(2)}, u32[]{:S(2)}) collective-permute-start(bf16[384,256]{1,0:T(8,128)(2,1)S(1)} %get-tuple-element.8), channel_id=1, source_target_pairs={{0,3},{2,5},{4,7},{6,9},{8,11},{10,13},{12,15},{14,1},{1,0},{3,2},... | collective-permute-start | bytes 589832 | tf_op jit(solution)/shard_map/ppermute | solution.py:26
  161.1 5.6 %collective-permute-done.5 = bf16[384,256]{1,0:T(8,128)(2,1)S(1)} collective-permute-done((bf16[384,256]{1,0:T(8,128)(2,1)S(1)}, bf16[384,256]{1,0:T(8,128)(2,1)S(1)}, u32[]{:S(2)}, u32[]{:S(2)}) %collective-permute-start.5) | collective-permute-done | bytes 196640 | tf_op jit(solution)/shard_map/ppermute | solution.py:26
  167.4 3.8 %all-to-all-done.1 = bf16[32,24,256]{2,1,0:T(8,128)(2,1)S(1)} async-done(((bf16[32,24,256]{2,1,0:T(8,128)(2,1)}), bf16[32,24,256]{2,1,0:T(8,128)(2,1)S(1)}, u32[]{:S(2)}, u32[]{:S(2)}) %all-to-all-start.1) | async-done | bytes 393248 | tf_op jit(solution)/shard_map/all_to_all | solution.py:173
  (91 shorter events, 29.7 us)
Async XLA Ops:
  0.6 26.9 %copy-start = (bf16[16,128,128]{2,1,0:T(8,128)(2,1)S(1)}, bf16[16,128,128]{2,1,0:T(8,128)(2,1)}, u32[]{:S(2)}) copy-start(bf16[16,128,128]{2,1,0:T(8,128)(2,1)} %param.19) | copy-start | bytes 1572868
  0.7 2.9 %copy-start.5 = (f32[4096]{0:T(1024)S(1)}, f32[4096]{0:T(1024)}, u32[]{:S(2)}) copy-start(f32[4096]{0:T(1024)} %param.23) | copy-start | bytes 49156
  3.5 15.5 %copy-start.4 = (bf16[256,128]{1,0:T(8,128)(2,1)S(1)}, bf16[256,128]{1,0:T(8,128)(2,1)}, u32[]{:S(2)}) copy-start(bf16[256,128]{1,0:T(8,128)(2,1)} %param.18) | copy-start | bytes 196612
  5.3 34.8 %all-to-all-start = ((bf16[32,24,512]{2,1,0:T(8,128)(2,1)}), bf16[32,24,512]{2,1,0:T(8,128)(2,1)S(1)}, u32[]{:S(2)}, u32[]{:S(2)}) async-start(bf16[32,24,512]{2,1,0:T(8,128)(2,1)} %bitcast.29), calls=%async_computation | async-start | bytes 1572864 | tf_op jit(solution)/shard_map/all_to_all | solution.py:173
  19.1 8.4 %collective-permute-start = (bf16[15,128]{1,0:T(8,128)(2,1)S(1)}, bf16[15,128]{1,0:T(8,128)(2,1)S(1)}, u32[]{:S(2)}, u32[]{:S(2)}) collective-permute-start(bf16[15,128]{1,0:T(8,128)(2,1)S(1)} %slice.140), channel_id=1, source_target_pairs={{0,16},{16,32},{32,48},{48,64},{64,80},{80,96},{96,112},{112,128},... | collective-permute-start | bytes 11528 | tf_op jit(solution)/shard_map/ppermute | solution.py:18
  22.6 3.4 %copy-start.9 = (s32[4]{0:T(128)S(1)}, s32[4]{0:T(128)}, u32[]{:S(2)}) copy-start(s32[4]{0:T(128)} %constant.180.clone) | copy-start | bytes 52
  22.7 3.4 %copy-start.10 = (s32[4]{0:T(128)S(1)}, s32[4]{0:T(128)}, u32[]{:S(2)}) copy-start(s32[4]{0:T(128)} %constant.181.clone) | copy-start | bytes 52
  27.5 26.6 %copy-start.7 = (s32[5]{0:T(128)S(1)}, s32[5]{0:T(128)}, u32[]{:S(2)}) copy-start(s32[5]{0:T(128)} %constant.182.clone) | copy-start | bytes 64
  27.5 26.6 %copy-start.8 = (s32[5]{0:T(128)S(1)}, s32[5]{0:T(128)}, u32[]{:S(2)}) copy-start(s32[5]{0:T(128)} %constant.183.clone) | copy-start | bytes 64
  32.1 26.9 %collective-permute-start.1 = (bf16[4,384,512]{2,1,0:T(8,128)(2,1)}, bf16[4,384,512]{2,1,0:T(8,128)(2,1)}, u32[]{:S(2)}, u32[]{:S(2)}) collective-permute-start(bf16[4,384,512]{2,1,0:T(8,128)(2,1)} %get-tuple-element.7), channel_id=1, source_target_pairs={{0,1},{1,0},{2,3},{3,2},{4,5},{5,4},{6,7},{7,6},{8,9},{9,8},{10,11... | collective-permute-start | bytes 4718600 | tf_op jit(solution)/shard_map/ppermute | solution.py:31
  40.1 25.1 %collective-permute-start.10 = (bf16[768,512]{1,0:T(8,128)(2,1)S(1)}, bf16[768,512]{1,0:T(8,128)(2,1)S(1)}, u32[]{:S(2)}, u32[]{:S(2)}) collective-permute-start(bf16[768,512]{1,0:T(8,128)(2,1)S(1)} %bitcast.115), channel_id=1, source_target_pairs={{0,14},{2,0},{4,2},{6,4},{8,6},{10,8},{12,10},{14,12},{1,3},{3,5},... | collective-permute-start | bytes 2359304 | tf_op jit(solution)/shard_map/ppermute | solution.py:26
  43.3 22.6 %collective-permute-start.9 = (bf16[768,512]{1,0:T(8,128)(2,1)S(1)}, bf16[768,512]{1,0:T(8,128)(2,1)S(1)}, u32[]{:S(2)}, u32[]{:S(2)}) collective-permute-start(bf16[768,512]{1,0:T(8,128)(2,1)S(1)} %bitcast.116), channel_id=1, source_target_pairs={{0,2},{2,4},{4,6},{6,8},{8,10},{10,12},{12,14},{14,0},{1,15},{3,1}... | collective-permute-start | bytes 2359304 | tf_op jit(solution)/shard_map/ppermute | solution.py:26
  47.2 7.5 %collective-permute-start.7 = (bf16[64,4096]{1,0:T(8,128)(2,1)}, bf16[64,4096]{1,0:T(8,128)(2,1)}, u32[]{:S(2)}, u32[]{:S(2)}) collective-permute-start(bf16[64,4096]{1,0:T(8,128)(2,1)} %bitcast.118), channel_id=1, source_target_pairs={{0,1},{1,0},{2,3},{3,2},{4,5},{5,4},{6,7},{7,6},{8,9},{9,8},{10,11... | collective-permute-start | bytes 1572872 | tf_op jit(solution)/shard_map/ppermute | solution.py:31
  52.1 4.1 %collective-permute-start.8 = (bf16[64,4096]{1,0:T(8,128)(2,1)}, bf16[64,4096]{1,0:T(8,128)(2,1)}, u32[]{:S(2)}, u32[]{:S(2)}) collective-permute-start(bf16[64,4096]{1,0:T(8,128)(2,1)} %bitcast.120), channel_id=1, source_target_pairs={{0,1},{1,0},{2,3},{3,2},{4,5},{5,4},{6,7},{7,6},{8,9},{9,8},{10,11... | collective-permute-start | bytes 1572872 | tf_op jit(solution)/shard_map/ppermute | solution.py:31
  59.0 9.0 %copy-start.2 = (bf16[5,256,512]{2,1,0:T(8,128)(2,1)S(1)}, bf16[5,256,512]{2,1,0:T(8,128)(2,1)}, u32[]{:S(2)}) copy-start(bf16[5,256,512]{2,1,0:T(8,128)(2,1)} %shard_map.186) | copy-start | bytes 3932164
  60.3 27.7 %collective-permute-start.2 = (bf16[384,512]{1,0:T(8,128)(2,1)S(1)}, bf16[384,512]{1,0:T(8,128)(2,1)S(1)}, u32[]{:S(2)}, u32[]{:S(2)}) collective-permute-start(bf16[384,512]{1,0:T(8,128)(2,1)S(1)} %fusion.20), channel_id=1, source_target_pairs={{0,2},{2,4},{4,6},{6,8},{8,10},{10,12},{12,14},{14,0},{1,15},{3,1}... | collective-permute-start | bytes 1179656 | tf_op jit(solution)/shard_map/ppermute | solution.py:26
  65.2 3.6 %collective-permute-start.12 = (bf16[768,512]{1,0:T(8,128)(2,1)S(1)}, bf16[768,512]{1,0:T(8,128)(2,1)S(1)}, u32[]{:S(2)}, u32[]{:S(2)}) collective-permute-start(bf16[768,512]{1,0:T(8,128)(2,1)S(1)} %collective-permute-done.10), channel_id=1, source_target_pairs={{0,14},{2,0},{4,2},{6,4},{8,6},{10,8},{12,10},{14,12},{16,30},{18,... | collective-permute-start | bytes 2359304 | tf_op jit(solution)/shard_map/ppermute | solution.py:26
  65.9 3.3 %collective-permute-start.11 = (bf16[768,512]{1,0:T(8,128)(2,1)S(1)}, bf16[768,512]{1,0:T(8,128)(2,1)S(1)}, u32[]{:S(2)}, u32[]{:S(2)}) collective-permute-start(bf16[768,512]{1,0:T(8,128)(2,1)S(1)} %collective-permute-done.9), channel_id=1, source_target_pairs={{0,2},{2,4},{4,6},{6,8},{8,10},{10,12},{12,14},{14,0},{16,18},{18,... | collective-permute-start | bytes 2359304 | tf_op jit(solution)/shard_map/ppermute | solution.py:26
  69.6 23.7 %copy-start.6 = (f32[128,4]{0,1:T(4,128)S(1)}, f32[128,4]{0,1:T(4,128)}, u32[]{:S(2)}) copy-start(f32[128,4]{0,1:T(4,128)} %param.25) | copy-start | bytes 6148
  69.7 28.6 %copy-start.3 = (bf16[4,384,512]{2,1,0:T(8,128)(2,1)S(1)}, bf16[4,384,512]{2,1,0:T(8,128)(2,1)}, u32[]{:S(2)}) copy-start(bf16[4,384,512]{2,1,0:T(8,128)(2,1)} %get-tuple-element.6) | copy-start | bytes 4718596
  69.7 32.7 %collective-permute-start.13 = (f32[256,768]{1,0:T(8,128)S(1)}, f32[256,768]{1,0:T(8,128)}, u32[]{:S(2)}, u32[]{:S(2)}) collective-permute-start(f32[256,768]{1,0:T(8,128)S(1)} %fusion.11), channel_id=1, source_target_pairs={{0,1},{1,0},{2,3},{3,2},{4,5},{5,4},{6,7},{7,6},{8,9},{9,8},{10,11... | collective-permute-start | bytes 2359304 | tf_op jit(solution)/shard_map/ppermute | solution.py:31
  89.3 8.9 %collective-permute-start.3 = (bf16[384,512]{1,0:T(8,128)(2,1)S(1)}, bf16[384,512]{1,0:T(8,128)(2,1)}, u32[]{:S(2)}, u32[]{:S(2)}) collective-permute-start(bf16[384,512]{1,0:T(8,128)(2,1)S(1)} %fusion.18), channel_id=1, source_target_pairs={{0,2},{2,4},{4,6},{6,8},{8,10},{10,12},{12,14},{14,0},{1,15},{3,1}... | collective-permute-start | bytes 1179656 | tf_op jit(solution)/shard_map/ppermute | solution.py:26
  91.3 34.7 %collective-permute-start.18 = (bf16[1024,256]{1,0:T(8,128)(2,1)}, bf16[1024,256]{1,0:T(8,128)(2,1)}, u32[]{:S(2)}, u32[]{:S(2)}) collective-permute-start(bf16[1024,256]{1,0:T(8,128)(2,1)} %bitcast.40), channel_id=1, source_target_pairs={{0,1},{1,0},{2,3},{3,2},{4,5},{5,4},{6,7},{7,6},{8,9},{9,8},{10,11... | collective-permute-start | bytes 1572872 | tf_op jit(solution)/shard_map/ppermute | solution.py:31
  99.5 57.3 %collective-permute-start.4 = (bf16[384,512]{1,0:T(8,128)(2,1)S(1)}, bf16[384,512]{1,0:T(8,128)(2,1)}, u32[]{:S(2)}, u32[]{:S(2)}) collective-permute-start(bf16[384,512]{1,0:T(8,128)(2,1)S(1)} %fusion.19), channel_id=1, source_target_pairs={{0,2},{2,4},{4,6},{6,8},{8,10},{10,12},{12,14},{14,0},{1,15},{3,1}... | collective-permute-start | bytes 1179656 | tf_op jit(solution)/shard_map/ppermute | solution.py:26
  103.8 23.2 %collective-permute-start.17 = (bf16[128,768]{1,0:T(8,128)(2,1)S(1)}, bf16[128,768]{1,0:T(8,128)(2,1)S(1)}, u32[]{:S(2)}, u32[]{:S(2)}) collective-permute-start(bf16[128,768]{1,0:T(8,128)(2,1)S(1)} %fusion.21), channel_id=1, source_target_pairs={{0,2},{2,4},{4,6},{6,8},{8,10},{10,12},{12,14},{14,0},{1,15},{3,1}... | collective-permute-start | bytes 589832 | tf_op jit(solution)/shard_map/ppermute | solution.py:26
  105.7 22.5 %collective-permute-start.16 = (bf16[128,768]{1,0:T(8,128)(2,1)S(1)}, bf16[128,768]{1,0:T(8,128)(2,1)S(1)}, u32[]{:S(2)}, u32[]{:S(2)}) collective-permute-start(bf16[128,768]{1,0:T(8,128)(2,1)S(1)} %fusion.21), channel_id=1, source_target_pairs={{0,4},{2,6},{4,8},{6,10},{8,12},{10,14},{12,0},{14,2},{1,13},{3,15... | collective-permute-start | bytes 589832 | tf_op jit(solution)/shard_map/ppermute | solution.py:26
  109.9 13.1 %collective-permute-start.14 = (bf16[64,768]{1,0:T(8,128)(2,1)S(1)}, bf16[64,768]{1,0:T(8,128)(2,1)S(1)}, u32[]{:S(2)}, u32[]{:S(2)}) collective-permute-start(bf16[64,768]{1,0:T(8,128)(2,1)S(1)} %slice_select_fusion), channel_id=1, source_target_pairs={{0,8},{2,10},{4,12},{6,14},{8,0},{10,2},{12,4},{14,6},{1,9},{3,11}... | collective-permute-start | bytes 294920 | tf_op jit(solution)/shard_map/ppermute | solution.py:26
  123.0 11.0 %collective-permute-start.15 = (bf16[128,768]{1,0:T(8,128)(2,1)S(1)}, bf16[128,768]{1,0:T(8,128)(2,1)S(1)}, u32[]{:S(2)}, u32[]{:S(2)}) collective-permute-start(bf16[128,768]{1,0:T(8,128)(2,1)S(1)} %fusion.21), channel_id=1, source_target_pairs={{0,6},{2,8},{4,10},{6,12},{8,14},{10,0},{12,2},{14,4},{1,11},{3,13... | collective-permute-start | bytes 589832 | tf_op jit(solution)/shard_map/ppermute | solution.py:26
  136.2 7.9 %collective-permute-start.19 = (bf16[768,256]{1,0:T(8,128)(2,1)S(1)}, bf16[768,256]{1,0:T(8,128)(2,1)S(1)}, u32[]{:S(2)}, u32[]{:S(2)}) collective-permute-start(bf16[768,256]{1,0:T(8,128)(2,1)S(1)} %fusion.14), channel_id=1, source_target_pairs={{0,1},{1,0},{2,3},{3,2},{4,5},{5,4},{6,7},{7,6},{8,9},{9,8},{10,11... | collective-permute-start | bytes 1179656 | tf_op jit(solution)/shard_map/ppermute | solution.py:31
  146.0 25.2 %all-to-all-start.1 = ((bf16[32,24,256]{2,1,0:T(8,128)(2,1)}), bf16[32,24,256]{2,1,0:T(8,128)(2,1)S(1)}, u32[]{:S(2)}, u32[]{:S(2)}) async-start(bf16[32,24,256]{2,1,0:T(8,128)(2,1)} %bitcast.41), calls=%async_computation.1 | async-start | bytes 786432 | tf_op jit(solution)/shard_map/all_to_all | solution.py:173
  158.2 8.5 %collective-permute-start.5 = (bf16[384,256]{1,0:T(8,128)(2,1)S(1)}, bf16[384,256]{1,0:T(8,128)(2,1)S(1)}, u32[]{:S(2)}, u32[]{:S(2)}) collective-permute-start(bf16[384,256]{1,0:T(8,128)(2,1)S(1)} %get-tuple-element.8), channel_id=1, source_target_pairs={{0,3},{2,5},{4,7},{6,9},{8,11},{10,13},{12,15},{14,1},{1,0},{3,2},... | collective-permute-start | bytes 589832 | tf_op jit(solution)/shard_map/ppermute | solution.py:26
  160.4 6.3 %collective-permute-start.6 = (bf16[384,256]{1,0:T(8,128)(2,1)S(1)}, bf16[384,256]{1,0:T(8,128)(2,1)S(1)}, u32[]{:S(2)}, u32[]{:S(2)}) collective-permute-start(bf16[384,256]{1,0:T(8,128)(2,1)S(1)} %get-tuple-element.9), channel_id=1, source_target_pairs={{0,2},{2,4},{4,6},{6,8},{8,10},{10,12},{12,14},{14,0},{16,18},{18,... | collective-permute-start | bytes 589832 | tf_op jit(solution)/shard_map/ppermute | solution.py:26
  (1 other events, 2.5 us)

commit v8 on v7

--- a/solution.py
+++ b/solution.py
@@ -73,6 +73,20 @@
             at = lanes(index[side, j], width)
             to[j, :rows] = jnp.dot(group[...], proj[:, at], preferred_element_type=f32).astype(bf16)
             to[j, rows:] = jnp.dot(hidden[...], down[:, at], preferred_element_type=f32).astype(bf16)
+
+
+def down_kernel(index, *refs):
+    *pieces, own, partner, own_sum, partner_sum = refs
+    unit = pieces[0].shape[0]
+    for weight, to in ((partner, partner_sum), (own, own_sum)):
+        total = None
+        for i, piece in enumerate(pieces):
+            rows = pl.ds(pl.multiple_of(index[i] * unit, unit), piece.shape[0])
+            product = lax.dot_general(
+                piece[...], weight[rows, :], (((0,), (0,)), ((), ())), preferred_element_type=f32
+            )
+            total = product if total is None else total + product
+        to[...] = total.astype(to.dtype)
 
 
 def after(x, event):
@@ -177,8 +191,8 @@
     pool_input = after(pool_input, outgoing)
     upward = jnp.array([4, 3, 2, 1], jnp.int32)
     downward = jnp.array([5, 6, 7, 0], jnp.int32)
-    kept_ids = jnp.where(core == 0, upward, downward)
-    sent_ids = jnp.where(core == 0, downward, upward)
+    kept_ids = jnp.where(core == 0, downward, upward)
+    sent_ids = jnp.where(core == 0, upward, downward)
     index = (y + jnp.stack([kept_ids, sent_ids])) % y_size
     offsets = jnp.where(core == 0, jnp.array([0, -1, 1, -2, 2], jnp.int32), jnp.array([0, 1, -1, 0, 0], jnp.int32))
     near_index = (home + y_size + offsets) % y_size
@@ -211,7 +225,7 @@
         return (part(j) + ring.astype(f32)).astype(bf16)
 
     def ring_step(x):
-        return sent(x.astype(bf16), {0: (1, 0), 1: (-1, 1)})
+        return sent(x.astype(bf16), {0: (-1, 0), 1: (1, 1)})
 
     one = sent(arrived, {0: (1, 0), 1: (-1, 1)})
     other = sent(arrived, {0: (-1, 0), 1: (1, 1)})
@@ -227,24 +241,20 @@
     hidden = (jax.nn.silu(full[:chip_units]) * full[chip_units:]).astype(bf16)
 
     half = jnp.where(core == 0, hidden[:units], hidden[units:])
-    pieces = [(half, 0, units)]
-    for distance in range(y_size // 2, 0, -1):
-        block = half if 2 * distance == y_size else hidden
+    side = jnp.where(core == 0, -1, 1)
+    pieces = [half]
+    begins = [2 * y + core]
+    for distance in range(1, y_size // 2 + 1):
+        farthest = 2 * distance == y_size
         route = {0: (distance, 0), 1: (-distance, 1)}
-        pieces.append((sent(block, route), distance, block.shape[0]))
-    own_sum = partner_sum = 0.0
-    for h, distance, rows in pieces:
-        chip = (y + y_size + jnp.where(core == 0, -distance, distance)) % y_size
-        begin = chip * chip_units + (core * units if rows == units else 0)
-
-        def down_product(weight):
-            w = lax.dynamic_slice_in_dim(weight, begin, rows, 0)
-            return lax.dot_general(h, w, (((0,), (0,)), ((), ())), preferred_element_type=f32)
-
-        own_sum = own_sum + down_product(own_down)
-        partner_sum = partner_sum + down_product(partner_down)
+        pieces.append(sent(half if farthest else hidden, route))
+        begins.append(2 * ((y + y_size + side * distance) % y_size) + (core if farthest else 0))
+    sums = [jax.ShapeDtypeStruct((buffer_len, slice_width), kind) for kind in (f32, bf16)]
+    own_sum, partner_sum = local_kernel(
+        down_kernel, jnp.stack(begins).astype(jnp.int32), (*pieces, own_down, partner_down), sums
+    )
     ring = ring_step(ring_sum(2, ring))
-    expert_result = own_sum + to_partner(partner_sum.astype(bf16)).astype(f32)
+    expert_result = own_sum + to_partner(partner_sum).astype(f32)
     expert_result = expert_result.astype(bf16)
     returned = exchanged(expert_result)
     routed = lax.dot_general(combine, returned, (((0,), (0,)), ((), ())), preferred_element_type=f32)
@@ -252,9 +262,9 @@
     done = part(3) + ring.astype(f32)
     low = done[:, :slice_width]
     high = done[:, slice_width:]
-    cross = sent(jnp.where(core == 0, high, low).astype(bf16), {0: (1, 1), 1: (0, 0)})
-    straight = sent(low.astype(bf16), {0: (1, 0)})
-    total = cross.astype(f32) + straight.astype(f32) + jnp.where(core == 0, 0.0, high)
+    cross = sent(jnp.where(core == 0, high, low).astype(bf16), {0: (0, 1), 1: (1, 0)})
+    straight = sent(high.astype(bf16), {1: (1, 1)})
+    total = cross.astype(f32) + straight.astype(f32) + jnp.where(core == 0, low, 0.0)
     return (total[:row_count].astype(bf16), (routed + total[row_count:]).astype(bf16))
 
 

time: 174 us -> 166 us (0.954)
  the two profiles are of different devices: /device:TPU:1 before, /device:TPU:9 now
where the time goes in v8:
time: 166 us; the launch traced here: 164 us
  starting transfers between devices  90 us (54%)
  waiting for transfers between devices  38 us (23%)
  other arithmetic  10.4 us (6%)
  Pallas kernels  10.1 us (6%)
  matrix products  8.92 us (5%)
  local copies, waits for them, and re-layouts  5.59 us (3%)
    ppermute x13, starting transfers between devices, sent(): return lax.ppermute(x, 'tp', route)  35.5 us
    ppermute x6, starting transfers between devices, to_partner(): return lax.ppermute(x, 'tp', [(i, i ^ 1) for i in range(n)])  33.4 us
    ppermute x13, waiting for transfers between devices, sent(): return lax.ppermute(x, 'tp', route)  19.2 us
    all_to_all x2, waiting for transfers between devices, exchanged(): return lax.all_to_all(rows, 'ep', split_axis=0, concat_axis=0, tiled=True)  18.8 us
    all_to_all x2, starting transfers between devices, exchanged(): return lax.all_to_all(rows, 'ep', split_axis=0, concat_axis=0, tiled=True)  18 us
    pallas_call x3, Pallas kernels, local_kernel(): pl.pallas_call(body, in_specs=[smem] + [vmem] * len(operands), out_specs=...  10.1 us
    dot_general x5, matrix products, tdot(): lax.dot_general(a, b, (((1,), (1,)), ((), ())), preferred_element_type=f32)  4.07 us
  transfers between devices with their start and end apart: 22, of which 7 were waited for; matrix products, arithmetic and copies ran while one was open for 13% of the time, Pallas kernels for 6%

profile of v8, /device:TPU:9, one launch (start us, length us, event | category | flops | bytes accessed | tf_op | source)
XLA Modules:
  0.0 164.5 jit_solution(13448171633379931703)
XLA Ops:
  1.5 3.1 %collective-permute-start = (bf16[15,128]{1,0:T(8,128)(2,1)S(1)}, bf16[15,128]{1,0:T(8,128)(2,1)S(1)}, u32[]{:S(2)}, u32[]{:S(2)}) collective-permute-start(bf16[15,128]{1,0:T(8,128)(2,1)S(1)} %slice.140), channel_id=1, source_target_pairs={{0,16},{16,32},{32,48},{48,64},{64,80},{80,96},{96,112},{112,128},... | collective-permute-start | bytes 11528 | tf_op jit(solution)/shard_map/ppermute | solution.py:18
  5.6 1.5 convert_reduce_fusion
  7.9 1.3 convolution_convert_fusion
  9.3 12.7 %all-to-all-start = ((bf16[32,24,512]{2,1,0:T(8,128)(2,1)}), bf16[32,24,512]{2,1,0:T(8,128)(2,1)S(1)}, u32[]{:S(2)}, u32[]{:S(2)}) async-start(bf16[32,24,512]{2,1,0:T(8,128)(2,1)} %bitcast.34), calls=%async_computation | async-start | bytes 1572864 | tf_op jit(solution)/shard_map/all_to_all | solution.py:187
  22.0 3.1 %collective-permute-start.7 = (bf16[64,4096]{1,0:T(8,128)(2,1)}, bf16[64,4096]{1,0:T(8,128)(2,1)}, u32[]{:S(2)}, u32[]{:S(2)}) collective-permute-start(bf16[64,4096]{1,0:T(8,128)(2,1)} %bitcast.28.gate), channel_id=1, source_target_pairs={{0,1},{1,0},{2,3},{3,2},{4,5},{5,4},{6,7},{7,6},{8,9},{9,8},{10,11... | collective-permute-start | bytes 1572872 | tf_op jit(solution)/shard_map/ppermute | solution.py:31
  25.1 1.9 %collective-permute-start.8 = (bf16[64,4096]{1,0:T(8,128)(2,1)}, bf16[64,4096]{1,0:T(8,128)(2,1)}, u32[]{:S(2)}, u32[]{:S(2)}) collective-permute-start(bf16[64,4096]{1,0:T(8,128)(2,1)} %bitcast.30.up), channel_id=1, source_target_pairs={{0,1},{1,0},{2,3},{3,2},{4,5},{5,4},{6,7},{7,6},{8,9},{9,8},{10,11... | collective-permute-start | bytes 1572872 | tf_op jit(solution)/shard_map/ppermute | solution.py:31
  29.1 13.9 %all-to-all-done = bf16[32,24,512]{2,1,0:T(8,128)(2,1)S(1)} async-done(((bf16[32,24,512]{2,1,0:T(8,128)(2,1)}), bf16[32,24,512]{2,1,0:T(8,128)(2,1)S(1)}, u32[]{:S(2)}, u32[]{:S(2)}) %all-to-all-start) | async-done | bytes 786464 | tf_op jit(solution)/shard_map/all_to_all | solution.py:187
  43.1 3.2 %collective-permute-start.10 = (bf16[768,512]{1,0:T(8,128)(2,1)S(1)}, bf16[768,512]{1,0:T(8,128)(2,1)S(1)}, u32[]{:S(2)}, u32[]{:S(2)}) collective-permute-start(bf16[768,512]{1,0:T(8,128)(2,1)S(1)} %bitcast.97), channel_id=1, source_target_pairs={{0,14},{2,0},{4,2},{6,4},{8,6},{10,8},{12,10},{14,12},{1,3},{3,5},... | collective-permute-start | bytes 2359304 | tf_op jit(solution)/shard_map/ppermute | solution.py:26
  46.3 2.1 %collective-permute-start.9 = (bf16[768,512]{1,0:T(8,128)(2,1)S(1)}, bf16[768,512]{1,0:T(8,128)(2,1)}, u32[]{:S(2)}, u32[]{:S(2)}) collective-permute-start(bf16[768,512]{1,0:T(8,128)(2,1)S(1)} %bitcast.98), channel_id=1, source_target_pairs={{0,2},{2,4},{4,6},{6,8},{8,10},{10,12},{12,14},{14,0},{1,15},{3,1}... | collective-permute-start | bytes 2359304 | tf_op jit(solution)/shard_map/ppermute | solution.py:26
  50.8 3.6 %shard_map.185 = (bf16[4,384,512]{2,1,0:T(8,128)(2,1)}, bf16[4,384,512]{2,1,0:T(8,128)(2,1)}) custom-call(s32[2,4]{1,0:T(2,128)} %and_select_fusion.3.index, bf16[256,128]{1,0:T(8,128)(2,1)} %fusion.8.group, bf16[128,32]{1,0:T(8,128)(2,1)} %fusion.9.hidden, bf16[128,4096]{1,0:T(8,128)(2,1)} %proj.1, bf16[32,4096]{1,0:T(8,128)(2,1)} %down.1), custom_call_target="tpu_custom_call" | custom-call | tf_op jit(solution)/shard_map/pallas_call | solution.py:46
  54.4 5.3 %collective-permute-start.1 = (bf16[4,384,512]{2,1,0:T(8,128)(2,1)}, bf16[4,384,512]{2,1,0:T(8,128)(2,1)}, u32[]{:S(2)}, u32[]{:S(2)}) collective-permute-start(bf16[4,384,512]{2,1,0:T(8,128)(2,1)} %get-tuple-element.9), channel_id=1, source_target_pairs={{0,1},{1,0},{2,3},{3,2},{4,5},{5,4},{6,7},{7,6},{8,9},{9,8},{10,11... | collective-permute-start | bytes 4718600 | tf_op jit(solution)/shard_map/ppermute | solution.py:31
  60.4 2.7 %shard_map.186 = bf16[5,256,512]{2,1,0:T(8,128)(2,1)} custom-call(s32[6]{0:T(128)} %pad_add_fusion.index, bf16[64,4096]{1,0:T(8,128)(2,1)} %bitcast.28.gate, bf16[64,4096]{1,0:T(8,128)(2,1)} %bitcast.30.up, bf16[64,4096]{1,0:T(8,128)(2,1)} %collective-permute-done.7.partner_gate, bf16[64,4096]{1,0:T(8,128)(2,1)} %collective-permute-done.8.partner_up), custom_call_target="tpu_custom_call" | custom-call | tf_op jit(solution)/shard_map/pallas_call | solution.py:46
  63.9 3.7 %collective-permute-done.9 = bf16[768,512]{1,0:T(8,128)(2,1)} collective-permute-done((bf16[768,512]{1,0:T(8,128)(2,1)S(1)}, bf16[768,512]{1,0:T(8,128)(2,1)}, u32[]{:S(2)}, u32[]{:S(2)}) %collective-permute-start.9) | collective-permute-done | bytes 786464 | tf_op jit(solution)/shard_map/ppermute | solution.py:26
  69.7 1.5 fusion.16
  72.5 15.8 %collective-permute-start.13 = (f32[256,768]{1,0:T(8,128)S(1)}, f32[256,768]{1,0:T(8,128)S(1)}, u32[]{:S(2)}, u32[]{:S(2)}) collective-permute-start(f32[256,768]{1,0:T(8,128)S(1)} %fusion.5), channel_id=1, source_target_pairs={{0,1},{1,0},{2,3},{3,2},{4,5},{5,4},{6,7},{7,6},{8,9},{9,8},{10,11... | collective-permute-start | bytes 2359304 | tf_op jit(solution)/shard_map/ppermute | solution.py:31
  89.4 1.9 %collective-permute-start.2 = (bf16[384,512]{1,0:T(8,128)(2,1)S(1)}, bf16[384,512]{1,0:T(8,128)(2,1)S(1)}, u32[]{:S(2)}, u32[]{:S(2)}) collective-permute-start(bf16[384,512]{1,0:T(8,128)(2,1)S(1)} %fusion.12), channel_id=1, source_target_pairs={{0,14},{2,0},{4,2},{6,4},{8,6},{10,8},{12,10},{14,12},{1,3},{3,5},... | collective-permute-start | bytes 1179656 | tf_op jit(solution)/shard_map/ppermute | solution.py:26
  91.4 5.1 %collective-permute-start.18 = (bf16[1024,256]{1,0:T(8,128)(2,1)S(1)}, bf16[1024,256]{1,0:T(8,128)(2,1)S(1)}, u32[]{:S(2)}, u32[]{:S(2)}) collective-permute-start(bf16[1024,256]{1,0:T(8,128)(2,1)S(1)} %bitcast.101), channel_id=1, source_target_pairs={{0,1},{1,0},{2,3},{3,2},{4,5},{5,4},{6,7},{7,6},{8,9},{9,8},{10,11... | collective-permute-start | bytes 1572872 | tf_op jit(solution)/shard_map/ppermute | solution.py:31
  96.5 2.9 %collective-permute-done.2 = bf16[384,512]{1,0:T(8,128)(2,1)S(1)} collective-permute-done((bf16[384,512]{1,0:T(8,128)(2,1)S(1)}, bf16[384,512]{1,0:T(8,128)(2,1)S(1)}, u32[]{:S(2)}, u32[]{:S(2)}) %collective-permute-start.2) | collective-permute-done | bytes 393248 | tf_op jit(solution)/shard_map/ppermute | solution.py:26
  99.4 1.9 %fusion.10 = bf16[384,512]{1,0:T(8,128)(2,1)} fusion(bf16[384,512]{1,0:T(8,128)(2,1)S(1)} %collective-permute-done.2, bf16[4,384,512]{2,1,0:T(8,128)(2,1)} %collective-permute-done.1, bf16[4,384,512]{2,1,0:T(8,128)(2,1)S(1)} %copy-done.3), kind=kLoop, calls=%fused_computation.34 | loop fusion | flops 1179648 | bytes 1572864 | tf_op jit(solution)/shard_map/convert_element_type | solution.py:225
  101.3 1.9 %collective-permute-start.3 = (bf16[384,512]{1,0:T(8,128)(2,1)}, bf16[384,512]{1,0:T(8,128)(2,1)}, u32[]{:S(2)}, u32[]{:S(2)}) collective-permute-start(bf16[384,512]{1,0:T(8,128)(2,1)} %fusion.10), channel_id=1, source_target_pairs={{0,14},{2,0},{4,2},{6,4},{8,6},{10,8},{12,10},{14,12},{1,3},{3,5},... | collective-permute-start | bytes 1179656 | tf_op jit(solution)/shard_map/ppermute | solution.py:26
  103.5 4.6 %collective-permute-start.14 = (bf16[128,768]{1,0:T(8,128)(2,1)S(1)}, bf16[128,768]{1,0:T(8,128)(2,1)S(1)}, u32[]{:S(2)}, u32[]{:S(2)}) collective-permute-start(bf16[128,768]{1,0:T(8,128)(2,1)S(1)} %fusion.13), channel_id=1, source_target_pairs={{0,2},{2,4},{4,6},{6,8},{8,10},{10,12},{12,14},{14,0},{1,15},{3,1}... | collective-permute-start | bytes 589832 | tf_op jit(solution)/shard_map/ppermute | solution.py:26
  108.0 4.3 %collective-permute-start.15 = (bf16[128,768]{1,0:T(8,128)(2,1)S(1)}, bf16[128,768]{1,0:T(8,128)(2,1)S(1)}, u32[]{:S(2)}, u32[]{:S(2)}) collective-permute-start(bf16[128,768]{1,0:T(8,128)(2,1)S(1)} %fusion.13), channel_id=1, source_target_pairs={{0,4},{2,6},{4,8},{6,10},{8,12},{10,14},{12,0},{14,2},{1,13},{3,15... | collective-permute-start | bytes 589832 | tf_op jit(solution)/shard_map/ppermute | solution.py:26
  112.4 5.0 %collective-permute-start.16 = (bf16[128,768]{1,0:T(8,128)(2,1)S(1)}, bf16[128,768]{1,0:T(8,128)(2,1)}, u32[]{:S(2)}, u32[]{:S(2)}) collective-permute-start(bf16[128,768]{1,0:T(8,128)(2,1)S(1)} %fusion.13), channel_id=1, source_target_pairs={{0,6},{2,8},{4,10},{6,12},{8,14},{10,0},{12,2},{14,4},{1,11},{3,13... | collective-permute-start | bytes 589832 | tf_op jit(solution)/shard_map/ppermute | solution.py:26
  118.2 4.5 %collective-permute-start.17 = (bf16[64,768]{1,0:T(8,128)(2,1)S(1)}, bf16[64,768]{1,0:T(8,128)(2,1)S(1)}, u32[]{:S(2)}, u32[]{:S(2)}) collective-permute-start(bf16[64,768]{1,0:T(8,128)(2,1)S(1)} %slice_select_fusion.refs_0_), channel_id=1, source_target_pairs={{0,8},{2,10},{4,12},{6,14},{8,0},{10,2},{12,4},{14,6},{1,9},{3,11}... | collective-permute-start | bytes 294920 | tf_op jit(solution)/shard_map/ppermute | solution.py:26
  123.4 7.9 %collective-permute-done.17.refs_4_ = bf16[64,768]{1,0:T(8,128)(2,1)S(1)} collective-permute-done((bf16[64,768]{1,0:T(8,128)(2,1)S(1)}, bf16[64,768]{1,0:T(8,128)(2,1)S(1)}, u32[]{:S(2)}, u32[]{:S(2)}) %collective-permute-start.17) | collective-permute-done | bytes 98336 | tf_op jit(solution)/shard_map/ppermute | solution.py:26
  132.1 3.8 %shard_map.187 = (f32[768,256]{1,0:T(8,128)}, bf16[768,256]{1,0:T(8,128)(2,1)}) custom-call(s32[5]{0:T(128)} %stack.35.index, bf16[64,768]{1,0:T(8,128)(2,1)} %copy-done.7, bf16[128,768]{1,0:T(8,128)(2,1)} %copy-done.9, bf16[128,768]{1,0:T(8,128)(2,1)} %copy-done.10, bf16[128,768]{1,0:T(8,128)(2,1)} %collective-permute-done.16.refs_3_, ...), custom_call_target="tpu_custom_call" | custom-call | tf_op jit(solution)/shard_map/pallas_call | solution.py:46
  136.0 2.0 %collective-permute-start.19 = (bf16[768,256]{1,0:T(8,128)(2,1)}, bf16[768,256]{1,0:T(8,128)(2,1)S(1)}, u32[]{:S(2)}, u32[]{:S(2)}) collective-permute-start(bf16[768,256]{1,0:T(8,128)(2,1)} %get-tuple-element.11), channel_id=1, source_target_pairs={{0,1},{1,0},{2,3},{3,2},{4,5},{5,4},{6,7},{7,6},{8,9},{9,8},{10,11... | collective-permute-start | bytes 1179656 | tf_op jit(solution)/shard_map/ppermute | solution.py:31
  139.3 3.8 %collective-permute-start.4 = (bf16[384,512]{1,0:T(8,128)(2,1)S(1)}, bf16[384,512]{1,0:T(8,128)(2,1)}, u32[]{:S(2)}, u32[]{:S(2)}) collective-permute-start(bf16[384,512]{1,0:T(8,128)(2,1)S(1)} %fusion.11), channel_id=1, source_target_pairs={{0,14},{2,0},{4,2},{6,4},{8,6},{10,8},{12,10},{14,12},{1,3},{3,5},... | collective-permute-start | bytes 1179656 | tf_op jit(solution)/shard_map/ppermute | solution.py:26
  144.0 5.2 %all-to-all-start.1 = ((bf16[32,24,256]{2,1,0:T(8,128)(2,1)}), bf16[32,24,256]{2,1,0:T(8,128)(2,1)S(1)}, u32[]{:S(2)}, u32[]{:S(2)}) async-start(bf16[32,24,256]{2,1,0:T(8,128)(2,1)} %bitcast.41), calls=%async_computation.1 | async-start | bytes 786432 | tf_op jit(solution)/shard_map/all_to_all | solution.py:187
  150.5 2.8 %collective-permute-start.6 = (bf16[384,256]{1,0:T(8,128)(2,1)S(1)}, bf16[384,256]{1,0:T(8,128)(2,1)S(1)}, u32[]{:S(2)}, u32[]{:S(2)}) collective-permute-start(bf16[384,256]{1,0:T(8,128)(2,1)S(1)} %get-tuple-element.13), channel_id=1, source_target_pairs={{1,3},{3,5},{5,7},{7,9},{9,11},{11,13},{13,15},{15,1},{17,19},{19,... | collective-permute-start | bytes 589832 | tf_op jit(solution)/shard_map/ppermute | solution.py:26
  153.4 3.9 %collective-permute-done.6 = bf16[384,256]{1,0:T(8,128)(2,1)S(1)} collective-permute-done((bf16[384,256]{1,0:T(8,128)(2,1)S(1)}, bf16[384,256]{1,0:T(8,128)(2,1)S(1)}, u32[]{:S(2)}, u32[]{:S(2)}) %collective-permute-start.6) | collective-permute-done | bytes 196640 | tf_op jit(solution)/shard_map/ppermute | solution.py:26
  158.8 4.8 %all-to-all-done.1 = bf16[32,24,256]{2,1,0:T(8,128)(2,1)S(1)} async-done(((bf16[32,24,256]{2,1,0:T(8,128)(2,1)}), bf16[32,24,256]{2,1,0:T(8,128)(2,1)S(1)}, u32[]{:S(2)}, u32[]{:S(2)}) %all-to-all-start.1) | async-done | bytes 393248 | tf_op jit(solution)/shard_map/all_to_all | solution.py:187
  (102 shorter events, 21.1 us)
Async XLA Ops:
  0.6 49.1 %copy-start = (bf16[16,128,128]{2,1,0:T(8,128)(2,1)S(1)}, bf16[16,128,128]{2,1,0:T(8,128)(2,1)}, u32[]{:S(2)}) copy-start(bf16[16,128,128]{2,1,0:T(8,128)(2,1)} %param.19) | copy-start | bytes 1572868
  1.5 48.3 %collective-permute-start = (bf16[15,128]{1,0:T(8,128)(2,1)S(1)}, bf16[15,128]{1,0:T(8,128)(2,1)S(1)}, u32[]{:S(2)}, u32[]{:S(2)}) collective-permute-start(bf16[15,128]{1,0:T(8,128)(2,1)S(1)} %slice.140), channel_id=1, source_target_pairs={{0,16},{16,32},{32,48},{48,64},{64,80},{80,96},{96,112},{112,128},... | collective-permute-start | bytes 11528 | tf_op jit(solution)/shard_map/ppermute | solution.py:18
  7.5 19.7 %copy-start.17 = (s32[4]{0:T(128)S(1)}, s32[4]{0:T(128)}, u32[]{:S(2)}) copy-start(s32[4]{0:T(128)} %constant.162.clone) | copy-start | bytes 52
  7.5 19.7 %copy-start.18 = (s32[4]{0:T(128)S(1)}, s32[4]{0:T(128)}, u32[]{:S(2)}) copy-start(s32[4]{0:T(128)} %constant.161.clone) | copy-start | bytes 52
  9.2 18.4 %copy-start.8 = (bf16[4096,32]{0,1:T(8,128)(2,1)S(1)}, bf16[4096,32]{0,1:T(8,128)(2,1)}, u32[]{:S(2)}) copy-start(bf16[4096,32]{0,1:T(8,128)(2,1)} %param.29) | copy-start | bytes 786436
  9.3 33.8 %all-to-all-start = ((bf16[32,24,512]{2,1,0:T(8,128)(2,1)}), bf16[32,24,512]{2,1,0:T(8,128)(2,1)S(1)}, u32[]{:S(2)}, u32[]{:S(2)}) async-start(bf16[32,24,512]{2,1,0:T(8,128)(2,1)} %bitcast.34), calls=%async_computation | async-start | bytes 1572864 | tf_op jit(solution)/shard_map/all_to_all | solution.py:187
  22.0 38.4 %collective-permute-start.7 = (bf16[64,4096]{1,0:T(8,128)(2,1)}, bf16[64,4096]{1,0:T(8,128)(2,1)}, u32[]{:S(2)}, u32[]{:S(2)}) collective-permute-start(bf16[64,4096]{1,0:T(8,128)(2,1)} %bitcast.28.gate), channel_id=1, source_target_pairs={{0,1},{1,0},{2,3},{3,2},{4,5},{5,4},{6,7},{7,6},{8,9},{9,8},{10,11... | collective-permute-start | bytes 1572872 | tf_op jit(solution)/shard_map/ppermute | solution.py:31
  25.1 35.2 %collective-permute-start.8 = (bf16[64,4096]{1,0:T(8,128)(2,1)}, bf16[64,4096]{1,0:T(8,128)(2,1)}, u32[]{:S(2)}, u32[]{:S(2)}) collective-permute-start(bf16[64,4096]{1,0:T(8,128)(2,1)} %bitcast.30.up), channel_id=1, source_target_pairs={{0,1},{1,0},{2,3},{3,2},{4,5},{5,4},{6,7},{7,6},{8,9},{9,8},{10,11... | collective-permute-start | bytes 1572872 | tf_op jit(solution)/shard_map/ppermute | solution.py:31
  27.6 21.4 %copy-start.12 = (bf16[256,128]{1,0:T(8,128)(2,1)S(1)}, bf16[256,128]{1,0:T(8,128)(2,1)}, u32[]{:S(2)}) copy-start(bf16[256,128]{1,0:T(8,128)(2,1)} %param.18) | copy-start | bytes 196612
  43.1 20.0 %collective-permute-start.10 = (bf16[768,512]{1,0:T(8,128)(2,1)S(1)}, bf16[768,512]{1,0:T(8,128)(2,1)S(1)}, u32[]{:S(2)}, u32[]{:S(2)}) collective-permute-start(bf16[768,512]{1,0:T(8,128)(2,1)S(1)} %bitcast.97), channel_id=1, source_target_pairs={{0,14},{2,0},{4,2},{6,4},{8,6},{10,8},{12,10},{14,12},{1,3},{3,5},... | collective-permute-start | bytes 2359304 | tf_op jit(solution)/shard_map/ppermute | solution.py:26
  46.3 21.3 %collective-permute-start.9 = (bf16[768,512]{1,0:T(8,128)(2,1)S(1)}, bf16[768,512]{1,0:T(8,128)(2,1)}, u32[]{:S(2)}, u32[]{:S(2)}) collective-permute-start(bf16[768,512]{1,0:T(8,128)(2,1)S(1)} %bitcast.98), channel_id=1, source_target_pairs={{0,2},{2,4},{4,6},{6,8},{8,10},{10,12},{12,14},{14,0},{1,15},{3,1}... | collective-permute-start | bytes 2359304 | tf_op jit(solution)/shard_map/ppermute | solution.py:26
  49.8 9.9 %copy-start.15 = (s32[5]{0:T(128)S(1)}, s32[5]{0:T(128)}, u32[]{:S(2)}) copy-start(s32[5]{0:T(128)} %constant.163.clone) | copy-start | bytes 64
  54.4 33.9 %collective-permute-start.1 = (bf16[4,384,512]{2,1,0:T(8,128)(2,1)}, bf16[4,384,512]{2,1,0:T(8,128)(2,1)}, u32[]{:S(2)}, u32[]{:S(2)}) collective-permute-start(bf16[4,384,512]{2,1,0:T(8,128)(2,1)} %get-tuple-element.9), channel_id=1, source_target_pairs={{0,1},{1,0},{2,3},{3,2},{4,5},{5,4},{6,7},{7,6},{8,9},{9,8},{10,11... | collective-permute-start | bytes 4718600 | tf_op jit(solution)/shard_map/ppermute | solution.py:31
  63.1 8.5 %collective-permute-start.12 = (bf16[768,512]{1,0:T(8,128)(2,1)S(1)}, bf16[768,512]{1,0:T(8,128)(2,1)S(1)}, u32[]{:S(2)}, u32[]{:S(2)}) collective-permute-start(bf16[768,512]{1,0:T(8,128)(2,1)S(1)} %collective-permute-done.10), channel_id=1, source_target_pairs={{0,14},{2,0},{4,2},{6,4},{8,6},{10,8},{12,10},{14,12},{16,30},{18,... | collective-permute-start | bytes 2359304 | tf_op jit(solution)/shard_map/ppermute | solution.py:26
  67.6 4.5 %collective-permute-start.11 = (bf16[768,512]{1,0:T(8,128)(2,1)}, bf16[768,512]{1,0:T(8,128)(2,1)S(1)}, u32[]{:S(2)}, u32[]{:S(2)}) collective-permute-start(bf16[768,512]{1,0:T(8,128)(2,1)} %collective-permute-done.9), channel_id=1, source_target_pairs={{0,2},{2,4},{4,6},{6,8},{8,10},{10,12},{12,14},{14,0},{16,18},{18,... | collective-permute-start | bytes 2359304 | tf_op jit(solution)/shard_map/ppermute | solution.py:26
  72.1 16.3 %copy-start.3 = (bf16[4,384,512]{2,1,0:T(8,128)(2,1)S(1)}, bf16[4,384,512]{2,1,0:T(8,128)(2,1)}, u32[]{:S(2)}) copy-start(bf16[4,384,512]{2,1,0:T(8,128)(2,1)} %get-tuple-element.8) | copy-start | bytes 4718596
  72.1 19.3 %copy-start.5 = (bf16[1,1024,256]{2,1,0:T(8,128)(2,1)S(1)}, bf16[1,1024,256]{2,1,0:T(8,128)(2,1)}, u32[]{:S(2)}) copy-start(bf16[1,1024,256]{2,1,0:T(8,128)(2,1)} %param.28) | copy-start | bytes 1572868
  72.5 30.7 %collective-permute-start.13 = (f32[256,768]{1,0:T(8,128)S(1)}, f32[256,768]{1,0:T(8,128)S(1)}, u32[]{:S(2)}, u32[]{:S(2)}) collective-permute-start(f32[256,768]{1,0:T(8,128)S(1)} %fusion.5), channel_id=1, source_target_pairs={{0,1},{1,0},{2,3},{3,2},{4,5},{5,4},{6,7},{7,6},{8,9},{9,8},{10,11... | collective-permute-start | bytes 2359304 | tf_op jit(solution)/shard_map/ppermute | solution.py:31
  89.4 10.0 %collective-permute-start.2 = (bf16[384,512]{1,0:T(8,128)(2,1)S(1)}, bf16[384,512]{1,0:T(8,128)(2,1)S(1)}, u32[]{:S(2)}, u32[]{:S(2)}) collective-permute-start(bf16[384,512]{1,0:T(8,128)(2,1)S(1)} %fusion.12), channel_id=1, source_target_pairs={{0,14},{2,0},{4,2},{6,4},{8,6},{10,8},{12,10},{14,12},{1,3},{3,5},... | collective-permute-start | bytes 1179656 | tf_op jit(solution)/shard_map/ppermute | solution.py:26
  91.4 26.0 %collective-permute-start.18 = (bf16[1024,256]{1,0:T(8,128)(2,1)S(1)}, bf16[1024,256]{1,0:T(8,128)(2,1)S(1)}, u32[]{:S(2)}, u32[]{:S(2)}) collective-permute-start(bf16[1024,256]{1,0:T(8,128)(2,1)S(1)} %bitcast.101), channel_id=1, source_target_pairs={{0,1},{1,0},{2,3},{3,2},{4,5},{5,4},{6,7},{7,6},{8,9},{9,8},{10,11... | collective-permute-start | bytes 1572872 | tf_op jit(solution)/shard_map/ppermute | solution.py:31
  101.3 36.7 %collective-permute-start.3 = (bf16[384,512]{1,0:T(8,128)(2,1)}, bf16[384,512]{1,0:T(8,128)(2,1)}, u32[]{:S(2)}, u32[]{:S(2)}) collective-permute-start(bf16[384,512]{1,0:T(8,128)(2,1)} %fusion.10), channel_id=1, source_target_pairs={{0,14},{2,0},{4,2},{6,4},{8,6},{10,8},{12,10},{14,12},{1,3},{3,5},... | collective-permute-start | bytes 1179656 | tf_op jit(solution)/shard_map/ppermute | solution.py:26
  103.5 27.9 %collective-permute-start.14 = (bf16[128,768]{1,0:T(8,128)(2,1)S(1)}, bf16[128,768]{1,0:T(8,128)(2,1)S(1)}, u32[]{:S(2)}, u32[]{:S(2)}) collective-permute-start(bf16[128,768]{1,0:T(8,128)(2,1)S(1)} %fusion.13), channel_id=1, source_target_pairs={{0,2},{2,4},{4,6},{6,8},{8,10},{10,12},{12,14},{14,0},{1,15},{3,1}... | collective-permute-start | bytes 589832 | tf_op jit(solution)/shard_map/ppermute | solution.py:26
  108.0 23.3 %collective-permute-start.15 = (bf16[128,768]{1,0:T(8,128)(2,1)S(1)}, bf16[128,768]{1,0:T(8,128)(2,1)S(1)}, u32[]{:S(2)}, u32[]{:S(2)}) collective-permute-start(bf16[128,768]{1,0:T(8,128)(2,1)S(1)} %fusion.13), channel_id=1, source_target_pairs={{0,4},{2,6},{4,8},{6,10},{8,12},{10,14},{12,0},{14,2},{1,13},{3,15... | collective-permute-start | bytes 589832 | tf_op jit(solution)/shard_map/ppermute | solution.py:26
  112.4 19.0 %collective-permute-start.16 = (bf16[128,768]{1,0:T(8,128)(2,1)S(1)}, bf16[128,768]{1,0:T(8,128)(2,1)}, u32[]{:S(2)}, u32[]{:S(2)}) collective-permute-start(bf16[128,768]{1,0:T(8,128)(2,1)S(1)} %fusion.13), channel_id=1, source_target_pairs={{0,6},{2,8},{4,10},{6,12},{8,14},{10,0},{12,2},{14,4},{1,11},{3,13... | collective-permute-start | bytes 589832 | tf_op jit(solution)/shard_map/ppermute | solution.py:26
  117.4 14.0 %copy-start.7 = (bf16[64,768]{1,0:T(8,128)(2,1)}, bf16[64,768]{1,0:T(8,128)(2,1)S(1)}, u32[]{:S(2)}) copy-start(bf16[64,768]{1,0:T(8,128)(2,1)S(1)} %slice_select_fusion.refs_0_) | copy-start | bytes 294916
  118.2 13.1 %collective-permute-start.17 = (bf16[64,768]{1,0:T(8,128)(2,1)S(1)}, bf16[64,768]{1,0:T(8,128)(2,1)S(1)}, u32[]{:S(2)}, u32[]{:S(2)}) collective-permute-start(bf16[64,768]{1,0:T(8,128)(2,1)S(1)} %slice_select_fusion.refs_0_), channel_id=1, source_target_pairs={{0,8},{2,10},{4,12},{6,14},{8,0},{10,2},{12,4},{14,6},{1,9},{3,11}... | collective-permute-start | bytes 294920 | tf_op jit(solution)/shard_map/ppermute | solution.py:26
  123.4 19.7 %copy-start.14 = (f32[128,4]{0,1:T(4,128)S(1)}, f32[128,4]{0,1:T(4,128)}, u32[]{:S(2)}) copy-start(f32[128,4]{0,1:T(4,128)} %param.25) | copy-start | bytes 6148
  136.0 7.1 %collective-permute-start.19 = (bf16[768,256]{1,0:T(8,128)(2,1)}, bf16[768,256]{1,0:T(8,128)(2,1)S(1)}, u32[]{:S(2)}, u32[]{:S(2)}) collective-permute-start(bf16[768,256]{1,0:T(8,128)(2,1)} %get-tuple-element.11), channel_id=1, source_target_pairs={{0,1},{1,0},{2,3},{3,2},{4,5},{5,4},{6,7},{7,6},{8,9},{9,8},{10,11... | collective-permute-start | bytes 1179656 | tf_op jit(solution)/shard_map/ppermute | solution.py:31
  139.3 9.9 %collective-permute-start.4 = (bf16[384,512]{1,0:T(8,128)(2,1)S(1)}, bf16[384,512]{1,0:T(8,128)(2,1)}, u32[]{:S(2)}, u32[]{:S(2)}) collective-permute-start(bf16[384,512]{1,0:T(8,128)(2,1)S(1)} %fusion.11), channel_id=1, source_target_pairs={{0,14},{2,0},{4,2},{6,4},{8,6},{10,8},{12,10},{14,12},{1,3},{3,5},... | collective-permute-start | bytes 1179656 | tf_op jit(solution)/shard_map/ppermute | solution.py:26
  144.0 19.6 %all-to-all-start.1 = ((bf16[32,24,256]{2,1,0:T(8,128)(2,1)}), bf16[32,24,256]{2,1,0:T(8,128)(2,1)S(1)}, u32[]{:S(2)}, u32[]{:S(2)}) async-start(bf16[32,24,256]{2,1,0:T(8,128)(2,1)} %bitcast.41), calls=%async_computation.1 | async-start | bytes 786432 | tf_op jit(solution)/shard_map/all_to_all | solution.py:187
  150.5 6.7 %collective-permute-start.6 = (bf16[384,256]{1,0:T(8,128)(2,1)S(1)}, bf16[384,256]{1,0:T(8,128)(2,1)S(1)}, u32[]{:S(2)}, u32[]{:S(2)}) collective-permute-start(bf16[384,256]{1,0:T(8,128)(2,1)S(1)} %get-tuple-element.13), channel_id=1, source_target_pairs={{1,3},{3,5},{5,7},{7,9},{9,11},{11,13},{13,15},{15,1},{17,19},{19,... | collective-permute-start | bytes 589832 | tf_op jit(solution)/shard_map/ppermute | solution.py:26
  153.3 4.7 %collective-permute-start.5 = (bf16[384,256]{1,0:T(8,128)(2,1)S(1)}, bf16[384,256]{1,0:T(8,128)(2,1)S(1)}, u32[]{:S(2)}, u32[]{:S(2)}) collective-permute-start(bf16[384,256]{1,0:T(8,128)(2,1)S(1)} %get-tuple-element.12), channel_id=1, source_target_pairs={{0,1},{2,3},{4,5},{6,7},{8,9},{10,11},{12,13},{14,15},{1,2},{3,4},... | collective-permute-start | bytes 589832 | tf_op jit(solution)/shard_map/ppermute | solution.py:26
  (10 other events, 41.1 us)

commit v9 on v8

--- a/solution.py
+++ b/solution.py
@@ -75,18 +75,30 @@
             to[j, rows:] = jnp.dot(hidden[...], down[:, at], preferred_element_type=f32).astype(bf16)
 
 
-def down_kernel(index, *refs):
-    *pieces, own, partner, own_sum, partner_sum = refs
-    unit = pieces[0].shape[0]
-    for weight, to in ((partner, partner_sum), (own, own_sum)):
-        total = None
-        for i, piece in enumerate(pieces):
-            rows = pl.ds(pl.multiple_of(index[i] * unit, unit), piece.shape[0])
-            product = lax.dot_general(
-                piece[...], weight[rows, :], (((0,), (0,)), ((), ())), preferred_element_type=f32
-            )
-            total = product if total is None else total + product
-        to[...] = total.astype(to.dtype)
+def down_rows_kernel(index, own, partner, blocks):
+    unit = blocks.shape[0] // 8
+    width = own.shape[1]
+    counts = (1, 2, 2, 2, 1)
+    to = 0
+    for i, count in enumerate(counts):
+        rows = pl.ds(pl.multiple_of(index[i] * unit, unit), count * unit)
+        for side, source in enumerate((own, partner)):
+            blocks[to : to + count * unit, side * width : (side + 1) * width] = source[rows, :]
+        to += count * unit
+
+
+def down_kernel(*refs):
+    *pieces, blocks, own_sum, partner_sum, joined = refs
+    to = 0
+    for piece in pieces:
+        count = piece.shape[0]
+        joined[to : to + count, :] = piece[...]
+        to += count
+    width = own_sum.shape[1]
+    for part, out in enumerate((own_sum, partner_sum)):
+        weight = blocks[:, part * width : (part + 1) * width]
+        product = lax.dot_general(joined[...], weight, (((0,), (0,)), ((), ())), preferred_element_type=f32)
+        out[...] = product.astype(out.dtype)
 
 
 def after(x, event):
@@ -155,6 +167,12 @@
 
     earlier_rows = halo(pool_input[row_count - reach_back :])
 
+    values = moe_input.astype(f32)
+    mean = jnp.mean(values, axis=1, keepdims=True)
+    routes = after(routes, mean)
+    centre = values - mean
+    rstd = lax.rsqrt(jnp.mean(centre * centre, axis=1, keepdims=True) + eps)
+
     routes_t = routes.T
     experts = jnp.arange(expert_count, dtype=jnp.int32)[:, None]
     named = jnp.zeros((expert_count, tok_count), f32)
@@ -171,10 +189,6 @@
     placing = match.astype(bf16).reshape(buffer_len, tok_count)
     combine = jnp.where(match, weight_t[:, None, :], 0.0).astype(bf16).reshape(buffer_len, tok_count)
 
-    values = moe_input.astype(f32)
-    mean = jnp.mean(values, axis=1, keepdims=True)
-    centre = values - mean
-    rstd = lax.rsqrt(jnp.mean(centre * centre, axis=1, keepdims=True) + eps)
 
     home = y + core * (y_size // 2)
     chip_width = 2 * slice_width
@@ -204,14 +218,14 @@
     shared_up_val = jnp.dot(normed, shared_up, preferred_element_type=f32)
     shared_hidden = (jax.nn.silu(shared_gate_val) * shared_up_val).astype(bf16)
 
-    shape = jax.ShapeDtypeStruct((y_size // 2, row_count + tok_count, chip_width), bf16)
+    shape = pltpu.VMEM((y_size // 2, row_count + tok_count, chip_width), bf16)
     kept, given = local_kernel(project_kernel, index, (group_out, shared_hidden, out_proj, shared_down), [shape, shape])
     from_partner = to_partner(given)
 
     gate_t = expert_gate[0].T
     up_t = expert_up[0].T
     units = gate_t.shape[0]
-    blocks = jax.ShapeDtypeStruct((5, 4 * units, chip_width), bf16)
+    blocks = pltpu.VMEM((5, 4 * units, chip_width), bf16)
     partner_gate = to_partner(gate_t)
     partner_up = to_partner(up_t)
     own_down = expert_down[0]
@@ -249,10 +263,17 @@
         route = {0: (distance, 0), 1: (-distance, 1)}
         pieces.append(sent(half if farthest else hidden, route))
         begins.append(2 * ((y + y_size + side * distance) % y_size) + (core if farthest else 0))
-    sums = [jax.ShapeDtypeStruct((buffer_len, slice_width), kind) for kind in (f32, bf16)]
-    own_sum, partner_sum = local_kernel(
-        down_kernel, jnp.stack(begins).astype(jnp.int32), (*pieces, own_down, partner_down), sums
-    )
+    blocks = pltpu.VMEM((y_size * units, 2 * slice_width), bf16)
+    rows_index = jnp.stack(begins).astype(jnp.int32)
+    down_blocks = local_kernel(down_rows_kernel, rows_index, (own_down, partner_down), blocks)
+    vmem = pl.BlockSpec(memory_space=pltpu.VMEM)
+    own_sum, partner_sum = pl.pallas_call(
+        down_kernel,
+        in_specs=[vmem] * (len(pieces) + 1),
+        out_specs=[vmem] * 2,
+        out_shape=[pltpu.VMEM((buffer_len, slice_width), kind) for kind in (f32, bf16)],
+        scratch_shapes=[pltpu.VMEM((y_size * units, buffer_len), bf16)],
+    )(*[pltpu.with_memory_space_constraint(a, pltpu.VMEM) for a in (*pieces, down_blocks)])
     ring = ring_step(ring_sum(2, ring))
     expert_result = own_sum + to_partner(partner_sum).astype(f32)
     expert_result = expert_result.astype(bf16)

time: 166 us -> 162 us (0.976)
  the two profiles are of different devices: /device:TPU:9 before, /device:TPU:1 now
where the time goes in v9:
time: 162 us; the launch traced here: 160 us
  starting transfers between devices  89.4 us (55%)
  waiting for transfers between devices  37.1 us (23%)
  matrix products  11 us (7%)
  other arithmetic  10.4 us (6%)
  Pallas kernels  6.52 us (4%)
  local copies, waits for them, and re-layouts  4.05 us (2%)
    ppermute x13, starting transfers between devices, sent(): return lax.ppermute(x, 'tp', route)  36.3 us
    ppermute x6, starting transfers between devices, to_partner(): return lax.ppermute(x, 'tp', [(i, i ^ 1) for i in range(n)])  31.7 us
    ppermute x13, waiting for transfers between devices, sent(): return lax.ppermute(x, 'tp', route)  20.3 us
    all_to_all x2, starting transfers between devices, exchanged(): return lax.all_to_all(rows, 'ep', split_axis=0, concat_axis=0, tiled=True)  17.5 us
    all_to_all x2, waiting for transfers between devices, exchanged(): return lax.all_to_all(rows, 'ep', split_axis=0, concat_axis=0, tiled=True)  16.8 us
    pallas_call x3, Pallas kernels, local_kernel(): pl.pallas_call(body, in_specs=[smem] + [vmem] * len(operands), out_specs=...  5.91 us
    dot_general x5, matrix products, tdot(): lax.dot_general(a, b, (((1,), (1,)), ((), ())), preferred_element_type=f32)  5.38 us
    ppermute x1, starting transfers between devices, halo(): return lax.ppermute(block, 'ep', [(i - 1, i) for i in devices if i > 0])  3.92 us
  transfers between devices with their start and end apart: 22, of which 7 were waited for; matrix products, arithmetic and copies ran while one was open for 15% of the time, Pallas kernels for 4%

profile of v9, /device:TPU:1, one launch (start us, length us, event | category | flops | bytes accessed | tf_op | source)
XLA Modules:
  0.0 159.9 jit_solution(1765833716973745104)
XLA Ops:
  1.5 3.9 %collective-permute-start = (bf16[15,128]{1,0:T(8,128)(2,1)S(1)}, bf16[15,128]{1,0:T(8,128)(2,1)S(1)}, u32[]{:S(2)}, u32[]{:S(2)}) collective-permute-start(bf16[15,128]{1,0:T(8,128)(2,1)S(1)} %slice.140), channel_id=1, source_target_pairs={{0,16},{16,32},{32,48},{48,64},{64,80},{80,96},{96,112},{112,128},... | collective-permute-start | bytes 11528 | tf_op jit(solution)/shard_map/ppermute | solution.py:18
  10.0 12.7 %all-to-all-start = ((bf16[32,24,512]{2,1,0:T(8,128)(2,1)}), bf16[32,24,512]{2,1,0:T(8,128)(2,1)}, u32[]{:S(2)}, u32[]{:S(2)}) async-start(bf16[32,24,512]{2,1,0:T(8,128)(2,1)} %bitcast.29), calls=%async_computation | async-start | bytes 1572864 | tf_op jit(solution)/shard_map/all_to_all | solution.py:201
  22.8 3.1 %collective-permute-start.7 = (bf16[64,4096]{1,0:T(8,128)(2,1)}, bf16[64,4096]{1,0:T(8,128)(2,1)}, u32[]{:S(2)}, u32[]{:S(2)}) collective-permute-start(bf16[64,4096]{1,0:T(8,128)(2,1)} %bitcast.23.gate), channel_id=1, source_target_pairs={{0,1},{1,0},{2,3},{3,2},{4,5},{5,4},{6,7},{7,6},{8,9},{9,8},{10,11... | collective-permute-start | bytes 1572872 | tf_op jit(solution)/shard_map/ppermute | solution.py:31
  25.9 1.9 %collective-permute-start.8 = (bf16[64,4096]{1,0:T(8,128)(2,1)}, bf16[64,4096]{1,0:T(8,128)(2,1)}, u32[]{:S(2)}, u32[]{:S(2)}) collective-permute-start(bf16[64,4096]{1,0:T(8,128)(2,1)} %bitcast.25.up), channel_id=1, source_target_pairs={{0,1},{1,0},{2,3},{3,2},{4,5},{5,4},{6,7},{7,6},{8,9},{9,8},{10,11... | collective-permute-start | bytes 1572872 | tf_op jit(solution)/shard_map/ppermute | solution.py:31
  29.9 13.9 %all-to-all-done = bf16[32,24,512]{2,1,0:T(8,128)(2,1)} async-done(((bf16[32,24,512]{2,1,0:T(8,128)(2,1)}), bf16[32,24,512]{2,1,0:T(8,128)(2,1)}, u32[]{:S(2)}, u32[]{:S(2)}) %all-to-all-start) | async-done | bytes 786464 | tf_op jit(solution)/shard_map/all_to_all | solution.py:201
  43.9 3.2 %collective-permute-start.10 = (bf16[768,512]{1,0:T(8,128)(2,1)}, bf16[768,512]{1,0:T(8,128)(2,1)}, u32[]{:S(2)}, u32[]{:S(2)}) collective-permute-start(bf16[768,512]{1,0:T(8,128)(2,1)} %bitcast.30), channel_id=1, source_target_pairs={{0,14},{2,0},{4,2},{6,4},{8,6},{10,8},{12,10},{14,12},{1,3},{3,5},... | collective-permute-start | bytes 2359304 | tf_op jit(solution)/shard_map/ppermute | solution.py:26
  47.1 3.8 %collective-permute-start.9 = (bf16[768,512]{1,0:T(8,128)(2,1)}, bf16[768,512]{1,0:T(8,128)(2,1)}, u32[]{:S(2)}, u32[]{:S(2)}) collective-permute-start(bf16[768,512]{1,0:T(8,128)(2,1)} %bitcast.30), channel_id=1, source_target_pairs={{0,2},{2,4},{4,6},{6,8},{8,10},{10,12},{12,14},{14,0},{1,15},{3,1}... | collective-permute-start | bytes 2359304 | tf_op jit(solution)/shard_map/ppermute | solution.py:26
  52.2 1.8 %fusion.8.group = bf16[256,128]{1,0:T(8,128)(2,1)} fusion(f32[128]{0:T(128)S(1)} %dynamic_slice.15, f32[256,128]{1,0:T(8,128)S(1)} %convert_element_type.181, f32[15,128]{1,0:T(8,128)S(1)} %convert_element_type.183, f32[256]{0:T(256)S(1)} %get-tuple-element.28, f32[128]{0:T(128)S(1)} %get-tuple-element.24, f32[256]{0:T(256)S(1)} %get-tuple-element.29, ...), kind=kOutput, calls=%fused_computation.15 | convolution fusion | flops 9895936 | bytes 243716 | tf_op jit(solution)/shard_map/rgc,gcd->rgd/dot_general | solution.py:129
  54.0 3.0 %shard_map.185 = (bf16[4,384,512]{2,1,0:T(8,128)(2,1)S(1)}, bf16[4,384,512]{2,1,0:T(8,128)(2,1)}) custom-call(s32[2,4]{1,0:T(2,128)} %and_select_fusion.3.index, bf16[256,128]{1,0:T(8,128)(2,1)} %fusion.8.group, bf16[128,32]{1,0:T(8,128)(2,1)} %fusion.9.hidden, bf16[128,4096]{1,0:T(8,128)(2,1)} %proj.1, bf16[32,4096]{1,0:T(8,128)(2,1)} %down.1), custom_call_target="tpu_custom_call" | custom-call | tf_op jit(solution)/shard_map/pallas_call | solution.py:46
  57.1 5.0 %collective-permute-start.1 = (bf16[4,384,512]{2,1,0:T(8,128)(2,1)}, bf16[4,384,512]{2,1,0:T(8,128)(2,1)}, u32[]{:S(2)}, u32[]{:S(2)}) collective-permute-start(bf16[4,384,512]{2,1,0:T(8,128)(2,1)} %get-tuple-element.9), channel_id=1, source_target_pairs={{0,1},{1,0},{2,3},{3,2},{4,5},{5,4},{6,7},{7,6},{8,9},{9,8},{10,11... | collective-permute-start | bytes 4718600 | tf_op jit(solution)/shard_map/ppermute | solution.py:31
  62.8 1.6 %shard_map.186 = bf16[5,256,512]{2,1,0:T(8,128)(2,1)S(1)} custom-call(s32[6]{0:T(128)} %pad_add_fusion.index, bf16[64,4096]{1,0:T(8,128)(2,1)} %bitcast.23.gate, bf16[64,4096]{1,0:T(8,128)(2,1)} %bitcast.25.up, bf16[64,4096]{1,0:T(8,128)(2,1)} %collective-permute-done.7.partner_gate, bf16[64,4096]{1,0:T(8,128)(2,1)} %collective-permute-done.8.partner_up), custom_call_target="tpu_custom_call" | custom-call | tf_op jit(solution)/shard_map/pallas_call | solution.py:46
  65.1 3.6 %collective-permute-done.9 = bf16[768,512]{1,0:T(8,128)(2,1)} collective-permute-done((bf16[768,512]{1,0:T(8,128)(2,1)}, bf16[768,512]{1,0:T(8,128)(2,1)}, u32[]{:S(2)}, u32[]{:S(2)}) %collective-permute-start.9) | collective-permute-done | bytes 786464 | tf_op jit(solution)/shard_map/ppermute | solution.py:26
  69.4 1.5 fusion.15
  71.0 1.5 fusion.16
  72.5 1.5 fusion.6
  74.9 17.3 %collective-permute-start.13 = (f32[256,768]{1,0:T(8,128)S(1)}, f32[256,768]{1,0:T(8,128)S(1)}, u32[]{:S(2)}, u32[]{:S(2)}) collective-permute-start(f32[256,768]{1,0:T(8,128)S(1)} %fusion.5), channel_id=1, source_target_pairs={{0,1},{1,0},{2,3},{3,2},{4,5},{5,4},{6,7},{7,6},{8,9},{9,8},{10,11... | collective-permute-start | bytes 2359304 | tf_op jit(solution)/shard_map/ppermute | solution.py:31
  93.3 1.9 %collective-permute-start.2 = (bf16[384,512]{1,0:T(8,128)(2,1)S(1)}, bf16[384,512]{1,0:T(8,128)(2,1)S(1)}, u32[]{:S(2)}, u32[]{:S(2)}) collective-permute-start(bf16[384,512]{1,0:T(8,128)(2,1)S(1)} %fusion.12), channel_id=1, source_target_pairs={{0,14},{2,0},{4,2},{6,4},{8,6},{10,8},{12,10},{14,12},{1,3},{3,5},... | collective-permute-start | bytes 1179656 | tf_op jit(solution)/shard_map/ppermute | solution.py:26
  95.2 1.9 %collective-permute-start.18 = (bf16[1024,256]{1,0:T(8,128)(2,1)S(1)}, bf16[1024,256]{1,0:T(8,128)(2,1)S(1)}, u32[]{:S(2)}, u32[]{:S(2)}) collective-permute-start(bf16[1024,256]{1,0:T(8,128)(2,1)S(1)} %bitcast.98), channel_id=1, source_target_pairs={{0,1},{1,0},{2,3},{3,2},{4,5},{5,4},{6,7},{7,6},{8,9},{9,8},{10,11... | collective-permute-start | bytes 1572872 | tf_op jit(solution)/shard_map/ppermute | solution.py:31
  97.1 5.9 %collective-permute-done.2 = bf16[384,512]{1,0:T(8,128)(2,1)S(1)} collective-permute-done((bf16[384,512]{1,0:T(8,128)(2,1)S(1)}, bf16[384,512]{1,0:T(8,128)(2,1)S(1)}, u32[]{:S(2)}, u32[]{:S(2)}) %collective-permute-start.2) | collective-permute-done | bytes 393248 | tf_op jit(solution)/shard_map/ppermute | solution.py:26
  103.0 1.9 %fusion.10 = bf16[384,512]{1,0:T(8,128)(2,1)} fusion(bf16[384,512]{1,0:T(8,128)(2,1)S(1)} %collective-permute-done.2, bf16[4,384,512]{2,1,0:T(8,128)(2,1)} %collective-permute-done.1, bf16[4,384,512]{2,1,0:T(8,128)(2,1)S(1)} %get-tuple-element.8), kind=kLoop, calls=%fused_computation.34 | loop fusion | flops 1179648 | bytes 1572864 | tf_op jit(solution)/shard_map/convert_element_type | solution.py:239
  104.9 1.9 %collective-permute-start.3 = (bf16[384,512]{1,0:T(8,128)(2,1)}, bf16[384,512]{1,0:T(8,128)(2,1)S(1)}, u32[]{:S(2)}, u32[]{:S(2)}) collective-permute-start(bf16[384,512]{1,0:T(8,128)(2,1)} %fusion.10), channel_id=1, source_target_pairs={{0,14},{2,0},{4,2},{6,4},{8,6},{10,8},{12,10},{14,12},{1,3},{3,5},... | collective-permute-start | bytes 1179656 | tf_op jit(solution)/shard_map/ppermute | solution.py:26
  107.0 4.6 %collective-permute-start.14 = (bf16[128,768]{1,0:T(8,128)(2,1)S(1)}, bf16[128,768]{1,0:T(8,128)(2,1)S(1)}, u32[]{:S(2)}, u32[]{:S(2)}) collective-permute-start(bf16[128,768]{1,0:T(8,128)(2,1)S(1)} %fusion.13), channel_id=1, source_target_pairs={{0,2},{2,4},{4,6},{6,8},{8,10},{10,12},{12,14},{14,0},{1,15},{3,1}... | collective-permute-start | bytes 589832 | tf_op jit(solution)/shard_map/ppermute | solution.py:26
  111.6 1.9 %collective-permute-start.15 = (bf16[128,768]{1,0:T(8,128)(2,1)S(1)}, bf16[128,768]{1,0:T(8,128)(2,1)S(1)}, u32[]{:S(2)}, u32[]{:S(2)}) collective-permute-start(bf16[128,768]{1,0:T(8,128)(2,1)S(1)} %fusion.13), channel_id=1, source_target_pairs={{0,4},{2,6},{4,8},{6,10},{8,12},{10,14},{12,0},{14,2},{1,13},{3,15... | collective-permute-start | bytes 589832 | tf_op jit(solution)/shard_map/ppermute | solution.py:26
  113.6 4.7 %collective-permute-start.16 = (bf16[128,768]{1,0:T(8,128)(2,1)S(1)}, bf16[128,768]{1,0:T(8,128)(2,1)S(1)}, u32[]{:S(2)}, u32[]{:S(2)}) collective-permute-start(bf16[128,768]{1,0:T(8,128)(2,1)S(1)} %fusion.13), channel_id=1, source_target_pairs={{0,6},{2,8},{4,10},{6,12},{8,14},{10,0},{12,2},{14,4},{1,11},{3,13... | collective-permute-start | bytes 589832 | tf_op jit(solution)/shard_map/ppermute | solution.py:26
  118.3 4.5 %collective-permute-start.17 = (bf16[64,768]{1,0:T(8,128)(2,1)S(1)}, bf16[64,768]{1,0:T(8,128)(2,1)S(1)}, u32[]{:S(2)}, u32[]{:S(2)}) collective-permute-start(bf16[64,768]{1,0:T(8,128)(2,1)S(1)} %slice_select_fusion.refs_0_), channel_id=1, source_target_pairs={{0,8},{2,10},{4,12},{6,14},{8,0},{10,2},{12,4},{14,6},{1,9},{3,11}... | collective-permute-start | bytes 294920 | tf_op jit(solution)/shard_map/ppermute | solution.py:26
  124.8 6.2 %collective-permute-done.17.refs_4_ = bf16[64,768]{1,0:T(8,128)(2,1)S(1)} collective-permute-done((bf16[64,768]{1,0:T(8,128)(2,1)S(1)}, bf16[64,768]{1,0:T(8,128)(2,1)S(1)}, u32[]{:S(2)}, u32[]{:S(2)}) %collective-permute-start.17) | collective-permute-done | bytes 98336 | tf_op jit(solution)/shard_map/ppermute | solution.py:26
  131.6 2.4 %collective-permute-start.19 = (bf16[768,256]{1,0:T(8,128)(2,1)S(1)}, bf16[768,256]{1,0:T(8,128)(2,1)S(1)}, u32[]{:S(2)}, u32[]{:S(2)}) collective-permute-start(bf16[768,256]{1,0:T(8,128)(2,1)S(1)} %get-tuple-element.11), channel_id=1, source_target_pairs={{0,1},{1,0},{2,3},{3,2},{4,5},{5,4},{6,7},{7,6},{8,9},{9,8},{10,11... | collective-permute-start | bytes 1179656 | tf_op jit(solution)/shard_map/ppermute | solution.py:31
  135.3 4.2 %collective-permute-start.4 = (bf16[384,512]{1,0:T(8,128)(2,1)S(1)}, bf16[384,512]{1,0:T(8,128)(2,1)S(1)}, u32[]{:S(2)}, u32[]{:S(2)}) collective-permute-start(bf16[384,512]{1,0:T(8,128)(2,1)S(1)} %fusion.11), channel_id=1, source_target_pairs={{0,14},{2,0},{4,2},{6,4},{8,6},{10,8},{12,10},{14,12},{1,3},{3,5},... | collective-permute-start | bytes 1179656 | tf_op jit(solution)/shard_map/ppermute | solution.py:26
  140.4 4.8 %all-to-all-start.1 = ((bf16[32,24,256]{2,1,0:T(8,128)(2,1)}), bf16[32,24,256]{2,1,0:T(8,128)(2,1)S(1)}, u32[]{:S(2)}, u32[]{:S(2)}) async-start(bf16[32,24,256]{2,1,0:T(8,128)(2,1)} %bitcast.41), calls=%async_computation.1 | async-start | bytes 786432 | tf_op jit(solution)/shard_map/all_to_all | solution.py:201
  146.5 4.2 %collective-permute-start.6 = (bf16[384,256]{1,0:T(8,128)(2,1)S(1)}, bf16[384,256]{1,0:T(8,128)(2,1)S(1)}, u32[]{:S(2)}, u32[]{:S(2)}) collective-permute-start(bf16[384,256]{1,0:T(8,128)(2,1)S(1)} %get-tuple-element.13), channel_id=1, source_target_pairs={{1,3},{3,5},{5,7},{7,9},{9,11},{11,13},{13,15},{15,1},{17,19},{19,... | collective-permute-start | bytes 589832 | tf_op jit(solution)/shard_map/ppermute | solution.py:26
  150.7 3.7 %collective-permute-done.6 = bf16[384,256]{1,0:T(8,128)(2,1)S(1)} collective-permute-done((bf16[384,256]{1,0:T(8,128)(2,1)S(1)}, bf16[384,256]{1,0:T(8,128)(2,1)S(1)}, u32[]{:S(2)}, u32[]{:S(2)}) %collective-permute-start.6) | collective-permute-done | bytes 196640 | tf_op jit(solution)/shard_map/ppermute | solution.py:26
  156.2 2.9 %all-to-all-done.1 = bf16[32,24,256]{2,1,0:T(8,128)(2,1)S(1)} async-done(((bf16[32,24,256]{2,1,0:T(8,128)(2,1)}), bf16[32,24,256]{2,1,0:T(8,128)(2,1)S(1)}, u32[]{:S(2)}, u32[]{:S(2)}) %all-to-all-start.1) | async-done | bytes 393248 | tf_op jit(solution)/shard_map/all_to_all | solution.py:201
  (89 shorter events, 21.4 us)
Async XLA Ops:
  0.6 27.7 %copy-start = (bf16[4096,32]{0,1:T(8,128)(2,1)S(1)}, bf16[4096,32]{0,1:T(8,128)(2,1)}, u32[]{:S(2)}) copy-start(bf16[4096,32]{0,1:T(8,128)(2,1)} %param.29) | copy-start | bytes 786436
  0.7 8.0 %copy-start.6 = (f32[4096]{0:T(1024)S(1)}, f32[4096]{0:T(1024)}, u32[]{:S(2)}) copy-start(f32[4096]{0:T(1024)} %param.23) | copy-start | bytes 49156
  1.5 50.8 %collective-permute-start = (bf16[15,128]{1,0:T(8,128)(2,1)S(1)}, bf16[15,128]{1,0:T(8,128)(2,1)S(1)}, u32[]{:S(2)}, u32[]{:S(2)}) collective-permute-start(bf16[15,128]{1,0:T(8,128)(2,1)S(1)} %slice.140), channel_id=1, source_target_pairs={{0,16},{16,32},{32,48},{48,64},{64,80},{80,96},{96,112},{112,128},... | collective-permute-start | bytes 11528 | tf_op jit(solution)/shard_map/ppermute | solution.py:18
  8.3 19.6 %copy-start.10 = (s32[4]{0:T(128)S(1)}, s32[4]{0:T(128)}, u32[]{:S(2)}) copy-start(s32[4]{0:T(128)} %constant.162.clone) | copy-start | bytes 52
  8.3 19.6 %copy-start.11 = (s32[4]{0:T(128)S(1)}, s32[4]{0:T(128)}, u32[]{:S(2)}) copy-start(s32[4]{0:T(128)} %constant.161.clone) | copy-start | bytes 52
  10.0 33.8 %all-to-all-start = ((bf16[32,24,512]{2,1,0:T(8,128)(2,1)}), bf16[32,24,512]{2,1,0:T(8,128)(2,1)}, u32[]{:S(2)}, u32[]{:S(2)}) async-start(bf16[32,24,512]{2,1,0:T(8,128)(2,1)} %bitcast.29), calls=%async_computation | async-start | bytes 1572864 | tf_op jit(solution)/shard_map/all_to_all | solution.py:201
  22.8 40.0 %collective-permute-start.7 = (bf16[64,4096]{1,0:T(8,128)(2,1)}, bf16[64,4096]{1,0:T(8,128)(2,1)}, u32[]{:S(2)}, u32[]{:S(2)}) collective-permute-start(bf16[64,4096]{1,0:T(8,128)(2,1)} %bitcast.23.gate), channel_id=1, source_target_pairs={{0,1},{1,0},{2,3},{3,2},{4,5},{5,4},{6,7},{7,6},{8,9},{9,8},{10,11... | collective-permute-start | bytes 1572872 | tf_op jit(solution)/shard_map/ppermute | solution.py:31
  25.9 36.8 %collective-permute-start.8 = (bf16[64,4096]{1,0:T(8,128)(2,1)}, bf16[64,4096]{1,0:T(8,128)(2,1)}, u32[]{:S(2)}, u32[]{:S(2)}) collective-permute-start(bf16[64,4096]{1,0:T(8,128)(2,1)} %bitcast.25.up), channel_id=1, source_target_pairs={{0,1},{1,0},{2,3},{3,2},{4,5},{5,4},{6,7},{7,6},{8,9},{9,8},{10,11... | collective-permute-start | bytes 1572872 | tf_op jit(solution)/shard_map/ppermute | solution.py:31
  28.4 23.1 %copy-start.5 = (bf16[256,128]{1,0:T(8,128)(2,1)S(1)}, bf16[256,128]{1,0:T(8,128)(2,1)}, u32[]{:S(2)}) copy-start(bf16[256,128]{1,0:T(8,128)(2,1)} %param.18) | copy-start | bytes 196612
  43.9 20.5 %collective-permute-start.10 = (bf16[768,512]{1,0:T(8,128)(2,1)}, bf16[768,512]{1,0:T(8,128)(2,1)}, u32[]{:S(2)}, u32[]{:S(2)}) collective-permute-start(bf16[768,512]{1,0:T(8,128)(2,1)} %bitcast.30), channel_id=1, source_target_pairs={{0,14},{2,0},{4,2},{6,4},{8,6},{10,8},{12,10},{14,12},{1,3},{3,5},... | collective-permute-start | bytes 2359304 | tf_op jit(solution)/shard_map/ppermute | solution.py:26
  47.1 21.7 %collective-permute-start.9 = (bf16[768,512]{1,0:T(8,128)(2,1)}, bf16[768,512]{1,0:T(8,128)(2,1)}, u32[]{:S(2)}, u32[]{:S(2)}) collective-permute-start(bf16[768,512]{1,0:T(8,128)(2,1)} %bitcast.30), channel_id=1, source_target_pairs={{0,2},{2,4},{4,6},{6,8},{8,10},{10,12},{12,14},{14,0},{1,15},{3,1}... | collective-permute-start | bytes 2359304 | tf_op jit(solution)/shard_map/ppermute | solution.py:26
  52.2 9.9 %copy-start.8 = (s32[5]{0:T(128)S(1)}, s32[5]{0:T(128)}, u32[]{:S(2)}) copy-start(s32[5]{0:T(128)} %constant.163.clone) | copy-start | bytes 64
  52.2 9.9 %copy-start.9 = (s32[5]{0:T(128)S(1)}, s32[5]{0:T(128)}, u32[]{:S(2)}) copy-start(s32[5]{0:T(128)} %constant.164.clone) | copy-start | bytes 64
  57.1 45.9 %copy-start.1 = (bf16[4,384,512]{2,1,0:T(8,128)(2,1)}, bf16[4,384,512]{2,1,0:T(8,128)(2,1)S(1)}, u32[]{:S(2)}) copy-start(bf16[4,384,512]{2,1,0:T(8,128)(2,1)S(1)} %get-tuple-element.8) | copy-start | bytes 4718596
  57.1 35.1 %collective-permute-start.1 = (bf16[4,384,512]{2,1,0:T(8,128)(2,1)}, bf16[4,384,512]{2,1,0:T(8,128)(2,1)}, u32[]{:S(2)}, u32[]{:S(2)}) collective-permute-start(bf16[4,384,512]{2,1,0:T(8,128)(2,1)} %get-tuple-element.9), channel_id=1, source_target_pairs={{0,1},{1,0},{2,3},{3,2},{4,5},{5,4},{6,7},{7,6},{8,9},{9,8},{10,11... | collective-permute-start | bytes 4718600 | tf_op jit(solution)/shard_map/ppermute | solution.py:31
  64.4 9.6 %collective-permute-start.12 = (bf16[768,512]{1,0:T(8,128)(2,1)}, bf16[768,512]{1,0:T(8,128)(2,1)S(1)}, u32[]{:S(2)}, u32[]{:S(2)}) collective-permute-start(bf16[768,512]{1,0:T(8,128)(2,1)} %collective-permute-done.10), channel_id=1, source_target_pairs={{0,14},{2,0},{4,2},{6,4},{8,6},{10,8},{12,10},{14,12},{16,30},{18,... | collective-permute-start | bytes 2359304 | tf_op jit(solution)/shard_map/ppermute | solution.py:26
  68.7 5.7 %collective-permute-start.11 = (bf16[768,512]{1,0:T(8,128)(2,1)}, bf16[768,512]{1,0:T(8,128)(2,1)S(1)}, u32[]{:S(2)}, u32[]{:S(2)}) collective-permute-start(bf16[768,512]{1,0:T(8,128)(2,1)} %collective-permute-done.9), channel_id=1, source_target_pairs={{0,2},{2,4},{4,6},{6,8},{8,10},{10,12},{12,14},{14,0},{16,18},{18,... | collective-permute-start | bytes 2359304 | tf_op jit(solution)/shard_map/ppermute | solution.py:26
  74.5 20.7 %copy-start.3 = (bf16[1,1024,256]{2,1,0:T(8,128)(2,1)S(1)}, bf16[1,1024,256]{2,1,0:T(8,128)(2,1)}, u32[]{:S(2)}) copy-start(bf16[1,1024,256]{2,1,0:T(8,128)(2,1)} %param.28) | copy-start | bytes 1572868
  74.9 31.9 %collective-permute-start.13 = (f32[256,768]{1,0:T(8,128)S(1)}, f32[256,768]{1,0:T(8,128)S(1)}, u32[]{:S(2)}, u32[]{:S(2)}) collective-permute-start(f32[256,768]{1,0:T(8,128)S(1)} %fusion.5), channel_id=1, source_target_pairs={{0,1},{1,0},{2,3},{3,2},{4,5},{5,4},{6,7},{7,6},{8,9},{9,8},{10,11... | collective-permute-start | bytes 2359304 | tf_op jit(solution)/shard_map/ppermute | solution.py:31
  93.3 9.7 %collective-permute-start.2 = (bf16[384,512]{1,0:T(8,128)(2,1)S(1)}, bf16[384,512]{1,0:T(8,128)(2,1)S(1)}, u32[]{:S(2)}, u32[]{:S(2)}) collective-permute-start(bf16[384,512]{1,0:T(8,128)(2,1)S(1)} %fusion.12), channel_id=1, source_target_pairs={{0,14},{2,0},{4,2},{6,4},{8,6},{10,8},{12,10},{14,12},{1,3},{3,5},... | collective-permute-start | bytes 1179656 | tf_op jit(solution)/shard_map/ppermute | solution.py:26
  95.2 23.1 %collective-permute-start.18 = (bf16[1024,256]{1,0:T(8,128)(2,1)S(1)}, bf16[1024,256]{1,0:T(8,128)(2,1)S(1)}, u32[]{:S(2)}, u32[]{:S(2)}) collective-permute-start(bf16[1024,256]{1,0:T(8,128)(2,1)S(1)} %bitcast.98), channel_id=1, source_target_pairs={{0,1},{1,0},{2,3},{3,2},{4,5},{5,4},{6,7},{7,6},{8,9},{9,8},{10,11... | collective-permute-start | bytes 1572872 | tf_op jit(solution)/shard_map/ppermute | solution.py:31
  104.9 29.1 %collective-permute-start.3 = (bf16[384,512]{1,0:T(8,128)(2,1)}, bf16[384,512]{1,0:T(8,128)(2,1)S(1)}, u32[]{:S(2)}, u32[]{:S(2)}) collective-permute-start(bf16[384,512]{1,0:T(8,128)(2,1)} %fusion.10), channel_id=1, source_target_pairs={{0,14},{2,0},{4,2},{6,4},{8,6},{10,8},{12,10},{14,12},{1,3},{3,5},... | collective-permute-start | bytes 1179656 | tf_op jit(solution)/shard_map/ppermute | solution.py:26
  107.0 24.0 %collective-permute-start.14 = (bf16[128,768]{1,0:T(8,128)(2,1)S(1)}, bf16[128,768]{1,0:T(8,128)(2,1)S(1)}, u32[]{:S(2)}, u32[]{:S(2)}) collective-permute-start(bf16[128,768]{1,0:T(8,128)(2,1)S(1)} %fusion.13), channel_id=1, source_target_pairs={{0,2},{2,4},{4,6},{6,8},{8,10},{10,12},{12,14},{14,0},{1,15},{3,1}... | collective-permute-start | bytes 589832 | tf_op jit(solution)/shard_map/ppermute | solution.py:26
  111.6 19.4 %collective-permute-start.15 = (bf16[128,768]{1,0:T(8,128)(2,1)S(1)}, bf16[128,768]{1,0:T(8,128)(2,1)S(1)}, u32[]{:S(2)}, u32[]{:S(2)}) collective-permute-start(bf16[128,768]{1,0:T(8,128)(2,1)S(1)} %fusion.13), channel_id=1, source_target_pairs={{0,4},{2,6},{4,8},{6,10},{8,12},{10,14},{12,0},{14,2},{1,13},{3,15... | collective-permute-start | bytes 589832 | tf_op jit(solution)/shard_map/ppermute | solution.py:26
  113.6 17.5 %collective-permute-start.16 = (bf16[128,768]{1,0:T(8,128)(2,1)S(1)}, bf16[128,768]{1,0:T(8,128)(2,1)S(1)}, u32[]{:S(2)}, u32[]{:S(2)}) collective-permute-start(bf16[128,768]{1,0:T(8,128)(2,1)S(1)} %fusion.13), channel_id=1, source_target_pairs={{0,6},{2,8},{4,10},{6,12},{8,14},{10,0},{12,2},{14,4},{1,11},{3,13... | collective-permute-start | bytes 589832 | tf_op jit(solution)/shard_map/ppermute | solution.py:26
  118.3 12.7 %collective-permute-start.17 = (bf16[64,768]{1,0:T(8,128)(2,1)S(1)}, bf16[64,768]{1,0:T(8,128)(2,1)S(1)}, u32[]{:S(2)}, u32[]{:S(2)}) collective-permute-start(bf16[64,768]{1,0:T(8,128)(2,1)S(1)} %slice_select_fusion.refs_0_), channel_id=1, source_target_pairs={{0,8},{2,10},{4,12},{6,14},{8,0},{10,2},{12,4},{14,6},{1,9},{3,11}... | collective-permute-start | bytes 294920 | tf_op jit(solution)/shard_map/ppermute | solution.py:26
  124.8 14.7 %copy-start.7 = (f32[128,4]{0,1:T(4,128)S(1)}, f32[128,4]{0,1:T(4,128)}, u32[]{:S(2)}) copy-start(f32[128,4]{0,1:T(4,128)} %param.25) | copy-start | bytes 6148
  131.6 7.9 %collective-permute-start.19 = (bf16[768,256]{1,0:T(8,128)(2,1)S(1)}, bf16[768,256]{1,0:T(8,128)(2,1)S(1)}, u32[]{:S(2)}, u32[]{:S(2)}) collective-permute-start(bf16[768,256]{1,0:T(8,128)(2,1)S(1)} %get-tuple-element.11), channel_id=1, source_target_pairs={{0,1},{1,0},{2,3},{3,2},{4,5},{5,4},{6,7},{7,6},{8,9},{9,8},{10,11... | collective-permute-start | bytes 1179656 | tf_op jit(solution)/shard_map/ppermute | solution.py:31
  135.3 9.9 %collective-permute-start.4 = (bf16[384,512]{1,0:T(8,128)(2,1)S(1)}, bf16[384,512]{1,0:T(8,128)(2,1)S(1)}, u32[]{:S(2)}, u32[]{:S(2)}) collective-permute-start(bf16[384,512]{1,0:T(8,128)(2,1)S(1)} %fusion.11), channel_id=1, source_target_pairs={{0,14},{2,0},{4,2},{6,4},{8,6},{10,8},{12,10},{14,12},{1,3},{3,5},... | collective-permute-start | bytes 1179656 | tf_op jit(solution)/shard_map/ppermute | solution.py:26
  140.4 18.6 %all-to-all-start.1 = ((bf16[32,24,256]{2,1,0:T(8,128)(2,1)}), bf16[32,24,256]{2,1,0:T(8,128)(2,1)S(1)}, u32[]{:S(2)}, u32[]{:S(2)}) async-start(bf16[32,24,256]{2,1,0:T(8,128)(2,1)} %bitcast.41), calls=%async_computation.1 | async-start | bytes 786432 | tf_op jit(solution)/shard_map/all_to_all | solution.py:201
  146.5 7.9 %collective-permute-start.6 = (bf16[384,256]{1,0:T(8,128)(2,1)S(1)}, bf16[384,256]{1,0:T(8,128)(2,1)S(1)}, u32[]{:S(2)}, u32[]{:S(2)}) collective-permute-start(bf16[384,256]{1,0:T(8,128)(2,1)S(1)} %get-tuple-element.13), channel_id=1, source_target_pairs={{1,3},{3,5},{5,7},{7,9},{9,11},{11,13},{13,15},{15,1},{17,19},{19,... | collective-permute-start | bytes 589832 | tf_op jit(solution)/shard_map/ppermute | solution.py:26
  150.7 4.7 %collective-permute-start.5 = (bf16[384,256]{1,0:T(8,128)(2,1)S(1)}, bf16[384,256]{1,0:T(8,128)(2,1)S(1)}, u32[]{:S(2)}, u32[]{:S(2)}) collective-permute-start(bf16[384,256]{1,0:T(8,128)(2,1)S(1)} %get-tuple-element.12), channel_id=1, source_target_pairs={{0,1},{2,3},{4,5},{6,7},{8,9},{10,11},{12,13},{14,15},{1,2},{3,4},... | collective-permute-start | bytes 589832 | tf_op jit(solution)/shard_map/ppermute | solution.py:26
  (3 other events, 13.3 us)

commit v10 on v9

--- a/solution.py
+++ b/solution.py
@@ -11,6 +11,7 @@
 eps = 1e-05
 f32 = jnp.float32
 bf16 = jnp.bfloat16
+grant = pltpu.CompilerParams(vmem_limit_bytes=16 * 1024 * 1024)
 
 
 def halo(block):
@@ -48,6 +49,7 @@
         in_specs=[smem] + [vmem] * len(operands),
         out_specs=[vmem] * len(out_shape) if several else vmem,
         out_shape=out_shape,
+        compiler_params=grant,
     )(index, *operands)
 
 
@@ -73,6 +75,44 @@
             at = lanes(index[side, j], width)
             to[j, :rows] = jnp.dot(group[...], proj[:, at], preferred_element_type=f32).astype(bf16)
             to[j, rows:] = jnp.dot(hidden[...], down[:, at], preferred_element_type=f32).astype(bf16)
+
+
+def in_vmem(body, operands, out_shape, **options):
+    vmem = pl.BlockSpec(memory_space=pltpu.VMEM)
+    several = isinstance(out_shape, list)
+    return pl.pallas_call(
+        body,
+        in_specs=[vmem] * len(operands),
+        out_specs=[vmem] * len(out_shape) if several else vmem,
+        out_shape=out_shape,
+        compiler_params=grant,
+        **options,
+    )(*[pltpu.with_memory_space_constraint(a, pltpu.VMEM) for a in operands])
+
+
+def rows_sum(weights, chunks, first, base):
+    rows = chunks[0].shape[0]
+    step = rows // 3
+
+    def body(*refs):
+        weight, *sources, out = refs
+        before = sources.pop() if base is not None else None
+        for lo in range(0, rows, step):
+            total = None if before is None else before[:, lo : lo + step]
+            for i, source in enumerate(sources):
+                product = tdot(weight[first + i], source[lo : lo + step, :])
+                total = product if total is None else total + product
+            out[:, lo : lo + step] = total
+
+    operands = [weights, *chunks] + ([] if base is None else [base])
+    return in_vmem(body, operands, pltpu.VMEM((weights.shape[1], rows), f32))
+
+
+def gate_kernel(mine, other, hidden):
+    units = hidden.shape[0]
+    gate = mine[:units] + other[:units]
+    up = mine[units:] + other[units:]
+    hidden[...] = (jax.nn.silu(gate) * up).astype(bf16)
 
 
 def down_rows_kernel(index, own, partner, blocks):
@@ -247,12 +287,12 @@
     down_two = sent(other, {0: (-1, 0)})
     ring = ring_step(part(0))
     ring = ring_step(ring_sum(1, ring))
-    summed = tdot(weights[0], arrived)
-    for j, rows in enumerate((one, other, up_two, down_two)):
-        summed = summed + tdot(weights[j + 1], rows)
-    full = summed + to_partner(summed)
+    summed = rows_sum(weights, (arrived,), 0, None)
+    summed = rows_sum(weights, (one, other), 1, summed)
+    summed = rows_sum(weights, (up_two, down_two), 3, summed)
     chip_units = 2 * units
-    hidden = (jax.nn.silu(full[:chip_units]) * full[chip_units:]).astype(bf16)
+    shape = pltpu.VMEM((chip_units, buffer_len), bf16)
+    hidden = in_vmem(gate_kernel, (summed, to_partner(summed)), shape)
 
     half = jnp.where(core == 0, hidden[:units], hidden[units:])
     side = jnp.where(core == 0, -1, 1)
@@ -266,14 +306,12 @@
     blocks = pltpu.VMEM((y_size * units, 2 * slice_width), bf16)
     rows_index = jnp.stack(begins).astype(jnp.int32)
     down_blocks = local_kernel(down_rows_kernel, rows_index, (own_down, partner_down), blocks)
-    vmem = pl.BlockSpec(memory_space=pltpu.VMEM)
-    own_sum, partner_sum = pl.pallas_call(
+    own_sum, partner_sum = in_vmem(
         down_kernel,
-        in_specs=[vmem] * (len(pieces) + 1),
-        out_specs=[vmem] * 2,
-        out_shape=[pltpu.VMEM((buffer_len, slice_width), kind) for kind in (f32, bf16)],
+        (*pieces, down_blocks),
+        [pltpu.VMEM((buffer_len, slice_width), kind) for kind in (f32, bf16)],
         scratch_shapes=[pltpu.VMEM((y_size * units, buffer_len), bf16)],
-    )(*[pltpu.with_memory_space_constraint(a, pltpu.VMEM) for a in (*pieces, down_blocks)])
+    )
     ring = ring_step(ring_sum(2, ring))
     expert_result = own_sum + to_partner(partner_sum).astype(f32)
     expert_result = expert_result.astype(bf16)

time: 162 us -> 165 us (1.019)
  waiting for transfers between devices: 37.1 us -> 45.3 us
  matrix products: 11 us -> 3.61 us
  Pallas kernels: 6.52 us -> 10.6 us
  starting transfers between devices: 89.4 us -> 86.9 us
  local copies, waits for them, and re-layouts: 4.05 us -> 5.95 us
    ppermute x6, starting transfers between devices: 31.7 us -> 24 us  [to_partner(): return lax.ppermute(x, 'tp', [(i, i ^ 1) for i in range(n)])]
    pallas_call x1 -> x5, Pallas kernels: 0.61 us -> 6.22 us  [in_vmem(): pl.pallas_call(body, in_specs=[vmem] * len(operands), out_specs=[vmem] *...]
    dot_general x5 -> x0, matrix products: 5.38 us -> none  [tdot(): lax.dot_general(a, b, (((1,), (1,)), ((), ())), preferred_element_type=f32)]
    ppermute x13, waiting for transfers between devices: 20.3 us -> 25.4 us  [sent(): return lax.ppermute(x, 'tp', route)]
    ppermute x13, starting transfers between devices: 36.3 us -> 40.3 us  [sent(): return lax.ppermute(x, 'tp', route)]
    unnamed x26 -> x40, local copies, waits for them, and re-layouts: 0.16 us -> 3.41 us
    ppermute x6, waiting for transfers between devices: 0.02 us -> 2.11 us  [to_partner(): return lax.ppermute(x, 'tp', [(i, i ^ 1) for i in range(n)])]
    all_to_all x2, starting transfers between devices: 17.5 us -> 19.5 us  [exchanged(): return lax.all_to_all(rows, 'ep', split_axis=0, concat_axis=0, tiled=True)]
  transfers between devices with their start and end apart: 22 -> 22, of which waited for: 7 -> 8; matrix products, arithmetic and copies ran while one was open for 15% -> 6% of each run, Pallas kernels for 4% -> 7%
where the time goes in v10:
time: 165 us; the launch traced here: 164 us
  starting transfers between devices  86.9 us (53%)
  waiting for transfers between devices  45.3 us (27%)
  Pallas kernels  10.6 us (6%)
  other arithmetic  9.91 us (6%)
  local copies, waits for them, and re-layouts  5.95 us (4%)
  matrix products  3.61 us (2%)
    ppermute x13, starting transfers between devices, sent(): return lax.ppermute(x, 'tp', route)  40.3 us
    ppermute x13, waiting for transfers between devices, sent(): return lax.ppermute(x, 'tp', route)  25.4 us
    ppermute x6, starting transfers between devices, to_partner(): return lax.ppermute(x, 'tp', [(i, i ^ 1) for i in range(n)])  24 us
    all_to_all x2, starting transfers between devices, exchanged(): return lax.all_to_all(rows, 'ep', split_axis=0, concat_axis=0, tiled=True)  19.5 us
    all_to_all x2, waiting for transfers between devices, exchanged(): return lax.all_to_all(rows, 'ep', split_axis=0, concat_axis=0, tiled=True)  17.7 us
    pallas_call x5, Pallas kernels, in_vmem(): pl.pallas_call(body, in_specs=[vmem] * len(operands), out_specs=[vmem] *...  6.22 us
    pallas_call x3, Pallas kernels, local_kernel(): pl.pallas_call(body, in_specs=[smem] + [vmem] * len(operands), out_specs=...  4.42 us
    convert_element_type x2, other arithmetic, ring_sum(): return (part(j) + ring.astype(f32)).astype(bf16)  3.95 us
  transfers between devices with their start and end apart: 22, of which 8 were waited for; matrix products, arithmetic and copies ran while one was open for 6% of the time, Pallas kernels for 7%

profile of v10, /device:TPU:1, one launch (start us, length us, event | category | flops | bytes accessed | tf_op | source)
XLA Modules:
  0.0 163.6 jit_solution(5598903751913481317)
XLA Ops:
  5.4 13.8 %all-to-all-start = ((bf16[32,24,512]{2,1,0:T(8,128)(2,1)}), bf16[32,24,512]{2,1,0:T(8,128)(2,1)S(1)}, u32[]{:S(2)}, u32[]{:S(2)}) async-start(bf16[32,24,512]{2,1,0:T(8,128)(2,1)} %bitcast.86), calls=%async_computation | async-start | bytes 1572864 | tf_op jit(solution)/shard_map/all_to_all | solution.py:241
  19.2 3.1 %collective-permute-start = (bf16[15,128]{1,0:T(8,128)(2,1)S(1)}, bf16[15,128]{1,0:T(8,128)(2,1)S(1)}, u32[]{:S(2)}, u32[]{:S(2)}) collective-permute-start(bf16[15,128]{1,0:T(8,128)(2,1)S(1)} %slice.119), channel_id=1, source_target_pairs={{0,16},{16,32},{32,48},{48,64},{64,80},{80,96},{96,112},{112,128},... | collective-permute-start | bytes 11528 | tf_op jit(solution)/shard_map/ppermute | solution.py:19
  25.1 15.2 %all-to-all-done = bf16[32,24,512]{2,1,0:T(8,128)(2,1)S(1)} async-done(((bf16[32,24,512]{2,1,0:T(8,128)(2,1)}), bf16[32,24,512]{2,1,0:T(8,128)(2,1)S(1)}, u32[]{:S(2)}, u32[]{:S(2)}) %all-to-all-start) | async-done | bytes 786464 | tf_op jit(solution)/shard_map/all_to_all | solution.py:241
  40.3 5.1 %collective-permute-start.9 = (bf16[768,512]{1,0:T(8,128)(2,1)S(1)}, bf16[768,512]{1,0:T(8,128)(2,1)}, u32[]{:S(2)}, u32[]{:S(2)}) collective-permute-start(bf16[768,512]{1,0:T(8,128)(2,1)S(1)} %bitcast.77), channel_id=1, source_target_pairs={{0,2},{2,4},{4,6},{6,8},{8,10},{10,12},{12,14},{14,0},{1,15},{3,1}... | collective-permute-start | bytes 2359304 | tf_op jit(solution)/shard_map/ppermute | solution.py:27
  45.4 1.9 %collective-permute-start.11 = (bf16[768,512]{1,0:T(8,128)(2,1)S(1)}, bf16[768,512]{1,0:T(8,128)(2,1)}, u32[]{:S(2)}, u32[]{:S(2)}) collective-permute-start(bf16[768,512]{1,0:T(8,128)(2,1)S(1)} %bitcast.78), channel_id=1, source_target_pairs={{0,14},{2,0},{4,2},{6,4},{8,6},{10,8},{12,10},{14,12},{1,3},{3,5},... | collective-permute-start | bytes 2359304 | tf_op jit(solution)/shard_map/ppermute | solution.py:27
  49.5 2.5 %shard_map.185 = (bf16[4,384,512]{2,1,0:T(8,128)(2,1)S(1)}, bf16[4,384,512]{2,1,0:T(8,128)(2,1)}) custom-call(s32[2,4]{1,0:T(2,128)S(1)} %and_select_fusion.3.index, bf16[256,128]{1,0:T(8,128)(2,1)S(1)} %fusion.6.group, bf16[128,32]{1,0:T(8,128)(2,1)S(1)} %fusion.7.hidden, bf16[128,4096]{1,0:T(8,128)(2,1)S(1)} %copy-done.1, bf16[32,4096]{1,0:T(8,128)(2,1)S(1)} %copy-done.5), custom_call_target="tpu_custom_call" | custom-call | tf_op jit(solution)/shard_map/pallas_call | solution.py:47
  52.0 4.9 %collective-permute-start.1 = (bf16[4,384,512]{2,1,0:T(8,128)(2,1)}, bf16[4,384,512]{2,1,0:T(8,128)(2,1)}, u32[]{:S(2)}, u32[]{:S(2)}) collective-permute-start(bf16[4,384,512]{2,1,0:T(8,128)(2,1)} %get-tuple-element.9), channel_id=1, source_target_pairs={{0,1},{1,0},{2,3},{3,2},{4,5},{5,4},{6,7},{7,6},{8,9},{9,8},{10,11... | collective-permute-start | bytes 4718600 | tf_op jit(solution)/shard_map/ppermute | solution.py:32
  59.2 7.1 %collective-permute-done.11.refs_2_ = bf16[768,512]{1,0:T(8,128)(2,1)} collective-permute-done((bf16[768,512]{1,0:T(8,128)(2,1)S(1)}, bf16[768,512]{1,0:T(8,128)(2,1)}, u32[]{:S(2)}, u32[]{:S(2)}) %collective-permute-start.11) | collective-permute-done | bytes 786464 | tf_op jit(solution)/shard_map/ppermute | solution.py:27
  67.8 6.7 %collective-permute-start.7 = (bf16[64,4096]{1,0:T(8,128)(2,1)S(1)}, bf16[64,4096]{1,0:T(8,128)(2,1)}, u32[]{:S(2)}, u32[]{:S(2)}) collective-permute-start(bf16[64,4096]{1,0:T(8,128)(2,1)S(1)} %bitcast.82), channel_id=1, source_target_pairs={{0,1},{1,0},{2,3},{3,2},{4,5},{5,4},{6,7},{7,6},{8,9},{9,8},{10,11... | collective-permute-start | bytes 1572872 | tf_op jit(solution)/shard_map/ppermute | solution.py:32
  74.5 1.9 %collective-permute-start.8 = (bf16[64,4096]{1,0:T(8,128)(2,1)}, bf16[64,4096]{1,0:T(8,128)(2,1)}, u32[]{:S(2)}, u32[]{:S(2)}) collective-permute-start(bf16[64,4096]{1,0:T(8,128)(2,1)} %bitcast.84), channel_id=1, source_target_pairs={{0,1},{1,0},{2,3},{3,2},{4,5},{5,4},{6,7},{7,6},{8,9},{9,8},{10,11... | collective-permute-start | bytes 1572872 | tf_op jit(solution)/shard_map/ppermute | solution.py:32
  76.5 2.1 %collective-permute-done.8.partner_up = bf16[64,4096]{1,0:T(8,128)(2,1)} collective-permute-done((bf16[64,4096]{1,0:T(8,128)(2,1)}, bf16[64,4096]{1,0:T(8,128)(2,1)}, u32[]{:S(2)}, u32[]{:S(2)}) %collective-permute-start.8) | collective-permute-done | bytes 524320 | tf_op jit(solution)/shard_map/ppermute | solution.py:32
  81.4 2.0 %shard_map.188.refs_3_ = f32[256,768]{1,0:T(8,128)S(1)} custom-call(bf16[5,256,512]{2,1,0:T(8,128)(2,1)S(1)} %shard_map.186.refs_0_, bf16[768,512]{1,0:T(8,128)(2,1)} %collective-permute-done.9.refs_1_, bf16[768,512]{1,0:T(8,128)(2,1)} %collective-permute-done.11.refs_2_, f32[256,768]{1,0:T(8,128)S(1)} %shard_map.187.refs_3_), custom_call_target="tpu_custom_call" | custom-call | tf_op jit(solution)/shard_map/pallas_call | solution.py:83
  83.4 2.0 %shard_map.189.mine = f32[256,768]{1,0:T(8,128)S(1)} custom-call(bf16[5,256,512]{2,1,0:T(8,128)(2,1)S(1)} %shard_map.186.refs_0_, bf16[768,512]{1,0:T(8,128)(2,1)} %collective-permute-done.10.refs_1_, bf16[768,512]{1,0:T(8,128)(2,1)} %collective-permute-done.12.refs_2_, f32[256,768]{1,0:T(8,128)S(1)} %shard_map.188.refs_3_), custom_call_target="tpu_custom_call" | custom-call | tf_op jit(solution)/shard_map/pallas_call | solution.py:83
  85.4 2.0 %collective-permute-start.13 = (f32[256,768]{1,0:T(8,128)S(1)}, f32[256,768]{1,0:T(8,128)S(1)}, u32[]{:S(2)}, u32[]{:S(2)}) collective-permute-start(f32[256,768]{1,0:T(8,128)S(1)} %shard_map.189.mine), channel_id=1, source_target_pairs={{0,1},{1,0},{2,3},{3,2},{4,5},{5,4},{6,7},{7,6},{8,9},{9,8},{10,11... | collective-permute-start | bytes 2359304 | tf_op jit(solution)/shard_map/ppermute | solution.py:32
  88.6 1.9 %collective-permute-start.2 = (bf16[384,512]{1,0:T(8,128)(2,1)S(1)}, bf16[384,512]{1,0:T(8,128)(2,1)S(1)}, u32[]{:S(2)}, u32[]{:S(2)}) collective-permute-start(bf16[384,512]{1,0:T(8,128)(2,1)S(1)} %fusion.10), channel_id=1, source_target_pairs={{0,14},{2,0},{4,2},{6,4},{8,6},{10,8},{12,10},{14,12},{1,3},{3,5},... | collective-permute-start | bytes 1179656 | tf_op jit(solution)/shard_map/ppermute | solution.py:27
  90.5 4.4 %collective-permute-start.18 = (bf16[1024,256]{1,0:T(8,128)(2,1)S(1)}, bf16[1024,256]{1,0:T(8,128)(2,1)S(1)}, u32[]{:S(2)}, u32[]{:S(2)}) collective-permute-start(bf16[1024,256]{1,0:T(8,128)(2,1)S(1)} %bitcast.80), channel_id=1, source_target_pairs={{0,1},{1,0},{2,3},{3,2},{4,5},{5,4},{6,7},{7,6},{8,9},{9,8},{10,11... | collective-permute-start | bytes 1572872 | tf_op jit(solution)/shard_map/ppermute | solution.py:32
  94.9 3.4 %collective-permute-done.2 = bf16[384,512]{1,0:T(8,128)(2,1)S(1)} collective-permute-done((bf16[384,512]{1,0:T(8,128)(2,1)S(1)}, bf16[384,512]{1,0:T(8,128)(2,1)S(1)}, u32[]{:S(2)}, u32[]{:S(2)}) %collective-permute-start.2) | collective-permute-done | bytes 393248 | tf_op jit(solution)/shard_map/ppermute | solution.py:27
  98.3 1.9 %fusion.8 = bf16[384,512]{1,0:T(8,128)(2,1)} fusion(bf16[384,512]{1,0:T(8,128)(2,1)S(1)} %collective-permute-done.2, bf16[4,384,512]{2,1,0:T(8,128)(2,1)} %collective-permute-done.1, bf16[4,384,512]{2,1,0:T(8,128)(2,1)S(1)} %get-tuple-element.8), kind=kLoop, calls=%fused_computation.30 | loop fusion | flops 1179648 | bytes 1572864 | tf_op jit(solution)/shard_map/convert_element_type | solution.py:279
  100.2 1.9 %collective-permute-start.3 = (bf16[384,512]{1,0:T(8,128)(2,1)}, bf16[384,512]{1,0:T(8,128)(2,1)}, u32[]{:S(2)}, u32[]{:S(2)}) collective-permute-start(bf16[384,512]{1,0:T(8,128)(2,1)} %fusion.8), channel_id=1, source_target_pairs={{0,14},{2,0},{4,2},{6,4},{8,6},{10,8},{12,10},{14,12},{1,3},{3,5},... | collective-permute-start | bytes 1179656 | tf_op jit(solution)/shard_map/ppermute | solution.py:27
  102.2 4.6 %collective-permute-start.14 = (bf16[128,768]{1,0:T(8,128)(2,1)S(1)}, bf16[128,768]{1,0:T(8,128)(2,1)}, u32[]{:S(2)}, u32[]{:S(2)}) collective-permute-start(bf16[128,768]{1,0:T(8,128)(2,1)S(1)} %shard_map.190), channel_id=1, source_target_pairs={{0,2},{2,4},{4,6},{6,8},{8,10},{10,12},{12,14},{14,0},{1,15},{3,1}... | collective-permute-start | bytes 589832 | tf_op jit(solution)/shard_map/ppermute | solution.py:27
  106.8 2.8 %collective-permute-start.15 = (bf16[128,768]{1,0:T(8,128)(2,1)S(1)}, bf16[128,768]{1,0:T(8,128)(2,1)}, u32[]{:S(2)}, u32[]{:S(2)}) collective-permute-start(bf16[128,768]{1,0:T(8,128)(2,1)S(1)} %shard_map.190), channel_id=1, source_target_pairs={{0,4},{2,6},{4,8},{6,10},{8,12},{10,14},{12,0},{14,2},{1,13},{3,15... | collective-permute-start | bytes 589832 | tf_op jit(solution)/shard_map/ppermute | solution.py:27
  109.6 6.7 %collective-permute-start.16 = (bf16[128,768]{1,0:T(8,128)(2,1)S(1)}, bf16[128,768]{1,0:T(8,128)(2,1)}, u32[]{:S(2)}, u32[]{:S(2)}) collective-permute-start(bf16[128,768]{1,0:T(8,128)(2,1)S(1)} %shard_map.190), channel_id=1, source_target_pairs={{0,6},{2,8},{4,10},{6,12},{8,14},{10,0},{12,2},{14,4},{1,11},{3,13... | collective-permute-start | bytes 589832 | tf_op jit(solution)/shard_map/ppermute | solution.py:27
  116.4 1.9 %collective-permute-start.17 = (bf16[64,768]{1,0:T(8,128)(2,1)S(1)}, bf16[64,768]{1,0:T(8,128)(2,1)S(1)}, u32[]{:S(2)}, u32[]{:S(2)}) collective-permute-start(bf16[64,768]{1,0:T(8,128)(2,1)S(1)} %slice_select_fusion.refs_0_), channel_id=1, source_target_pairs={{0,8},{2,10},{4,12},{6,14},{8,0},{10,2},{12,4},{14,6},{1,9},{3,11}... | collective-permute-start | bytes 294920 | tf_op jit(solution)/shard_map/ppermute | solution.py:27
  119.0 9.0 %collective-permute-done.17.refs_4_ = bf16[64,768]{1,0:T(8,128)(2,1)S(1)} collective-permute-done((bf16[64,768]{1,0:T(8,128)(2,1)S(1)}, bf16[64,768]{1,0:T(8,128)(2,1)S(1)}, u32[]{:S(2)}, u32[]{:S(2)}) %collective-permute-start.17) | collective-permute-done | bytes 98336 | tf_op jit(solution)/shard_map/ppermute | solution.py:27
  129.8 4.0 %collective-permute-start.19 = (bf16[768,256]{1,0:T(8,128)(2,1)S(1)}, bf16[768,256]{1,0:T(8,128)(2,1)S(1)}, u32[]{:S(2)}, u32[]{:S(2)}) collective-permute-start(bf16[768,256]{1,0:T(8,128)(2,1)S(1)} %get-tuple-element.11), channel_id=1, source_target_pairs={{0,1},{1,0},{2,3},{3,2},{4,5},{5,4},{6,7},{7,6},{8,9},{9,8},{10,11... | collective-permute-start | bytes 1179656 | tf_op jit(solution)/shard_map/ppermute | solution.py:32
  133.8 2.0 %fusion.9 = bf16[384,512]{1,0:T(8,128)(2,1)} fusion(bf16[384,512]{1,0:T(8,128)(2,1)} %collective-permute-done.3, bf16[4,384,512]{2,1,0:T(8,128)(2,1)} %collective-permute-done.1, bf16[4,384,512]{2,1,0:T(8,128)(2,1)S(1)} %get-tuple-element.8), kind=kLoop, calls=%fused_computation.32 | loop fusion | flops 1179648 | bytes 1572864 | tf_op jit(solution)/shard_map/convert_element_type | solution.py:279
  135.9 5.8 %collective-permute-start.4 = (bf16[384,512]{1,0:T(8,128)(2,1)}, bf16[384,512]{1,0:T(8,128)(2,1)}, u32[]{:S(2)}, u32[]{:S(2)}) collective-permute-start(bf16[384,512]{1,0:T(8,128)(2,1)} %fusion.9), channel_id=1, source_target_pairs={{0,14},{2,0},{4,2},{6,4},{8,6},{10,8},{12,10},{14,12},{1,3},{3,5},... | collective-permute-start | bytes 1179656 | tf_op jit(solution)/shard_map/ppermute | solution.py:27
  142.6 5.6 %all-to-all-start.1 = ((bf16[32,24,256]{2,1,0:T(8,128)(2,1)}), bf16[32,24,256]{2,1,0:T(8,128)(2,1)S(1)}, u32[]{:S(2)}, u32[]{:S(2)}) async-start(bf16[32,24,256]{2,1,0:T(8,128)(2,1)} %bitcast.36), calls=%async_computation.1 | async-start | bytes 786432 | tf_op jit(solution)/shard_map/all_to_all | solution.py:241
  149.6 1.9 %collective-permute-start.5 = (bf16[384,256]{1,0:T(8,128)(2,1)S(1)}, bf16[384,256]{1,0:T(8,128)(2,1)S(1)}, u32[]{:S(2)}, u32[]{:S(2)}) collective-permute-start(bf16[384,256]{1,0:T(8,128)(2,1)S(1)} %get-tuple-element.12), channel_id=1, source_target_pairs={{0,1},{2,3},{4,5},{6,7},{8,9},{10,11},{12,13},{14,15},{1,2},{3,4},... | collective-permute-start | bytes 589832 | tf_op jit(solution)/shard_map/ppermute | solution.py:27
  151.5 2.5 %collective-permute-start.6 = (bf16[384,256]{1,0:T(8,128)(2,1)S(1)}, bf16[384,256]{1,0:T(8,128)(2,1)S(1)}, u32[]{:S(2)}, u32[]{:S(2)}) collective-permute-start(bf16[384,256]{1,0:T(8,128)(2,1)S(1)} %get-tuple-element.13), channel_id=1, source_target_pairs={{1,3},{3,5},{5,7},{7,9},{9,11},{11,13},{13,15},{15,1},{17,19},{19,... | collective-permute-start | bytes 589832 | tf_op jit(solution)/shard_map/ppermute | solution.py:27
  154.1 5.3 %collective-permute-done.6 = bf16[384,256]{1,0:T(8,128)(2,1)S(1)} collective-permute-done((bf16[384,256]{1,0:T(8,128)(2,1)S(1)}, bf16[384,256]{1,0:T(8,128)(2,1)S(1)}, u32[]{:S(2)}, u32[]{:S(2)}) %collective-permute-start.6) | collective-permute-done | bytes 196640 | tf_op jit(solution)/shard_map/ppermute | solution.py:27
  160.2 2.6 %all-to-all-done.1 = bf16[32,24,256]{2,1,0:T(8,128)(2,1)S(1)} async-done(((bf16[32,24,256]{2,1,0:T(8,128)(2,1)}), bf16[32,24,256]{2,1,0:T(8,128)(2,1)S(1)}, u32[]{:S(2)}, u32[]{:S(2)}) %all-to-all-start.1) | async-done | bytes 393248 | tf_op jit(solution)/shard_map/all_to_all | solution.py:241
  (100 shorter events, 23.4 us)
Async XLA Ops:
  0.6 24.0 %copy-start = (bf16[16,128,128]{2,1,0:T(8,128)(2,1)S(1)}, bf16[16,128,128]{2,1,0:T(8,128)(2,1)}, u32[]{:S(2)}) copy-start(bf16[16,128,128]{2,1,0:T(8,128)(2,1)} %param.19) | copy-start | bytes 1572868
  3.5 15.7 %copy-start.8 = (bf16[256,128]{1,0:T(8,128)(2,1)S(1)}, bf16[256,128]{1,0:T(8,128)(2,1)}, u32[]{:S(2)}) copy-start(bf16[256,128]{1,0:T(8,128)(2,1)} %param.18) | copy-start | bytes 196612
  3.6 18.9 %copy-start.17 = (s32[4]{0:T(128)S(1)}, s32[4]{0:T(128)}, u32[]{:S(2)}) copy-start(s32[4]{0:T(128)} %constant.159.clone) | copy-start | bytes 52
  3.6 18.9 %copy-start.18 = (s32[4]{0:T(128)S(1)}, s32[4]{0:T(128)}, u32[]{:S(2)}) copy-start(s32[4]{0:T(128)} %constant.160.clone) | copy-start | bytes 52
  5.4 17.5 %copy-start.7 = (bf16[4096,32]{0,1:T(8,128)(2,1)S(1)}, bf16[4096,32]{0,1:T(8,128)(2,1)}, u32[]{:S(2)}) copy-start(bf16[4096,32]{0,1:T(8,128)(2,1)} %param.29) | copy-start | bytes 786436
  5.4 34.9 %all-to-all-start = ((bf16[32,24,512]{2,1,0:T(8,128)(2,1)}), bf16[32,24,512]{2,1,0:T(8,128)(2,1)S(1)}, u32[]{:S(2)}, u32[]{:S(2)}) async-start(bf16[32,24,512]{2,1,0:T(8,128)(2,1)} %bitcast.86), calls=%async_computation | async-start | bytes 1572864 | tf_op jit(solution)/shard_map/all_to_all | solution.py:241
  19.2 5.4 %collective-permute-start = (bf16[15,128]{1,0:T(8,128)(2,1)S(1)}, bf16[15,128]{1,0:T(8,128)(2,1)S(1)}, u32[]{:S(2)}, u32[]{:S(2)}) collective-permute-start(bf16[15,128]{1,0:T(8,128)(2,1)S(1)} %slice.119), channel_id=1, source_target_pairs={{0,16},{16,32},{32,48},{48,64},{64,80},{80,96},{96,112},{112,128},... | collective-permute-start | bytes 11528 | tf_op jit(solution)/shard_map/ppermute | solution.py:19
  24.7 43.1 %copy-start.3 = (bf16[1,4096,64]{1,2,0:T(8,128)(2,1)S(1)}, bf16[1,4096,64]{1,2,0:T(8,128)(2,1)}, u32[]{:S(2)}) copy-start(bf16[1,4096,64]{1,2,0:T(8,128)(2,1)} %param.26) | copy-start | bytes 1572868
  24.7 51.7 %copy-start.15 = (s32[5]{0:T(128)S(1)}, s32[5]{0:T(128)}, u32[]{:S(2)}) copy-start(s32[5]{0:T(128)} %constant.161.clone) | copy-start | bytes 64
  24.7 51.7 %copy-start.16 = (s32[5]{0:T(128)S(1)}, s32[5]{0:T(128)}, u32[]{:S(2)}) copy-start(s32[5]{0:T(128)} %constant.162.clone) | copy-start | bytes 64
  40.3 17.3 %collective-permute-start.9 = (bf16[768,512]{1,0:T(8,128)(2,1)S(1)}, bf16[768,512]{1,0:T(8,128)(2,1)}, u32[]{:S(2)}, u32[]{:S(2)}) collective-permute-start(bf16[768,512]{1,0:T(8,128)(2,1)S(1)} %bitcast.77), channel_id=1, source_target_pairs={{0,2},{2,4},{4,6},{6,8},{8,10},{10,12},{12,14},{14,0},{1,15},{3,1}... | collective-permute-start | bytes 2359304 | tf_op jit(solution)/shard_map/ppermute | solution.py:27
  45.4 20.8 %collective-permute-start.11 = (bf16[768,512]{1,0:T(8,128)(2,1)S(1)}, bf16[768,512]{1,0:T(8,128)(2,1)}, u32[]{:S(2)}, u32[]{:S(2)}) collective-permute-start(bf16[768,512]{1,0:T(8,128)(2,1)S(1)} %bitcast.78), channel_id=1, source_target_pairs={{0,14},{2,0},{4,2},{6,4},{8,6},{10,8},{12,10},{14,12},{1,3},{3,5},... | collective-permute-start | bytes 2359304 | tf_op jit(solution)/shard_map/ppermute | solution.py:27
  52.0 35.4 %collective-permute-start.1 = (bf16[4,384,512]{2,1,0:T(8,128)(2,1)}, bf16[4,384,512]{2,1,0:T(8,128)(2,1)}, u32[]{:S(2)}, u32[]{:S(2)}) collective-permute-start(bf16[4,384,512]{2,1,0:T(8,128)(2,1)} %get-tuple-element.9), channel_id=1, source_target_pairs={{0,1},{1,0},{2,3},{3,2},{4,5},{5,4},{6,7},{7,6},{8,9},{9,8},{10,11... | collective-permute-start | bytes 4718600 | tf_op jit(solution)/shard_map/ppermute | solution.py:32
  57.6 25.8 %collective-permute-start.10 = (bf16[768,512]{1,0:T(8,128)(2,1)}, bf16[768,512]{1,0:T(8,128)(2,1)}, u32[]{:S(2)}, u32[]{:S(2)}) collective-permute-start(bf16[768,512]{1,0:T(8,128)(2,1)} %collective-permute-done.9.refs_1_), channel_id=1, source_target_pairs={{0,2},{2,4},{4,6},{6,8},{8,10},{10,12},{12,14},{14,0},{16,18},{18,... | collective-permute-start | bytes 2359304 | tf_op jit(solution)/shard_map/ppermute | solution.py:27
  66.2 17.1 %collective-permute-start.12 = (bf16[768,512]{1,0:T(8,128)(2,1)}, bf16[768,512]{1,0:T(8,128)(2,1)}, u32[]{:S(2)}, u32[]{:S(2)}) collective-permute-start(bf16[768,512]{1,0:T(8,128)(2,1)} %collective-permute-done.11.refs_2_), channel_id=1, source_target_pairs={{0,14},{2,0},{4,2},{6,4},{8,6},{10,8},{12,10},{14,12},{16,30},{18,... | collective-permute-start | bytes 2359304 | tf_op jit(solution)/shard_map/ppermute | solution.py:27
  67.8 8.7 %collective-permute-start.7 = (bf16[64,4096]{1,0:T(8,128)(2,1)S(1)}, bf16[64,4096]{1,0:T(8,128)(2,1)}, u32[]{:S(2)}, u32[]{:S(2)}) collective-permute-start(bf16[64,4096]{1,0:T(8,128)(2,1)S(1)} %bitcast.82), channel_id=1, source_target_pairs={{0,1},{1,0},{2,3},{3,2},{4,5},{5,4},{6,7},{7,6},{8,9},{9,8},{10,11... | collective-permute-start | bytes 1572872 | tf_op jit(solution)/shard_map/ppermute | solution.py:32
  74.5 4.1 %collective-permute-start.8 = (bf16[64,4096]{1,0:T(8,128)(2,1)}, bf16[64,4096]{1,0:T(8,128)(2,1)}, u32[]{:S(2)}, u32[]{:S(2)}) collective-permute-start(bf16[64,4096]{1,0:T(8,128)(2,1)} %bitcast.84), channel_id=1, source_target_pairs={{0,1},{1,0},{2,3},{3,2},{4,5},{5,4},{6,7},{7,6},{8,9},{9,8},{10,11... | collective-permute-start | bytes 1572872 | tf_op jit(solution)/shard_map/ppermute | solution.py:32
  85.4 16.7 %collective-permute-start.13 = (f32[256,768]{1,0:T(8,128)S(1)}, f32[256,768]{1,0:T(8,128)S(1)}, u32[]{:S(2)}, u32[]{:S(2)}) collective-permute-start(f32[256,768]{1,0:T(8,128)S(1)} %shard_map.189.mine), channel_id=1, source_target_pairs={{0,1},{1,0},{2,3},{3,2},{4,5},{5,4},{6,7},{7,6},{8,9},{9,8},{10,11... | collective-permute-start | bytes 2359304 | tf_op jit(solution)/shard_map/ppermute | solution.py:32
  88.6 9.7 %collective-permute-start.2 = (bf16[384,512]{1,0:T(8,128)(2,1)S(1)}, bf16[384,512]{1,0:T(8,128)(2,1)S(1)}, u32[]{:S(2)}, u32[]{:S(2)}) collective-permute-start(bf16[384,512]{1,0:T(8,128)(2,1)S(1)} %fusion.10), channel_id=1, source_target_pairs={{0,14},{2,0},{4,2},{6,4},{8,6},{10,8},{12,10},{14,12},{1,3},{3,5},... | collective-permute-start | bytes 1179656 | tf_op jit(solution)/shard_map/ppermute | solution.py:27
  90.5 25.8 %collective-permute-start.18 = (bf16[1024,256]{1,0:T(8,128)(2,1)S(1)}, bf16[1024,256]{1,0:T(8,128)(2,1)S(1)}, u32[]{:S(2)}, u32[]{:S(2)}) collective-permute-start(bf16[1024,256]{1,0:T(8,128)(2,1)S(1)} %bitcast.80), channel_id=1, source_target_pairs={{0,1},{1,0},{2,3},{3,2},{4,5},{5,4},{6,7},{7,6},{8,9},{9,8},{10,11... | collective-permute-start | bytes 1572872 | tf_op jit(solution)/shard_map/ppermute | solution.py:32
  100.2 33.6 %collective-permute-start.3 = (bf16[384,512]{1,0:T(8,128)(2,1)}, bf16[384,512]{1,0:T(8,128)(2,1)}, u32[]{:S(2)}, u32[]{:S(2)}) collective-permute-start(bf16[384,512]{1,0:T(8,128)(2,1)} %fusion.8), channel_id=1, source_target_pairs={{0,14},{2,0},{4,2},{6,4},{8,6},{10,8},{12,10},{14,12},{1,3},{3,5},... | collective-permute-start | bytes 1179656 | tf_op jit(solution)/shard_map/ppermute | solution.py:27
  102.2 25.8 %collective-permute-start.14 = (bf16[128,768]{1,0:T(8,128)(2,1)S(1)}, bf16[128,768]{1,0:T(8,128)(2,1)}, u32[]{:S(2)}, u32[]{:S(2)}) collective-permute-start(bf16[128,768]{1,0:T(8,128)(2,1)S(1)} %shard_map.190), channel_id=1, source_target_pairs={{0,2},{2,4},{4,6},{6,8},{8,10},{10,12},{12,14},{14,0},{1,15},{3,1}... | collective-permute-start | bytes 589832 | tf_op jit(solution)/shard_map/ppermute | solution.py:27
  106.8 21.2 %collective-permute-start.15 = (bf16[128,768]{1,0:T(8,128)(2,1)S(1)}, bf16[128,768]{1,0:T(8,128)(2,1)}, u32[]{:S(2)}, u32[]{:S(2)}) collective-permute-start(bf16[128,768]{1,0:T(8,128)(2,1)S(1)} %shard_map.190), channel_id=1, source_target_pairs={{0,4},{2,6},{4,8},{6,10},{8,12},{10,14},{12,0},{14,2},{1,13},{3,15... | collective-permute-start | bytes 589832 | tf_op jit(solution)/shard_map/ppermute | solution.py:27
  109.6 18.5 %collective-permute-start.16 = (bf16[128,768]{1,0:T(8,128)(2,1)S(1)}, bf16[128,768]{1,0:T(8,128)(2,1)}, u32[]{:S(2)}, u32[]{:S(2)}) collective-permute-start(bf16[128,768]{1,0:T(8,128)(2,1)S(1)} %shard_map.190), channel_id=1, source_target_pairs={{0,6},{2,8},{4,10},{6,12},{8,14},{10,0},{12,2},{14,4},{1,11},{3,13... | collective-permute-start | bytes 589832 | tf_op jit(solution)/shard_map/ppermute | solution.py:27
  116.4 11.7 %collective-permute-start.17 = (bf16[64,768]{1,0:T(8,128)(2,1)S(1)}, bf16[64,768]{1,0:T(8,128)(2,1)S(1)}, u32[]{:S(2)}, u32[]{:S(2)}) collective-permute-start(bf16[64,768]{1,0:T(8,128)(2,1)S(1)} %slice_select_fusion.refs_0_), channel_id=1, source_target_pairs={{0,8},{2,10},{4,12},{6,14},{8,0},{10,2},{12,4},{14,6},{1,9},{3,11}... | collective-permute-start | bytes 294920 | tf_op jit(solution)/shard_map/ppermute | solution.py:27
  119.0 22.7 %copy-start.12 = (f32[128,4]{0,1:T(4,128)S(1)}, f32[128,4]{0,1:T(4,128)}, u32[]{:S(2)}) copy-start(f32[128,4]{0,1:T(4,128)} %param.25) | copy-start | bytes 6148
  129.8 12.0 %collective-permute-start.19 = (bf16[768,256]{1,0:T(8,128)(2,1)S(1)}, bf16[768,256]{1,0:T(8,128)(2,1)S(1)}, u32[]{:S(2)}, u32[]{:S(2)}) collective-permute-start(bf16[768,256]{1,0:T(8,128)(2,1)S(1)} %get-tuple-element.11), channel_id=1, source_target_pairs={{0,1},{1,0},{2,3},{3,2},{4,5},{5,4},{6,7},{7,6},{8,9},{9,8},{10,11... | collective-permute-start | bytes 1179656 | tf_op jit(solution)/shard_map/ppermute | solution.py:32
  135.9 12.4 %collective-permute-start.4 = (bf16[384,512]{1,0:T(8,128)(2,1)}, bf16[384,512]{1,0:T(8,128)(2,1)}, u32[]{:S(2)}, u32[]{:S(2)}) collective-permute-start(bf16[384,512]{1,0:T(8,128)(2,1)} %fusion.9), channel_id=1, source_target_pairs={{0,14},{2,0},{4,2},{6,4},{8,6},{10,8},{12,10},{14,12},{1,3},{3,5},... | collective-permute-start | bytes 1179656 | tf_op jit(solution)/shard_map/ppermute | solution.py:27
  142.6 20.1 %all-to-all-start.1 = ((bf16[32,24,256]{2,1,0:T(8,128)(2,1)}), bf16[32,24,256]{2,1,0:T(8,128)(2,1)S(1)}, u32[]{:S(2)}, u32[]{:S(2)}) async-start(bf16[32,24,256]{2,1,0:T(8,128)(2,1)} %bitcast.36), calls=%async_computation.1 | async-start | bytes 786432 | tf_op jit(solution)/shard_map/all_to_all | solution.py:241
  149.5 13.2 %copy-start.11 = (f32[32,128]{1,0:T(8,128)S(1)}, f32[32,128]{1,0:T(8,128)}, u32[]{:S(2)}) copy-start(f32[32,128]{1,0:T(8,128)} %copy-done.10) | copy-start | bytes 49156
  149.6 4.5 %collective-permute-start.5 = (bf16[384,256]{1,0:T(8,128)(2,1)S(1)}, bf16[384,256]{1,0:T(8,128)(2,1)S(1)}, u32[]{:S(2)}, u32[]{:S(2)}) collective-permute-start(bf16[384,256]{1,0:T(8,128)(2,1)S(1)} %get-tuple-element.12), channel_id=1, source_target_pairs={{0,1},{2,3},{4,5},{6,7},{8,9},{10,11},{12,13},{14,15},{1,2},{3,4},... | collective-permute-start | bytes 589832 | tf_op jit(solution)/shard_map/ppermute | solution.py:27
  151.5 7.9 %collective-permute-start.6 = (bf16[384,256]{1,0:T(8,128)(2,1)S(1)}, bf16[384,256]{1,0:T(8,128)(2,1)S(1)}, u32[]{:S(2)}, u32[]{:S(2)}) collective-permute-start(bf16[384,256]{1,0:T(8,128)(2,1)S(1)} %get-tuple-element.13), channel_id=1, source_target_pairs={{1,3},{3,5},{5,7},{7,9},{9,11},{11,13},{13,15},{15,1},{17,19},{19,... | collective-permute-start | bytes 589832 | tf_op jit(solution)/shard_map/ppermute | solution.py:27
  (10 other events, 27.9 us)
